TPU v7x, 512 devices: a whole 4x4x16 slice. The times are simulated.
512 devices in a mesh: sp: 16 (over z), dp: 32 (over y, x, core).
Axes of the slice: x: 4, y: 4, z: 16, core: 2. Of those that a mesh axis runs over, the one named last changes fastest.
Arguments:
- tokens: bfloat16 [64, 1024, 1024], P('dp', 'sp'), may hold values from -6 to 6
- norm_gain: float32 [1024], replicated, may hold values from 0.1 to 1.9
- w_query: bfloat16 [1024, 512], P('dp'), may hold values from -0.1875 to 0.1875
- w_key: bfloat16 [1024, 512], P('dp'), may hold values from -0.1875 to 0.1875
- w_value: bfloat16 [1024, 512], P('dp'), may hold values from -0.1875 to 0.1875
- w_rank_forward: bfloat16 [1024, 16], P('dp'), may hold values from -0.1875 to 0.1875
- w_rank_backward: bfloat16 [1024, 16], P('dp'), may hold values from -0.1875 to 0.1875
- up_forward: bfloat16 [16, 512], replicated, may hold values from -1.5 to 1.5
- up_backward: bfloat16 [16, 512], replicated, may hold values from -1.5 to 1.5
- bias_forward: float32 [512], replicated, may hold values from -1.5 to 3
- bias_backward: float32 [512], replicated, may hold values from -1.5 to 3
- out_gain: float32 [32], replicated, may hold values from 0.1 to 1.9
- w_out: bfloat16 [512, 1024], P('dp'), may hold values from -0.25 to 0.25
Outputs:
- mixed_out: bfloat16 [64, 1024, 1024], P('dp', 'sp')
All inputs are finite; a program needn't handle non-finite values.
Results may differ from a plain program's by a relative error of at most 0.005.
Values may be sent and summed in bfloat16 or wider, within the bound.
No kernel may reach another device: no remote copies, remote signals or barrier semaphores. Data moves between devices by JAX's collectives and lax.ppermute only.
A program may use at most 64 MiB of HBM per device.

v0:
```python
import jax
import jax.numpy as jnp
from jax import lax
from jax.sharding import Mesh
from jax.sharding import PartitionSpec as P

HK = 32
HV = 32
BLOCK = 64
DP = ("dp_0", "dp_1", "dp_2")


eps = 1e-06
precise = lax.Precision.HIGHEST


def over_all(x, axis, dim, take_in, carry):
    whole = jax.tree.map(lambda part: lax.all_gather(part, axis, axis=dim, tiled=True), x)
    return take_in(carry, whole, jnp.int32(0))


def for_sending(x):
    return jax.tree.map(lambda a: a.astype(jnp.bfloat16) if a.dtype == jnp.float32 else a, x)


def joined_along(pieces, dim):
    pieces = jnp.moveaxis(pieces, 0, dim)
    lengths = pieces.shape
    return pieces.reshape(*lengths[:dim], lengths[dim] * lengths[dim + 1], *lengths[dim + 2 :])


def stacked_from(x, axes, sequence):
    pieces = x
    for k in sequence:
        pieces = lax.all_gather(pieces, axes[k])
    done = sequence[::-1]
    back = [done.index(k) for k in range(len(axes))]
    pieces = pieces.transpose(*back, *range(len(axes), pieces.ndim))
    return pieces.reshape(-1, *x.shape)


def whole_of(x, axes, sequence, dim):
    return joined_along(stacked_from(x, axes, sequence), dim)


def folded(x, axes, sequence, dim, take_in, carry):
    everything = jax.tree.map(lambda part: whole_of(part, axes, sequence, dim), x)
    return take_in(carry, everything, jnp.int32(0))


def rms_norm(values, norm_scale):
    return values * lax.rsqrt(jnp.mean(values * values, axis=-1, keepdims=True) + eps) * norm_scale


def one_way(queries, key_rows, value_rows, decay_rates):
    head_count, length, key_width = queries.shape
    value_width = value_rows.shape[-1]
    blocks = length // BLOCK

    def in_blocks(tensor):
        return tensor.reshape(head_count, blocks, BLOCK, tensor.shape[-1])

    query_blocks = in_blocks(queries)
    key_blocks = in_blocks(key_rows)
    value_blocks = in_blocks(value_rows)
    running = jnp.cumsum(in_blocks(decay_rates), axis=2)
    closing = running[:, :, -1:, :]
    query_decayed = query_blocks * jnp.exp(running)
    key_inverse = key_blocks * jnp.exp(-running)
    key_remain = key_blocks * jnp.exp(closing - running)
    triangle = jnp.tril(jnp.ones((BLOCK, BLOCK), jnp.float32))
    scores = jnp.einsum("hnid,hnjd->hnij", query_decayed, key_inverse, precision=precise) * triangle
    within = jnp.einsum("hnij,hnjv->hniv", scores, value_blocks, precision=precise)
    block_decay = jnp.exp(closing[:, :, 0, :])

    def advance(carried, inputs):
        query_now, key_now, value_now, decay_now = inputs
        emitted = jnp.einsum("hid,hdv->hiv", query_now, carried, precision=precise)
        carried = decay_now[..., None] * carried + jnp.einsum(
            "hid,hiv->hdv", key_now, value_now, precision=precise
        )
        return (carried, emitted)

    initial = jnp.zeros((head_count, key_width, value_width), jnp.float32)
    stacked = tuple(
        (
            jnp.moveaxis(tensor, 1, 0)
            for tensor in (query_decayed, key_remain, value_blocks, block_decay)
        )
    )
    final_state, across = lax.scan(advance, initial, stacked)
    return (within + jnp.moveaxis(across, 0, 1)).reshape(head_count, length, value_width)


def both_ways(queries, key_rows, value_rows, rates_forward, rates_backward):
    forward = one_way(queries, key_rows, value_rows, rates_forward)
    backward = one_way(
        jnp.flip(queries, 1),
        jnp.flip(key_rows, 1),
        jnp.flip(value_rows, 1),
        jnp.flip(rates_backward, 1),
    )
    return forward + jnp.flip(backward, 1)


def by_head(tensor, head_width):
    length = tensor.shape[0]
    return tensor.reshape(length, -1, head_width).transpose(1, 0, 2).astype(jnp.float32)


def attend(queries, key_rows, value_rows, rates_forward, rates_backward, out_gain):
    combined = both_ways(
        by_head(queries, HK) * HK ** (-0.5),
        by_head(key_rows, HK),
        by_head(value_rows, HV),
        by_head(rates_forward, HK),
        by_head(rates_backward, HK),
    )
    normed = rms_norm(combined, out_gain).astype(jnp.bfloat16)
    return normed.transpose(1, 0, 2).reshape(normed.shape[1], -1)


def body(
    tokens,
    norm_gain,
    w_query,
    w_key,
    w_value,
    w_rank_forward,
    w_rank_backward,
    up_forward,
    up_backward,
    bias_forward,
    bias_backward,
    out_gain,
    w_out,
):
    seq_local, tok_local, model_width = tokens.shape
    sp_count = lax.axis_size("sp")
    length = tok_local * sp_count
    rate_scale = 2.0 / length
    row_count = seq_local * tok_local
    normed = rms_norm(tokens.reshape(row_count, model_width).astype(jnp.float32), norm_gain).astype(
        jnp.bfloat16
    )

    def add_rows(totals, pieces, offset):
        span_rows = pieces[0].shape[0]
        left_part = lax.dynamic_slice_in_dim(normed, offset, span_rows, 1)
        return tuple(
            (
                running_sum + jnp.dot(left_part, shard_piece, preferred_element_type=jnp.float32)
                for running_sum, shard_piece in zip(totals, pieces)
            )
        )

    starting = tuple(
        (
            jnp.zeros((row_count, weight.shape[1]), jnp.float32)
            for weight in (w_query, w_key, w_value, w_rank_forward, w_rank_backward)
        )
    )
    projected = over_all(
        (w_query, w_key, w_value, w_rank_forward, w_rank_backward), DP, 0, add_rows, starting
    )
    queries = projected[0].astype(jnp.bfloat16).reshape(seq_local, tok_local, -1)
    key_rows = projected[1].astype(jnp.bfloat16).reshape(seq_local, tok_local, -1)
    value_rows = projected[2].astype(jnp.bfloat16).reshape(seq_local, tok_local, -1)
    rank_forward = projected[3].astype(jnp.bfloat16)
    rank_backward = projected[4].astype(jnp.bfloat16)
    head_queries, head_keys, head_values = (
        lax.all_to_all(queries, "sp", split_axis=2, concat_axis=1, tiled=True),
        lax.all_to_all(key_rows, "sp", split_axis=2, concat_axis=1, tiled=True),
        lax.all_to_all(value_rows, "sp", split_axis=2, concat_axis=1, tiled=True),
    )
    all_forward, all_backward = (
        lax.all_gather(rank_forward.reshape(seq_local, tok_local, -1), "sp", axis=1, tiled=True),
        lax.all_gather(rank_backward.reshape(seq_local, tok_local, -1), "sp", axis=1, tiled=True),
    )
    local_width = head_queries.shape[2]
    column = lax.axis_index("sp") * local_width
    up_fwd_local = lax.dynamic_slice_in_dim(up_forward, column, local_width, 1)
    up_bwd_local = lax.dynamic_slice_in_dim(up_backward, column, local_width, 1)
    bias_fwd_local = lax.dynamic_slice_in_dim(bias_forward, column, local_width, 0)
    bias_bwd_local = lax.dynamic_slice_in_dim(bias_backward, column, local_width, 0)
    rates_forward = (
        jax.nn.log_sigmoid(
            jnp.dot(all_forward, up_fwd_local, preferred_element_type=jnp.float32) + bias_fwd_local
        )
        * rate_scale
    )
    rates_backward = (
        jax.nn.log_sigmoid(
            jnp.dot(all_backward, up_bwd_local, preferred_element_type=jnp.float32) + bias_bwd_local
        )
        * rate_scale
    )
    attended = jax.vmap(attend, in_axes=(0, 0, 0, 0, 0, None))(
        head_queries, head_keys, head_values, rates_forward, rates_backward, out_gain
    )
    gathered_heads = jax.tree.map(
        lambda part, own: part.astype(own.dtype),
        lax.all_to_all(for_sending(attended), "sp", split_axis=1, concat_axis=2, tiled=True),
        attended,
    ).reshape(row_count, -1)

    def add_out(running_sum, shard_piece, offset):
        left_part = lax.dynamic_slice_in_dim(gathered_heads, offset, shard_piece.shape[0], 1)
        return running_sum + jnp.dot(left_part, shard_piece, preferred_element_type=jnp.float32)

    mixed_out = folded(
        w_out,
        (("dp_0", "dp_1"), "dp_2"),
        (0, 1),
        0,
        add_out,
        jnp.zeros((row_count, w_out.shape[1]), jnp.float32),
    )
    return mixed_out.astype(jnp.bfloat16).reshape(seq_local, tok_local, -1)


def solution(mesh):
    finer = Mesh(mesh.devices.reshape(mesh.shape["sp"], 4, 4, 2), ("sp", "dp_0", "dp_1", "dp_2"))
    in_specs = (
        P(DP, "sp", None),
        P(),
        P(DP, None),
        P(DP, None),
        P(DP, None),
        P(DP, None),
        P(DP, None),
        P(),
        P(),
        P(),
        P(),
        P(),
        P(DP, None),
    )
    out_specs = P(DP, "sp", None)
    return jax.shard_map(body, mesh=finer, in_specs=in_specs, out_specs=out_specs, check_vma=False)
```

profile of v0, /device:TPU:24, one launch (start us, length us, event | category | flops | bytes accessed | tf_op | source)
XLA Modules:
  0.0 393.3 jit_solution(9699959497070522098)
XLA Ops:
  8.8 28.4 %all-gather = bf16[256,1024]{1,0:T(8,128)(2,1)} all-gather(bf16[16,1024]{1,0:T(8,128)(2,1)S(1)} %copy-done.10), channel_id=2, replica_groups=mesh['sp'=16,'dp_0'=4,'dp_1'=4,'dp_2'=2] {'dp_0','dp_1'}, dimensions={0}, use_global_device_ids=true | all-gather | bytes 557056 | tf_op jit(solution)/shard_map/all_gather | solution.py:35
  39.0 22.0 %all-gather.2 = bf16[32,32,16]{1,2,0:T(8,128)(2,1)S(1)} all-gather(bf16[1,32,16]{1,2,0:T(8,128)(2,1)S(1)} %bitcast.301), channel_id=1, replica_groups=mesh['sp'=16,'dp_0'=4,'dp_1'=4,'dp_2'=2] {'dp_0','dp_1','dp_2'}, dimensions={0}, use_global_device_ids=true | all-gather | bytes 33792 | tf_op jit(solution)/shard_map/all_gather | solution.py:18
  62.3 35.7 %all_gather.35 = bf16[2,1024,16]{2,0,1:T(2,128)(2,1)S(1)} all-gather(bf16[2,64,16]{2,0,1:T(2,128)(2,1)S(1)} %copy.154), channel_id=1, replica_groups=mesh['sp'=16,'dp_0'=4,'dp_1'=4,'dp_2'=2] {'sp'}, dimensions={1}, use_global_device_ids=true | all-gather | bytes 69632 | tf_op jit(solution)/shard_map/all_gather | solution.py:177
  100.0 13.2 %fusion.64 = f32[2,1,16,64,32]{4,2,3,1,0:T(8,128)S(1)} fusion(f32[2,1,16,64,32]{4,2,3,1,0:T(8,128)S(1)} %copy.156), kind=kOutput, calls=%fused_computation.107 | output fusion | flops 4128768 | bytes 524288 | tf_op jit(solution)/shard_map/vmap(jit(cumsum))/reduce_window_sum | solution.py:66
  113.1 23.8 %all-gather.3 = bf16[32,32,16]{1,2,0:T(8,128)(2,1)S(1)} all-gather(bf16[1,32,16]{1,2,0:T(8,128)(2,1)S(1)} %bitcast.302), channel_id=1, replica_groups=mesh['sp'=16,'dp_0'=4,'dp_1'=4,'dp_2'=2] {'dp_0','dp_1','dp_2'}, dimensions={0}, use_global_device_ids=true | all-gather | bytes 33792 | tf_op jit(solution)/shard_map/all_gather | solution.py:18
  137.5 29.1 %all_gather.39 = bf16[2,1024,16]{2,0,1:T(2,128)(2,1)S(1)} all-gather(bf16[2,64,16]{2,0,1:T(2,128)(2,1)S(1)} %copy.172), channel_id=1, replica_groups=mesh['sp'=16,'dp_0'=4,'dp_1'=4,'dp_2'=2] {'sp'}, dimensions={1}, use_global_device_ids=true | all-gather | bytes 69632 | tf_op jit(solution)/shard_map/all_gather | solution.py:178
  173.5 7.3 %all-to-all-start.1 = ((bf16[16,2,2048]{2,1,0:T(2,128)(2,1)}), bf16[16,2,2048]{2,1,0:T(2,128)(2,1)S(1)}, u32[]{:S(2)}, u32[]{:S(2)}) async-start(bf16[16,2,2048]{2,1,0:T(2,128)(2,1)} %reshape.375), calls=%async_computation.1 | async-start | bytes 262144 | tf_op jit(solution)/shard_map/all_to_all | solution.py:173
  185.4 9.2 %all-to-all-done.1 = bf16[16,2,2048]{2,1,0:T(2,128)(2,1)S(1)} async-done(((bf16[16,2,2048]{2,1,0:T(2,128)(2,1)}), bf16[16,2,2048]{2,1,0:T(2,128)(2,1)S(1)}, u32[]{:S(2)}, u32[]{:S(2)}) %all-to-all-start.1) | async-done | bytes 131104 | tf_op jit(solution)/shard_map/all_to_all | solution.py:173
  194.5 3.6 all-to-all-start
  202.1 9.5 %all-to-all-done = bf16[16,2,2048]{2,1,0:T(2,128)(2,1)S(1)} async-done(((bf16[16,2,2048]{2,1,0:T(2,128)(2,1)}), bf16[16,2,2048]{2,1,0:T(2,128)(2,1)S(1)}, u32[]{:S(2)}, u32[]{:S(2)}) %all-to-all-start) | async-done | bytes 131104 | tf_op jit(solution)/shard_map/all_to_all | solution.py:172
  212.2 4.3 %all-to-all-start.2 = ((bf16[16,2,2048]{2,1,0:T(2,128)(2,1)}), bf16[16,2,2048]{2,1,0:T(2,128)(2,1)}, u32[]{:S(2)}, u32[]{:S(2)}) async-start(bf16[16,2,2048]{2,1,0:T(2,128)(2,1)} %reshape.373), calls=%async_computation.2 | async-start | bytes 262144 | tf_op jit(solution)/shard_map/all_to_all | solution.py:174
  221.3 8.1 %all-to-all-done.2 = bf16[16,2,2048]{2,1,0:T(2,128)(2,1)} async-done(((bf16[16,2,2048]{2,1,0:T(2,128)(2,1)}), bf16[16,2,2048]{2,1,0:T(2,128)(2,1)}, u32[]{:S(2)}, u32[]{:S(2)}) %all-to-all-start.2) | async-done | bytes 131104 | tf_op jit(solution)/shard_map/all_to_all | solution.py:174
  242.6 3.6 fusion.32
  246.2 2.4 copy.165
  250.7 52.4 %while.26 = (s32[]{:T(128)}, f32[2,1,32,32]{3,2,0,1:T(8,128)S(1)}, f32[16,2,1,64,32]{3,4,0,1,2:T(8,128)}, f32[16,2,1,32]{3,0,1,2:T(8,128)}, f32[16,2,1,64,32]{3,...) while((s32[]{:T(128)}, f32[2,1,32,32]{3,2,0,1:T(8,128)S(1)}, ...), condition=%wide.region_3.4_spmd.clone, body=%wide.region_2.3_spmd.clone.sunk | while | flops 3153923 | bytes 159602 | solution.py:91
  250.7 1.6 fusion.101
  254.0 1.6 fusion.101
  263.8 1.6 fusion.101
  267.1 1.6 fusion.101
  270.4 1.6 fusion.101
  276.9 1.6 fusion.101
  286.8 1.6 fusion.101
  290.0 1.6 fusion.101
  293.3 1.6 fusion.101
  296.6 1.6 fusion.101
  303.2 3.7 convolution_multiply_fusion.1
  311.0 2.5 copy.185
  313.8 46.3 %while.27 = (s32[]{:T(128)}, f32[2,1,32,32]{3,2,0,1:T(8,128)S(1)}, f32[16,2,1,64,32]{3,4,0,1,2:T(8,128)S(1)}, f32[16,2,1,32]{3,0,1,2:T(8,128)}, f32[16,2,1,64,32...) while((s32[]{:T(128)}, f32[2,1,32,32]{3,2,0,1:T(8,128)S(1)}, ...), condition=%wide.region_6.7_spmd.clone, body=%wide.region_5.6_spmd.clone.sunk | while | flops 3153923 | bytes 199035 | solution.py:91
  360.1 2.1 convolution_multiply_fusion
  362.1 1.8 fusion.29
  367.5 3.9 all-to-all-start.3
  372.8 12.1 %all-to-all-done.3 = bf16[16,2,2048]{2,1,0:T(2,128)(2,1)S(1)} async-done(((bf16[16,2,2048]{2,1,0:T(2,128)(2,1)}), bf16[16,2,2048]{2,1,0:T(2,128)(2,1)S(1)}, u32[]{:S(2)}, u32[]{:S(2)}) %all-to-all-start.3) | async-done | bytes 131104 | tf_op jit(solution)/shard_map/all_to_all | solution.py:203
  (233 shorter events, 136.1 us)
Async XLA Ops:
  6.5 92.2 %copy-start = (bf16[16,512]{1,0:T(8,128)(2,1)S(1)}, bf16[16,512]{1,0:T(8,128)(2,1)}, u32[]{:S(2)}) copy-start(bf16[16,512]{1,0:T(8,128)(2,1)} %param.24) | copy-start | bytes 49156
  6.5 164.3 %all-gather.11.cloned.1.call-start = ((), (), s32[]{:S(2)}) async-start(), calls=%async_computation.5 | async-start | bytes 1081344 | tf_op jit(solution)/shard_map/all_gather | solution.py:18
  7.3 1.5 copy-start.10
  7.3 175.5 %all-gather.9.cloned.1.call-start = ((), (), s32[]{:S(2)}) async-start(), calls=%async_computation.4 | async-start | bytes 1081344 | tf_op jit(solution)/shard_map/all_gather | solution.py:18
  8.0 191.2 %all-gather.13.cloned.1.call-start = ((), (), s32[]{:S(2)}) async-start(), calls=%async_computation.6 | async-start | bytes 1081344 | tf_op jit(solution)/shard_map/all_gather | solution.py:18
  8.8 362.7 %all-gather.15.cloned.1.call-start = ((), (), s32[]{:S(2)}) async-start(), calls=%async_computation.7 | async-start | bytes 1572864 | tf_op jit(solution)/shard_map/all_gather | solution.py:35
  37.3 1.0 copy-start.7
  38.3 0.7 copy-start.12
  61.1 0.7 copy-start.11
  100.0 13.2 %copy-start.13 = (bf16[32,16]{0,1:T(8,128)(2,1)S(1)}, bf16[32,16]{0,1:T(8,128)(2,1)}, u32[]{:S(2)}) copy-start(bf16[32,16]{0,1:T(8,128)(2,1)} %param.23) | copy-start | bytes 3076
  113.1 85.4 %copy-start.1 = (f32[2,1,16,64,32]{4,2,3,1,0:T(8,128)}, f32[2,1,16,64,32]{4,2,3,1,0:T(8,128)S(1)}, u32[]{:S(2)}) copy-start(f32[2,1,16,64,32]{4,2,3,1,0:T(8,128)S(1)} %fusion.64) | copy-start | bytes 786436
  173.5 21.1 %all-to-all-start.1 = ((bf16[16,2,2048]{2,1,0:T(2,128)(2,1)}), bf16[16,2,2048]{2,1,0:T(2,128)(2,1)S(1)}, u32[]{:S(2)}, u32[]{:S(2)}) async-start(bf16[16,2,2048]{2,1,0:T(2,128)(2,1)} %reshape.375), calls=%async_computation.1 | async-start | bytes 262144 | tf_op jit(solution)/shard_map/all_to_all | solution.py:173
  194.5 17.0 %all-to-all-start = ((bf16[16,2,2048]{2,1,0:T(2,128)(2,1)}), bf16[16,2,2048]{2,1,0:T(2,128)(2,1)S(1)}, u32[]{:S(2)}, u32[]{:S(2)}) async-start(bf16[16,2,2048]{2,1,0:T(2,128)(2,1)} %reshape.377), calls=%async_computation | async-start | bytes 262144 | tf_op jit(solution)/shard_map/all_to_all | solution.py:172
  211.6 0.7 copy-start.8
  212.2 17.2 %all-to-all-start.2 = ((bf16[16,2,2048]{2,1,0:T(2,128)(2,1)}), bf16[16,2,2048]{2,1,0:T(2,128)(2,1)}, u32[]{:S(2)}, u32[]{:S(2)}) async-start(bf16[16,2,2048]{2,1,0:T(2,128)(2,1)} %reshape.373), calls=%async_computation.2 | async-start | bytes 262144 | tf_op jit(solution)/shard_map/all_to_all | solution.py:174
  219.2 1.0 copy-start.9
  231.4 1.2 copy-start.5
  303.1 3.7 copy-start.6
  311.0 2.5 copy-start.4
  313.7 46.3 %copy-start.2 = (f32[2,16,64,32]{2,1,3,0:T(8,128)S(1)}, f32[2,16,64,32]{2,1,3,0:T(8,128)}, u32[]{:S(2)}) copy-start(f32[2,16,64,32]{2,1,3,0:T(8,128)} %reshape.338) | copy-start | bytes 786436
  360.0 2.1 copy-start.3
  365.2 0.7 copy-start.14
  367.5 17.4 %all-to-all-start.3 = ((bf16[16,2,2048]{2,1,0:T(2,128)(2,1)}), bf16[16,2,2048]{2,1,0:T(2,128)(2,1)S(1)}, u32[]{:S(2)}, u32[]{:S(2)}) async-start(bf16[16,2,2048]{2,1,0:T(2,128)(2,1)} %reshape.379), calls=%async_computation.3 | async-start | bytes 262144 | tf_op jit(solution)/shard_map/all_to_all | solution.py:203
Sparse Core Ops, SparseCore 0:
  10.5 61.6 all-gather.10
  75.3 57.3 all-gather.8
  135.8 57.3 all-gather.12
  195.2 19.3 all-gather.14
where the time goes:
time: 401 us; the launch traced here: 393 us
  blocking collectives  139 us (35%)
  local copies, waits for them, and re-layouts  82.1 us (20%)
  matrix products  75.5 us (19%)
  waiting for transfers between devices  41 us (10%)
  other arithmetic  21.7 us (5%)
  starting transfers between devices  19.3 us (5%)
  between operations  13.6 us (3%)
    all_gather x2, blocking collectives, over_all(): lax.all_gather(part, axis, axis=dim, tiled=True)  45.8 us
    dynamic_slice x48, local copies, waits for them, and re-layouts, one_way(): final_state, across = lax.scan(advance, initial, stacked)  38.2 us
    all_gather x1, blocking collectives, body(): lax.all_gather(rank_forward.reshape(seq_local, tok_local, -1), 'sp', axis...  35.7 us
    dot_general x32, matrix products, advance(): jnp.einsum('hid,hiv->hdv', key_now, value_now, precision=precise)  30 us
    dot_general x32, matrix products, advance(): emitted = jnp.einsum('hid,hdv->hiv', query_now, carried, precision=precise)  29.4 us
    all_gather x1, blocking collectives, body(): lax.all_gather(rank_backward.reshape(seq_local, tok_local, -1), 'sp', axi...  29.1 us
    all_gather x1, blocking collectives, stacked_from(): pieces = lax.all_gather(pieces, axes[k])  28.4 us
    unnamed x43, local copies, waits for them, and re-layouts  15.8 us
  transfers between devices with their start and end apart: 8, of which 4 were waited for; matrix products, arithmetic and copies ran while one was open for 44% of the time, Pallas kernels for 0%

commit v1 on v0

v1 whole, which is shorter than its diff:
```python
import functools

import jax
import jax.numpy as jnp
from jax import lax
from jax.experimental import pallas as pl
from jax.experimental.pallas import tpu as pltpu
from jax.sharding import Mesh
from jax.sharding import PartitionSpec as P

DP = ("dp_0", "dp_1", "dp_2")
PLANE = ("dp_0", "dp_1")
HEAD = 32
HEADS = 16
WIDTH = 512
BLOCK = 64
LANES = 128
EPS = 1e-06
f32 = jnp.float32
bf16 = jnp.bfloat16


def dot(a, b):
    return jnp.dot(a, b, preferred_element_type=f32)


def dot_tn(a, b):
    return lax.dot_general(a, b, (((0,), (0,)), ((), ())), preferred_element_type=f32)


def dot_nt(a, b):
    return lax.dot_general(a, b, (((1,), (1,)), ((), ())), preferred_element_type=f32)


def halves(x):
    high = x.astype(bf16)
    return high, (x - high.astype(f32)).astype(bf16)


def grid_of(shape):
    return lax.broadcasted_iota(jnp.int32, shape, 0), lax.broadcasted_iota(jnp.int32, shape, 1)


def as_bf16(mask):
    return jnp.where(mask, 1.0, 0.0).astype(bf16)


def norm_kernel(tokens_ref, gain_ref, normed_ref):
    values = tokens_ref[...].astype(f32)
    scale = lax.rsqrt(jnp.mean(values * values, axis=-1, keepdims=True) + EPS)
    normed = (values * scale * gain_ref[...]).astype(bf16)
    for core in range(2):
        normed_ref[core] = jnp.concatenate(
            [normed[:, (2 * i + core) * 32 : (2 * i + core) * 32 + 32] for i in range(16)], axis=1
        )


def block_kernel(
    core_ref, normed_ref, own_ref, other_ref, up_ref, bias_ref,
    payload_ref, keys_ref, values_ref, running_ref,
):
    core = core_ref[0]
    length = BLOCK * HEADS
    projected = dot(normed_ref[core], own_ref[...]) + dot(normed_ref[1 - core], other_ref[...])
    rounded = projected.astype(bf16)
    keys = rounded[:, :WIDTH]
    values = rounded[:, WIDTH : 2 * WIDTH]
    ranks = rounded[:, 2 * WIDTH :]
    keys_ref[...] = keys
    values_ref[...] = values
    gates = dot(ranks, up_ref[...]) + bias_ref[...]
    rates = jax.nn.log_sigmoid(gates) * (2.0 / length)
    high, low = halves(rates)
    row, col = grid_of((128, 128))
    same = (row // BLOCK) == (col // BLOCK)

    def summed(mask, span):
        ones = as_bf16(mask)
        return dot(ones, high[:, span]) + dot(ones, low[:, span])

    fwd, bwd = slice(0, WIDTH), slice(WIDTH, 2 * WIDTH)
    running_ref[:, fwd] = summed(same & (col <= row), fwd)
    running_ref[:, bwd] = summed(same & (col >= row), bwd)
    keys32 = keys.astype(f32)
    remain = (
        (keys32 * jnp.exp(summed(same & (col > row), fwd))).astype(bf16),
        (keys32 * jnp.exp(summed(same & (col < row), bwd))).astype(bf16),
    )
    closing = 0.0
    for way, span in ((0, fwd), (1, bwd)):
        pick = as_bf16((col // HEAD) == 2 * way + row // BLOCK)
        closing = closing + dot_tn(high[:, span], pick) + dot_tn(low[:, span], pick)
    close_high, close_low = halves(closing)
    lane = lax.broadcasted_iota(jnp.int32, (WIDTH, LANES), 1)
    close_both = jnp.where(lane % 2 == 0, close_high.astype(f32), close_low.astype(f32))
    payload_ref[:, LANES:] = close_both.astype(bf16)
    diagonal = (row // HEAD) == (col // HEAD)
    erow, ecol = grid_of((4 * LANES, LANES))
    fold = as_bf16(((erow // LANES) * HEAD + erow % HEAD) == ecol)
    for group in range(4):
        lanes = slice(group * LANES, (group + 1) * LANES)
        parts = []
        for way in range(2):
            for seq in range(2):
                span = slice(seq * BLOCK, (seq + 1) * BLOCK)
                state = dot_tn(remain[way][span, lanes], values[span, lanes])
                parts.append(jnp.where(diagonal, state, 0.0).astype(bf16))
        folded = dot(jnp.concatenate(parts, axis=1), fold)
        payload_ref[lanes, :LANES] = folded.astype(bf16)


def scan_kernel(payload_ref, out_ref):
    row, col = grid_of((LANES, LANES))
    spread = as_bf16(((row // HEAD) == (col // HEAD)) & (row % HEAD < 2))
    closing = dot(payload_ref[:, LANES:], spread)
    decay = jnp.exp(closing)
    states = payload_ref[:, :LANES].astype(f32)
    lane = lax.broadcasted_iota(jnp.int32, (HEAD, LANES), 1)
    ahead = [None] * HEADS
    behind = [None] * HEADS

    def at(x, i):
        return x[i * HEAD : (i + 1) * HEAD, :]

    carried = jnp.zeros((HEAD, LANES), f32)
    for i in range(HEADS):
        ahead[i] = carried
        carried = at(decay, i) * carried + at(states, i)
    carried = jnp.zeros((HEAD, LANES), f32)
    for i in range(HEADS - 1, -1, -1):
        behind[i] = carried
        carried = at(decay, i) * carried + at(states, i)
    for i in range(HEADS):
        out_ref[i * HEAD : (i + 1) * HEAD, :] = jnp.where(
            lane < LANES // 2, ahead[i], behind[i]
        ).astype(bf16)


def query_kernel(
    core_ref, normed_ref, own_ref, other_ref, keys_ref, values_ref, running_ref,
    within_ref, queries_ref,
):
    core = core_ref[0]

    def weights(ref):
        both = jnp.concatenate([ref[:, 16:32, :WIDTH], ref[:, 16:32, WIDTH:]], axis=1)
        return both.reshape(WIDTH, WIDTH)

    projected = dot(normed_ref[core], weights(own_ref)) + dot(
        normed_ref[1 - core], weights(other_ref)
    )
    queries = projected.astype(bf16).astype(f32) * HEAD ** (-0.5)
    keys = keys_ref[...].astype(f32)
    decayed, inverse = [], []
    for way in range(2):
        running = running_ref[:, way * WIDTH : (way + 1) * WIDTH]
        decayed.append((queries * jnp.exp(running)).astype(bf16))
        inverse.append((keys * jnp.exp(-running)).astype(bf16))
        queries_ref[:, way * WIDTH : (way + 1) * WIDTH] = decayed[way]
    row, col = grid_of((4 * BLOCK, LANES))
    own_lanes = (row // BLOCK) == (col // HEAD)
    own_lanes_bf = as_bf16(own_lanes)
    srow, scol = grid_of((4 * BLOCK, BLOCK))
    lower = (srow % BLOCK) >= scol
    upper = (srow % BLOCK) <= scol
    for seq in range(2):
        span = slice(seq * BLOCK, (seq + 1) * BLOCK)
        for group in range(4):
            lanes = slice(group * LANES, (group + 1) * LANES)
            scores = 0.0
            for way, mask in ((0, lower), (1, upper)):
                one = decayed[way][span, lanes]
                stacked = jnp.concatenate([one] * 4, axis=0) * own_lanes_bf
                scores = scores + jnp.where(mask, dot_nt(stacked, inverse[way][span, lanes]), 0.0)
            spread = jnp.where(own_lanes, dot(scores.astype(bf16), values_ref[span, lanes]), 0.0)
            within_ref[span, lanes] = (
                spread[:BLOCK] + spread[BLOCK : 2 * BLOCK]
                + spread[2 * BLOCK : 3 * BLOCK] + spread[3 * BLOCK :]
            )


def out_kernel(core_ref, states_ref, within_ref, queries_ref, gain_ref, own_ref, other_ref, out_ref):
    core = core_ref[0]
    row, col = grid_of((LANES, LANES))
    diagonal = (row // HEAD) == (col // HEAD)
    rows = []
    for seq in range(2):
        span = slice(seq * BLOCK, (seq + 1) * BLOCK)
        pieces = []
        for group in range(4):
            lanes = slice(group * LANES, (group + 1) * LANES)
            total = within_ref[span, lanes]
            for way in range(2):
                widen = as_bf16(row == (2 * way + seq) * HEAD + col % HEAD)
                full = dot(states_ref[lanes, :], widen)
                full = jnp.where(diagonal, full, 0.0).astype(bf16)
                query = queries_ref[span, way * WIDTH + group * LANES : way * WIDTH + (group + 1) * LANES]
                total = total + dot(query, full)
            pieces.append(total)
        rows.append(jnp.concatenate(pieces, axis=1))
    combined = jnp.concatenate(rows, axis=0)
    high, low = halves(combined * combined)
    ones = as_bf16(diagonal)
    mean = jnp.concatenate(
        [
            dot(high[:, g * LANES : (g + 1) * LANES], ones)
            + dot(low[:, g * LANES : (g + 1) * LANES], ones)
            for g in range(4)
        ],
        axis=1,
    ) * (1.0 / HEAD)
    attended = (combined * lax.rsqrt(mean + EPS) * gain_ref[...]).astype(bf16)
    prow, pcol = grid_of((WIDTH, WIDTH))
    source = ((pcol % 256) // 16) * 32 + (pcol // 256) * 16 + pcol % 16
    shuffled = dot(attended, as_bf16(prow == source)).astype(bf16)
    first, second = shuffled[:, :256], shuffled[:, 256:]
    mine = jnp.where(core == 0, first, second)
    theirs = jnp.where(core == 0, second, first)
    out_ref[...] = (
        dot(mine, own_ref[:, :16, :].reshape(256, 1024))
        + dot(theirs, other_ref[:, :16, :].reshape(256, 1024))
    ).astype(bf16)


VMEM = pl.BlockSpec(memory_space=pltpu.VMEM)
SMEM = pl.BlockSpec(memory_space=pltpu.SMEM)


def call(kernel, outs, specs, cycles, *args):
    many = isinstance(outs, tuple)
    return pl.pallas_call(
        kernel,
        out_shape=outs,
        in_specs=specs,
        out_specs=(VMEM,) * len(outs) if many else VMEM,
        cost_estimate=pl.CostEstimate(flops=cycles, bytes_accessed=1 << 20, transcendentals=0),
        name=kernel.__name__,
    )(*args)


def spread_out(block):
    return jnp.broadcast_to(block[None], (16, *block.shape))


def swapped(x):
    return lax.ppermute(x, "dp_2", [(0, 1), (1, 0)])


def body(
    tokens, norm_gain, w_query, w_key, w_value, w_rank_forward, w_rank_backward,
    up_forward, up_backward, bias_forward, bias_backward, out_gain, w_out,
):
    seqs, toks, width = tokens.shape
    rows = seqs * toks
    shape = jax.ShapeDtypeStruct
    core = lax.axis_index("dp_2").astype(jnp.int32).reshape(1)
    first = jnp.concatenate(
        [w_key, w_value, w_rank_forward, w_rank_backward, jnp.zeros((32, 96), bf16)], axis=1
    )
    own = lax.all_to_all(spread_out(first), PLANE, 0, 0)
    other = swapped(own)
    normed = call(
        norm_kernel, shape((2, rows, 512), bf16), [VMEM, VMEM], 1 << 28,
        tokens.reshape(rows, width), norm_gain.reshape(1, width),
    )
    up = jnp.zeros((128, 1024), bf16)
    up = up.at[:16, :512].set(up_forward).at[16:32, 512:].set(up_backward)
    bias = jnp.concatenate([bias_forward, bias_backward]).reshape(1, 1024)
    payload, keys, values, running = call(
        block_kernel,
        (
            shape((WIDTH, 2 * LANES), bf16), shape((rows, WIDTH), bf16),
            shape((rows, WIDTH), bf16), shape((rows, 2 * WIDTH), f32),
        ),
        [SMEM] + [VMEM] * 5, 1 << 30,
        core, normed, own.reshape(512, 1152), other.reshape(512, 1152), up, bias,
    )
    inbound = lax.all_to_all(payload.reshape(HEADS, HEAD, 2 * LANES), "sp", 0, 0)
    second = jnp.concatenate(
        [w_out, jnp.concatenate([w_query[:16], w_query[16:]], axis=1)], axis=0
    )
    second, _ = lax.optimization_barrier((second, payload))
    own2 = lax.all_to_all(spread_out(second), PLANE, 0, 0)
    other2 = swapped(own2)
    states = call(
        scan_kernel, shape((WIDTH, LANES), bf16), [VMEM], 1 << 28,
        inbound.reshape(WIDTH, 2 * LANES),
    )
    returned = lax.all_to_all(states.reshape(HEADS, HEAD, LANES), "sp", 0, 0)
    within, queries = call(
        query_kernel,
        (shape((rows, WIDTH), f32), shape((rows, 2 * WIDTH), bf16)),
        [SMEM] + [VMEM] * 6, 1 << 30,
        core, normed, own2, other2, keys, values, running,
    )
    mixed = call(
        out_kernel, shape((rows, width), bf16), [SMEM] + [VMEM] * 6, 1 << 30,
        core, returned.reshape(WIDTH, LANES), within, queries,
        jnp.tile(out_gain, HEADS).reshape(1, WIDTH), own2, other2,
    )
    return mixed.reshape(seqs, toks, width)


def solution(mesh):
    finer = Mesh(mesh.devices.reshape(mesh.shape["sp"], 4, 4, 2), ("sp", "dp_0", "dp_1", "dp_2"))
    rows = P(DP, None)
    in_specs = (
        P(DP, "sp", None), P(), rows, rows, rows, rows, rows, P(), P(), P(), P(), P(), rows,
    )
    return jax.shard_map(
        body, mesh=finer, in_specs=in_specs, out_specs=P(DP, "sp", None), check_vma=False
    )
```

time: 401 us -> 123 us (0.31); the launches traced: 393 us -> 122 us
  blocking collectives: 139 us -> 45 us
  matrix products: 75.5 us -> 0 us
  local copies, waits for them, and re-layouts: 82.1 us -> 6.7 us
  other arithmetic: 21.7 us -> 0.61 us
  Pallas kernels: 0 us -> 16.6 us
  waiting for transfers between devices: 41 us -> 26 us
  between operations: 13.6 us -> 0.15 us
  starting transfers between devices: 19.3 us -> 27 us
    all_gather x5 -> x0, blocking collectives: 139 us -> none  [the longest x2 45.8 us: over_all(): lax.all_gather(part, axis, axis=dim, tiled=True)]
    dot_general x76 -> x0, matrix products: 75.5 us -> none  [the longest x32 30 us: advance(): jnp.einsum('hid,hiv->hdv', key_now, value_now, precision=precise)]
    all_to_all x0 -> x2, blocking collectives: none -> 45 us  [the longest x1 23.8 us: body(): own = lax.all_to_all(spread_out(first), PLANE, 0, 0)]
    dynamic_slice x50 -> x0, local copies, waits for them, and re-layouts: 39.7 us -> none  [the longest x48 38.2 us: one_way(): final_state, across = lax.scan(advance, initial, stacked)]
    pallas_call x0 -> x5, Pallas kernels: none -> 16.6 us  [call(): pl.pallas_call(kernel, out_shape=outs, in_specs=specs, out_specs=(VMEM,)...]
    another operation x3 -> x0, other arithmetic: 14.5 us -> none  [the longest x2 14.5 us: one_way(): running = jnp.cumsum(in_blocks(decay_rates), axis=2)]
    all_to_all x4 -> x2, waiting for transfers between devices: 38.9 us -> 25.9 us  [the longest x1 16.3 us: body(): lax.all_to_all(payload.reshape(HEADS, HEAD, 2 * LANES), 'sp', 0, 0)]
    unnamed x43 -> x30, local copies, waits for them, and re-layouts: 15.8 us -> 4.93 us
  transfers between devices with their start and end apart: 8 -> 4, of which waited for: 4 -> 3; matrix products, arithmetic and copies ran while one was open for 44% -> 1% of each run, Pallas kernels for 0% -> 7%
where the time goes in v1:
time: 123 us; the launch traced here: 122 us
  blocking collectives  45 us (37%)
  starting transfers between devices  27 us (22%)
  waiting for transfers between devices  26 us (21%)
  Pallas kernels  16.6 us (13%)
  local copies, waits for them, and re-layouts  6.7 us (5%)
    all_to_all x1, blocking collectives, body(): own = lax.all_to_all(spread_out(first), PLANE, 0, 0)  23.8 us
    all_to_all x1, blocking collectives, body(): own2 = lax.all_to_all(spread_out(second), PLANE, 0, 0)  21.2 us
    pallas_call x5, Pallas kernels, call(): pl.pallas_call(kernel, out_shape=outs, in_specs=specs, out_specs=(VMEM,)...  16.6 us
    all_to_all x1, waiting for transfers between devices, body(): lax.all_to_all(payload.reshape(HEADS, HEAD, 2 * LANES), 'sp', 0, 0)  16.3 us
    all_to_all x1, starting transfers between devices, body(): lax.all_to_all(payload.reshape(HEADS, HEAD, 2 * LANES), 'sp', 0, 0)  15.4 us
    all_to_all x1, waiting for transfers between devices, body(): returned = lax.all_to_all(states.reshape(HEADS, HEAD, LANES), 'sp', 0, 0)  9.61 us
    all_to_all x1, starting transfers between devices, body(): returned = lax.all_to_all(states.reshape(HEADS, HEAD, LANES), 'sp', 0, 0)  7.58 us
    unnamed x30, local copies, waits for them, and re-layouts  4.93 us
  transfers between devices with their start and end apart: 4, of which 3 were waited for; matrix products, arithmetic and copies ran while one was open for 1% of the time, Pallas kernels for 7%

profile of v1, /device:TPU:24, one launch (start us, length us, event | category | flops | bytes accessed | tf_op | source)
XLA Modules:
  0.0 122.0 jit_solution(14375955860693910567)
XLA Ops:
  0.0 0.8 copy.14
  0.8 0.8 copy.15
  1.5 0.9 concatenate.16
  2.4 0.1 broadcast_in_dim.7
  2.5 0.0 copy-start.7
  2.5 23.8 %all_to_all.20 = bf16[16,32,1152]{2,1,0:T(8,128)(2,1)S(1)} all-to-all(bf16[16,32,1152]{2,1,0:T(8,128)(2,1)S(1)} %broadcast_in_dim.7), channel_id=1, replica_groups=mesh['sp'=16,'dp_0'=4,'dp_1'=4,'dp_2'=2] {'dp_0','dp_1'}, dimensions={0} | all-to-all | bytes 2359296 | tf_op jit(solution)/shard_map/all_to_all | solution.py:260
  26.3 0.0 copy-start.5
  26.3 0.0 copy-start.6
  26.3 2.1 %collective-permute-start = (bf16[16,32,1152]{2,1,0:T(8,128)(2,1)S(1)}, bf16[16,32,1152]{2,1,0:T(8,128)(2,1)S(1)}, u32[]{:S(2)}, u32[]{:S(2)}) collective-permute-start(bf16[16,32,1152]{2,1,0:T(8,128)(2,1)S(1)} %all_to_all.20), channel_id=1, source_target_pairs={{0,1},{1,0},{2,3},{3,2},{4,5},{5,4},{6,7},{7,6},{8,9},{9,8},{10,11... | collective-permute-start | bytes 3538952 | tf_op jit(solution)/shard_map/ppermute | solution.py:246
  28.5 2.0 %norm_kernel.1.normed_ref = bf16[2,128,512]{2,1,0:T(8,128)(2,1)} custom-call(bf16[128,1024]{1,0:T(8,128)(2,1)} %bitcast.17, f32[1,1024]{1,0:T(1,128)} %bitcast.18), custom_call_target="tpu_custom_call" | custom-call | flops 268435456 | bytes 1048576 | tf_op jit(solution)/shard_map/norm_kernel/pallas_call | solution.py:231
  30.5 0.6 pad_maximum_fusion
  31.1 0.0 copy-done.5
  31.1 0.1 collective-permute-done
  31.2 0.5 copy-done.3
  31.8 0.5 copy-done.12
  32.2 4.8 %block_kernel.1 = (bf16[512,256]{1,0:T(8,128)(2,1)}, bf16[128,512]{1,0:T(8,128)(2,1)}, bf16[128,512]{1,0:T(8,128)(2,1)}, f32[128,1024]{1,0:T(8,128)}) custom-call(s32[1]{0:T(128)} %bitcast.core_ref, bf16[2,128,512]{2,1,0:T(8,128)(2,1)} %norm_kernel.1.normed_ref, bf16[512,1152]{1,0:T(8,128)(2,1)} %bitcast.11, bf16[512,1152]{1,0:T(8,128)(2,1)} %bitcast.16, ...), custom_call_target="tpu_custom_call" | custom-call | flops 1073741824 | bytes 1048576 | tf_op jit(solution)/shard_map/block_kernel/pallas_call | solution.py:231
  37.1 0.1 broadcast_in_dim.8
  37.2 21.2 %all_to_all.21.own_ref = bf16[16,32,1024]{2,1,0:T(8,128)(2,1)S(1)} all-to-all(bf16[16,32,1024]{2,1,0:T(8,128)(2,1)S(1)} %broadcast_in_dim.8), channel_id=1, replica_groups=mesh['sp'=16,'dp_0'=4,'dp_1'=4,'dp_2'=2] {'dp_0','dp_1'}, dimensions={0} | all-to-all | bytes 2097152 | tf_op jit(solution)/shard_map/all_to_all | solution.py:283
  58.4 15.4 %all-to-all-start.1 = ((bf16[16,32,256]{2,1,0:T(8,128)(2,1)}), bf16[16,32,256]{2,1,0:T(8,128)(2,1)S(1)}, u32[]{:S(2)}, u32[]{:S(2)}) async-start(bf16[16,32,256]{2,1,0:T(8,128)(2,1)} %bitcast.6), calls=%async_computation.1 | async-start | bytes 524288 | tf_op jit(solution)/shard_map/all_to_all | solution.py:278
  73.8 1.9 %collective-permute-start.1 = (bf16[16,32,1024]{2,1,0:T(8,128)(2,1)S(1)}, bf16[16,32,1024]{2,1,0:T(8,128)(2,1)S(1)}, u32[]{:S(2)}, u32[]{:S(2)}) collective-permute-start(bf16[16,32,1024]{2,1,0:T(8,128)(2,1)S(1)} %all_to_all.21.own_ref), channel_id=1, source_target_pairs={{0,1},{1,0},{2,3},{3,2},{4,5},{5,4},{6,7},{7,6},{8,9},{9,8},{10,11... | collective-permute-start | bytes 3145736 | tf_op jit(solution)/shard_map/ppermute | solution.py:246
  75.8 16.3 %all-to-all-done.1 = bf16[16,32,256]{2,1,0:T(8,128)(2,1)S(1)} async-done(((bf16[16,32,256]{2,1,0:T(8,128)(2,1)}), bf16[16,32,256]{2,1,0:T(8,128)(2,1)S(1)}, u32[]{:S(2)}, u32[]{:S(2)}) %all-to-all-start.1) | async-done | bytes 262176 | tf_op jit(solution)/shard_map/all_to_all | solution.py:278
  92.1 0.7 copy-done.2
  92.8 1.8 %scan_kernel.1 = bf16[512,128]{1,0:T(8,128)(2,1)} custom-call(bf16[512,256]{1,0:T(8,128)(2,1)} %bitcast.12), custom_call_target="tpu_custom_call" | custom-call | flops 268435456 | bytes 1048576 | tf_op jit(solution)/shard_map/scan_kernel/pallas_call | solution.py:231
  94.6 7.6 %all-to-all-start.2 = ((bf16[16,32,128]{2,1,0:T(8,128)(2,1)}), bf16[16,32,128]{2,1,0:T(8,128)(2,1)S(1)}, u32[]{:S(2)}, u32[]{:S(2)}) async-start(bf16[16,32,128]{2,1,0:T(8,128)(2,1)} %bitcast.14), calls=%async_computation.2 | async-start | bytes 262144 | tf_op jit(solution)/shard_map/all_to_all | solution.py:289
  102.2 0.0 copy-done.11
  102.2 0.7 reshape_tile.3.gain_ref
  102.9 0.0 collective-permute-done.1.other_ref
  102.9 1.0 copy-done.13
  103.8 4.2 %query_kernel.1 = (f32[128,512]{1,0:T(8,128)}, bf16[128,1024]{1,0:T(8,128)(2,1)}) custom-call(s32[1]{0:T(128)} %bitcast.core_ref, bf16[2,128,512]{2,1,0:T(8,128)(2,1)} %norm_kernel.1.normed_ref, bf16[16,32,1024]{2,1,0:T(8,128)(2,1)} %copy-done.1, bf16[16,32,1024]{2,1,0:T(8,128)(2,1)} %copy-done.13, bf16[128,512]{1,0:T(8,128)(2,1)} %get-tuple-element.38.keys_ref, ...), custom_call_target="tpu_custom_call" | custom-call | flops 1073741824 | bytes 1048576 | tf_op jit(solution)/shard_map/query_kernel/pallas_call | solution.py:231
  108.1 9.6 %all-to-all-done.2 = bf16[16,32,128]{2,1,0:T(8,128)(2,1)S(1)} async-done(((bf16[16,32,128]{2,1,0:T(8,128)(2,1)}), bf16[16,32,128]{2,1,0:T(8,128)(2,1)S(1)}, u32[]{:S(2)}, u32[]{:S(2)}) %all-to-all-start.2) | async-done | bytes 131104 | tf_op jit(solution)/shard_map/all_to_all | solution.py:289
  117.7 0.7 copy-done.4
  118.4 3.7 %out_kernel.1 = bf16[128,1024]{1,0:T(8,128)(2,1)} custom-call(s32[1]{0:T(128)} %bitcast.core_ref, bf16[512,128]{1,0:T(8,128)(2,1)} %bitcast.13, f32[128,512]{1,0:T(8,128)} %get-tuple-element.41.within_ref, bf16[128,1024]{1,0:T(8,128)(2,1)} %get-tuple-element.42.queries_ref, f32[1,512]{1,0:T(1,128)} %reshape_tile.3.gain_ref, bf16[16,32,1024]{2,1,0:T(8,128)(2,1)} %copy-done.1, ...), custom_call_target="tpu_custom_call" | custom-call | flops 1073741824 | bytes 1048576 | tf_op jit(solution)/shard_map/out_kernel/pallas_call | solution.py:231
  (24 shorter events, 0.1 us)
Async XLA Ops:
  2.5 25.9 %copy-start.7 = (bf16[16,512]{1,0:T(8,128)(2,1)S(1)}, bf16[16,512]{1,0:T(8,128)(2,1)}, u32[]{:S(2)}) copy-start(bf16[16,512]{1,0:T(8,128)(2,1)} %param.24) | copy-start | bytes 49156
  26.3 4.9 %copy-start = (bf16[16,32,1152]{2,1,0:T(8,128)(2,1)}, bf16[16,32,1152]{2,1,0:T(8,128)(2,1)S(1)}, u32[]{:S(2)}) copy-start(bf16[16,32,1152]{2,1,0:T(8,128)(2,1)S(1)} %all_to_all.20) | copy-start | bytes 3538948
  26.3 4.1 %copy-start.9 = (f32[512]{0:T(512)S(1)}, f32[512]{0:T(512)}, u32[]{:S(2)}) copy-start(f32[512]{0:T(512)} %param.27) | copy-start | bytes 6148
  26.3 4.1 %copy-start.10 = (f32[512]{0:T(512)S(1)}, f32[512]{0:T(512)}, u32[]{:S(2)}) copy-start(f32[512]{0:T(512)} %param.26) | copy-start | bytes 6148
  26.3 4.7 %copy-start.8 = (bf16[16,512]{1,0:T(8,128)(2,1)S(1)}, bf16[16,512]{1,0:T(8,128)(2,1)}, u32[]{:S(2)}) copy-start(bf16[16,512]{1,0:T(8,128)(2,1)} %param.25) | copy-start | bytes 49156
  26.3 4.7 %copy-start.5 = (bf16[32,512]{1,0:T(8,128)(2,1)S(1)}, bf16[32,512]{1,0:T(8,128)(2,1)}, u32[]{:S(2)}) copy-start(bf16[32,512]{1,0:T(8,128)(2,1)} %param.19) | copy-start | bytes 98308
  26.3 4.7 %copy-start.6 = (bf16[16,1024]{1,0:T(8,128)(2,1)S(1)}, bf16[16,1024]{1,0:T(8,128)(2,1)}, u32[]{:S(2)}) copy-start(bf16[16,1024]{1,0:T(8,128)(2,1)} %param.29) | copy-start | bytes 98308
  26.3 4.9 %collective-permute-start = (bf16[16,32,1152]{2,1,0:T(8,128)(2,1)S(1)}, bf16[16,32,1152]{2,1,0:T(8,128)(2,1)S(1)}, u32[]{:S(2)}, u32[]{:S(2)}) collective-permute-start(bf16[16,32,1152]{2,1,0:T(8,128)(2,1)S(1)} %all_to_all.20), channel_id=1, source_target_pairs={{0,1},{1,0},{2,3},{3,2},{4,5},{5,4},{6,7},{7,6},{8,9},{9,8},{10,11... | collective-permute-start | bytes 3538952 | tf_op jit(solution)/shard_map/ppermute | solution.py:246
  31.1 0.7 copy-start.3
  31.2 1.0 copy-start.12
  58.4 44.4 %copy-start.1 = (bf16[16,32,1024]{2,1,0:T(8,128)(2,1)}, bf16[16,32,1024]{2,1,0:T(8,128)(2,1)S(1)}, u32[]{:S(2)}) copy-start(bf16[16,32,1024]{2,1,0:T(8,128)(2,1)S(1)} %all_to_all.21.own_ref) | copy-start | bytes 3145732
  58.4 43.7 %copy-start.11 = (f32[32]{0:T(128)S(1)}, f32[32]{0:T(128)}, u32[]{:S(2)}) copy-start(f32[32]{0:T(128)} %param.28) | copy-start | bytes 388
  58.4 33.6 %all-to-all-start.1 = ((bf16[16,32,256]{2,1,0:T(8,128)(2,1)}), bf16[16,32,256]{2,1,0:T(8,128)(2,1)S(1)}, u32[]{:S(2)}, u32[]{:S(2)}) async-start(bf16[16,32,256]{2,1,0:T(8,128)(2,1)} %bitcast.6), calls=%async_computation.1 | async-start | bytes 524288 | tf_op jit(solution)/shard_map/all_to_all | solution.py:278
  73.8 29.0 %collective-permute-start.1 = (bf16[16,32,1024]{2,1,0:T(8,128)(2,1)S(1)}, bf16[16,32,1024]{2,1,0:T(8,128)(2,1)S(1)}, u32[]{:S(2)}, u32[]{:S(2)}) collective-permute-start(bf16[16,32,1024]{2,1,0:T(8,128)(2,1)S(1)} %all_to_all.21.own_ref), channel_id=1, source_target_pairs={{0,1},{1,0},{2,3},{3,2},{4,5},{5,4},{6,7},{7,6},{8,9},{9,8},{10,11... | collective-permute-start | bytes 3145736 | tf_op jit(solution)/shard_map/ppermute | solution.py:246
  92.1 0.7 copy-start.2
  94.6 23.1 %all-to-all-start.2 = ((bf16[16,32,128]{2,1,0:T(8,128)(2,1)}), bf16[16,32,128]{2,1,0:T(8,128)(2,1)S(1)}, u32[]{:S(2)}, u32[]{:S(2)}) async-start(bf16[16,32,128]{2,1,0:T(8,128)(2,1)} %bitcast.14), calls=%async_computation.2 | async-start | bytes 262144 | tf_op jit(solution)/shard_map/all_to_all | solution.py:289
  102.9 1.0 copy-start.13
  117.7 0.7 copy-start.4

commit v2 on v1

--- a/solution.py
+++ b/solution.py
@@ -1,5 +1,3 @@
-import functools
-
 import jax
 import jax.numpy as jnp
 from jax import lax
@@ -45,6 +43,37 @@
     return jnp.where(mask, 1.0, 0.0).astype(bf16)
 
 
+def pack_kernel(key_ref, value_ref, forward_ref, backward_ref, out_ref):
+    block = jnp.concatenate(
+        [key_ref[...], value_ref[...], forward_ref[...], backward_ref[...], jnp.zeros((32, 96), bf16)],
+        axis=1,
+    )
+    for i in range(16):
+        out_ref[i] = block
+
+
+def join_kernel(query_ref, query_in_ref, out_ref, out_in_ref, queries_ref, outs_ref):
+    count = query_ref.shape[0]
+    queries_ref[:count] = query_ref[...]
+    queries_ref[count:] = query_in_ref[...]
+    outs_ref[:count] = out_ref[...]
+    outs_ref[count:] = out_in_ref[...]
+
+
+def slot_of(index, axis):
+    apart = index ^ lax.axis_index(axis)
+    return apart ^ (apart >> 1)
+
+
+def in_order(ref, major, minor):
+    pieces = []
+    for y in range(4):
+        for x in range(4):
+            at = {"dp_0": slot_of(y, "dp_0"), "dp_1": slot_of(x, "dp_1")}
+            pieces.append(ref[at[major] * 4 + at[minor]])
+    return jnp.concatenate(pieces, axis=0)
+
+
 def norm_kernel(tokens_ref, gain_ref, normed_ref):
     values = tokens_ref[...].astype(f32)
     scale = lax.rsqrt(jnp.mean(values * values, axis=-1, keepdims=True) + EPS)
@@ -56,10 +85,10 @@
 
 
 def block_kernel(
-    core_ref, normed_ref, own_ref, other_ref, up_ref, bias_ref,
-    payload_ref, keys_ref, values_ref, running_ref,
+    normed_ref, own_ref, other_ref, up_forward_ref, up_backward_ref,
+    bias_forward_ref, bias_backward_ref, payload_ref, keys_ref, values_ref, running_ref,
 ):
-    core = core_ref[0]
+    core = lax.axis_index("dp_2")
     length = BLOCK * HEADS
     projected = dot(normed_ref[core], own_ref[...]) + dot(normed_ref[1 - core], other_ref[...])
     rounded = projected.astype(bf16)
@@ -68,7 +97,13 @@
     ranks = rounded[:, 2 * WIDTH :]
     keys_ref[...] = keys
     values_ref[...] = values
-    gates = dot(ranks, up_ref[...]) + bias_ref[...]
+    gates = jnp.concatenate(
+        [
+            dot(ranks[:, :16], up_forward_ref[...]) + bias_forward_ref[...],
+            dot(ranks[:, 16:32], up_backward_ref[...]) + bias_backward_ref[...],
+        ],
+        axis=1,
+    )
     rates = jax.nn.log_sigmoid(gates) * (2.0 / length)
     high, low = halves(rates)
     row, col = grid_of((128, 128))
@@ -83,8 +118,8 @@
     running_ref[:, bwd] = summed(same & (col >= row), bwd)
     keys32 = keys.astype(f32)
     remain = (
-        (keys32 * jnp.exp(summed(same & (col > row), fwd))).astype(bf16),
-        (keys32 * jnp.exp(summed(same & (col < row), bwd))).astype(bf16),
+        halves(keys32 * jnp.exp(summed(same & (col > row), fwd))),
+        halves(keys32 * jnp.exp(summed(same & (col < row), bwd))),
     )
     closing = 0.0
     for way, span in ((0, fwd), (1, bwd)):
@@ -103,7 +138,10 @@
         for way in range(2):
             for seq in range(2):
                 span = slice(seq * BLOCK, (seq + 1) * BLOCK)
-                state = dot_tn(remain[way][span, lanes], values[span, lanes])
+                value = values[span, lanes]
+                state = dot_tn(remain[way][0][span, lanes], value) + dot_tn(
+                    remain[way][1][span, lanes], value
+                )
                 parts.append(jnp.where(diagonal, state, 0.0).astype(bf16))
         folded = dot(jnp.concatenate(parts, axis=1), fold)
         payload_ref[lanes, :LANES] = folded.astype(bf16)
@@ -136,27 +174,32 @@
         ).astype(bf16)
 
 
+def prepare_kernel(keys_ref, running_ref, inverse_ref, decay_ref):
+    keys = keys_ref[...].astype(f32)
+    for way in range(2):
+        lanes = slice(way * WIDTH, (way + 1) * WIDTH)
+        running = running_ref[:, lanes]
+        inverse_ref[:, lanes] = (keys * jnp.exp(-running)).astype(bf16)
+        decay_ref[:, lanes] = jnp.exp(running)
+
+
 def query_kernel(
-    core_ref, normed_ref, own_ref, other_ref, keys_ref, values_ref, running_ref,
-    within_ref, queries_ref,
+    normed_ref, own_ref, other_ref, inverse_ref, values_ref, decay_ref,
+    within_ref, high_ref, low_ref,
 ):
-    core = core_ref[0]
-
-    def weights(ref):
-        both = jnp.concatenate([ref[:, 16:32, :WIDTH], ref[:, 16:32, WIDTH:]], axis=1)
-        return both.reshape(WIDTH, WIDTH)
-
-    projected = dot(normed_ref[core], weights(own_ref)) + dot(
-        normed_ref[1 - core], weights(other_ref)
+    core = lax.axis_index("dp_2")
+
+    projected = dot(normed_ref[core], in_order(own_ref, "dp_1", "dp_0")) + dot(
+        normed_ref[1 - core], in_order(other_ref, "dp_1", "dp_0")
     )
     queries = projected.astype(bf16).astype(f32) * HEAD ** (-0.5)
-    keys = keys_ref[...].astype(f32)
-    decayed, inverse = [], []
+    decayed = []
     for way in range(2):
-        running = running_ref[:, way * WIDTH : (way + 1) * WIDTH]
-        decayed.append((queries * jnp.exp(running)).astype(bf16))
-        inverse.append((keys * jnp.exp(-running)).astype(bf16))
-        queries_ref[:, way * WIDTH : (way + 1) * WIDTH] = decayed[way]
+        lanes = slice(way * WIDTH, (way + 1) * WIDTH)
+        high, low = halves(queries * decay_ref[:, lanes])
+        decayed.append(high)
+        high_ref[:, lanes] = high
+        low_ref[:, lanes] = low
     row, col = grid_of((4 * BLOCK, LANES))
     own_lanes = (row // BLOCK) == (col // HEAD)
     own_lanes_bf = as_bf16(own_lanes)
@@ -170,8 +213,9 @@
             scores = 0.0
             for way, mask in ((0, lower), (1, upper)):
                 one = decayed[way][span, lanes]
+                wide = slice(way * WIDTH + group * LANES, way * WIDTH + (group + 1) * LANES)
                 stacked = jnp.concatenate([one] * 4, axis=0) * own_lanes_bf
-                scores = scores + jnp.where(mask, dot_nt(stacked, inverse[way][span, lanes]), 0.0)
+                scores = scores + jnp.where(mask, dot_nt(stacked, inverse_ref[span, wide]), 0.0)
             spread = jnp.where(own_lanes, dot(scores.astype(bf16), values_ref[span, lanes]), 0.0)
             within_ref[span, lanes] = (
                 spread[:BLOCK] + spread[BLOCK : 2 * BLOCK]
@@ -179,8 +223,10 @@
             )
 
 
-def out_kernel(core_ref, states_ref, within_ref, queries_ref, gain_ref, own_ref, other_ref, out_ref):
-    core = core_ref[0]
+def out_kernel(
+    states_ref, within_ref, high_ref, low_ref, gain_ref, own_ref, other_ref, out_ref
+):
+    core = lax.axis_index("dp_2")
     row, col = grid_of((LANES, LANES))
     diagonal = (row // HEAD) == (col // HEAD)
     rows = []
@@ -194,8 +240,8 @@
                 widen = as_bf16(row == (2 * way + seq) * HEAD + col % HEAD)
                 full = dot(states_ref[lanes, :], widen)
                 full = jnp.where(diagonal, full, 0.0).astype(bf16)
-                query = queries_ref[span, way * WIDTH + group * LANES : way * WIDTH + (group + 1) * LANES]
-                total = total + dot(query, full)
+                wide = slice(way * WIDTH + group * LANES, way * WIDTH + (group + 1) * LANES)
+                total = total + dot(high_ref[span, wide], full) + dot(low_ref[span, wide], full)
             pieces.append(total)
         rows.append(jnp.concatenate(pieces, axis=1))
     combined = jnp.concatenate(rows, axis=0)
@@ -217,13 +263,12 @@
     mine = jnp.where(core == 0, first, second)
     theirs = jnp.where(core == 0, second, first)
     out_ref[...] = (
-        dot(mine, own_ref[:, :16, :].reshape(256, 1024))
-        + dot(theirs, other_ref[:, :16, :].reshape(256, 1024))
+        dot(mine, in_order(own_ref, "dp_0", "dp_1"))
+        + dot(theirs, in_order(other_ref, "dp_0", "dp_1"))
     ).astype(bf16)
 
 
 VMEM = pl.BlockSpec(memory_space=pltpu.VMEM)
-SMEM = pl.BlockSpec(memory_space=pltpu.SMEM)
 
 
 def call(kernel, outs, specs, cycles, *args):
@@ -234,12 +279,8 @@
         in_specs=specs,
         out_specs=(VMEM,) * len(outs) if many else VMEM,
         cost_estimate=pl.CostEstimate(flops=cycles, bytes_accessed=1 << 20, transcendentals=0),
-        name=kernel.__name__,
+        compiler_params=pltpu.CompilerParams(vmem_limit_bytes=16 << 20),
     )(*args)
-
-
-def spread_out(block):
-    return jnp.broadcast_to(block[None], (16, *block.shape))
 
 
 def swapped(x):
@@ -253,50 +294,68 @@
     seqs, toks, width = tokens.shape
     rows = seqs * toks
     shape = jax.ShapeDtypeStruct
-    core = lax.axis_index("dp_2").astype(jnp.int32).reshape(1)
-    first = jnp.concatenate(
-        [w_key, w_value, w_rank_forward, w_rank_backward, jnp.zeros((32, 96), bf16)], axis=1
-    )
-    own = lax.all_to_all(spread_out(first), PLANE, 0, 0)
+    send = call(
+        pack_kernel, shape((16, 32, 1152), bf16), [VMEM] * 4, 1 << 26,
+        w_key, w_value, w_rank_forward, w_rank_backward,
+    )
+    own = lax.all_to_all(send, PLANE, 0, 0)
     other = swapped(own)
     normed = call(
         norm_kernel, shape((2, rows, 512), bf16), [VMEM, VMEM], 1 << 28,
         tokens.reshape(rows, width), norm_gain.reshape(1, width),
     )
-    up = jnp.zeros((128, 1024), bf16)
-    up = up.at[:16, :512].set(up_forward).at[16:32, 512:].set(up_backward)
-    bias = jnp.concatenate([bias_forward, bias_backward]).reshape(1, 1024)
+    query_blocks, out_blocks = w_query[None], w_out[None]
+
+    def widen(query_axis, out_axis, flip):
+        pairs = [(i, i ^ flip) for i in range(4)]
+        query_in = lax.ppermute(query_blocks, query_axis, pairs)
+        out_in = lax.ppermute(out_blocks, out_axis, pairs)
+        count = 2 * query_blocks.shape[0]
+        return call(
+            join_kernel, (shape((count, 32, 512), bf16), shape((count, 16, 1024), bf16)),
+            [VMEM] * 4, 1 << 26, query_blocks, query_in, out_blocks, out_in,
+        )
+
+    query_blocks, out_blocks = widen("dp_0", "dp_1", 1)
+    query_blocks, out_blocks = widen("dp_0", "dp_1", 3)
+    query_blocks, out_blocks = widen("dp_1", "dp_0", 1)
+    query_blocks, out_blocks = widen("dp_1", "dp_0", 3)
     payload, keys, values, running = call(
         block_kernel,
         (
             shape((WIDTH, 2 * LANES), bf16), shape((rows, WIDTH), bf16),
             shape((rows, WIDTH), bf16), shape((rows, 2 * WIDTH), f32),
         ),
-        [SMEM] + [VMEM] * 5, 1 << 30,
-        core, normed, own.reshape(512, 1152), other.reshape(512, 1152), up, bias,
+        [VMEM] * 7, 1 << 30,
+        normed, own.reshape(512, 1152), other.reshape(512, 1152), up_forward, up_backward,
+        bias_forward.reshape(1, WIDTH), bias_backward.reshape(1, WIDTH),
     )
     inbound = lax.all_to_all(payload.reshape(HEADS, HEAD, 2 * LANES), "sp", 0, 0)
-    second = jnp.concatenate(
-        [w_out, jnp.concatenate([w_query[:16], w_query[16:]], axis=1)], axis=0
-    )
-    second, _ = lax.optimization_barrier((second, payload))
-    own2 = lax.all_to_all(spread_out(second), PLANE, 0, 0)
-    other2 = swapped(own2)
+    inverse, decay = call(
+        prepare_kernel,
+        (shape((rows, 2 * WIDTH), bf16), shape((rows, 2 * WIDTH), f32)),
+        [VMEM] * 2, 1 << 28, keys, running,
+    )
+    query_other = swapped(query_blocks)
+    out_other = swapped(out_blocks)
     states = call(
         scan_kernel, shape((WIDTH, LANES), bf16), [VMEM], 1 << 28,
         inbound.reshape(WIDTH, 2 * LANES),
     )
     returned = lax.all_to_all(states.reshape(HEADS, HEAD, LANES), "sp", 0, 0)
-    within, queries = call(
+    within, high, low = call(
         query_kernel,
-        (shape((rows, WIDTH), f32), shape((rows, 2 * WIDTH), bf16)),
-        [SMEM] + [VMEM] * 6, 1 << 30,
-        core, normed, own2, other2, keys, values, running,
+        (
+            shape((rows, WIDTH), f32), shape((rows, 2 * WIDTH), bf16),
+            shape((rows, 2 * WIDTH), bf16),
+        ),
+        [VMEM] * 6, 1 << 30,
+        normed, query_blocks, query_other, inverse, values, decay,
     )
     mixed = call(
-        out_kernel, shape((rows, width), bf16), [SMEM] + [VMEM] * 6, 1 << 30,
-        core, returned.reshape(WIDTH, LANES), within, queries,
-        jnp.tile(out_gain, HEADS).reshape(1, WIDTH), own2, other2,
+        out_kernel, shape((rows, width), bf16), [VMEM] * 7, 1 << 30,
+        returned.reshape(WIDTH, LANES), within, high, low,
+        jnp.tile(out_gain, HEADS).reshape(1, WIDTH), out_blocks, out_other,
     )
     return mixed.reshape(seqs, toks, width)
 
@@ -307,6 +366,7 @@
     in_specs = (
         P(DP, "sp", None), P(), rows, rows, rows, rows, rows, P(), P(), P(), P(), P(), rows,
     )
+
     return jax.shard_map(
         body, mesh=finer, in_specs=in_specs, out_specs=P(DP, "sp", None), check_vma=False
     )

time: 123 us -> 127 us (1.033)
  starting transfers between devices: 27 us -> 56.6 us
  blocking collectives: 45 us -> 23.6 us
  Pallas kernels: 16.6 us -> 9.31 us
  waiting for transfers between devices: 26 us -> 32.6 us
  local copies, waits for them, and re-layouts: 6.7 us -> 3.19 us
    ppermute x0 -> x8, starting transfers between devices: none -> 23.4 us  [the longest x4 11.9 us: widen(): out_in = lax.ppermute(out_blocks, out_axis, pairs)]
    all_to_all x2 -> x1, blocking collectives: 45 us -> 23.6 us  [body(): own = lax.all_to_all(send, PLANE, 0, 0)]
    ppermute x0 -> x8, waiting for transfers between devices: none -> 17.6 us  [the longest x4 11.6 us: widen(): out_in = lax.ppermute(out_blocks, out_axis, pairs)]
    all_to_all x1, waiting for transfers between devices: 16.3 us -> 0.01 us  [body(): lax.all_to_all(payload.reshape(HEADS, HEAD, 2 * LANES), 'sp', 0, 0)]
    pallas_call x5 -> x11, Pallas kernels: 16.6 us -> 9.31 us  [call(): pl.pallas_call(kernel, out_shape=outs, in_specs=specs, out_specs=(VMEM,)...]
    all_to_all x1, starting transfers between devices: 7.58 us -> 12 us  [body(): returned = lax.all_to_all(states.reshape(HEADS, HEAD, LANES), 'sp', 0, 0)]
    all_to_all x1, waiting for transfers between devices: 9.61 us -> 12.5 us  [body(): returned = lax.all_to_all(states.reshape(HEADS, HEAD, LANES), 'sp', 0, 0)]
    ppermute x2 -> x3, waiting for transfers between devices: 0.12 us -> 2.46 us  [swapped(): return lax.ppermute(x, 'dp_2', [(0, 1), (1, 0)])]
  transfers between devices with their start and end apart: 4 -> 13, of which waited for: 3 -> 10; matrix products, arithmetic and copies ran while one was open for 1% -> 0% of each run, Pallas kernels for 7% -> 3%
where the time goes in v2:
time: 127 us; the launch traced here: 126 us
  starting transfers between devices  56.6 us (45%)
  waiting for transfers between devices  32.6 us (26%)
  blocking collectives  23.6 us (19%)
  Pallas kernels  9.31 us (7%)
  local copies, waits for them, and re-layouts  3.19 us (3%)
    all_to_all x1, blocking collectives, body(): own = lax.all_to_all(send, PLANE, 0, 0)  23.6 us
    all_to_all x1, starting transfers between devices, body(): lax.all_to_all(payload.reshape(HEADS, HEAD, 2 * LANES), 'sp', 0, 0)  14.9 us
    all_to_all x1, waiting for transfers between devices, body(): returned = lax.all_to_all(states.reshape(HEADS, HEAD, LANES), 'sp', 0, 0)  12.5 us
    all_to_all x1, starting transfers between devices, body(): returned = lax.all_to_all(states.reshape(HEADS, HEAD, LANES), 'sp', 0, 0)  12 us
    ppermute x4, starting transfers between devices, widen(): out_in = lax.ppermute(out_blocks, out_axis, pairs)  11.9 us
    ppermute x4, waiting for transfers between devices, widen(): out_in = lax.ppermute(out_blocks, out_axis, pairs)  11.6 us
    ppermute x4, starting transfers between devices, widen(): query_in = lax.ppermute(query_blocks, query_axis, pairs)  11.5 us
    pallas_call x11, Pallas kernels, call(): pl.pallas_call(kernel, out_shape=outs, in_specs=specs, out_specs=(VMEM,)...  9.31 us
  transfers between devices with their start and end apart: 13, of which 10 were waited for; matrix products, arithmetic and copies ran while one was open for 0% of the time, Pallas kernels for 3%

profile of v2, /device:TPU:24, one launch (start us, length us, event | category | flops | bytes accessed | tf_op | source)
XLA Modules:
  0.0 125.6 jit_solution(10410627668345370497)
XLA Ops:
  0.0 0.8 copy.14.forward_ref
  0.8 0.8 copy.15.backward_ref
  1.5 0.8 copy-done
  2.3 0.8 copy-done.1
  3.2 23.6 %all_to_all.15 = bf16[16,32,1152]{2,1,0:T(8,128)(2,1)S(1)} all-to-all(bf16[16,32,1152]{2,1,0:T(8,128)(2,1)S(1)} %shard_map.128), channel_id=1, replica_groups=mesh['sp'=16,'dp_0'=4,'dp_1'=4,'dp_2'=2] {'dp_0','dp_1'}, dimensions={0} | all-to-all | bytes 2359296 | tf_op jit(solution)/shard_map/all_to_all | solution.py:301
  26.9 1.9 %collective-permute-start = (bf16[16,32,1152]{2,1,0:T(8,128)(2,1)S(1)}, bf16[16,32,1152]{2,1,0:T(8,128)(2,1)S(1)}, u32[]{:S(2)}, u32[]{:S(2)}) collective-permute-start(bf16[16,32,1152]{2,1,0:T(8,128)(2,1)S(1)} %all_to_all.15), channel_id=1, source_target_pairs={{0,1},{1,0},{2,3},{3,2},{4,5},{5,4},{6,7},{7,6},{8,9},{9,8},{10,11... | collective-permute-start | bytes 3538952 | tf_op jit(solution)/shard_map/ppermute | solution.py:287
  28.8 0.3 shard_map.127.normed_ref
  29.1 2.5 %collective-permute-done = bf16[16,32,1152]{2,1,0:T(8,128)(2,1)S(1)} collective-permute-done((bf16[16,32,1152]{2,1,0:T(8,128)(2,1)S(1)}, bf16[16,32,1152]{2,1,0:T(8,128)(2,1)S(1)}, u32[]{:S(2)}, u32[]{:S(2)}) %collective-permute-start) | collective-permute-done | bytes 1179680 | tf_op jit(solution)/shard_map/ppermute | solution.py:287
  31.6 3.2 %shard_map.129 = (bf16[512,256]{1,0:T(8,128)(2,1)}, bf16[128,512]{1,0:T(8,128)(2,1)S(1)}, bf16[128,512]{1,0:T(8,128)(2,1)S(1)}, f32[128,1024]{1,0:T(8,128)S(1)}) custom-call(bf16[2,128,512]{2,1,0:T(8,128)(2,1)S(1)} %shard_map.127.normed_ref, bf16[512,1152]{1,0:T(8,128)(2,1)S(1)} %bitcast.13, bf16[512,1152]{1,0:T(8,128)(2,1)S(1)} %bitcast.16, ...), custom_call_target="tpu_custom_call" | custom-call | flops 1073741824 | bytes 1048576 | tf_op jit(solution)/shard_map/pallas_call | solution.py:276
  34.8 14.9 %all-to-all-start.1 = ((bf16[16,32,256]{2,1,0:T(8,128)(2,1)}), bf16[16,32,256]{2,1,0:T(8,128)(2,1)S(1)}, u32[]{:S(2)}, u32[]{:S(2)}) async-start(bf16[16,32,256]{2,1,0:T(8,128)(2,1)} %bitcast.6), calls=%async_computation.1 | async-start | bytes 524288 | tf_op jit(solution)/shard_map/all_to_all | solution.py:333
  49.8 2.6 %collective-permute-start.1 = (bf16[1,32,512]{2,1,0:T(8,128)(2,1)S(1)}, bf16[1,32,512]{2,1,0:T(8,128)(2,1)S(1)}, u32[]{:S(2)}, u32[]{:S(2)}) collective-permute-start(bf16[1,32,512]{2,1,0:T(8,128)(2,1)S(1)} %bitcast.18), channel_id=1, source_target_pairs={{0,8},{8,0},{16,24},{24,16},{1,9},{9,1},{17,25},{25,17},{2,10},{10... | collective-permute-start | bytes 98312 | tf_op jit(solution)/shard_map/ppermute | solution.py:311
  52.4 2.5 %collective-permute-start.2 = (bf16[1,16,1024]{2,1,0:T(8,128)(2,1)S(1)}, bf16[1,16,1024]{2,1,0:T(8,128)(2,1)S(1)}, u32[]{:S(2)}, u32[]{:S(2)}) collective-permute-start(bf16[1,16,1024]{2,1,0:T(8,128)(2,1)S(1)} %bitcast.20), channel_id=1, source_target_pairs={{0,2},{2,0},{4,6},{6,4},{1,3},{3,1},{5,7},{7,5},{8,10},{10,8},{12,... | collective-permute-start | bytes 98312 | tf_op jit(solution)/shard_map/ppermute | solution.py:312
  54.8 0.8 collective-permute-done.1.query_in_ref
  55.6 2.6 %collective-permute-done.2.out_in_ref = bf16[1,16,1024]{2,1,0:T(8,128)(2,1)S(1)} collective-permute-done((bf16[1,16,1024]{2,1,0:T(8,128)(2,1)S(1)}, bf16[1,16,1024]{2,1,0:T(8,128)(2,1)S(1)}, u32[]{:S(2)}, u32[]{:S(2)}) %collective-permute-start.2) | collective-permute-done | bytes 32800 | tf_op jit(solution)/shard_map/ppermute | solution.py:312
  58.2 3.9 %collective-permute-start.3 = (bf16[2,32,512]{2,1,0:T(8,128)(2,1)S(1)}, bf16[2,32,512]{2,1,0:T(8,128)(2,1)S(1)}, u32[]{:S(2)}, u32[]{:S(2)}) collective-permute-start(bf16[2,32,512]{2,1,0:T(8,128)(2,1)S(1)} %get-tuple-element.23.query_ref), channel_id=1, source_target_pairs={{0,24},{8,16},{16,8},{24,0},{1,25},{9,17},{17,9},{25,1},{2,26},{10... | collective-permute-start | bytes 196616 | tf_op jit(solution)/shard_map/ppermute | solution.py:311
  62.1 3.2 %collective-permute-start.4 = (bf16[2,16,1024]{2,1,0:T(8,128)(2,1)S(1)}, bf16[2,16,1024]{2,1,0:T(8,128)(2,1)S(1)}, u32[]{:S(2)}, u32[]{:S(2)}) collective-permute-start(bf16[2,16,1024]{2,1,0:T(8,128)(2,1)S(1)} %get-tuple-element.24.out_ref), channel_id=1, source_target_pairs={{0,6},{2,4},{4,2},{6,0},{1,7},{3,5},{5,3},{7,1},{8,14},{10,12},{12... | collective-permute-start | bytes 196616 | tf_op jit(solution)/shard_map/ppermute | solution.py:312
  65.6 3.9 %collective-permute-done.4.out_in_ref = bf16[2,16,1024]{2,1,0:T(8,128)(2,1)S(1)} collective-permute-done((bf16[2,16,1024]{2,1,0:T(8,128)(2,1)S(1)}, bf16[2,16,1024]{2,1,0:T(8,128)(2,1)S(1)}, u32[]{:S(2)}, u32[]{:S(2)}) %collective-permute-start.4) | collective-permute-done | bytes 65568 | tf_op jit(solution)/shard_map/ppermute | solution.py:312
  69.5 1.9 %collective-permute-start.5 = (bf16[4,32,512]{2,1,0:T(8,128)(2,1)S(1)}, bf16[4,32,512]{2,1,0:T(8,128)(2,1)S(1)}, u32[]{:S(2)}, u32[]{:S(2)}) collective-permute-start(bf16[4,32,512]{2,1,0:T(8,128)(2,1)S(1)} %get-tuple-element.25.query_ref), channel_id=1, source_target_pairs={{0,2},{2,0},{4,6},{6,4},{1,3},{3,1},{5,7},{7,5},{8,10},{10,8},{12,... | collective-permute-start | bytes 393224 | tf_op jit(solution)/shard_map/ppermute | solution.py:311
  71.4 3.1 %collective-permute-start.6 = (bf16[4,16,1024]{2,1,0:T(8,128)(2,1)S(1)}, bf16[4,16,1024]{2,1,0:T(8,128)(2,1)S(1)}, u32[]{:S(2)}, u32[]{:S(2)}) collective-permute-start(bf16[4,16,1024]{2,1,0:T(8,128)(2,1)S(1)} %get-tuple-element.26.out_ref), channel_id=1, source_target_pairs={{0,8},{8,0},{16,24},{24,16},{1,9},{9,1},{17,25},{25,17},{2,10},{10... | collective-permute-start | bytes 393224 | tf_op jit(solution)/shard_map/ppermute | solution.py:312
  74.5 1.8 %collective-permute-done.5.query_in_ref = bf16[4,32,512]{2,1,0:T(8,128)(2,1)S(1)} collective-permute-done((bf16[4,32,512]{2,1,0:T(8,128)(2,1)S(1)}, bf16[4,32,512]{2,1,0:T(8,128)(2,1)S(1)}, u32[]{:S(2)}, u32[]{:S(2)}) %collective-permute-start.5) | collective-permute-done | bytes 131104 | tf_op jit(solution)/shard_map/ppermute | solution.py:311
  76.3 1.9 %collective-permute-done.6.out_in_ref = bf16[4,16,1024]{2,1,0:T(8,128)(2,1)S(1)} collective-permute-done((bf16[4,16,1024]{2,1,0:T(8,128)(2,1)S(1)}, bf16[4,16,1024]{2,1,0:T(8,128)(2,1)S(1)}, u32[]{:S(2)}, u32[]{:S(2)}) %collective-permute-start.6) | collective-permute-done | bytes 131104 | tf_op jit(solution)/shard_map/ppermute | solution.py:312
  78.3 3.2 %collective-permute-start.7 = (bf16[8,32,512]{2,1,0:T(8,128)(2,1)S(1)}, bf16[8,32,512]{2,1,0:T(8,128)(2,1)S(1)}, u32[]{:S(2)}, u32[]{:S(2)}) collective-permute-start(bf16[8,32,512]{2,1,0:T(8,128)(2,1)S(1)} %get-tuple-element.27.query_ref), channel_id=1, source_target_pairs={{0,6},{2,4},{4,2},{6,0},{1,7},{3,5},{5,3},{7,1},{8,14},{10,12},{12... | collective-permute-start | bytes 786440 | tf_op jit(solution)/shard_map/ppermute | solution.py:311
  81.5 3.2 %collective-permute-start.8 = (bf16[8,16,1024]{2,1,0:T(8,128)(2,1)S(1)}, bf16[8,16,1024]{2,1,0:T(8,128)(2,1)S(1)}, u32[]{:S(2)}, u32[]{:S(2)}) collective-permute-start(bf16[8,16,1024]{2,1,0:T(8,128)(2,1)S(1)} %get-tuple-element.28.out_ref), channel_id=1, source_target_pairs={{0,24},{8,16},{16,8},{24,0},{1,25},{9,17},{17,9},{25,1},{2,26},{10... | collective-permute-start | bytes 786440 | tf_op jit(solution)/shard_map/ppermute | solution.py:312
  84.7 3.1 %collective-permute-done.7.query_in_ref = bf16[8,32,512]{2,1,0:T(8,128)(2,1)S(1)} collective-permute-done((bf16[8,32,512]{2,1,0:T(8,128)(2,1)S(1)}, bf16[8,32,512]{2,1,0:T(8,128)(2,1)S(1)}, u32[]{:S(2)}, u32[]{:S(2)}) %collective-permute-start.7) | collective-permute-done | bytes 262176 | tf_op jit(solution)/shard_map/ppermute | solution.py:311
  87.8 3.2 %collective-permute-done.8.out_in_ref = bf16[8,16,1024]{2,1,0:T(8,128)(2,1)S(1)} collective-permute-done((bf16[8,16,1024]{2,1,0:T(8,128)(2,1)S(1)}, bf16[8,16,1024]{2,1,0:T(8,128)(2,1)S(1)}, u32[]{:S(2)}, u32[]{:S(2)}) %collective-permute-start.8) | collective-permute-done | bytes 262176 | tf_op jit(solution)/shard_map/ppermute | solution.py:312
  91.0 1.9 %collective-permute-start.9 = (bf16[16,32,512]{2,1,0:T(8,128)(2,1)S(1)}, bf16[16,32,512]{2,1,0:T(8,128)(2,1)S(1)}, u32[]{:S(2)}, u32[]{:S(2)}) collective-permute-start(bf16[16,32,512]{2,1,0:T(8,128)(2,1)S(1)} %get-tuple-element.29.own_ref), channel_id=1, source_target_pairs={{0,1},{1,0},{2,3},{3,2},{4,5},{5,4},{6,7},{7,6},{8,9},{9,8},{10,11... | collective-permute-start | bytes 1572872 | tf_op jit(solution)/shard_map/ppermute | solution.py:287
  93.0 2.4 %collective-permute-start.10 = (bf16[16,16,1024]{2,1,0:T(8,128)(2,1)S(1)}, bf16[16,16,1024]{2,1,0:T(8,128)(2,1)S(1)}, u32[]{:S(2)}, u32[]{:S(2)}) collective-permute-start(bf16[16,16,1024]{2,1,0:T(8,128)(2,1)S(1)} %get-tuple-element.38.own_ref), channel_id=1, source_target_pairs={{0,1},{1,0},{2,3},{3,2},{4,5},{5,4},{6,7},{7,6},{8,9},{9,8},{10,11... | collective-permute-start | bytes 1572872 | tf_op jit(solution)/shard_map/ppermute | solution.py:287
  95.4 0.9 shard_map.130
  96.3 12.0 %all-to-all-start.2 = ((bf16[16,32,128]{2,1,0:T(8,128)(2,1)}), bf16[16,32,128]{2,1,0:T(8,128)(2,1)S(1)}, u32[]{:S(2)}, u32[]{:S(2)}) async-start(bf16[16,32,128]{2,1,0:T(8,128)(2,1)} %bitcast.8), calls=%async_computation.2 | async-start | bytes 262144 | tf_op jit(solution)/shard_map/all_to_all | solution.py:345
  108.6 1.7 %shard_map.136 = (f32[128,512]{1,0:T(8,128)S(1)}, bf16[128,1024]{1,0:T(8,128)(2,1)S(1)}, bf16[128,1024]{1,0:T(8,128)(2,1)S(1)}) custom-call(bf16[2,128,512]{2,1,0:T(8,128)(2,1)S(1)} %shard_map.127.normed_ref, bf16[16,32,512]{2,1,0:T(8,128)(2,1)S(1)} %get-tuple-element.29.own_ref, bf16[16,32,512]{2,1,0:T(8,128)(2,1)S(1)} %collective-permute-done.9.other_ref, ...), custom_call_target="tpu_custom_call" | custom-call | flops 1073741824 | bytes 1048576 | tf_op jit(solution)/shard_map/pallas_call | solution.py:276
  110.4 12.5 %all-to-all-done.2 = bf16[16,32,128]{2,1,0:T(8,128)(2,1)S(1)} async-done(((bf16[16,32,128]{2,1,0:T(8,128)(2,1)}), bf16[16,32,128]{2,1,0:T(8,128)(2,1)S(1)}, u32[]{:S(2)}, u32[]{:S(2)}) %all-to-all-start.2) | async-done | bytes 131104 | tf_op jit(solution)/shard_map/all_to_all | solution.py:345
  122.9 2.7 %shard_map.137 = bf16[128,1024]{1,0:T(8,128)(2,1)} custom-call(bf16[512,128]{1,0:T(8,128)(2,1)S(1)} %bitcast.15, f32[128,512]{1,0:T(8,128)S(1)} %get-tuple-element.35.within_ref, bf16[128,1024]{1,0:T(8,128)(2,1)S(1)} %get-tuple-element.36.high_ref, bf16[128,1024]{1,0:T(8,128)(2,1)S(1)} %get-tuple-element.37.low_ref, f32[1,512]{1,0:T(1,128)S(1)} %reshape_tile.3.gain_ref, ...), custom_call_target="tpu_custom_call" | custom-call | flops 1073741824 | bytes 1048576 | tf_op jit(solution)/shard_map/pallas_call | solution.py:276
  (32 shorter events, 0.8 us)
Async XLA Ops:
  1.5 0.8 copy-start
  2.3 0.8 copy-start.1
  3.2 25.6 %copy-start.2 = (bf16[2,64,1024]{2,1,0:T(8,128)(2,1)S(1)}, bf16[2,64,1024]{2,1,0:T(8,128)(2,1)}, u32[]{:S(2)}) copy-start(bf16[2,64,1024]{2,1,0:T(8,128)(2,1)} %param.13) | copy-start | bytes 786436
  3.2 25.6 %copy-start.7 = (f32[1024]{0:T(1024)S(1)}, f32[1024]{0:T(1024)}, u32[]{:S(2)}) copy-start(f32[1024]{0:T(1024)} %param.14) | copy-start | bytes 12292
  3.2 28.4 %copy-start.5 = (bf16[16,512]{1,0:T(8,128)(2,1)S(1)}, bf16[16,512]{1,0:T(8,128)(2,1)}, u32[]{:S(2)}) copy-start(bf16[16,512]{1,0:T(8,128)(2,1)} %up_forward_ref.1) | copy-start | bytes 49156
  3.2 28.4 %copy-start.6 = (bf16[16,512]{1,0:T(8,128)(2,1)S(1)}, bf16[16,512]{1,0:T(8,128)(2,1)}, u32[]{:S(2)}) copy-start(bf16[16,512]{1,0:T(8,128)(2,1)} %up_backward_ref.1) | copy-start | bytes 49156
  3.2 28.4 %copy-start.8 = (f32[512]{0:T(512)S(1)}, f32[512]{0:T(512)}, u32[]{:S(2)}) copy-start(f32[512]{0:T(512)} %param.22) | copy-start | bytes 6148
  3.2 28.4 %copy-start.9 = (f32[512]{0:T(512)S(1)}, f32[512]{0:T(512)}, u32[]{:S(2)}) copy-start(f32[512]{0:T(512)} %param.23) | copy-start | bytes 6148
  26.9 4.7 %collective-permute-start = (bf16[16,32,1152]{2,1,0:T(8,128)(2,1)S(1)}, bf16[16,32,1152]{2,1,0:T(8,128)(2,1)S(1)}, u32[]{:S(2)}, u32[]{:S(2)}) collective-permute-start(bf16[16,32,1152]{2,1,0:T(8,128)(2,1)S(1)} %all_to_all.15), channel_id=1, source_target_pairs={{0,1},{1,0},{2,3},{3,2},{4,5},{5,4},{6,7},{7,6},{8,9},{9,8},{10,11... | collective-permute-start | bytes 3538952 | tf_op jit(solution)/shard_map/ppermute | solution.py:287
  31.6 18.2 %copy-start.3 = (bf16[32,512]{1,0:T(8,128)(2,1)S(1)}, bf16[32,512]{1,0:T(8,128)(2,1)}, u32[]{:S(2)}) copy-start(bf16[32,512]{1,0:T(8,128)(2,1)} %param.15) | copy-start | bytes 98308
  31.6 20.7 %copy-start.4 = (bf16[16,1024]{1,0:T(8,128)(2,1)S(1)}, bf16[16,1024]{1,0:T(8,128)(2,1)}, u32[]{:S(2)}) copy-start(bf16[16,1024]{1,0:T(8,128)(2,1)} %param.25) | copy-start | bytes 98308
  34.8 60.5 %all-to-all-start.1 = ((bf16[16,32,256]{2,1,0:T(8,128)(2,1)}), bf16[16,32,256]{2,1,0:T(8,128)(2,1)S(1)}, u32[]{:S(2)}, u32[]{:S(2)}) async-start(bf16[16,32,256]{2,1,0:T(8,128)(2,1)} %bitcast.6), calls=%async_computation.1 | async-start | bytes 524288 | tf_op jit(solution)/shard_map/all_to_all | solution.py:333
  49.8 5.8 %collective-permute-start.1 = (bf16[1,32,512]{2,1,0:T(8,128)(2,1)S(1)}, bf16[1,32,512]{2,1,0:T(8,128)(2,1)S(1)}, u32[]{:S(2)}, u32[]{:S(2)}) collective-permute-start(bf16[1,32,512]{2,1,0:T(8,128)(2,1)S(1)} %bitcast.18), channel_id=1, source_target_pairs={{0,8},{8,0},{16,24},{24,16},{1,9},{9,1},{17,25},{25,17},{2,10},{10... | collective-permute-start | bytes 98312 | tf_op jit(solution)/shard_map/ppermute | solution.py:311
  52.4 5.8 %collective-permute-start.2 = (bf16[1,16,1024]{2,1,0:T(8,128)(2,1)S(1)}, bf16[1,16,1024]{2,1,0:T(8,128)(2,1)S(1)}, u32[]{:S(2)}, u32[]{:S(2)}) collective-permute-start(bf16[1,16,1024]{2,1,0:T(8,128)(2,1)S(1)} %bitcast.20), channel_id=1, source_target_pairs={{0,2},{2,0},{4,6},{6,4},{1,3},{3,1},{5,7},{7,5},{8,10},{10,8},{12,... | collective-permute-start | bytes 98312 | tf_op jit(solution)/shard_map/ppermute | solution.py:312
  58.2 7.4 %collective-permute-start.3 = (bf16[2,32,512]{2,1,0:T(8,128)(2,1)S(1)}, bf16[2,32,512]{2,1,0:T(8,128)(2,1)S(1)}, u32[]{:S(2)}, u32[]{:S(2)}) collective-permute-start(bf16[2,32,512]{2,1,0:T(8,128)(2,1)S(1)} %get-tuple-element.23.query_ref), channel_id=1, source_target_pairs={{0,24},{8,16},{16,8},{24,0},{1,25},{9,17},{17,9},{25,1},{2,26},{10... | collective-permute-start | bytes 196616 | tf_op jit(solution)/shard_map/ppermute | solution.py:311
  62.1 7.4 %collective-permute-start.4 = (bf16[2,16,1024]{2,1,0:T(8,128)(2,1)S(1)}, bf16[2,16,1024]{2,1,0:T(8,128)(2,1)S(1)}, u32[]{:S(2)}, u32[]{:S(2)}) collective-permute-start(bf16[2,16,1024]{2,1,0:T(8,128)(2,1)S(1)} %get-tuple-element.24.out_ref), channel_id=1, source_target_pairs={{0,6},{2,4},{4,2},{6,0},{1,7},{3,5},{5,3},{7,1},{8,14},{10,12},{12... | collective-permute-start | bytes 196616 | tf_op jit(solution)/shard_map/ppermute | solution.py:312
  69.5 6.9 %collective-permute-start.5 = (bf16[4,32,512]{2,1,0:T(8,128)(2,1)S(1)}, bf16[4,32,512]{2,1,0:T(8,128)(2,1)S(1)}, u32[]{:S(2)}, u32[]{:S(2)}) collective-permute-start(bf16[4,32,512]{2,1,0:T(8,128)(2,1)S(1)} %get-tuple-element.25.query_ref), channel_id=1, source_target_pairs={{0,2},{2,0},{4,6},{6,4},{1,3},{3,1},{5,7},{7,5},{8,10},{10,8},{12,... | collective-permute-start | bytes 393224 | tf_op jit(solution)/shard_map/ppermute | solution.py:311
  71.4 6.9 %collective-permute-start.6 = (bf16[4,16,1024]{2,1,0:T(8,128)(2,1)S(1)}, bf16[4,16,1024]{2,1,0:T(8,128)(2,1)S(1)}, u32[]{:S(2)}, u32[]{:S(2)}) collective-permute-start(bf16[4,16,1024]{2,1,0:T(8,128)(2,1)S(1)} %get-tuple-element.26.out_ref), channel_id=1, source_target_pairs={{0,8},{8,0},{16,24},{24,16},{1,9},{9,1},{17,25},{25,17},{2,10},{10... | collective-permute-start | bytes 393224 | tf_op jit(solution)/shard_map/ppermute | solution.py:312
  78.3 30.0 %copy-start.10 = (f32[32]{0:T(128)S(1)}, f32[32]{0:T(128)}, u32[]{:S(2)}) copy-start(f32[32]{0:T(128)} %param.24) | copy-start | bytes 388
  78.3 9.5 %collective-permute-start.7 = (bf16[8,32,512]{2,1,0:T(8,128)(2,1)S(1)}, bf16[8,32,512]{2,1,0:T(8,128)(2,1)S(1)}, u32[]{:S(2)}, u32[]{:S(2)}) collective-permute-start(bf16[8,32,512]{2,1,0:T(8,128)(2,1)S(1)} %get-tuple-element.27.query_ref), channel_id=1, source_target_pairs={{0,6},{2,4},{4,2},{6,0},{1,7},{3,5},{5,3},{7,1},{8,14},{10,12},{12... | collective-permute-start | bytes 786440 | tf_op jit(solution)/shard_map/ppermute | solution.py:311
  81.5 9.5 %collective-permute-start.8 = (bf16[8,16,1024]{2,1,0:T(8,128)(2,1)S(1)}, bf16[8,16,1024]{2,1,0:T(8,128)(2,1)S(1)}, u32[]{:S(2)}, u32[]{:S(2)}) collective-permute-start(bf16[8,16,1024]{2,1,0:T(8,128)(2,1)S(1)} %get-tuple-element.28.out_ref), channel_id=1, source_target_pairs={{0,24},{8,16},{16,8},{24,0},{1,25},{9,17},{17,9},{25,1},{2,26},{10... | collective-permute-start | bytes 786440 | tf_op jit(solution)/shard_map/ppermute | solution.py:312
  91.0 17.5 %collective-permute-start.9 = (bf16[16,32,512]{2,1,0:T(8,128)(2,1)S(1)}, bf16[16,32,512]{2,1,0:T(8,128)(2,1)S(1)}, u32[]{:S(2)}, u32[]{:S(2)}) collective-permute-start(bf16[16,32,512]{2,1,0:T(8,128)(2,1)S(1)} %get-tuple-element.29.own_ref), channel_id=1, source_target_pairs={{0,1},{1,0},{2,3},{3,2},{4,5},{5,4},{6,7},{7,6},{8,9},{9,8},{10,11... | collective-permute-start | bytes 1572872 | tf_op jit(solution)/shard_map/ppermute | solution.py:287
  93.0 17.4 %collective-permute-start.10 = (bf16[16,16,1024]{2,1,0:T(8,128)(2,1)S(1)}, bf16[16,16,1024]{2,1,0:T(8,128)(2,1)S(1)}, u32[]{:S(2)}, u32[]{:S(2)}) collective-permute-start(bf16[16,16,1024]{2,1,0:T(8,128)(2,1)S(1)} %get-tuple-element.38.own_ref), channel_id=1, source_target_pairs={{0,1},{1,0},{2,3},{3,2},{4,5},{5,4},{6,7},{7,6},{8,9},{9,8},{10,11... | collective-permute-start | bytes 1572872 | tf_op jit(solution)/shard_map/ppermute | solution.py:287
  96.3 26.6 %all-to-all-start.2 = ((bf16[16,32,128]{2,1,0:T(8,128)(2,1)}), bf16[16,32,128]{2,1,0:T(8,128)(2,1)S(1)}, u32[]{:S(2)}, u32[]{:S(2)}) async-start(bf16[16,32,128]{2,1,0:T(8,128)(2,1)} %bitcast.8), calls=%async_computation.2 | async-start | bytes 262144 | tf_op jit(solution)/shard_map/all_to_all | solution.py:345

commit v3 on v1

v3 whole, which is shorter than its diff:
```python
import jax
import jax.numpy as jnp
from jax import lax
from jax.experimental import pallas as pl
from jax.experimental.pallas import tpu as pltpu
from jax.sharding import Mesh
from jax.sharding import PartitionSpec as P

DP = ("dp_0", "dp_1", "dp_2")
PLANE = ("dp_0", "dp_1")
HEAD = 32
HEADS = 16
WIDTH = 512
BLOCK = 64
LANES = 128
FIRST = 2 * WIDTH + LANES
EPS = 1e-06
f32 = jnp.float32
bf16 = jnp.bfloat16


def dot(a, b):
    return jnp.dot(a, b, preferred_element_type=f32)


def dot_tn(a, b):
    return lax.dot_general(a, b, (((0,), (0,)), ((), ())), preferred_element_type=f32)


def dot_nt(a, b):
    return lax.dot_general(a, b, (((1,), (1,)), ((), ())), preferred_element_type=f32)


def halves(x):
    high = x.astype(bf16)
    return high, (x - high.astype(f32)).astype(bf16)


def grid_of(shape):
    return lax.broadcasted_iota(jnp.int32, shape, 0), lax.broadcasted_iota(jnp.int32, shape, 1)


def as_bf16(mask):
    return jnp.where(mask, 1.0, 0.0).astype(bf16)


def pack_kernel(
    key_hbm, value_hbm, query_hbm, mix_hbm, forward_hbm, backward_hbm,
    out_ref, key_ref, value_ref, query_ref, mix_ref, forward_ref, backward_ref, sems,
):
    sources = (key_hbm, value_hbm, query_hbm, mix_hbm, forward_hbm, backward_hbm)
    targets = (key_ref, value_ref, query_ref, mix_ref, forward_ref, backward_ref)
    copies = [
        pltpu.make_async_copy(source, target, sems.at[i])
        for i, (source, target) in enumerate(zip(sources, targets))
    ]
    for copy in copies:
        copy.start()
    for copy in copies:
        copy.wait()
    row, col = grid_of((16, LANES))
    ranks = dot_tn(forward_ref[...], as_bf16(row == col)) + dot_tn(
        backward_ref[...], as_bf16(row + 16 == col)
    )
    mix = jnp.concatenate([mix_ref[:, :WIDTH], mix_ref[:, WIDTH:]], axis=0)
    even = lax.rem(lax.axis_index("sp"), 2) == 0
    shared = jnp.where(even, query_ref[...].astype(f32), mix.astype(f32)).astype(bf16)
    block = jnp.concatenate(
        [key_ref[...], value_ref[...], ranks.astype(bf16), shared], axis=1
    )
    for i in range(16):
        out_ref[i] = block


def norm_kernel(tokens_ref, gain_ref, normed_ref):
    values = tokens_ref[...].astype(f32)
    scale = lax.rsqrt(jnp.mean(values * values, axis=-1, keepdims=True) + EPS)
    normed = (values * scale * gain_ref[...]).astype(bf16)
    for core in range(2):
        normed_ref[core] = jnp.concatenate(
            [normed[:, (2 * i + core) * 32 : (2 * i + core) * 32 + 32] for i in range(16)], axis=1
        )


def rates_of(ranks, up_forward_ref, up_backward_ref, bias_forward_ref, bias_backward_ref):
    gates = jnp.concatenate(
        [
            dot(ranks[:, :16], up_forward_ref[...]) + bias_forward_ref[...],
            dot(ranks[:, 16:32], up_backward_ref[...]) + bias_backward_ref[...],
        ],
        axis=1,
    )
    return halves(jax.nn.log_sigmoid(gates) * (2.0 / (BLOCK * HEADS)))


def summed(parts, mask, way):
    row, col = grid_of((LANES, LANES))
    ones = as_bf16(mask(row, col) & ((row // BLOCK) == (col // BLOCK)))
    lanes = slice(way * WIDTH, (way + 1) * WIDTH)
    return dot(ones, parts[0][:, lanes]) + dot(ones, parts[1][:, lanes])


def block_kernel(
    normed_ref, own_ref, other_ref, up_forward_ref, up_backward_ref,
    bias_forward_ref, bias_backward_ref, payload_ref, rounded_ref,
):
    core = lax.axis_index("dp_2")
    projected = dot(normed_ref[core], own_ref[...].reshape(WIDTH, FIRST)) + dot(
        normed_ref[1 - core], other_ref[...].reshape(WIDTH, FIRST)
    )
    rounded = projected.astype(bf16)
    rounded_ref[...] = rounded
    values = rounded[:, WIDTH : 2 * WIDTH]
    parts = rates_of(
        rounded[:, 2 * WIDTH :], up_forward_ref, up_backward_ref, bias_forward_ref, bias_backward_ref
    )
    high, low = parts
    row, col = grid_of((LANES, LANES))
    fwd, bwd = slice(0, WIDTH), slice(WIDTH, 2 * WIDTH)
    keys32 = rounded[:, :WIDTH].astype(f32)
    remain = (
        halves(keys32 * jnp.exp(summed(parts, lambda r, c: c > r, 0))),
        halves(keys32 * jnp.exp(summed(parts, lambda r, c: c < r, 1))),
    )
    hrow, hcol = grid_of((HEADS, WIDTH))
    mine = hrow == hcol // HEAD
    erow, ecol = grid_of((WIDTH, LANES))
    srow, scol = grid_of((8, 128))
    close = 0.0
    for way, span in ((0, fwd), (1, bwd)):
        pick = as_bf16(srow == scol // BLOCK)
        sums = dot(pick, high[:, span]) + dot(pick, low[:, span])
        for seq in range(2):
            line = jnp.where(mine, sums[seq : seq + 1], 0.0)
            place = as_bf16(ecol == (2 * way + seq) * HEAD + erow % HEAD)
            line_high, line_low = halves(line)
            both = jnp.concatenate([line_high, line_low], axis=0)
            close = close + dot(both, place)
    tail = lax.broadcasted_iota(jnp.int32, (HEADS, 16, LANES), 1)
    payload_ref[:, HEAD:, :] = jnp.where(
        tail == 0,
        close[:HEADS][:, None, :],
        jnp.where(tail == 1, close[HEADS:][:, None, :], 0.0),
    ).astype(bf16)
    diagonal = (row // HEAD) == (col // HEAD)
    erow, ecol = grid_of((4 * LANES, LANES))
    fold = as_bf16(((erow // LANES) * HEAD + erow % HEAD) == ecol)
    for group in range(4):
        lanes = slice(group * LANES, (group + 1) * LANES)
        parts = []
        for way in range(2):
            for seq in range(2):
                span = slice(seq * BLOCK, (seq + 1) * BLOCK)
                value = values[span, lanes]
                state = dot_tn(remain[way][0][span, lanes], value) + dot_tn(
                    remain[way][1][span, lanes], value
                )
                parts.append(jnp.where(diagonal, state, 0.0).astype(bf16))
        folded = dot(jnp.concatenate(parts, axis=1), fold).astype(bf16)
        payload_ref[4 * group : 4 * group + 4, :HEAD, :] = folded.reshape(4, HEAD, LANES)


def scan_kernel(payload_ref, out_ref):
    row, col = grid_of((LANES, LANES))
    spread = as_bf16((row // HEAD) == (col // HEAD))
    crow, ccol = grid_of((HEAD, LANES))
    mine = ccol % HEAD == crow
    lines = payload_ref[:, HEAD : HEAD + 16, :].astype(f32)
    closing = 0.0
    for part in range(2):
        line = jnp.where(mine[None], lines[:, part : part + 1, :], 0.0)
        closing = closing + dot(line.astype(bf16).reshape(WIDTH, LANES), spread)
    decay = jnp.exp(closing)
    states = payload_ref[:, :HEAD, :].astype(f32).reshape(WIDTH, LANES)
    lane = lax.broadcasted_iota(jnp.int32, (HEAD, LANES), 1)
    ahead = [None] * HEADS
    behind = [None] * HEADS

    def at(x, i):
        return x[i * HEAD : (i + 1) * HEAD, :]

    carried = jnp.zeros((HEAD, LANES), f32)
    for i in range(HEADS):
        ahead[i] = carried
        carried = at(decay, i) * carried + at(states, i)
    carried = jnp.zeros((HEAD, LANES), f32)
    for i in range(HEADS - 1, -1, -1):
        behind[i] = carried
        carried = at(decay, i) * carried + at(states, i)
    for i in range(HEADS):
        out_ref[i * HEAD : (i + 1) * HEAD, :] = jnp.where(
            lane < LANES // 2, ahead[i], behind[i]
        ).astype(bf16)


def sort_kernel(near_ref, far_ref, query_ref, mix_ref):
    parity = lax.rem(lax.axis_index("sp"), 2)

    @pl.when(parity == 0)
    def _():
        query_ref[...] = near_ref[...]
        mix_ref[...] = far_ref[...]

    @pl.when(parity == 1)
    def _():
        query_ref[...] = far_ref[...]
        mix_ref[...] = near_ref[...]


def query_kernel(
    normed_ref, own_ref, other_ref, rounded_ref, up_forward_ref, up_backward_ref,
    bias_forward_ref, bias_backward_ref, out_ref,
):
    core = lax.axis_index("dp_2")
    projected = dot(normed_ref[core], own_ref[...].reshape(WIDTH, WIDTH)) + dot(
        normed_ref[1 - core], other_ref[...].reshape(WIDTH, WIDTH)
    )
    queries = projected.astype(bf16).astype(f32) * HEAD ** (-0.5)
    keys = rounded_ref[:, :WIDTH].astype(f32)
    parts = rates_of(
        rounded_ref[:, 2 * WIDTH :], up_forward_ref, up_backward_ref, bias_forward_ref, bias_backward_ref
    )
    decayed, inverse = [], []
    for way, mask in ((0, lambda r, c: c <= r), (1, lambda r, c: c >= r)):
        running = summed(parts, mask, way)
        product = queries * jnp.exp(running)
        out_ref[:, (way + 1) * WIDTH : (way + 2) * WIDTH] = product
        decayed.append(product.astype(bf16))
        inverse.append((keys * jnp.exp(-running)).astype(bf16))
    row, col = grid_of((4 * BLOCK, LANES))
    own_lanes = (row // BLOCK) == (col // HEAD)
    own_lanes_bf = as_bf16(own_lanes)
    srow, scol = grid_of((4 * BLOCK, BLOCK))
    lower = (srow % BLOCK) >= scol
    upper = (srow % BLOCK) <= scol
    for seq in range(2):
        span = slice(seq * BLOCK, (seq + 1) * BLOCK)
        for group in range(4):
            lanes = slice(group * LANES, (group + 1) * LANES)
            scores = 0.0
            for way, mask in ((0, lower), (1, upper)):
                one = decayed[way][span, lanes]
                stacked = jnp.concatenate([one] * 4, axis=0) * own_lanes_bf
                scores = scores + jnp.where(mask, dot_nt(stacked, inverse[way][span, lanes]), 0.0)
            spread = jnp.where(own_lanes, dot(scores.astype(bf16), rounded_ref[span, slice(WIDTH + group * LANES, WIDTH + (group + 1) * LANES)]), 0.0)
            out_ref[span, lanes] = (
                spread[:BLOCK] + spread[BLOCK : 2 * BLOCK]
                + spread[2 * BLOCK : 3 * BLOCK] + spread[3 * BLOCK :]
            )


def out_kernel(
    states_ref, parts_ref, gain_ref, own_ref, other_ref, out_ref
):
    core = lax.axis_index("dp_2")
    row, col = grid_of((LANES, LANES))
    diagonal = (row // HEAD) == (col // HEAD)
    rows = []
    for seq in range(2):
        span = slice(seq * BLOCK, (seq + 1) * BLOCK)
        pieces = []
        for group in range(4):
            lanes = slice(group * LANES, (group + 1) * LANES)
            total = parts_ref[span, lanes]
            for way in range(2):
                widen = as_bf16(row == (2 * way + seq) * HEAD + col % HEAD)
                full = dot(states_ref[lanes, :], widen)
                full = jnp.where(diagonal, full, 0.0).astype(bf16)
                start = (way + 1) * WIDTH + group * LANES
                high, low = halves(parts_ref[span, start : start + LANES])
                total = total + dot(high, full) + dot(low, full)
            pieces.append(total)
        rows.append(jnp.concatenate(pieces, axis=1))
    combined = jnp.concatenate(rows, axis=0)
    high, low = halves(combined * combined)
    ones = as_bf16(diagonal)
    mean = jnp.concatenate(
        [
            dot(high[:, g * LANES : (g + 1) * LANES], ones)
            + dot(low[:, g * LANES : (g + 1) * LANES], ones)
            for g in range(4)
        ],
        axis=1,
    ) * (1.0 / HEAD)
    attended = (combined * lax.rsqrt(mean + EPS) * gain_ref[...]).astype(bf16)
    prow, pcol = grid_of((WIDTH, WIDTH))
    source = ((pcol % 256) // 16) * 32 + (pcol // 256) * 16 + pcol % 16
    shuffled = dot(attended, as_bf16(prow == source)).astype(bf16)
    first, second = shuffled[:, :256], shuffled[:, 256:]
    mine = jnp.where(core == 0, first, second)
    theirs = jnp.where(core == 0, second, first)
    for half in range(2):
        rows = slice(half * 16, half * 16 + 16)
        out_ref[:, half * WIDTH : (half + 1) * WIDTH] = (
            dot(mine, own_ref[:, rows, :].reshape(256, WIDTH))
            + dot(theirs, other_ref[:, rows, :].reshape(256, WIDTH))
        ).astype(bf16)


VMEM = pl.BlockSpec(memory_space=pltpu.VMEM)


def call(kernel, outs, specs, cycles, *args, scratch=(), grant=16 << 20):
    many = isinstance(outs, tuple)
    return pl.pallas_call(
        kernel,
        out_shape=outs,
        in_specs=specs,
        out_specs=(VMEM,) * len(outs) if many else VMEM,
        scratch_shapes=scratch,
        cost_estimate=pl.CostEstimate(flops=cycles, bytes_accessed=1 << 20, transcendentals=0),
        compiler_params=pltpu.CompilerParams(vmem_limit_bytes=grant),
    )(*args)


def swapped(x):
    return lax.ppermute(x, "dp_2", [(0, 1), (1, 0)])


def body(
    tokens, norm_gain, w_query, w_key, w_value, w_rank_forward, w_rank_backward,
    up_forward, up_backward, bias_forward, bias_backward, out_gain, w_out,
):
    seqs, toks, width = tokens.shape
    rows = seqs * toks
    shape = jax.ShapeDtypeStruct
    hbm = pl.BlockSpec(memory_space=pltpu.HBM)
    sources = (w_key, w_value, w_query, w_out, w_rank_forward.T, w_rank_backward.T)
    send = call(
        pack_kernel, shape((16, 32, FIRST + WIDTH), bf16), [hbm] * 6, 1 << 26, *sources,
        scratch=[pltpu.VMEM(x.shape, bf16) for x in sources] + [pltpu.SemaphoreType.DMA((6,))],
        grant=None,
    )
    own = lax.all_to_all(send, PLANE, 0, 0)
    first_own = own[:, :, :FIRST]
    other = swapped(first_own)
    near_part = own[:, :, FIRST:]
    far_part = lax.ppermute(near_part, "sp", [(i, i ^ 1) for i in range(16)])
    normed = call(
        norm_kernel, shape((2, rows, 512), bf16), [VMEM, VMEM], 1 << 28,
        tokens.reshape(rows, width), norm_gain.reshape(1, width),
    )
    decays = (
        up_forward, up_backward, bias_forward.reshape(1, WIDTH), bias_backward.reshape(1, WIDTH)
    )
    payload, rounded = call(
        block_kernel, (shape((HEADS, 48, LANES), bf16), shape((rows, FIRST), bf16)),
        [VMEM] * 7, 1 << 30, normed, first_own, other, *decays,
    )
    inbound = lax.all_to_all(payload, "sp", 0, 0)
    query_own, mix_own = call(
        sort_kernel, (shape(near_part.shape, bf16),) * 2, [VMEM] * 2, 1 << 28,
        near_part, far_part,
    )
    query_other = swapped(query_own)
    mix_other = swapped(mix_own)
    states = call(
        scan_kernel, shape((WIDTH, LANES), bf16), [VMEM], 1 << 28,
        inbound,
    )
    returned = lax.all_to_all(states.reshape(HEADS, HEAD, LANES), "sp", 0, 0)
    parts = call(
        query_kernel, shape((rows, 3 * WIDTH), f32), [VMEM] * 8, 1 << 30,
        normed, query_own, query_other, rounded, *decays,
    )
    mixed = call(
        out_kernel, shape((rows, width), bf16), [VMEM] * 5, 1 << 30,
        returned.reshape(WIDTH, LANES), parts,
        jnp.tile(out_gain, HEADS).reshape(1, WIDTH), mix_own, mix_other,
    )
    return mixed.reshape(seqs, toks, width)


def solution(mesh):
    finer = Mesh(mesh.devices.reshape(mesh.shape["sp"], 4, 4, 2), ("sp", "dp_0", "dp_1", "dp_2"))
    rows = P(DP, None)
    in_specs = (
        P(DP, "sp", None), P(), rows, rows, rows, rows, rows, P(), P(), P(), P(), P(), rows,
    )

    return jax.shard_map(
        body, mesh=finer, in_specs=in_specs, out_specs=P(DP, "sp", None), check_vma=False
    )
```

time: 123 us -> 113 us (0.919)
  blocking collectives: 45 us -> 29.1 us
  starting transfers between devices: 27 us -> 36 us
  waiting for transfers between devices: 26 us -> 30.9 us
  Pallas kernels: 16.6 us -> 11.9 us
  local copies, waits for them, and re-layouts: 6.7 us -> 2.99 us
    ppermute x0 -> x1, waiting for transfers between devices: none -> 17.3 us  [body(): far_part = lax.ppermute(near_part, 'sp', [(i, i ^ 1) for i in range(16)])]
    all_to_all x1, waiting for transfers between devices: 16.3 us -> 0.01 us  [body(): inbound = lax.all_to_all(payload, 'sp', 0, 0)]
    all_to_all x2 -> x1, blocking collectives: 45 us -> 29.1 us  [body(): own = lax.all_to_all(send, PLANE, 0, 0)]
    pallas_call x5 -> x7, Pallas kernels: 16.6 us -> 11.9 us  [call(): pl.pallas_call(kernel, out_shape=outs, in_specs=specs, out_specs=(VMEM,)...]
    ppermute x0 -> x1, starting transfers between devices: none -> 3.83 us  [body(): far_part = lax.ppermute(near_part, 'sp', [(i, i ^ 1) for i in range(16)])]
    unnamed x30 -> x20, local copies, waits for them, and re-layouts: 4.93 us -> 1.74 us
    all_to_all x1, starting transfers between devices: 7.58 us -> 10.7 us  [body(): returned = lax.all_to_all(states.reshape(HEADS, HEAD, LANES), 'sp', 0, 0)]
    ppermute x2 -> x3, starting transfers between devices: 3.97 us -> 6.38 us  [swapped(): return lax.ppermute(x, 'dp_2', [(0, 1), (1, 0)])]
  transfers between devices with their start and end apart: 4 -> 6, of which waited for: 3 -> 3; matrix products, arithmetic and copies ran while one was open for 1% -> 1% of each run, Pallas kernels for 7% -> 3%
where the time goes in v3:
time: 113 us; the launch traced here: 111 us
  starting transfers between devices  36 us (32%)
  waiting for transfers between devices  30.9 us (27%)
  blocking collectives  29.1 us (26%)
  Pallas kernels  11.9 us (11%)
  local copies, waits for them, and re-layouts  2.99 us (3%)
    all_to_all x1, blocking collectives, body(): own = lax.all_to_all(send, PLANE, 0, 0)  29.1 us
    ppermute x1, waiting for transfers between devices, body(): far_part = lax.ppermute(near_part, 'sp', [(i, i ^ 1) for i in range(16)])  17.3 us
    all_to_all x1, starting transfers between devices, body(): inbound = lax.all_to_all(payload, 'sp', 0, 0)  15.1 us
    pallas_call x7, Pallas kernels, call(): pl.pallas_call(kernel, out_shape=outs, in_specs=specs, out_specs=(VMEM,)...  11.9 us
    all_to_all x1, waiting for transfers between devices, body(): returned = lax.all_to_all(states.reshape(HEADS, HEAD, LANES), 'sp', 0, 0)  11.1 us
    all_to_all x1, starting transfers between devices, body(): returned = lax.all_to_all(states.reshape(HEADS, HEAD, LANES), 'sp', 0, 0)  10.7 us
    ppermute x3, starting transfers between devices, swapped(): return lax.ppermute(x, 'dp_2', [(0, 1), (1, 0)])  6.38 us
    ppermute x1, starting transfers between devices, body(): far_part = lax.ppermute(near_part, 'sp', [(i, i ^ 1) for i in range(16)])  3.83 us
  transfers between devices with their start and end apart: 6, of which 3 were waited for; matrix products, arithmetic and copies ran while one was open for 1% of the time, Pallas kernels for 3%

profile of v3, /device:TPU:24, one launch (start us, length us, event | category | flops | bytes accessed | tf_op | source)
XLA Modules:
  0.0 111.1 jit_solution(9804128564968990708)
XLA Ops:
  0.0 2.3 %shard_map.128 = bf16[16,32,1664]{2,1,0:T(8,128)(2,1)} custom-call(bf16[32,512]{1,0:T(8,128)(2,1)} %key_hbm.1, bf16[32,512]{1,0:T(8,128)(2,1)} %value_hbm.1, bf16[32,512]{1,0:T(8,128)(2,1)} %query_hbm.1, bf16[16,1024]{1,0:T(8,128)(2,1)} %mix_hbm.1, bf16[16,32]{1,0:T(8,128)(2,1)} %bitcast.16, bf16[16,32]{1,0:T(8,128)(2,1)} %bitcast.17), custom_call_target="tpu_custom_call" | custom-call | flops 67108864 | bytes 1048576 | tf_op jit(solution)/shard_map/pallas_call | solution.py:305
  2.3 29.1 %all_to_all.15 = bf16[16,32,1664]{2,1,0:T(8,128)(2,1)S(1)} all-to-all(bf16[16,32,1664]{2,1,0:T(8,128)(2,1)} %shard_map.128), channel_id=1, replica_groups=mesh['sp'=16,'dp_0'=4,'dp_1'=4,'dp_2'=2] {'dp_0','dp_1'}, dimensions={0} | all-to-all | bytes 3407872 | tf_op jit(solution)/shard_map/all_to_all | solution.py:334
  31.4 0.0 copy-start.2
  31.5 0.0 copy-start.4
  31.5 0.0 copy-start.5
  31.5 0.1 slice.8.own_ref
  31.6 2.1 %collective-permute-start = (bf16[16,32,1152]{2,1,0:T(8,128)(2,1)S(1)}, bf16[16,32,1152]{2,1,0:T(8,128)(2,1)S(1)}, u32[]{:S(2)}, u32[]{:S(2)}) collective-permute-start(bf16[16,32,1152]{2,1,0:T(8,128)(2,1)S(1)} %slice.8.own_ref), channel_id=1, source_target_pairs={{0,1},{1,0},{2,3},{3,2},{4,5},{5,4},{6,7},{7,6},{8,9},{9,8},{10,11... | collective-permute-start | bytes 3538952 | tf_op jit(solution)/shard_map/ppermute | solution.py:317
  33.6 0.0 copy-done
  33.7 0.3 shard_map.127.normed_ref
  34.0 2.5 %collective-permute-done.other_ref = bf16[16,32,1152]{2,1,0:T(8,128)(2,1)S(1)} collective-permute-done((bf16[16,32,1152]{2,1,0:T(8,128)(2,1)S(1)}, bf16[16,32,1152]{2,1,0:T(8,128)(2,1)S(1)}, u32[]{:S(2)}, u32[]{:S(2)}) %collective-permute-start) | collective-permute-done | bytes 1179680 | tf_op jit(solution)/shard_map/ppermute | solution.py:317
  36.5 0.0 copy-done.5
  36.5 3.2 %shard_map.129 = (bf16[16,48,128]{2,1,0:T(8,128)(2,1)}, bf16[128,1152]{1,0:T(8,128)(2,1)S(1)}) custom-call(bf16[2,128,512]{2,1,0:T(8,128)(2,1)S(1)} %shard_map.127.normed_ref, bf16[16,32,1152]{2,1,0:T(8,128)(2,1)S(1)} %slice.8.own_ref, bf16[16,32,1152]{2,1,0:T(8,128)(2,1)S(1)} %collective-permute-done.other_ref, bf16[16,512]{1,0:T(8,128)(2,1)S(1)} %copy-done.1, ...), custom_call_target="tpu_custom_call" | custom-call | flops 1073741824 | bytes 1048576 | tf_op jit(solution)/shard_map/pallas_call | solution.py:305
  39.7 0.0 copy-done.8
  39.7 0.7 copy-done.6
  40.4 15.1 %all-to-all-start.1 = ((bf16[16,48,128]{2,1,0:T(8,128)(2,1)}), bf16[16,48,128]{2,1,0:T(8,128)(2,1)S(1)}, u32[]{:S(2)}, u32[]{:S(2)}) async-start(bf16[16,48,128]{2,1,0:T(8,128)(2,1)} %get-tuple-element.9), calls=%async_computation.1 | async-start | bytes 393216 | tf_op jit(solution)/shard_map/all_to_all | solution.py:350
  55.5 0.0 copy-start.9
  55.5 1.1 slice.9.near_ref
  56.6 3.8 %collective-permute-start.1 = (bf16[16,32,512]{2,1,0:T(8,128)(2,1)S(1)}, bf16[16,32,512]{2,1,0:T(8,128)(2,1)S(1)}, u32[]{:S(2)}, u32[]{:S(2)}) collective-permute-start(bf16[16,32,512]{2,1,0:T(8,128)(2,1)S(1)} %slice.9.near_ref), channel_id=1, source_target_pairs={{0,32},{32,0},{64,96},{96,64},{128,160},{160,128},{192,224},{224,1... | collective-permute-start | bytes 1572872 | tf_op jit(solution)/shard_map/ppermute | solution.py:338
  60.5 17.3 %collective-permute-done.1.far_ref = bf16[16,32,512]{2,1,0:T(8,128)(2,1)S(1)} collective-permute-done((bf16[16,32,512]{2,1,0:T(8,128)(2,1)S(1)}, bf16[16,32,512]{2,1,0:T(8,128)(2,1)S(1)}, u32[]{:S(2)}, u32[]{:S(2)}) %collective-permute-start.1) | collective-permute-done | bytes 524320 | tf_op jit(solution)/shard_map/ppermute | solution.py:338
  77.7 0.1 shard_map.131
  77.8 1.9 %collective-permute-start.2 = (bf16[16,32,512]{2,1,0:T(8,128)(2,1)S(1)}, bf16[16,32,512]{2,1,0:T(8,128)(2,1)S(1)}, u32[]{:S(2)}, u32[]{:S(2)}) collective-permute-start(bf16[16,32,512]{2,1,0:T(8,128)(2,1)S(1)} %get-tuple-element.10.own_ref), channel_id=1, source_target_pairs={{0,1},{1,0},{2,3},{3,2},{4,5},{5,4},{6,7},{7,6},{8,9},{9,8},{10,11... | collective-permute-start | bytes 1572872 | tf_op jit(solution)/shard_map/ppermute | solution.py:317
  79.7 2.4 %collective-permute-start.3 = (bf16[16,32,512]{2,1,0:T(8,128)(2,1)S(1)}, bf16[16,32,512]{2,1,0:T(8,128)(2,1)S(1)}, u32[]{:S(2)}, u32[]{:S(2)}) collective-permute-start(bf16[16,32,512]{2,1,0:T(8,128)(2,1)S(1)} %get-tuple-element.12.own_ref), channel_id=1, source_target_pairs={{0,1},{1,0},{2,3},{3,2},{4,5},{5,4},{6,7},{7,6},{8,9},{9,8},{10,11... | collective-permute-start | bytes 1572872 | tf_op jit(solution)/shard_map/ppermute | solution.py:317
  82.2 0.0 all-to-all-done.1.payload_ref
  82.2 0.9 shard_map.130
  83.1 10.7 %all-to-all-start.2 = ((bf16[16,32,128]{2,1,0:T(8,128)(2,1)}), bf16[16,32,128]{2,1,0:T(8,128)(2,1)S(1)}, u32[]{:S(2)}, u32[]{:S(2)}) async-start(bf16[16,32,128]{2,1,0:T(8,128)(2,1)} %bitcast.6), calls=%async_computation.2 | async-start | bytes 262144 | tf_op jit(solution)/shard_map/all_to_all | solution.py:361
  93.8 0.1 reshape_tile.3.gain_ref
  93.9 0.0 collective-permute-done.2.other_ref
  93.9 1.0 copy-done.7
  94.8 2.4 %shard_map.132.parts_ref = f32[128,1536]{1,0:T(8,128)S(1)} custom-call(bf16[2,128,512]{2,1,0:T(8,128)(2,1)S(1)} %shard_map.127.normed_ref, bf16[16,32,512]{2,1,0:T(8,128)(2,1)S(1)} %get-tuple-element.10.own_ref, bf16[16,32,512]{2,1,0:T(8,128)(2,1)S(1)} %collective-permute-done.2.other_ref, bf16[128,1152]{1,0:T(8,128)(2,1)S(1)} %copy-done.7, ...), custom_call_target="tpu_custom_call" | custom-call | flops 1073741824 | bytes 1048576 | tf_op jit(solution)/shard_map/pallas_call | solution.py:305
  97.2 0.0 collective-permute-done.3.other_ref
  97.2 11.1 %all-to-all-done.2 = bf16[16,32,128]{2,1,0:T(8,128)(2,1)S(1)} async-done(((bf16[16,32,128]{2,1,0:T(8,128)(2,1)}), bf16[16,32,128]{2,1,0:T(8,128)(2,1)S(1)}, u32[]{:S(2)}, u32[]{:S(2)}) %all-to-all-start.2) | async-done | bytes 131104 | tf_op jit(solution)/shard_map/all_to_all | solution.py:361
  108.3 2.7 %shard_map.133 = bf16[128,1024]{1,0:T(8,128)(2,1)} custom-call(bf16[512,128]{1,0:T(8,128)(2,1)S(1)} %bitcast.9, f32[128,1536]{1,0:T(8,128)S(1)} %shard_map.132.parts_ref, f32[1,512]{1,0:T(1,128)S(1)} %reshape_tile.3.gain_ref, bf16[16,32,512]{2,1,0:T(8,128)(2,1)S(1)} %get-tuple-element.12.own_ref, bf16[16,32,512]{2,1,0:T(8,128)(2,1)S(1)} %collective-permute-done.3.other_ref), custom_call_target="tpu_custom_call" | custom-call | flops 1073741824 | bytes 1048576 | tf_op jit(solution)/shard_map/pallas_call | solution.py:305
  (12 shorter events, 0.0 us)
Async XLA Ops:
  31.4 8.2 %copy-start.8 = (bf16[16,32,1664]{2,1,0:T(8,128)(2,1)}, bf16[16,32,1664]{2,1,0:T(8,128)(2,1)S(1)}, u32[]{:S(2)}) copy-start(bf16[16,32,1664]{2,1,0:T(8,128)(2,1)S(1)} %all_to_all.15) | copy-start | bytes 5111812
  31.4 2.2 %copy-start = (bf16[2,64,1024]{2,1,0:T(8,128)(2,1)S(1)}, bf16[2,64,1024]{2,1,0:T(8,128)(2,1)}, u32[]{:S(2)}) copy-start(bf16[2,64,1024]{2,1,0:T(8,128)(2,1)} %param.13) | copy-start | bytes 786436
  31.4 2.2 %copy-start.3 = (f32[1024]{0:T(1024)S(1)}, f32[1024]{0:T(1024)}, u32[]{:S(2)}) copy-start(f32[1024]{0:T(1024)} %param.14) | copy-start | bytes 12292
  31.4 5.0 %copy-start.1 = (bf16[16,512]{1,0:T(8,128)(2,1)S(1)}, bf16[16,512]{1,0:T(8,128)(2,1)}, u32[]{:S(2)}) copy-start(bf16[16,512]{1,0:T(8,128)(2,1)} %up_forward_ref.3) | copy-start | bytes 49156
  31.4 5.0 %copy-start.2 = (bf16[16,512]{1,0:T(8,128)(2,1)S(1)}, bf16[16,512]{1,0:T(8,128)(2,1)}, u32[]{:S(2)}) copy-start(bf16[16,512]{1,0:T(8,128)(2,1)} %up_backward_ref.3) | copy-start | bytes 49156
  31.5 5.0 %copy-start.4 = (f32[512]{0:T(512)S(1)}, f32[512]{0:T(512)}, u32[]{:S(2)}) copy-start(f32[512]{0:T(512)} %param.22) | copy-start | bytes 6148
  31.5 5.0 %copy-start.5 = (f32[512]{0:T(512)S(1)}, f32[512]{0:T(512)}, u32[]{:S(2)}) copy-start(f32[512]{0:T(512)} %param.23) | copy-start | bytes 6148
  31.6 4.9 %collective-permute-start = (bf16[16,32,1152]{2,1,0:T(8,128)(2,1)S(1)}, bf16[16,32,1152]{2,1,0:T(8,128)(2,1)S(1)}, u32[]{:S(2)}, u32[]{:S(2)}) collective-permute-start(bf16[16,32,1152]{2,1,0:T(8,128)(2,1)S(1)} %slice.8.own_ref), channel_id=1, source_target_pairs={{0,1},{1,0},{2,3},{3,2},{4,5},{5,4},{6,7},{7,6},{8,9},{9,8},{10,11... | collective-permute-start | bytes 3538952 | tf_op jit(solution)/shard_map/ppermute | solution.py:317
  39.7 0.7 copy-start.6
  40.4 41.7 %all-to-all-start.1 = ((bf16[16,48,128]{2,1,0:T(8,128)(2,1)}), bf16[16,48,128]{2,1,0:T(8,128)(2,1)S(1)}, u32[]{:S(2)}, u32[]{:S(2)}) async-start(bf16[16,48,128]{2,1,0:T(8,128)(2,1)} %get-tuple-element.9), calls=%async_computation.1 | async-start | bytes 393216 | tf_op jit(solution)/shard_map/all_to_all | solution.py:350
  55.5 38.2 %copy-start.9 = (f32[32]{0:T(128)S(1)}, f32[32]{0:T(128)}, u32[]{:S(2)}) copy-start(f32[32]{0:T(128)} %param.24) | copy-start | bytes 388
  56.6 21.1 %collective-permute-start.1 = (bf16[16,32,512]{2,1,0:T(8,128)(2,1)S(1)}, bf16[16,32,512]{2,1,0:T(8,128)(2,1)S(1)}, u32[]{:S(2)}, u32[]{:S(2)}) collective-permute-start(bf16[16,32,512]{2,1,0:T(8,128)(2,1)S(1)} %slice.9.near_ref), channel_id=1, source_target_pairs={{0,32},{32,0},{64,96},{96,64},{128,160},{160,128},{192,224},{224,1... | collective-permute-start | bytes 1572872 | tf_op jit(solution)/shard_map/ppermute | solution.py:338
  77.8 16.0 %collective-permute-start.2 = (bf16[16,32,512]{2,1,0:T(8,128)(2,1)S(1)}, bf16[16,32,512]{2,1,0:T(8,128)(2,1)S(1)}, u32[]{:S(2)}, u32[]{:S(2)}) collective-permute-start(bf16[16,32,512]{2,1,0:T(8,128)(2,1)S(1)} %get-tuple-element.10.own_ref), channel_id=1, source_target_pairs={{0,1},{1,0},{2,3},{3,2},{4,5},{5,4},{6,7},{7,6},{8,9},{9,8},{10,11... | collective-permute-start | bytes 1572872 | tf_op jit(solution)/shard_map/ppermute | solution.py:317
  79.7 17.5 %collective-permute-start.3 = (bf16[16,32,512]{2,1,0:T(8,128)(2,1)S(1)}, bf16[16,32,512]{2,1,0:T(8,128)(2,1)S(1)}, u32[]{:S(2)}, u32[]{:S(2)}) collective-permute-start(bf16[16,32,512]{2,1,0:T(8,128)(2,1)S(1)} %get-tuple-element.12.own_ref), channel_id=1, source_target_pairs={{0,1},{1,0},{2,3},{3,2},{4,5},{5,4},{6,7},{7,6},{8,9},{9,8},{10,11... | collective-permute-start | bytes 1572872 | tf_op jit(solution)/shard_map/ppermute | solution.py:317
  83.1 25.2 %all-to-all-start.2 = ((bf16[16,32,128]{2,1,0:T(8,128)(2,1)}), bf16[16,32,128]{2,1,0:T(8,128)(2,1)S(1)}, u32[]{:S(2)}, u32[]{:S(2)}) async-start(bf16[16,32,128]{2,1,0:T(8,128)(2,1)} %bitcast.6), calls=%async_computation.2 | async-start | bytes 262144 | tf_op jit(solution)/shard_map/all_to_all | solution.py:361
  93.9 1.0 copy-start.7

commit v4 on v3

--- a/solution.py
+++ b/solution.py
@@ -13,7 +13,7 @@
 WIDTH = 512
 BLOCK = 64
 LANES = 128
-FIRST = 2 * WIDTH + LANES
+ALL = 3 * WIDTH + LANES
 EPS = 1e-06
 f32 = jnp.float32
 bf16 = jnp.bfloat16
@@ -45,11 +45,11 @@
 
 
 def pack_kernel(
-    key_hbm, value_hbm, query_hbm, mix_hbm, forward_hbm, backward_hbm,
-    out_ref, key_ref, value_ref, query_ref, mix_ref, forward_ref, backward_ref, sems,
-):
-    sources = (key_hbm, value_hbm, query_hbm, mix_hbm, forward_hbm, backward_hbm)
-    targets = (key_ref, value_ref, query_ref, mix_ref, forward_ref, backward_ref)
+    key_hbm, value_hbm, query_hbm, forward_hbm, backward_hbm,
+    out_ref, key_ref, value_ref, query_ref, forward_ref, backward_ref, sems,
+):
+    sources = (key_hbm, value_hbm, query_hbm, forward_hbm, backward_hbm)
+    targets = (key_ref, value_ref, query_ref, forward_ref, backward_ref)
     copies = [
         pltpu.make_async_copy(source, target, sems.at[i])
         for i, (source, target) in enumerate(zip(sources, targets))
@@ -62,14 +62,30 @@
     ranks = dot_tn(forward_ref[...], as_bf16(row == col)) + dot_tn(
         backward_ref[...], as_bf16(row + 16 == col)
     )
-    mix = jnp.concatenate([mix_ref[:, :WIDTH], mix_ref[:, WIDTH:]], axis=0)
-    even = lax.rem(lax.axis_index("sp"), 2) == 0
-    shared = jnp.where(even, query_ref[...].astype(f32), mix.astype(f32)).astype(bf16)
     block = jnp.concatenate(
-        [key_ref[...], value_ref[...], ranks.astype(bf16), shared], axis=1
+        [key_ref[...], value_ref[...], query_ref[...], ranks.astype(bf16)], axis=1
     )
     for i in range(16):
         out_ref[i] = block
+
+
+def join_kernel(first_ref, second_ref, out_ref):
+    count = first_ref.shape[0]
+    out_ref[:count] = first_ref[...]
+    out_ref[count:] = second_ref[...]
+
+
+def slot_of(index, axis):
+    apart = index ^ lax.axis_index(axis)
+    return apart ^ (apart >> 1)
+
+
+def in_order(ref):
+    pieces = []
+    for y in range(4):
+        for x in range(4):
+            pieces.append(ref[slot_of(x, "dp_1") * 4 + slot_of(y, "dp_0")])
+    return jnp.concatenate(pieces, axis=0)
 
 
 def norm_kernel(tokens_ref, gain_ref, normed_ref):
@@ -105,14 +121,14 @@
     bias_forward_ref, bias_backward_ref, payload_ref, rounded_ref,
 ):
     core = lax.axis_index("dp_2")
-    projected = dot(normed_ref[core], own_ref[...].reshape(WIDTH, FIRST)) + dot(
-        normed_ref[1 - core], other_ref[...].reshape(WIDTH, FIRST)
+    projected = dot(normed_ref[core], own_ref[...].reshape(WIDTH, ALL)) + dot(
+        normed_ref[1 - core], other_ref[...].reshape(WIDTH, ALL)
     )
     rounded = projected.astype(bf16)
     rounded_ref[...] = rounded
     values = rounded[:, WIDTH : 2 * WIDTH]
     parts = rates_of(
-        rounded[:, 2 * WIDTH :], up_forward_ref, up_backward_ref, bias_forward_ref, bias_backward_ref
+        rounded[:, 3 * WIDTH :], up_forward_ref, up_backward_ref, bias_forward_ref, bias_backward_ref
     )
     high, low = parts
     row, col = grid_of((LANES, LANES))
@@ -193,32 +209,13 @@
         ).astype(bf16)
 
 
-def sort_kernel(near_ref, far_ref, query_ref, mix_ref):
-    parity = lax.rem(lax.axis_index("sp"), 2)
-
-    @pl.when(parity == 0)
-    def _():
-        query_ref[...] = near_ref[...]
-        mix_ref[...] = far_ref[...]
-
-    @pl.when(parity == 1)
-    def _():
-        query_ref[...] = far_ref[...]
-        mix_ref[...] = near_ref[...]
-
-
 def query_kernel(
-    normed_ref, own_ref, other_ref, rounded_ref, up_forward_ref, up_backward_ref,
-    bias_forward_ref, bias_backward_ref, out_ref,
-):
-    core = lax.axis_index("dp_2")
-    projected = dot(normed_ref[core], own_ref[...].reshape(WIDTH, WIDTH)) + dot(
-        normed_ref[1 - core], other_ref[...].reshape(WIDTH, WIDTH)
-    )
-    queries = projected.astype(bf16).astype(f32) * HEAD ** (-0.5)
+    rounded_ref, up_forward_ref, up_backward_ref, bias_forward_ref, bias_backward_ref, out_ref
+):
+    queries = rounded_ref[:, 2 * WIDTH : 3 * WIDTH].astype(f32) * HEAD ** (-0.5)
     keys = rounded_ref[:, :WIDTH].astype(f32)
     parts = rates_of(
-        rounded_ref[:, 2 * WIDTH :], up_forward_ref, up_backward_ref, bias_forward_ref, bias_backward_ref
+        rounded_ref[:, 3 * WIDTH :], up_forward_ref, up_backward_ref, bias_forward_ref, bias_backward_ref
     )
     decayed, inverse = [], []
     for way, mask in ((0, lambda r, c: c <= r), (1, lambda r, c: c >= r)):
@@ -289,12 +286,7 @@
     first, second = shuffled[:, :256], shuffled[:, 256:]
     mine = jnp.where(core == 0, first, second)
     theirs = jnp.where(core == 0, second, first)
-    for half in range(2):
-        rows = slice(half * 16, half * 16 + 16)
-        out_ref[:, half * WIDTH : (half + 1) * WIDTH] = (
-            dot(mine, own_ref[:, rows, :].reshape(256, WIDTH))
-            + dot(theirs, other_ref[:, rows, :].reshape(256, WIDTH))
-        ).astype(bf16)
+    out_ref[...] = (dot(mine, in_order(own_ref)) + dot(theirs, in_order(other_ref))).astype(bf16)
 
 
 VMEM = pl.BlockSpec(memory_space=pltpu.VMEM)
@@ -325,17 +317,22 @@
     rows = seqs * toks
     shape = jax.ShapeDtypeStruct
     hbm = pl.BlockSpec(memory_space=pltpu.HBM)
-    sources = (w_key, w_value, w_query, w_out, w_rank_forward.T, w_rank_backward.T)
+    sources = (w_key, w_value, w_query, w_rank_forward.T, w_rank_backward.T)
     send = call(
-        pack_kernel, shape((16, 32, FIRST + WIDTH), bf16), [hbm] * 6, 1 << 26, *sources,
-        scratch=[pltpu.VMEM(x.shape, bf16) for x in sources] + [pltpu.SemaphoreType.DMA((6,))],
+        pack_kernel, shape((16, 32, ALL), bf16), [hbm] * 5, 1 << 26, *sources,
+        scratch=[pltpu.VMEM(x.shape, bf16) for x in sources] + [pltpu.SemaphoreType.DMA((5,))],
         grant=None,
     )
     own = lax.all_to_all(send, PLANE, 0, 0)
-    first_own = own[:, :, :FIRST]
-    other = swapped(first_own)
-    near_part = own[:, :, FIRST:]
-    far_part = lax.ppermute(near_part, "sp", [(i, i ^ 1) for i in range(16)])
+    other = swapped(own)
+    mix = w_out[None]
+    for axis, flip in (("dp_0", 1), ("dp_0", 3), ("dp_1", 1), ("dp_1", 3)):
+        arrived = lax.ppermute(mix, axis, [(i, i ^ flip) for i in range(4)])
+        mix = call(
+            join_kernel, shape((2 * mix.shape[0], 16, width), bf16), [VMEM] * 2, 1 << 26,
+            mix, arrived,
+        )
+    mix_other = swapped(mix)
     normed = call(
         norm_kernel, shape((2, rows, 512), bf16), [VMEM, VMEM], 1 << 28,
         tokens.reshape(rows, width), norm_gain.reshape(1, width),
@@ -344,29 +341,20 @@
         up_forward, up_backward, bias_forward.reshape(1, WIDTH), bias_backward.reshape(1, WIDTH)
     )
     payload, rounded = call(
-        block_kernel, (shape((HEADS, 48, LANES), bf16), shape((rows, FIRST), bf16)),
-        [VMEM] * 7, 1 << 30, normed, first_own, other, *decays,
+        block_kernel, (shape((HEADS, 48, LANES), bf16), shape((rows, ALL), bf16)),
+        [VMEM] * 7, 1 << 30, normed, own, other, *decays,
     )
     inbound = lax.all_to_all(payload, "sp", 0, 0)
-    query_own, mix_own = call(
-        sort_kernel, (shape(near_part.shape, bf16),) * 2, [VMEM] * 2, 1 << 28,
-        near_part, far_part,
-    )
-    query_other = swapped(query_own)
-    mix_other = swapped(mix_own)
     states = call(
         scan_kernel, shape((WIDTH, LANES), bf16), [VMEM], 1 << 28,
         inbound,
     )
     returned = lax.all_to_all(states.reshape(HEADS, HEAD, LANES), "sp", 0, 0)
-    parts = call(
-        query_kernel, shape((rows, 3 * WIDTH), f32), [VMEM] * 8, 1 << 30,
-        normed, query_own, query_other, rounded, *decays,
-    )
+    parts = call(query_kernel, shape((rows, 3 * WIDTH), f32), [VMEM] * 5, 1 << 30, rounded, *decays)
     mixed = call(
         out_kernel, shape((rows, width), bf16), [VMEM] * 5, 1 << 30,
         returned.reshape(WIDTH, LANES), parts,
-        jnp.tile(out_gain, HEADS).reshape(1, WIDTH), mix_own, mix_other,
+        jnp.tile(out_gain, HEADS).reshape(1, WIDTH), mix, mix_other,
     )
     return mixed.reshape(seqs, toks, width)
 

time: 113 us -> 120 us (1.062)
  the two profiles are of different devices: /device:TPU:24 before, /device:TPU:32 now
where the time goes in v4:
time: 120 us; the launch traced here: 119 us
  starting transfers between devices  41.3 us (34%)
  waiting for transfers between devices  34.7 us (29%)
  blocking collectives  31.4 us (26%)
  Pallas kernels  11.8 us (10%)
    all_to_all x1, blocking collectives, body(): own = lax.all_to_all(send, PLANE, 0, 0)  31.4 us
    ppermute x4, waiting for transfers between devices, body(): arrived = lax.ppermute(mix, axis, [(i, i ^ flip) for i in range(4)])  19.3 us
    all_to_all x1, starting transfers between devices, body(): inbound = lax.all_to_all(payload, 'sp', 0, 0)  15.2 us
    all_to_all x1, waiting for transfers between devices, body(): returned = lax.all_to_all(states.reshape(HEADS, HEAD, LANES), 'sp', 0, 0)  12.2 us
    all_to_all x1, starting transfers between devices, body(): returned = lax.all_to_all(states.reshape(HEADS, HEAD, LANES), 'sp', 0, 0)  12 us
    pallas_call x10, Pallas kernels, call(): pl.pallas_call(kernel, out_shape=outs, in_specs=specs, out_specs=(VMEM,)...  11.8 us
    ppermute x4, starting transfers between devices, body(): arrived = lax.ppermute(mix, axis, [(i, i ^ flip) for i in range(4)])  10.2 us
    ppermute x2, starting transfers between devices, swapped(): return lax.ppermute(x, 'dp_2', [(0, 1), (1, 0)])  3.83 us
  transfers between devices with their start and end apart: 8, of which 6 were waited for; matrix products, arithmetic and copies ran while one was open for 0% of the time, Pallas kernels for 3%

profile of v4, /device:TPU:32, one launch (start us, length us, event | category | flops | bytes accessed | tf_op | source)
XLA Modules:
  0.0 119.5 jit_solution(6534342629164433826)
XLA Ops:
  0.0 2.3 %shard_map.128 = bf16[16,32,1664]{2,1,0:T(8,128)(2,1)} custom-call(bf16[32,512]{1,0:T(8,128)(2,1)} %key_hbm.1, bf16[32,512]{1,0:T(8,128)(2,1)} %value_hbm.1, bf16[32,512]{1,0:T(8,128)(2,1)} %query_hbm.1, bf16[16,32]{1,0:T(8,128)(2,1)} %bitcast.19, bf16[16,32]{1,0:T(8,128)(2,1)} %bitcast.20), custom_call_target="tpu_custom_call" | custom-call | flops 67108864 | bytes 1048576 | tf_op jit(solution)/shard_map/pallas_call | solution.py:297
  2.3 0.0 copy-start
  2.3 0.0 copy-start.4
  2.3 0.0 copy-start.2
  2.3 0.0 copy-start.3
  2.3 0.0 copy-start.5
  2.3 0.0 copy-start.6
  2.3 31.4 %all_to_all.15.own_ref = bf16[16,32,1664]{2,1,0:T(8,128)(2,1)S(1)} all-to-all(bf16[16,32,1664]{2,1,0:T(8,128)(2,1)} %shard_map.128), channel_id=1, replica_groups=mesh['sp'=16,'dp_0'=4,'dp_1'=4,'dp_2'=2] {'dp_0','dp_1'}, dimensions={0} | all-to-all | bytes 3407872 | tf_op jit(solution)/shard_map/all_to_all | solution.py:326
  33.7 1.9 %collective-permute-start = (bf16[16,32,1664]{2,1,0:T(8,128)(2,1)S(1)}, bf16[16,32,1664]{2,1,0:T(8,128)(2,1)S(1)}, u32[]{:S(2)}, u32[]{:S(2)}) collective-permute-start(bf16[16,32,1664]{2,1,0:T(8,128)(2,1)S(1)} %all_to_all.15.own_ref), channel_id=1, source_target_pairs={{0,1},{1,0},{2,3},{3,2},{4,5},{5,4},{6,7},{7,6},{8,9},{9,8},{10,11... | collective-permute-start | bytes 5111816 | tf_op jit(solution)/shard_map/ppermute | solution.py:309
  35.6 0.3 shard_map.127.normed_ref
  36.0 3.2 %collective-permute-done.other_ref = bf16[16,32,1664]{2,1,0:T(8,128)(2,1)S(1)} collective-permute-done((bf16[16,32,1664]{2,1,0:T(8,128)(2,1)S(1)}, bf16[16,32,1664]{2,1,0:T(8,128)(2,1)S(1)}, u32[]{:S(2)}, u32[]{:S(2)}) %collective-permute-start) | collective-permute-done | bytes 1703968 | tf_op jit(solution)/shard_map/ppermute | solution.py:309
  39.2 0.0 copy-done.3
  39.2 0.0 copy-start.1
  39.2 3.3 %shard_map.129 = (bf16[16,48,128]{2,1,0:T(8,128)(2,1)}, bf16[128,1664]{1,0:T(8,128)(2,1)S(1)}) custom-call(bf16[2,128,512]{2,1,0:T(8,128)(2,1)S(1)} %shard_map.127.normed_ref, bf16[16,32,1664]{2,1,0:T(8,128)(2,1)S(1)} %all_to_all.15.own_ref, bf16[16,32,1664]{2,1,0:T(8,128)(2,1)S(1)} %collective-permute-done.other_ref, bf16[16,512]{1,0:T(8,128)(2,1)S(1)} %copy-done.2, ...), custom_call_target="tpu_custom_call" | custom-call | flops 1073741824 | bytes 1048576 | tf_op jit(solution)/shard_map/pallas_call | solution.py:297
  42.5 15.2 %all-to-all-start.1 = ((bf16[16,48,128]{2,1,0:T(8,128)(2,1)}), bf16[16,48,128]{2,1,0:T(8,128)(2,1)S(1)}, u32[]{:S(2)}, u32[]{:S(2)}) async-start(bf16[16,48,128]{2,1,0:T(8,128)(2,1)} %get-tuple-element.7), calls=%async_computation.1 | async-start | bytes 393216 | tf_op jit(solution)/shard_map/all_to_all | solution.py:347
  57.7 2.2 %collective-permute-start.1 = (bf16[1,16,1024]{2,1,0:T(8,128)(2,1)S(1)}, bf16[1,16,1024]{2,1,0:T(8,128)(2,1)S(1)}, u32[]{:S(2)}, u32[]{:S(2)}) collective-permute-start(bf16[1,16,1024]{2,1,0:T(8,128)(2,1)S(1)} %bitcast.12), channel_id=1, source_target_pairs={{0,8},{8,0},{16,24},{24,16},{1,9},{9,1},{17,25},{25,17},{2,10},{10... | collective-permute-start | bytes 98312 | tf_op jit(solution)/shard_map/ppermute | solution.py:330
  59.9 3.6 %collective-permute-done.1.second_ref = bf16[1,16,1024]{2,1,0:T(8,128)(2,1)S(1)} collective-permute-done((bf16[1,16,1024]{2,1,0:T(8,128)(2,1)S(1)}, bf16[1,16,1024]{2,1,0:T(8,128)(2,1)S(1)}, u32[]{:S(2)}, u32[]{:S(2)}) %collective-permute-start.1) | collective-permute-done | bytes 32800 | tf_op jit(solution)/shard_map/ppermute | solution.py:330
  63.6 2.7 %collective-permute-start.2 = (bf16[2,16,1024]{2,1,0:T(8,128)(2,1)S(1)}, bf16[2,16,1024]{2,1,0:T(8,128)(2,1)S(1)}, u32[]{:S(2)}, u32[]{:S(2)}) collective-permute-start(bf16[2,16,1024]{2,1,0:T(8,128)(2,1)S(1)} %shard_map.132.first_ref), channel_id=1, source_target_pairs={{0,24},{8,16},{16,8},{24,0},{1,25},{9,17},{17,9},{25,1},{2,26},{10... | collective-permute-start | bytes 196616 | tf_op jit(solution)/shard_map/ppermute | solution.py:330
  66.3 4.6 %collective-permute-done.2.second_ref = bf16[2,16,1024]{2,1,0:T(8,128)(2,1)S(1)} collective-permute-done((bf16[2,16,1024]{2,1,0:T(8,128)(2,1)S(1)}, bf16[2,16,1024]{2,1,0:T(8,128)(2,1)S(1)}, u32[]{:S(2)}, u32[]{:S(2)}) %collective-permute-start.2) | collective-permute-done | bytes 65568 | tf_op jit(solution)/shard_map/ppermute | solution.py:330
  70.9 2.5 %collective-permute-start.3 = (bf16[4,16,1024]{2,1,0:T(8,128)(2,1)S(1)}, bf16[4,16,1024]{2,1,0:T(8,128)(2,1)S(1)}, u32[]{:S(2)}, u32[]{:S(2)}) collective-permute-start(bf16[4,16,1024]{2,1,0:T(8,128)(2,1)S(1)} %shard_map.133.first_ref), channel_id=1, source_target_pairs={{0,2},{2,0},{4,6},{6,4},{1,3},{3,1},{5,7},{7,5},{8,10},{10,8},{12,... | collective-permute-start | bytes 393224 | tf_op jit(solution)/shard_map/ppermute | solution.py:330
  73.4 4.4 %collective-permute-done.3.second_ref = bf16[4,16,1024]{2,1,0:T(8,128)(2,1)S(1)} collective-permute-done((bf16[4,16,1024]{2,1,0:T(8,128)(2,1)S(1)}, bf16[4,16,1024]{2,1,0:T(8,128)(2,1)S(1)}, u32[]{:S(2)}, u32[]{:S(2)}) %collective-permute-start.3) | collective-permute-done | bytes 131104 | tf_op jit(solution)/shard_map/ppermute | solution.py:330
  77.8 2.8 %collective-permute-start.4 = (bf16[8,16,1024]{2,1,0:T(8,128)(2,1)S(1)}, bf16[8,16,1024]{2,1,0:T(8,128)(2,1)S(1)}, u32[]{:S(2)}, u32[]{:S(2)}) collective-permute-start(bf16[8,16,1024]{2,1,0:T(8,128)(2,1)S(1)} %shard_map.134.first_ref), channel_id=1, source_target_pairs={{0,6},{2,4},{4,2},{6,0},{1,7},{3,5},{5,3},{7,1},{8,14},{10,12},{12... | collective-permute-start | bytes 786440 | tf_op jit(solution)/shard_map/ppermute | solution.py:330
  80.7 6.6 %collective-permute-done.4.second_ref = bf16[8,16,1024]{2,1,0:T(8,128)(2,1)S(1)} collective-permute-done((bf16[8,16,1024]{2,1,0:T(8,128)(2,1)S(1)}, bf16[8,16,1024]{2,1,0:T(8,128)(2,1)S(1)}, u32[]{:S(2)}, u32[]{:S(2)}) %collective-permute-start.4) | collective-permute-done | bytes 262176 | tf_op jit(solution)/shard_map/ppermute | solution.py:330
  87.3 1.9 %collective-permute-start.5 = (bf16[16,16,1024]{2,1,0:T(8,128)(2,1)S(1)}, bf16[16,16,1024]{2,1,0:T(8,128)(2,1)S(1)}, u32[]{:S(2)}, u32[]{:S(2)}) collective-permute-start(bf16[16,16,1024]{2,1,0:T(8,128)(2,1)S(1)} %shard_map.135.own_ref), channel_id=1, source_target_pairs={{0,1},{1,0},{2,3},{3,2},{4,5},{5,4},{6,7},{7,6},{8,9},{9,8},{10,11... | collective-permute-start | bytes 1572872 | tf_op jit(solution)/shard_map/ppermute | solution.py:309
  89.3 0.0 all-to-all-done.1.payload_ref
  89.3 0.9 shard_map.130
  90.2 12.0 %all-to-all-start.2 = ((bf16[16,32,128]{2,1,0:T(8,128)(2,1)}), bf16[16,32,128]{2,1,0:T(8,128)(2,1)S(1)}, u32[]{:S(2)}, u32[]{:S(2)}) async-start(bf16[16,32,128]{2,1,0:T(8,128)(2,1)} %bitcast.6), calls=%async_computation.2 | async-start | bytes 262144 | tf_op jit(solution)/shard_map/all_to_all | solution.py:352
  102.2 0.1 reshape_tile.3.gain_ref
  102.3 2.2 %shard_map.131.parts_ref = f32[128,1536]{1,0:T(8,128)S(1)} custom-call(bf16[128,1664]{1,0:T(8,128)(2,1)S(1)} %get-tuple-element.8.rounded_ref, bf16[16,512]{1,0:T(8,128)(2,1)S(1)} %copy-done.2, bf16[16,512]{1,0:T(8,128)(2,1)S(1)} %copy-done.3, f32[1,512]{1,0:T(1,128)S(1)} %bitcast.16, f32[1,512]{1,0:T(1,128)S(1)} %bitcast.18), custom_call_target="tpu_custom_call" | custom-call | flops 1073741824 | bytes 1048576 | tf_op jit(solution)/shard_map/pallas_call | solution.py:297
  104.5 0.0 collective-permute-done.5.other_ref
  104.5 12.2 %all-to-all-done.2 = bf16[16,32,128]{2,1,0:T(8,128)(2,1)S(1)} async-done(((bf16[16,32,128]{2,1,0:T(8,128)(2,1)}), bf16[16,32,128]{2,1,0:T(8,128)(2,1)S(1)}, u32[]{:S(2)}, u32[]{:S(2)}) %all-to-all-start.2) | async-done | bytes 131104 | tf_op jit(solution)/shard_map/all_to_all | solution.py:352
  116.7 2.8 %shard_map.136 = bf16[128,1024]{1,0:T(8,128)(2,1)} custom-call(bf16[512,128]{1,0:T(8,128)(2,1)S(1)} %bitcast.10, f32[128,1536]{1,0:T(8,128)S(1)} %shard_map.131.parts_ref, f32[1,512]{1,0:T(1,128)S(1)} %reshape_tile.3.gain_ref, bf16[16,16,1024]{2,1,0:T(8,128)(2,1)S(1)} %shard_map.135.own_ref, bf16[16,16,1024]{2,1,0:T(8,128)(2,1)S(1)} %collective-permute-done.5.other_ref), custom_call_target="tpu_custom_call" | custom-call | flops 1073741824 | bytes 1048576 | tf_op jit(solution)/shard_map/pallas_call | solution.py:297
  (13 shorter events, 0.1 us)
Async XLA Ops:
  2.3 33.3 %copy-start = (bf16[2,64,1024]{2,1,0:T(8,128)(2,1)S(1)}, bf16[2,64,1024]{2,1,0:T(8,128)(2,1)}, u32[]{:S(2)}) copy-start(bf16[2,64,1024]{2,1,0:T(8,128)(2,1)} %param.13) | copy-start | bytes 786436
  2.3 33.3 %copy-start.4 = (f32[1024]{0:T(1024)S(1)}, f32[1024]{0:T(1024)}, u32[]{:S(2)}) copy-start(f32[1024]{0:T(1024)} %param.14) | copy-start | bytes 12292
  2.3 36.9 %copy-start.2 = (bf16[16,512]{1,0:T(8,128)(2,1)S(1)}, bf16[16,512]{1,0:T(8,128)(2,1)}, u32[]{:S(2)}) copy-start(bf16[16,512]{1,0:T(8,128)(2,1)} %up_forward_ref.3) | copy-start | bytes 49156
  2.3 36.9 %copy-start.3 = (bf16[16,512]{1,0:T(8,128)(2,1)S(1)}, bf16[16,512]{1,0:T(8,128)(2,1)}, u32[]{:S(2)}) copy-start(bf16[16,512]{1,0:T(8,128)(2,1)} %up_backward_ref.3) | copy-start | bytes 49156
  2.3 36.9 %copy-start.5 = (f32[512]{0:T(512)S(1)}, f32[512]{0:T(512)}, u32[]{:S(2)}) copy-start(f32[512]{0:T(512)} %param.22) | copy-start | bytes 6148
  2.3 36.9 %copy-start.6 = (f32[512]{0:T(512)S(1)}, f32[512]{0:T(512)}, u32[]{:S(2)}) copy-start(f32[512]{0:T(512)} %param.23) | copy-start | bytes 6148
  33.7 5.5 %collective-permute-start = (bf16[16,32,1664]{2,1,0:T(8,128)(2,1)S(1)}, bf16[16,32,1664]{2,1,0:T(8,128)(2,1)S(1)}, u32[]{:S(2)}, u32[]{:S(2)}) collective-permute-start(bf16[16,32,1664]{2,1,0:T(8,128)(2,1)S(1)} %all_to_all.15.own_ref), channel_id=1, source_target_pairs={{0,1},{1,0},{2,3},{3,2},{4,5},{5,4},{6,7},{7,6},{8,9},{9,8},{10,11... | collective-permute-start | bytes 5111816 | tf_op jit(solution)/shard_map/ppermute | solution.py:309
  39.2 18.6 %copy-start.1 = (bf16[16,1024]{1,0:T(8,128)(2,1)S(1)}, bf16[16,1024]{1,0:T(8,128)(2,1)}, u32[]{:S(2)}) copy-start(bf16[16,1024]{1,0:T(8,128)(2,1)} %param.25) | copy-start | bytes 98308
  42.5 46.7 %all-to-all-start.1 = ((bf16[16,48,128]{2,1,0:T(8,128)(2,1)}), bf16[16,48,128]{2,1,0:T(8,128)(2,1)S(1)}, u32[]{:S(2)}, u32[]{:S(2)}) async-start(bf16[16,48,128]{2,1,0:T(8,128)(2,1)} %get-tuple-element.7), calls=%async_computation.1 | async-start | bytes 393216 | tf_op jit(solution)/shard_map/all_to_all | solution.py:347
  57.7 44.5 %copy-start.7 = (f32[32]{0:T(128)S(1)}, f32[32]{0:T(128)}, u32[]{:S(2)}) copy-start(f32[32]{0:T(128)} %param.24) | copy-start | bytes 388
  57.7 5.8 %collective-permute-start.1 = (bf16[1,16,1024]{2,1,0:T(8,128)(2,1)S(1)}, bf16[1,16,1024]{2,1,0:T(8,128)(2,1)S(1)}, u32[]{:S(2)}, u32[]{:S(2)}) collective-permute-start(bf16[1,16,1024]{2,1,0:T(8,128)(2,1)S(1)} %bitcast.12), channel_id=1, source_target_pairs={{0,8},{8,0},{16,24},{24,16},{1,9},{9,1},{17,25},{25,17},{2,10},{10... | collective-permute-start | bytes 98312 | tf_op jit(solution)/shard_map/ppermute | solution.py:330
  63.6 7.4 %collective-permute-start.2 = (bf16[2,16,1024]{2,1,0:T(8,128)(2,1)S(1)}, bf16[2,16,1024]{2,1,0:T(8,128)(2,1)S(1)}, u32[]{:S(2)}, u32[]{:S(2)}) collective-permute-start(bf16[2,16,1024]{2,1,0:T(8,128)(2,1)S(1)} %shard_map.132.first_ref), channel_id=1, source_target_pairs={{0,24},{8,16},{16,8},{24,0},{1,25},{9,17},{17,9},{25,1},{2,26},{10... | collective-permute-start | bytes 196616 | tf_op jit(solution)/shard_map/ppermute | solution.py:330
  70.9 6.9 %collective-permute-start.3 = (bf16[4,16,1024]{2,1,0:T(8,128)(2,1)S(1)}, bf16[4,16,1024]{2,1,0:T(8,128)(2,1)S(1)}, u32[]{:S(2)}, u32[]{:S(2)}) collective-permute-start(bf16[4,16,1024]{2,1,0:T(8,128)(2,1)S(1)} %shard_map.133.first_ref), channel_id=1, source_target_pairs={{0,2},{2,0},{4,6},{6,4},{1,3},{3,1},{5,7},{7,5},{8,10},{10,8},{12,... | collective-permute-start | bytes 393224 | tf_op jit(solution)/shard_map/ppermute | solution.py:330
  77.8 9.5 %collective-permute-start.4 = (bf16[8,16,1024]{2,1,0:T(8,128)(2,1)S(1)}, bf16[8,16,1024]{2,1,0:T(8,128)(2,1)S(1)}, u32[]{:S(2)}, u32[]{:S(2)}) collective-permute-start(bf16[8,16,1024]{2,1,0:T(8,128)(2,1)S(1)} %shard_map.134.first_ref), channel_id=1, source_target_pairs={{0,6},{2,4},{4,2},{6,0},{1,7},{3,5},{5,3},{7,1},{8,14},{10,12},{12... | collective-permute-start | bytes 786440 | tf_op jit(solution)/shard_map/ppermute | solution.py:330
  87.3 17.2 %collective-permute-start.5 = (bf16[16,16,1024]{2,1,0:T(8,128)(2,1)S(1)}, bf16[16,16,1024]{2,1,0:T(8,128)(2,1)S(1)}, u32[]{:S(2)}, u32[]{:S(2)}) collective-permute-start(bf16[16,16,1024]{2,1,0:T(8,128)(2,1)S(1)} %shard_map.135.own_ref), channel_id=1, source_target_pairs={{0,1},{1,0},{2,3},{3,2},{4,5},{5,4},{6,7},{7,6},{8,9},{9,8},{10,11... | collective-permute-start | bytes 1572872 | tf_op jit(solution)/shard_map/ppermute | solution.py:309
  90.2 26.5 %all-to-all-start.2 = ((bf16[16,32,128]{2,1,0:T(8,128)(2,1)}), bf16[16,32,128]{2,1,0:T(8,128)(2,1)S(1)}, u32[]{:S(2)}, u32[]{:S(2)}) async-start(bf16[16,32,128]{2,1,0:T(8,128)(2,1)} %bitcast.6), calls=%async_computation.2 | async-start | bytes 262144 | tf_op jit(solution)/shard_map/all_to_all | solution.py:352

commit v5 on v4

--- a/solution.py
+++ b/solution.py
@@ -152,7 +152,7 @@
             line_high, line_low = halves(line)
             both = jnp.concatenate([line_high, line_low], axis=0)
             close = close + dot(both, place)
-    tail = lax.broadcasted_iota(jnp.int32, (HEADS, 16, LANES), 1)
+    tail = lax.broadcasted_iota(jnp.int32, (HEADS, 8, LANES), 1)
     payload_ref[:, HEAD:, :] = jnp.where(
         tail == 0,
         close[:HEADS][:, None, :],
@@ -181,7 +181,7 @@
     spread = as_bf16((row // HEAD) == (col // HEAD))
     crow, ccol = grid_of((HEAD, LANES))
     mine = ccol % HEAD == crow
-    lines = payload_ref[:, HEAD : HEAD + 16, :].astype(f32)
+    lines = payload_ref[:, HEAD : HEAD + 8, :].astype(f32)
     closing = 0.0
     for part in range(2):
         line = jnp.where(mine[None], lines[:, part : part + 1, :], 0.0)
@@ -292,7 +292,7 @@
 VMEM = pl.BlockSpec(memory_space=pltpu.VMEM)
 
 
-def call(kernel, outs, specs, cycles, *args, scratch=(), grant=16 << 20):
+def call(kernel, outs, specs, cycles, *args, scratch=()):
     many = isinstance(outs, tuple)
     return pl.pallas_call(
         kernel,
@@ -301,7 +301,7 @@
         out_specs=(VMEM,) * len(outs) if many else VMEM,
         scratch_shapes=scratch,
         cost_estimate=pl.CostEstimate(flops=cycles, bytes_accessed=1 << 20, transcendentals=0),
-        compiler_params=pltpu.CompilerParams(vmem_limit_bytes=grant),
+        compiler_params=pltpu.CompilerParams(vmem_limit_bytes=16 << 20),
     )(*args)
 
 
@@ -317,11 +317,13 @@
     rows = seqs * toks
     shape = jax.ShapeDtypeStruct
     hbm = pl.BlockSpec(memory_space=pltpu.HBM)
-    sources = (w_key, w_value, w_query, w_rank_forward.T, w_rank_backward.T)
+    sources = [
+        pltpu.with_memory_space_constraint(x, pltpu.HBM)
+        for x in (w_key, w_value, w_query, w_rank_forward.T, w_rank_backward.T)
+    ]
     send = call(
         pack_kernel, shape((16, 32, ALL), bf16), [hbm] * 5, 1 << 26, *sources,
         scratch=[pltpu.VMEM(x.shape, bf16) for x in sources] + [pltpu.SemaphoreType.DMA((5,))],
-        grant=None,
     )
     own = lax.all_to_all(send, PLANE, 0, 0)
     other = swapped(own)
@@ -341,7 +343,7 @@
         up_forward, up_backward, bias_forward.reshape(1, WIDTH), bias_backward.reshape(1, WIDTH)
     )
     payload, rounded = call(
-        block_kernel, (shape((HEADS, 48, LANES), bf16), shape((rows, ALL), bf16)),
+        block_kernel, (shape((HEADS, 40, LANES), bf16), shape((rows, ALL), bf16)),
         [VMEM] * 7, 1 << 30, normed, own, other, *decays,
     )
     inbound = lax.all_to_all(payload, "sp", 0, 0)

time: 120 us -> 119 us (level)
  Pallas kernels: 11.8 us -> 10.6 us
    pallas_call x10, Pallas kernels: 11.8 us -> 10.6 us  [call(): pl.pallas_call(kernel, out_shape=outs, in_specs=specs, out_specs=(VMEM,)...]
where the time goes in v5:
time: 119 us; the launch traced here: 118 us
  starting transfers between devices  41.3 us (35%)
  waiting for transfers between devices  34.6 us (29%)
  blocking collectives  31.1 us (26%)
  Pallas kernels  10.6 us (9%)
    all_to_all x1, blocking collectives, body(): own = lax.all_to_all(send, PLANE, 0, 0)  31.1 us
    ppermute x4, waiting for transfers between devices, body(): arrived = lax.ppermute(mix, axis, [(i, i ^ flip) for i in range(4)])  19.2 us
    all_to_all x1, starting transfers between devices, body(): inbound = lax.all_to_all(payload, 'sp', 0, 0)  15.2 us
    all_to_all x1, waiting for transfers between devices, body(): returned = lax.all_to_all(states.reshape(HEADS, HEAD, LANES), 'sp', 0, 0)  12.2 us
    all_to_all x1, starting transfers between devices, body(): returned = lax.all_to_all(states.reshape(HEADS, HEAD, LANES), 'sp', 0, 0)  12 us
    pallas_call x10, Pallas kernels, call(): pl.pallas_call(kernel, out_shape=outs, in_specs=specs, out_specs=(VMEM,)...  10.6 us
    ppermute x4, starting transfers between devices, body(): arrived = lax.ppermute(mix, axis, [(i, i ^ flip) for i in range(4)])  10.2 us
    ppermute x2, starting transfers between devices, swapped(): return lax.ppermute(x, 'dp_2', [(0, 1), (1, 0)])  3.83 us
  transfers between devices with their start and end apart: 8, of which 6 were waited for; matrix products, arithmetic and copies ran while one was open for 0% of the time, Pallas kernels for 3%

profile of v5, /device:TPU:32, one launch (start us, length us, event | category | flops | bytes accessed | tf_op | source)
XLA Modules:
  0.0 118.0 jit_solution(13887554452233546114)
XLA Ops:
  0.0 1.1 shard_map.128
  1.1 0.0 copy-start
  1.1 0.0 copy-start.4
  1.1 0.0 copy-start.2
  1.1 0.0 copy-start.3
  1.1 0.0 copy-start.5
  1.1 0.0 copy-start.6
  1.2 31.1 %all_to_all.15.own_ref = bf16[16,32,1664]{2,1,0:T(8,128)(2,1)S(1)} all-to-all(bf16[16,32,1664]{2,1,0:T(8,128)(2,1)S(1)} %shard_map.128), channel_id=1, replica_groups=mesh['sp'=16,'dp_0'=4,'dp_1'=4,'dp_2'=2] {'dp_0','dp_1'}, dimensions={0} | all-to-all | bytes 3407872 | tf_op jit(solution)/shard_map/all_to_all | solution.py:328
  32.3 1.9 %collective-permute-start = (bf16[16,32,1664]{2,1,0:T(8,128)(2,1)S(1)}, bf16[16,32,1664]{2,1,0:T(8,128)(2,1)S(1)}, u32[]{:S(2)}, u32[]{:S(2)}) collective-permute-start(bf16[16,32,1664]{2,1,0:T(8,128)(2,1)S(1)} %all_to_all.15.own_ref), channel_id=1, source_target_pairs={{0,1},{1,0},{2,3},{3,2},{4,5},{5,4},{6,7},{7,6},{8,9},{9,8},{10,11... | collective-permute-start | bytes 5111816 | tf_op jit(solution)/shard_map/ppermute | solution.py:309
  34.2 0.3 shard_map.127.normed_ref
  34.6 3.2 %collective-permute-done.other_ref = bf16[16,32,1664]{2,1,0:T(8,128)(2,1)S(1)} collective-permute-done((bf16[16,32,1664]{2,1,0:T(8,128)(2,1)S(1)}, bf16[16,32,1664]{2,1,0:T(8,128)(2,1)S(1)}, u32[]{:S(2)}, u32[]{:S(2)}) %collective-permute-start) | collective-permute-done | bytes 1703968 | tf_op jit(solution)/shard_map/ppermute | solution.py:309
  37.8 0.0 copy-done.3
  37.8 0.0 copy-start.1
  37.8 3.3 %shard_map.129 = (bf16[16,40,128]{2,1,0:T(8,128)(2,1)}, bf16[128,1664]{1,0:T(8,128)(2,1)S(1)}) custom-call(bf16[2,128,512]{2,1,0:T(8,128)(2,1)S(1)} %shard_map.127.normed_ref, bf16[16,32,1664]{2,1,0:T(8,128)(2,1)S(1)} %all_to_all.15.own_ref, bf16[16,32,1664]{2,1,0:T(8,128)(2,1)S(1)} %collective-permute-done.other_ref, bf16[16,512]{1,0:T(8,128)(2,1)S(1)} %copy-done.2, ...), custom_call_target="tpu_custom_call" | custom-call | flops 1073741824 | bytes 1048576 | tf_op jit(solution)/shard_map/pallas_call | solution.py:297
  41.1 15.2 %all-to-all-start.1 = ((bf16[16,40,128]{2,1,0:T(8,128)(2,1)}), bf16[16,40,128]{2,1,0:T(8,128)(2,1)S(1)}, u32[]{:S(2)}, u32[]{:S(2)}) async-start(bf16[16,40,128]{2,1,0:T(8,128)(2,1)} %get-tuple-element.7), calls=%async_computation.1 | async-start | bytes 327680 | tf_op jit(solution)/shard_map/all_to_all | solution.py:349
  56.3 2.2 %collective-permute-start.1 = (bf16[1,16,1024]{2,1,0:T(8,128)(2,1)S(1)}, bf16[1,16,1024]{2,1,0:T(8,128)(2,1)S(1)}, u32[]{:S(2)}, u32[]{:S(2)}) collective-permute-start(bf16[1,16,1024]{2,1,0:T(8,128)(2,1)S(1)} %bitcast.12), channel_id=1, source_target_pairs={{0,8},{8,0},{16,24},{24,16},{1,9},{9,1},{17,25},{25,17},{2,10},{10... | collective-permute-start | bytes 98312 | tf_op jit(solution)/shard_map/ppermute | solution.py:332
  58.5 3.6 %collective-permute-done.1.second_ref = bf16[1,16,1024]{2,1,0:T(8,128)(2,1)S(1)} collective-permute-done((bf16[1,16,1024]{2,1,0:T(8,128)(2,1)S(1)}, bf16[1,16,1024]{2,1,0:T(8,128)(2,1)S(1)}, u32[]{:S(2)}, u32[]{:S(2)}) %collective-permute-start.1) | collective-permute-done | bytes 32800 | tf_op jit(solution)/shard_map/ppermute | solution.py:332
  62.2 2.7 %collective-permute-start.2 = (bf16[2,16,1024]{2,1,0:T(8,128)(2,1)S(1)}, bf16[2,16,1024]{2,1,0:T(8,128)(2,1)S(1)}, u32[]{:S(2)}, u32[]{:S(2)}) collective-permute-start(bf16[2,16,1024]{2,1,0:T(8,128)(2,1)S(1)} %shard_map.132.first_ref), channel_id=1, source_target_pairs={{0,24},{8,16},{16,8},{24,0},{1,25},{9,17},{17,9},{25,1},{2,26},{10... | collective-permute-start | bytes 196616 | tf_op jit(solution)/shard_map/ppermute | solution.py:332
  64.9 4.6 %collective-permute-done.2.second_ref = bf16[2,16,1024]{2,1,0:T(8,128)(2,1)S(1)} collective-permute-done((bf16[2,16,1024]{2,1,0:T(8,128)(2,1)S(1)}, bf16[2,16,1024]{2,1,0:T(8,128)(2,1)S(1)}, u32[]{:S(2)}, u32[]{:S(2)}) %collective-permute-start.2) | collective-permute-done | bytes 65568 | tf_op jit(solution)/shard_map/ppermute | solution.py:332
  69.5 2.5 %collective-permute-start.3 = (bf16[4,16,1024]{2,1,0:T(8,128)(2,1)S(1)}, bf16[4,16,1024]{2,1,0:T(8,128)(2,1)S(1)}, u32[]{:S(2)}, u32[]{:S(2)}) collective-permute-start(bf16[4,16,1024]{2,1,0:T(8,128)(2,1)S(1)} %shard_map.133.first_ref), channel_id=1, source_target_pairs={{0,2},{2,0},{4,6},{6,4},{1,3},{3,1},{5,7},{7,5},{8,10},{10,8},{12,... | collective-permute-start | bytes 393224 | tf_op jit(solution)/shard_map/ppermute | solution.py:332
  72.0 4.4 %collective-permute-done.3.second_ref = bf16[4,16,1024]{2,1,0:T(8,128)(2,1)S(1)} collective-permute-done((bf16[4,16,1024]{2,1,0:T(8,128)(2,1)S(1)}, bf16[4,16,1024]{2,1,0:T(8,128)(2,1)S(1)}, u32[]{:S(2)}, u32[]{:S(2)}) %collective-permute-start.3) | collective-permute-done | bytes 131104 | tf_op jit(solution)/shard_map/ppermute | solution.py:332
  76.4 2.9 %collective-permute-start.4 = (bf16[8,16,1024]{2,1,0:T(8,128)(2,1)S(1)}, bf16[8,16,1024]{2,1,0:T(8,128)(2,1)S(1)}, u32[]{:S(2)}, u32[]{:S(2)}) collective-permute-start(bf16[8,16,1024]{2,1,0:T(8,128)(2,1)S(1)} %shard_map.134.first_ref), channel_id=1, source_target_pairs={{0,6},{2,4},{4,2},{6,0},{1,7},{3,5},{5,3},{7,1},{8,14},{10,12},{12... | collective-permute-start | bytes 786440 | tf_op jit(solution)/shard_map/ppermute | solution.py:332
  79.3 6.6 %collective-permute-done.4.second_ref = bf16[8,16,1024]{2,1,0:T(8,128)(2,1)S(1)} collective-permute-done((bf16[8,16,1024]{2,1,0:T(8,128)(2,1)S(1)}, bf16[8,16,1024]{2,1,0:T(8,128)(2,1)S(1)}, u32[]{:S(2)}, u32[]{:S(2)}) %collective-permute-start.4) | collective-permute-done | bytes 262176 | tf_op jit(solution)/shard_map/ppermute | solution.py:332
  85.9 1.9 %collective-permute-start.5 = (bf16[16,16,1024]{2,1,0:T(8,128)(2,1)S(1)}, bf16[16,16,1024]{2,1,0:T(8,128)(2,1)S(1)}, u32[]{:S(2)}, u32[]{:S(2)}) collective-permute-start(bf16[16,16,1024]{2,1,0:T(8,128)(2,1)S(1)} %shard_map.135.own_ref), channel_id=1, source_target_pairs={{0,1},{1,0},{2,3},{3,2},{4,5},{5,4},{6,7},{7,6},{8,9},{9,8},{10,11... | collective-permute-start | bytes 1572872 | tf_op jit(solution)/shard_map/ppermute | solution.py:309
  87.9 0.0 all-to-all-done.1.payload_ref
  87.9 0.9 shard_map.130
  88.8 12.0 %all-to-all-start.2 = ((bf16[16,32,128]{2,1,0:T(8,128)(2,1)}), bf16[16,32,128]{2,1,0:T(8,128)(2,1)S(1)}, u32[]{:S(2)}, u32[]{:S(2)}) async-start(bf16[16,32,128]{2,1,0:T(8,128)(2,1)} %bitcast.6), calls=%async_computation.2 | async-start | bytes 262144 | tf_op jit(solution)/shard_map/all_to_all | solution.py:354
  100.8 0.1 reshape_tile.3.gain_ref
  100.9 2.2 %shard_map.131.parts_ref = f32[128,1536]{1,0:T(8,128)S(1)} custom-call(bf16[128,1664]{1,0:T(8,128)(2,1)S(1)} %get-tuple-element.8.rounded_ref, bf16[16,512]{1,0:T(8,128)(2,1)S(1)} %copy-done.2, bf16[16,512]{1,0:T(8,128)(2,1)S(1)} %copy-done.3, f32[1,512]{1,0:T(1,128)S(1)} %bitcast.16, f32[1,512]{1,0:T(1,128)S(1)} %bitcast.18), custom_call_target="tpu_custom_call" | custom-call | flops 1073741824 | bytes 1048576 | tf_op jit(solution)/shard_map/pallas_call | solution.py:297
  103.1 0.0 collective-permute-done.5.other_ref
  103.1 12.2 %all-to-all-done.2 = bf16[16,32,128]{2,1,0:T(8,128)(2,1)S(1)} async-done(((bf16[16,32,128]{2,1,0:T(8,128)(2,1)}), bf16[16,32,128]{2,1,0:T(8,128)(2,1)S(1)}, u32[]{:S(2)}, u32[]{:S(2)}) %all-to-all-start.2) | async-done | bytes 131104 | tf_op jit(solution)/shard_map/all_to_all | solution.py:354
  115.3 2.7 %shard_map.136 = bf16[128,1024]{1,0:T(8,128)(2,1)} custom-call(bf16[512,128]{1,0:T(8,128)(2,1)S(1)} %bitcast.10, f32[128,1536]{1,0:T(8,128)S(1)} %shard_map.131.parts_ref, f32[1,512]{1,0:T(1,128)S(1)} %reshape_tile.3.gain_ref, bf16[16,16,1024]{2,1,0:T(8,128)(2,1)S(1)} %shard_map.135.own_ref, bf16[16,16,1024]{2,1,0:T(8,128)(2,1)S(1)} %collective-permute-done.5.other_ref), custom_call_target="tpu_custom_call" | custom-call | flops 1073741824 | bytes 1048576 | tf_op jit(solution)/shard_map/pallas_call | solution.py:297
  (13 shorter events, 0.1 us)
Async XLA Ops:
  1.1 33.1 %copy-start = (bf16[2,64,1024]{2,1,0:T(8,128)(2,1)S(1)}, bf16[2,64,1024]{2,1,0:T(8,128)(2,1)}, u32[]{:S(2)}) copy-start(bf16[2,64,1024]{2,1,0:T(8,128)(2,1)} %param.13) | copy-start | bytes 786436
  1.1 33.1 %copy-start.4 = (f32[1024]{0:T(1024)S(1)}, f32[1024]{0:T(1024)}, u32[]{:S(2)}) copy-start(f32[1024]{0:T(1024)} %param.14) | copy-start | bytes 12292
  1.1 36.7 %copy-start.2 = (bf16[16,512]{1,0:T(8,128)(2,1)S(1)}, bf16[16,512]{1,0:T(8,128)(2,1)}, u32[]{:S(2)}) copy-start(bf16[16,512]{1,0:T(8,128)(2,1)} %up_forward_ref.3) | copy-start | bytes 49156
  1.1 36.7 %copy-start.3 = (bf16[16,512]{1,0:T(8,128)(2,1)S(1)}, bf16[16,512]{1,0:T(8,128)(2,1)}, u32[]{:S(2)}) copy-start(bf16[16,512]{1,0:T(8,128)(2,1)} %up_backward_ref.3) | copy-start | bytes 49156
  1.1 36.7 %copy-start.5 = (f32[512]{0:T(512)S(1)}, f32[512]{0:T(512)}, u32[]{:S(2)}) copy-start(f32[512]{0:T(512)} %param.22) | copy-start | bytes 6148
  1.1 36.6 %copy-start.6 = (f32[512]{0:T(512)S(1)}, f32[512]{0:T(512)}, u32[]{:S(2)}) copy-start(f32[512]{0:T(512)} %param.23) | copy-start | bytes 6148
  32.3 5.5 %collective-permute-start = (bf16[16,32,1664]{2,1,0:T(8,128)(2,1)S(1)}, bf16[16,32,1664]{2,1,0:T(8,128)(2,1)S(1)}, u32[]{:S(2)}, u32[]{:S(2)}) collective-permute-start(bf16[16,32,1664]{2,1,0:T(8,128)(2,1)S(1)} %all_to_all.15.own_ref), channel_id=1, source_target_pairs={{0,1},{1,0},{2,3},{3,2},{4,5},{5,4},{6,7},{7,6},{8,9},{9,8},{10,11... | collective-permute-start | bytes 5111816 | tf_op jit(solution)/shard_map/ppermute | solution.py:309
  37.8 18.5 %copy-start.1 = (bf16[16,1024]{1,0:T(8,128)(2,1)S(1)}, bf16[16,1024]{1,0:T(8,128)(2,1)}, u32[]{:S(2)}) copy-start(bf16[16,1024]{1,0:T(8,128)(2,1)} %param.25) | copy-start | bytes 98308
  41.1 46.7 %all-to-all-start.1 = ((bf16[16,40,128]{2,1,0:T(8,128)(2,1)}), bf16[16,40,128]{2,1,0:T(8,128)(2,1)S(1)}, u32[]{:S(2)}, u32[]{:S(2)}) async-start(bf16[16,40,128]{2,1,0:T(8,128)(2,1)} %get-tuple-element.7), calls=%async_computation.1 | async-start | bytes 327680 | tf_op jit(solution)/shard_map/all_to_all | solution.py:349
  56.3 44.5 %copy-start.7 = (f32[32]{0:T(128)S(1)}, f32[32]{0:T(128)}, u32[]{:S(2)}) copy-start(f32[32]{0:T(128)} %param.24) | copy-start | bytes 388
  56.3 5.8 %collective-permute-start.1 = (bf16[1,16,1024]{2,1,0:T(8,128)(2,1)S(1)}, bf16[1,16,1024]{2,1,0:T(8,128)(2,1)S(1)}, u32[]{:S(2)}, u32[]{:S(2)}) collective-permute-start(bf16[1,16,1024]{2,1,0:T(8,128)(2,1)S(1)} %bitcast.12), channel_id=1, source_target_pairs={{0,8},{8,0},{16,24},{24,16},{1,9},{9,1},{17,25},{25,17},{2,10},{10... | collective-permute-start | bytes 98312 | tf_op jit(solution)/shard_map/ppermute | solution.py:332
  62.2 7.4 %collective-permute-start.2 = (bf16[2,16,1024]{2,1,0:T(8,128)(2,1)S(1)}, bf16[2,16,1024]{2,1,0:T(8,128)(2,1)S(1)}, u32[]{:S(2)}, u32[]{:S(2)}) collective-permute-start(bf16[2,16,1024]{2,1,0:T(8,128)(2,1)S(1)} %shard_map.132.first_ref), channel_id=1, source_target_pairs={{0,24},{8,16},{16,8},{24,0},{1,25},{9,17},{17,9},{25,1},{2,26},{10... | collective-permute-start | bytes 196616 | tf_op jit(solution)/shard_map/ppermute | solution.py:332
  69.5 6.9 %collective-permute-start.3 = (bf16[4,16,1024]{2,1,0:T(8,128)(2,1)S(1)}, bf16[4,16,1024]{2,1,0:T(8,128)(2,1)S(1)}, u32[]{:S(2)}, u32[]{:S(2)}) collective-permute-start(bf16[4,16,1024]{2,1,0:T(8,128)(2,1)S(1)} %shard_map.133.first_ref), channel_id=1, source_target_pairs={{0,2},{2,0},{4,6},{6,4},{1,3},{3,1},{5,7},{7,5},{8,10},{10,8},{12,... | collective-permute-start | bytes 393224 | tf_op jit(solution)/shard_map/ppermute | solution.py:332
  76.4 9.5 %collective-permute-start.4 = (bf16[8,16,1024]{2,1,0:T(8,128)(2,1)S(1)}, bf16[8,16,1024]{2,1,0:T(8,128)(2,1)S(1)}, u32[]{:S(2)}, u32[]{:S(2)}) collective-permute-start(bf16[8,16,1024]{2,1,0:T(8,128)(2,1)S(1)} %shard_map.134.first_ref), channel_id=1, source_target_pairs={{0,6},{2,4},{4,2},{6,0},{1,7},{3,5},{5,3},{7,1},{8,14},{10,12},{12... | collective-permute-start | bytes 786440 | tf_op jit(solution)/shard_map/ppermute | solution.py:332
  85.9 17.2 %collective-permute-start.5 = (bf16[16,16,1024]{2,1,0:T(8,128)(2,1)S(1)}, bf16[16,16,1024]{2,1,0:T(8,128)(2,1)S(1)}, u32[]{:S(2)}, u32[]{:S(2)}) collective-permute-start(bf16[16,16,1024]{2,1,0:T(8,128)(2,1)S(1)} %shard_map.135.own_ref), channel_id=1, source_target_pairs={{0,1},{1,0},{2,3},{3,2},{4,5},{5,4},{6,7},{7,6},{8,9},{9,8},{10,11... | collective-permute-start | bytes 1572872 | tf_op jit(solution)/shard_map/ppermute | solution.py:309
  88.8 26.5 %all-to-all-start.2 = ((bf16[16,32,128]{2,1,0:T(8,128)(2,1)}), bf16[16,32,128]{2,1,0:T(8,128)(2,1)S(1)}, u32[]{:S(2)}, u32[]{:S(2)}) async-start(bf16[16,32,128]{2,1,0:T(8,128)(2,1)} %bitcast.6), calls=%async_computation.2 | async-start | bytes 262144 | tf_op jit(solution)/shard_map/all_to_all | solution.py:354

commit v6 on v5

--- a/solution.py
+++ b/solution.py
@@ -14,6 +14,7 @@
 BLOCK = 64
 LANES = 128
 ALL = 3 * WIDTH + LANES
+SENT = ALL + LANES
 EPS = 1e-06
 f32 = jnp.float32
 bf16 = jnp.bfloat16
@@ -45,11 +46,11 @@
 
 
 def pack_kernel(
-    key_hbm, value_hbm, query_hbm, forward_hbm, backward_hbm,
-    out_ref, key_ref, value_ref, query_ref, forward_ref, backward_ref, sems,
-):
-    sources = (key_hbm, value_hbm, query_hbm, forward_hbm, backward_hbm)
-    targets = (key_ref, value_ref, query_ref, forward_ref, backward_ref)
+    key_hbm, value_hbm, query_hbm, forward_hbm, backward_hbm, mix_hbm,
+    out_ref, key_ref, value_ref, query_ref, forward_ref, backward_ref, mix_ref, sems,
+):
+    sources = (key_hbm, value_hbm, query_hbm, forward_hbm, backward_hbm, mix_hbm)
+    targets = (key_ref, value_ref, query_ref, forward_ref, backward_ref, mix_ref)
     copies = [
         pltpu.make_async_copy(source, target, sems.at[i])
         for i, (source, target) in enumerate(zip(sources, targets))
@@ -66,7 +67,10 @@
         [key_ref[...], value_ref[...], query_ref[...], ranks.astype(bf16)], axis=1
     )
     for i in range(16):
-        out_ref[i] = block
+        start = (i // 4) * 2 * LANES
+        out_ref[i, :, :ALL] = block
+        out_ref[i, :16, ALL:] = mix_ref[:, start : start + LANES]
+        out_ref[i, 16:, ALL:] = mix_ref[:, start + LANES : start + 2 * LANES]
 
 
 def join_kernel(first_ref, second_ref, out_ref):
@@ -78,14 +82,6 @@
 def slot_of(index, axis):
     apart = index ^ lax.axis_index(axis)
     return apart ^ (apart >> 1)
-
-
-def in_order(ref):
-    pieces = []
-    for y in range(4):
-        for x in range(4):
-            pieces.append(ref[slot_of(x, "dp_1") * 4 + slot_of(y, "dp_0")])
-    return jnp.concatenate(pieces, axis=0)
 
 
 def norm_kernel(tokens_ref, gain_ref, normed_ref):
@@ -118,12 +114,13 @@
 
 def block_kernel(
     normed_ref, own_ref, other_ref, up_forward_ref, up_backward_ref,
-    bias_forward_ref, bias_backward_ref, payload_ref, rounded_ref,
+    bias_forward_ref, bias_backward_ref, payload_ref, rounded_ref, mix_ref,
 ):
     core = lax.axis_index("dp_2")
-    projected = dot(normed_ref[core], own_ref[...].reshape(WIDTH, ALL)) + dot(
-        normed_ref[1 - core], other_ref[...].reshape(WIDTH, ALL)
-    )
+    projected = dot(normed_ref[core], own_ref[:, :, :ALL].reshape(WIDTH, ALL)) + dot(
+        normed_ref[1 - core], other_ref[:, :, :ALL].reshape(WIDTH, ALL)
+    )
+    mix_ref[0] = own_ref[:, :, ALL:]
     rounded = projected.astype(bf16)
     rounded_ref[...] = rounded
     values = rounded[:, WIDTH : 2 * WIDTH]
@@ -286,7 +283,15 @@
     first, second = shuffled[:, :256], shuffled[:, 256:]
     mine = jnp.where(core == 0, first, second)
     theirs = jnp.where(core == 0, second, first)
-    out_ref[...] = (dot(mine, in_order(own_ref)) + dot(theirs, in_order(other_ref))).astype(bf16)
+    for quarter in range(4):
+        slot = slot_of(quarter, "dp_0")
+        for half in range(2):
+            rows = slice(16 * half, 16 * half + 16)
+            start = (2 * quarter + half) * LANES
+            out_ref[:, start : start + LANES] = (
+                dot(mine, own_ref[slot, :, rows, :].reshape(256, LANES))
+                + dot(theirs, other_ref[slot, :, rows, :].reshape(256, LANES))
+            ).astype(bf16)
 
 
 VMEM = pl.BlockSpec(memory_space=pltpu.VMEM)
@@ -319,34 +324,37 @@
     hbm = pl.BlockSpec(memory_space=pltpu.HBM)
     sources = [
         pltpu.with_memory_space_constraint(x, pltpu.HBM)
-        for x in (w_key, w_value, w_query, w_rank_forward.T, w_rank_backward.T)
+        for x in (w_key, w_value, w_query, w_rank_forward.T, w_rank_backward.T, w_out)
     ]
     send = call(
-        pack_kernel, shape((16, 32, ALL), bf16), [hbm] * 5, 1 << 26, *sources,
-        scratch=[pltpu.VMEM(x.shape, bf16) for x in sources] + [pltpu.SemaphoreType.DMA((5,))],
+        pack_kernel, shape((16, 32, SENT), bf16), [hbm] * 6, 1 << 26, *sources,
+        scratch=[pltpu.VMEM(x.shape, bf16) for x in sources] + [pltpu.SemaphoreType.DMA((6,))],
     )
     own = lax.all_to_all(send, PLANE, 0, 0)
     other = swapped(own)
-    mix = w_out[None]
-    for axis, flip in (("dp_0", 1), ("dp_0", 3), ("dp_1", 1), ("dp_1", 3)):
-        arrived = lax.ppermute(mix, axis, [(i, i ^ flip) for i in range(4)])
+    normed = call(
+        norm_kernel, shape((2, rows, 512), bf16), [VMEM, VMEM], 1 << 28,
+        tokens.reshape(rows, width), norm_gain.reshape(1, width),
+    )
+    decays = (
+        up_forward, up_backward, bias_forward.reshape(1, WIDTH), bias_backward.reshape(1, WIDTH)
+    )
+    payload, rounded, mix = call(
+        block_kernel,
+        (
+            shape((HEADS, 40, LANES), bf16), shape((rows, ALL), bf16),
+            shape((1, 16, 32, LANES), bf16),
+        ),
+        [VMEM] * 7, 1 << 30, normed, own, other, *decays,
+    )
+    inbound = lax.all_to_all(payload, "sp", 0, 0)
+    for flip in (1, 3):
+        arrived = lax.ppermute(mix, "dp_0", [(i, i ^ flip) for i in range(4)])
         mix = call(
-            join_kernel, shape((2 * mix.shape[0], 16, width), bf16), [VMEM] * 2, 1 << 26,
+            join_kernel, shape((2 * mix.shape[0], 16, 32, LANES), bf16), [VMEM] * 2, 1 << 26,
             mix, arrived,
         )
     mix_other = swapped(mix)
-    normed = call(
-        norm_kernel, shape((2, rows, 512), bf16), [VMEM, VMEM], 1 << 28,
-        tokens.reshape(rows, width), norm_gain.reshape(1, width),
-    )
-    decays = (
-        up_forward, up_backward, bias_forward.reshape(1, WIDTH), bias_backward.reshape(1, WIDTH)
-    )
-    payload, rounded = call(
-        block_kernel, (shape((HEADS, 40, LANES), bf16), shape((rows, ALL), bf16)),
-        [VMEM] * 7, 1 << 30, normed, own, other, *decays,
-    )
-    inbound = lax.all_to_all(payload, "sp", 0, 0)
     states = call(
         scan_kernel, shape((WIDTH, LANES), bf16), [VMEM], 1 << 28,
         inbound,

time: 119 us -> 108 us (0.908)
  waiting for transfers between devices: 34.6 us -> 27.8 us
  starting transfers between devices: 41.3 us -> 35.9 us
  blocking collectives: 31.1 us -> 32.5 us
    ppermute x4 -> x2, waiting for transfers between devices: 19.2 us -> 12.2 us  [body(): arrived = lax.ppermute(mix, 'dp_0', [(i, i ^ flip) for i in range(4)])]
    ppermute x4 -> x2, starting transfers between devices: 10.2 us -> 4.67 us  [body(): arrived = lax.ppermute(mix, 'dp_0', [(i, i ^ flip) for i in range(4)])]
    all_to_all x1, blocking collectives: 31.1 us -> 32.5 us  [body(): own = lax.all_to_all(send, PLANE, 0, 0)]
    pallas_call x10 -> x8, Pallas kernels: 10.6 us -> 10.8 us  [call(): pl.pallas_call(kernel, out_shape=outs, in_specs=specs, out_specs=(VMEM,)...]
  transfers between devices with their start and end apart: 8 -> 6, of which waited for: 6 -> 4; matrix products, arithmetic and copies ran while one was open for 0% -> 0% of each run, Pallas kernels for 3% -> 3%
where the time goes in v6:
time: 108 us; the launch traced here: 107 us
  starting transfers between devices  35.9 us (33%)
  blocking collectives  32.5 us (30%)
  waiting for transfers between devices  27.8 us (26%)
  Pallas kernels  10.8 us (10%)
    all_to_all x1, blocking collectives, body(): own = lax.all_to_all(send, PLANE, 0, 0)  32.5 us
    all_to_all x1, starting transfers between devices, body(): inbound = lax.all_to_all(payload, 'sp', 0, 0)  15.3 us
    all_to_all x1, waiting for transfers between devices, body(): returned = lax.all_to_all(states.reshape(HEADS, HEAD, LANES), 'sp', 0, 0)  12.2 us
    ppermute x2, waiting for transfers between devices, body(): arrived = lax.ppermute(mix, 'dp_0', [(i, i ^ flip) for i in range(4)])  12.2 us
    all_to_all x1, starting transfers between devices, body(): returned = lax.all_to_all(states.reshape(HEADS, HEAD, LANES), 'sp', 0, 0)  12 us
    pallas_call x8, Pallas kernels, call(): pl.pallas_call(kernel, out_shape=outs, in_specs=specs, out_specs=(VMEM,)...  10.8 us
    ppermute x2, starting transfers between devices, body(): arrived = lax.ppermute(mix, 'dp_0', [(i, i ^ flip) for i in range(4)])  4.67 us
    ppermute x2, starting transfers between devices, swapped(): return lax.ppermute(x, 'dp_2', [(0, 1), (1, 0)])  3.83 us
  transfers between devices with their start and end apart: 6, of which 4 were waited for; matrix products, arithmetic and copies ran while one was open for 0% of the time, Pallas kernels for 3%

profile of v6, /device:TPU:32, one launch (start us, length us, event | category | flops | bytes accessed | tf_op | source)
XLA Modules:
  0.0 107.3 jit_solution(6853754562866055899)
XLA Ops:
  0.0 1.2 %shard_map.128 = bf16[16,32,1792]{2,1,0:T(8,128)(2,1)S(1)} custom-call(bf16[32,512]{1,0:T(8,128)(2,1)} %key_hbm.1, bf16[32,512]{1,0:T(8,128)(2,1)} %value_hbm.1, bf16[32,512]{1,0:T(8,128)(2,1)} %query_hbm.1, bf16[16,32]{1,0:T(8,128)(2,1)} %bitcast.16, bf16[16,32]{1,0:T(8,128)(2,1)} %bitcast.17, bf16[16,1024]{1,0:T(8,128)(2,1)} %mix_hbm.1), custom_call_target="tpu_custom_call" | custom-call | flops 67108864 | bytes 1048576 | tf_op jit(solution)/shard_map/pallas_call | solution.py:302
  1.2 0.0 copy-start
  1.2 0.0 copy-start.3
  1.2 0.0 copy-start.1
  1.2 0.0 copy-start.2
  1.2 0.0 copy-start.4
  1.2 0.0 copy-start.5
  1.2 32.5 %all_to_all.15.own_ref = bf16[16,32,1792]{2,1,0:T(8,128)(2,1)S(1)} all-to-all(bf16[16,32,1792]{2,1,0:T(8,128)(2,1)S(1)} %shard_map.128), channel_id=1, replica_groups=mesh['sp'=16,'dp_0'=4,'dp_1'=4,'dp_2'=2] {'dp_0','dp_1'}, dimensions={0} | all-to-all | bytes 3670016 | tf_op jit(solution)/shard_map/all_to_all | solution.py:333
  33.8 1.9 %collective-permute-start = (bf16[16,32,1792]{2,1,0:T(8,128)(2,1)S(1)}, bf16[16,32,1792]{2,1,0:T(8,128)(2,1)S(1)}, u32[]{:S(2)}, u32[]{:S(2)}) collective-permute-start(bf16[16,32,1792]{2,1,0:T(8,128)(2,1)S(1)} %all_to_all.15.own_ref), channel_id=1, source_target_pairs={{0,1},{1,0},{2,3},{3,2},{4,5},{5,4},{6,7},{7,6},{8,9},{9,8},{10,11... | collective-permute-start | bytes 5505032 | tf_op jit(solution)/shard_map/ppermute | solution.py:314
  35.7 0.0 copy-done
  35.7 0.0 copy-done.3
  35.7 0.3 shard_map.127.normed_ref
  36.1 3.4 %collective-permute-done.other_ref = bf16[16,32,1792]{2,1,0:T(8,128)(2,1)S(1)} collective-permute-done((bf16[16,32,1792]{2,1,0:T(8,128)(2,1)S(1)}, bf16[16,32,1792]{2,1,0:T(8,128)(2,1)S(1)}, u32[]{:S(2)}, u32[]{:S(2)}) %collective-permute-start) | collective-permute-done | bytes 1835040 | tf_op jit(solution)/shard_map/ppermute | solution.py:314
  39.5 0.0 copy-done.1
  39.5 0.0 copy-done.2
  39.5 0.0 copy-done.4
  39.5 0.0 copy-done.5
  39.5 3.3 %shard_map.129 = (bf16[16,40,128]{2,1,0:T(8,128)(2,1)}, bf16[128,1664]{1,0:T(8,128)(2,1)S(1)}, bf16[1,16,32,128]{3,2,1,0:T(8,128)(2,1)S(1)}) custom-call(bf16[2,128,512]{2,1,0:T(8,128)(2,1)S(1)} %shard_map.127.normed_ref, bf16[16,32,1792]{2,1,0:T(8,128)(2,1)S(1)} %all_to_all.15.own_ref, bf16[16,32,1792]{2,1,0:T(8,128)(2,1)S(1)} %collective-permute-done.other_ref, ...), custom_call_target="tpu_custom_call" | custom-call | flops 1073741824 | bytes 1048576 | tf_op jit(solution)/shard_map/pallas_call | solution.py:302
  42.8 15.3 %all-to-all-start.1 = ((bf16[16,40,128]{2,1,0:T(8,128)(2,1)}), bf16[16,40,128]{2,1,0:T(8,128)(2,1)S(1)}, u32[]{:S(2)}, u32[]{:S(2)}) async-start(bf16[16,40,128]{2,1,0:T(8,128)(2,1)} %get-tuple-element.8), calls=%async_computation.1 | async-start | bytes 327680 | tf_op jit(solution)/shard_map/all_to_all | solution.py:350
  58.1 1.9 %collective-permute-start.1 = (bf16[1,16,32,128]{3,2,1,0:T(8,128)(2,1)S(1)}, bf16[1,16,32,128]{3,2,1,0:T(8,128)(2,1)S(1)}, u32[]{:S(2)}, u32[]{:S(2)}) collective-permute-start(bf16[1,16,32,128]{3,2,1,0:T(8,128)(2,1)S(1)} %get-tuple-element.10.first_ref), channel_id=1, source_target_pairs={{0,8},{8,0},{16,24},{24,16},{1,9},{9,1},{17,25},{25,17},{2,10},{10... | collective-permute-start | bytes 393224 | tf_op jit(solution)/shard_map/ppermute | solution.py:352
  60.0 4.9 %collective-permute-done.1.second_ref = bf16[1,16,32,128]{3,2,1,0:T(8,128)(2,1)S(1)} collective-permute-done((bf16[1,16,32,128]{3,2,1,0:T(8,128)(2,1)S(1)}, bf16[1,16,32,128]{3,2,1,0:T(8,128)(2,1)S(1)}, u32[]{:S(2)}, u32[]{:S(2)}) %collective-permute-start.1) | collective-permute-done | bytes 131104 | tf_op jit(solution)/shard_map/ppermute | solution.py:352
  65.0 2.8 %collective-permute-start.2 = (bf16[2,16,32,128]{3,2,1,0:T(8,128)(2,1)S(1)}, bf16[2,16,32,128]{3,2,1,0:T(8,128)(2,1)S(1)}, u32[]{:S(2)}, u32[]{:S(2)}) collective-permute-start(bf16[2,16,32,128]{3,2,1,0:T(8,128)(2,1)S(1)} %shard_map.132.first_ref), channel_id=1, source_target_pairs={{0,24},{8,16},{16,8},{24,0},{1,25},{9,17},{17,9},{25,1},{2,26},{10... | collective-permute-start | bytes 786440 | tf_op jit(solution)/shard_map/ppermute | solution.py:352
  67.8 7.3 %collective-permute-done.2.second_ref = bf16[2,16,32,128]{3,2,1,0:T(8,128)(2,1)S(1)} collective-permute-done((bf16[2,16,32,128]{3,2,1,0:T(8,128)(2,1)S(1)}, bf16[2,16,32,128]{3,2,1,0:T(8,128)(2,1)S(1)}, u32[]{:S(2)}, u32[]{:S(2)}) %collective-permute-start.2) | collective-permute-done | bytes 262176 | tf_op jit(solution)/shard_map/ppermute | solution.py:352
  75.1 1.9 %collective-permute-start.3 = (bf16[4,16,32,128]{3,2,1,0:T(8,128)(2,1)S(1)}, bf16[4,16,32,128]{3,2,1,0:T(8,128)(2,1)S(1)}, u32[]{:S(2)}, u32[]{:S(2)}) collective-permute-start(bf16[4,16,32,128]{3,2,1,0:T(8,128)(2,1)S(1)} %shard_map.133.own_ref), channel_id=1, source_target_pairs={{0,1},{1,0},{2,3},{3,2},{4,5},{5,4},{6,7},{7,6},{8,9},{9,8},{10,11... | collective-permute-start | bytes 1572872 | tf_op jit(solution)/shard_map/ppermute | solution.py:314
  77.0 0.0 all-to-all-done.1.payload_ref
  77.0 0.9 shard_map.130
  77.9 12.0 %all-to-all-start.2 = ((bf16[16,32,128]{2,1,0:T(8,128)(2,1)}), bf16[16,32,128]{2,1,0:T(8,128)(2,1)S(1)}, u32[]{:S(2)}, u32[]{:S(2)}) async-start(bf16[16,32,128]{2,1,0:T(8,128)(2,1)} %bitcast.6), calls=%async_computation.2 | async-start | bytes 262144 | tf_op jit(solution)/shard_map/all_to_all | solution.py:362
  90.0 0.1 reshape_tile.3.gain_ref
  90.0 2.2 %shard_map.131.parts_ref = f32[128,1536]{1,0:T(8,128)S(1)} custom-call(bf16[128,1664]{1,0:T(8,128)(2,1)S(1)} %get-tuple-element.9.rounded_ref, bf16[16,512]{1,0:T(8,128)(2,1)S(1)} %copy-done.1, bf16[16,512]{1,0:T(8,128)(2,1)S(1)} %copy-done.2, f32[1,512]{1,0:T(1,128)S(1)} %bitcast.13, f32[1,512]{1,0:T(1,128)S(1)} %bitcast.15), custom_call_target="tpu_custom_call" | custom-call | flops 1073741824 | bytes 1048576 | tf_op jit(solution)/shard_map/pallas_call | solution.py:302
  92.2 0.0 collective-permute-done.3.other_ref
  92.2 12.2 %all-to-all-done.2 = bf16[16,32,128]{2,1,0:T(8,128)(2,1)S(1)} async-done(((bf16[16,32,128]{2,1,0:T(8,128)(2,1)}), bf16[16,32,128]{2,1,0:T(8,128)(2,1)S(1)}, u32[]{:S(2)}, u32[]{:S(2)}) %all-to-all-start.2) | async-done | bytes 131104 | tf_op jit(solution)/shard_map/all_to_all | solution.py:362
  104.4 2.9 %shard_map.134 = bf16[128,1024]{1,0:T(8,128)(2,1)} custom-call(bf16[512,128]{1,0:T(8,128)(2,1)S(1)} %bitcast.9, f32[128,1536]{1,0:T(8,128)S(1)} %shard_map.131.parts_ref, f32[1,512]{1,0:T(1,128)S(1)} %reshape_tile.3.gain_ref, bf16[4,16,32,128]{3,2,1,0:T(8,128)(2,1)S(1)} %shard_map.133.own_ref, bf16[4,16,32,128]{3,2,1,0:T(8,128)(2,1)S(1)} %collective-permute-done.3.other_ref), custom_call_target="tpu_custom_call" | custom-call | flops 1073741824 | bytes 1048576 | tf_op jit(solution)/shard_map/pallas_call | solution.py:302
  (5 shorter events, 0.1 us)
Async XLA Ops:
  1.2 34.5 %copy-start = (bf16[2,64,1024]{2,1,0:T(8,128)(2,1)S(1)}, bf16[2,64,1024]{2,1,0:T(8,128)(2,1)}, u32[]{:S(2)}) copy-start(bf16[2,64,1024]{2,1,0:T(8,128)(2,1)} %param.13) | copy-start | bytes 786436
  1.2 34.5 %copy-start.3 = (f32[1024]{0:T(1024)S(1)}, f32[1024]{0:T(1024)}, u32[]{:S(2)}) copy-start(f32[1024]{0:T(1024)} %param.14) | copy-start | bytes 12292
  1.2 38.3 %copy-start.1 = (bf16[16,512]{1,0:T(8,128)(2,1)S(1)}, bf16[16,512]{1,0:T(8,128)(2,1)}, u32[]{:S(2)}) copy-start(bf16[16,512]{1,0:T(8,128)(2,1)} %up_forward_ref.3) | copy-start | bytes 49156
  1.2 38.3 %copy-start.2 = (bf16[16,512]{1,0:T(8,128)(2,1)S(1)}, bf16[16,512]{1,0:T(8,128)(2,1)}, u32[]{:S(2)}) copy-start(bf16[16,512]{1,0:T(8,128)(2,1)} %up_backward_ref.3) | copy-start | bytes 49156
  1.2 38.2 %copy-start.4 = (f32[512]{0:T(512)S(1)}, f32[512]{0:T(512)}, u32[]{:S(2)}) copy-start(f32[512]{0:T(512)} %param.22) | copy-start | bytes 6148
  1.2 38.2 %copy-start.5 = (f32[512]{0:T(512)S(1)}, f32[512]{0:T(512)}, u32[]{:S(2)}) copy-start(f32[512]{0:T(512)} %param.23) | copy-start | bytes 6148
  33.8 5.7 %collective-permute-start = (bf16[16,32,1792]{2,1,0:T(8,128)(2,1)S(1)}, bf16[16,32,1792]{2,1,0:T(8,128)(2,1)S(1)}, u32[]{:S(2)}, u32[]{:S(2)}) collective-permute-start(bf16[16,32,1792]{2,1,0:T(8,128)(2,1)S(1)} %all_to_all.15.own_ref), channel_id=1, source_target_pairs={{0,1},{1,0},{2,3},{3,2},{4,5},{5,4},{6,7},{7,6},{8,9},{9,8},{10,11... | collective-permute-start | bytes 5505032 | tf_op jit(solution)/shard_map/ppermute | solution.py:314
  42.8 47.2 %copy-start.6 = (f32[32]{0:T(128)S(1)}, f32[32]{0:T(128)}, u32[]{:S(2)}) copy-start(f32[32]{0:T(128)} %param.24) | copy-start | bytes 388
  42.8 34.2 %all-to-all-start.1 = ((bf16[16,40,128]{2,1,0:T(8,128)(2,1)}), bf16[16,40,128]{2,1,0:T(8,128)(2,1)S(1)}, u32[]{:S(2)}, u32[]{:S(2)}) async-start(bf16[16,40,128]{2,1,0:T(8,128)(2,1)} %get-tuple-element.8), calls=%async_computation.1 | async-start | bytes 327680 | tf_op jit(solution)/shard_map/all_to_all | solution.py:350
  58.1 6.8 %collective-permute-start.1 = (bf16[1,16,32,128]{3,2,1,0:T(8,128)(2,1)S(1)}, bf16[1,16,32,128]{3,2,1,0:T(8,128)(2,1)S(1)}, u32[]{:S(2)}, u32[]{:S(2)}) collective-permute-start(bf16[1,16,32,128]{3,2,1,0:T(8,128)(2,1)S(1)} %get-tuple-element.10.first_ref), channel_id=1, source_target_pairs={{0,8},{8,0},{16,24},{24,16},{1,9},{9,1},{17,25},{25,17},{2,10},{10... | collective-permute-start | bytes 393224 | tf_op jit(solution)/shard_map/ppermute | solution.py:352
  65.0 10.0 %collective-permute-start.2 = (bf16[2,16,32,128]{3,2,1,0:T(8,128)(2,1)S(1)}, bf16[2,16,32,128]{3,2,1,0:T(8,128)(2,1)S(1)}, u32[]{:S(2)}, u32[]{:S(2)}) collective-permute-start(bf16[2,16,32,128]{3,2,1,0:T(8,128)(2,1)S(1)} %shard_map.132.first_ref), channel_id=1, source_target_pairs={{0,24},{8,16},{16,8},{24,0},{1,25},{9,17},{17,9},{25,1},{2,26},{10... | collective-permute-start | bytes 786440 | tf_op jit(solution)/shard_map/ppermute | solution.py:352
  75.1 17.2 %collective-permute-start.3 = (bf16[4,16,32,128]{3,2,1,0:T(8,128)(2,1)S(1)}, bf16[4,16,32,128]{3,2,1,0:T(8,128)(2,1)S(1)}, u32[]{:S(2)}, u32[]{:S(2)}) collective-permute-start(bf16[4,16,32,128]{3,2,1,0:T(8,128)(2,1)S(1)} %shard_map.133.own_ref), channel_id=1, source_target_pairs={{0,1},{1,0},{2,3},{3,2},{4,5},{5,4},{6,7},{7,6},{8,9},{9,8},{10,11... | collective-permute-start | bytes 1572872 | tf_op jit(solution)/shard_map/ppermute | solution.py:314
  77.9 26.5 %all-to-all-start.2 = ((bf16[16,32,128]{2,1,0:T(8,128)(2,1)}), bf16[16,32,128]{2,1,0:T(8,128)(2,1)S(1)}, u32[]{:S(2)}, u32[]{:S(2)}) async-start(bf16[16,32,128]{2,1,0:T(8,128)(2,1)} %bitcast.6), calls=%async_computation.2 | async-start | bytes 262144 | tf_op jit(solution)/shard_map/all_to_all | solution.py:362

commit v7 on v6

--- a/solution.py
+++ b/solution.py
@@ -13,8 +13,8 @@
 WIDTH = 512
 BLOCK = 64
 LANES = 128
-ALL = 3 * WIDTH + LANES
-SENT = ALL + LANES
+ALL = 2 * WIDTH + LANES
+SENT = ALL + 2 * LANES
 EPS = 1e-06
 f32 = jnp.float32
 bf16 = jnp.bfloat16
@@ -64,13 +64,14 @@
         backward_ref[...], as_bf16(row + 16 == col)
     )
     block = jnp.concatenate(
-        [key_ref[...], value_ref[...], query_ref[...], ranks.astype(bf16)], axis=1
+        [key_ref[...], value_ref[...], ranks.astype(bf16)], axis=1
     )
     for i in range(16):
-        start = (i // 4) * 2 * LANES
+        start = (i // 4) * LANES
         out_ref[i, :, :ALL] = block
-        out_ref[i, :16, ALL:] = mix_ref[:, start : start + LANES]
-        out_ref[i, 16:, ALL:] = mix_ref[:, start + LANES : start + 2 * LANES]
+        out_ref[i, :, ALL : ALL + LANES] = query_ref[:, start : start + LANES]
+        out_ref[i, :16, ALL + LANES :] = mix_ref[:, 2 * start : 2 * start + LANES]
+        out_ref[i, 16:, ALL + LANES :] = mix_ref[:, 2 * start + LANES : 2 * start + 2 * LANES]
 
 
 def join_kernel(first_ref, second_ref, out_ref):
@@ -125,7 +126,7 @@
     rounded_ref[...] = rounded
     values = rounded[:, WIDTH : 2 * WIDTH]
     parts = rates_of(
-        rounded[:, 3 * WIDTH :], up_forward_ref, up_backward_ref, bias_forward_ref, bias_backward_ref
+        rounded[:, 2 * WIDTH :], up_forward_ref, up_backward_ref, bias_forward_ref, bias_backward_ref
     )
     high, low = parts
     row, col = grid_of((LANES, LANES))
@@ -207,12 +208,33 @@
 
 
 def query_kernel(
-    rounded_ref, up_forward_ref, up_backward_ref, bias_forward_ref, bias_backward_ref, out_ref
-):
-    queries = rounded_ref[:, 2 * WIDTH : 3 * WIDTH].astype(f32) * HEAD ** (-0.5)
+    normed_ref, own_ref, other_ref, rounded_ref, up_forward_ref, up_backward_ref,
+    bias_forward_ref, bias_backward_ref, out_ref, mix_ref,
+):
+    core = lax.axis_index("dp_2")
+
+    def weights(ref):
+        return jnp.concatenate(
+            [
+                ref[slot_of(quarter, "dp_0"), :, :, :LANES].reshape(WIDTH, LANES)
+                for quarter in range(4)
+            ],
+            axis=1,
+        )
+
+    projected = dot(normed_ref[core], weights(own_ref)) + dot(
+        normed_ref[1 - core], weights(other_ref)
+    )
+    queries = projected.astype(bf16).astype(f32) * HEAD ** (-0.5)
+    for quarter in range(4):
+        slot = slot_of(quarter, "dp_0")
+        for half in range(2):
+            rows = slice(16 * half, 16 * half + 16)
+            mix_ref[2 * quarter + half, :, core] = own_ref[slot, :, rows, LANES:]
+            mix_ref[2 * quarter + half, :, 1 - core] = other_ref[slot, :, rows, LANES:]
     keys = rounded_ref[:, :WIDTH].astype(f32)
     parts = rates_of(
-        rounded_ref[:, 3 * WIDTH :], up_forward_ref, up_backward_ref, bias_forward_ref, bias_backward_ref
+        rounded_ref[:, 2 * WIDTH :], up_forward_ref, up_backward_ref, bias_forward_ref, bias_backward_ref
     )
     decayed, inverse = [], []
     for way, mask in ((0, lambda r, c: c <= r), (1, lambda r, c: c >= r)):
@@ -244,9 +266,8 @@
 
 
 def out_kernel(
-    states_ref, parts_ref, gain_ref, own_ref, other_ref, out_ref
-):
-    core = lax.axis_index("dp_2")
+    states_ref, parts_ref, gain_ref, mix_ref, out_ref
+):
     row, col = grid_of((LANES, LANES))
     diagonal = (row // HEAD) == (col // HEAD)
     rows = []
@@ -277,21 +298,11 @@
         axis=1,
     ) * (1.0 / HEAD)
     attended = (combined * lax.rsqrt(mean + EPS) * gain_ref[...]).astype(bf16)
-    prow, pcol = grid_of((WIDTH, WIDTH))
-    source = ((pcol % 256) // 16) * 32 + (pcol // 256) * 16 + pcol % 16
-    shuffled = dot(attended, as_bf16(prow == source)).astype(bf16)
-    first, second = shuffled[:, :256], shuffled[:, 256:]
-    mine = jnp.where(core == 0, first, second)
-    theirs = jnp.where(core == 0, second, first)
-    for quarter in range(4):
-        slot = slot_of(quarter, "dp_0")
-        for half in range(2):
-            rows = slice(16 * half, 16 * half + 16)
-            start = (2 * quarter + half) * LANES
-            out_ref[:, start : start + LANES] = (
-                dot(mine, own_ref[slot, :, rows, :].reshape(256, LANES))
-                + dot(theirs, other_ref[slot, :, rows, :].reshape(256, LANES))
-            ).astype(bf16)
+    for part in range(4):
+        weights = jnp.concatenate(
+            [mix_ref[2 * part + half].reshape(WIDTH, LANES) for half in range(2)], axis=1
+        )
+        out_ref[:, part * 2 * LANES : (part + 1) * 2 * LANES] = dot(attended, weights).astype(bf16)
 
 
 VMEM = pl.BlockSpec(memory_space=pltpu.VMEM)
@@ -343,7 +354,7 @@
         block_kernel,
         (
             shape((HEADS, 40, LANES), bf16), shape((rows, ALL), bf16),
-            shape((1, 16, 32, LANES), bf16),
+            shape((1, 16, 32, 2 * LANES), bf16),
         ),
         [VMEM] * 7, 1 << 30, normed, own, other, *decays,
     )
@@ -351,7 +362,7 @@
     for flip in (1, 3):
         arrived = lax.ppermute(mix, "dp_0", [(i, i ^ flip) for i in range(4)])
         mix = call(
-            join_kernel, shape((2 * mix.shape[0], 16, 32, LANES), bf16), [VMEM] * 2, 1 << 26,
+            join_kernel, shape((2 * mix.shape[0], 16, 32, 2 * LANES), bf16), [VMEM] * 2, 1 << 26,
             mix, arrived,
         )
     mix_other = swapped(mix)
@@ -360,11 +371,15 @@
         inbound,
     )
     returned = lax.all_to_all(states.reshape(HEADS, HEAD, LANES), "sp", 0, 0)
-    parts = call(query_kernel, shape((rows, 3 * WIDTH), f32), [VMEM] * 5, 1 << 30, rounded, *decays)
+    parts, mix_all = call(
+        query_kernel,
+        (shape((rows, 3 * WIDTH), f32), shape((8, 16, 2, 16, LANES), bf16)),
+        [VMEM] * 8, 1 << 30, normed, mix, mix_other, rounded, *decays,
+    )
     mixed = call(
-        out_kernel, shape((rows, width), bf16), [VMEM] * 5, 1 << 30,
+        out_kernel, shape((rows, width), bf16), [VMEM] * 4, 1 << 30,
         returned.reshape(WIDTH, LANES), parts,
-        jnp.tile(out_gain, HEADS).reshape(1, WIDTH), mix, mix_other,
+        jnp.tile(out_gain, HEADS).reshape(1, WIDTH), mix_all,
     )
     return mixed.reshape(seqs, toks, width)
 

time: 108 us -> 121 us (1.12)
  blocking collectives: 32.5 us -> 58.7 us
  starting transfers between devices: 35.9 us -> 13.7 us
  waiting for transfers between devices: 27.8 us -> 34.5 us
  local copies, waits for them, and re-layouts: 0.12 us -> 3.29 us
    all_to_all x0 -> x1, blocking collectives: none -> 30.4 us  [body(): inbound = lax.all_to_all(payload, 'sp', 0, 0)]
    all_to_all x1 -> x0, starting transfers between devices: 15.3 us -> none  [body(): inbound = lax.all_to_all(payload, 'sp', 0, 0)]
    ppermute x2, waiting for transfers between devices: 12.2 us -> 21.8 us  [body(): arrived = lax.ppermute(mix, 'dp_0', [(i, i ^ flip) for i in range(4)])]
    all_to_all x1, starting transfers between devices: 12 us -> 5.2 us  [body(): returned = lax.all_to_all(states.reshape(HEADS, HEAD, LANES), 'sp', 0, 0)]
    all_to_all x1, blocking collectives: 32.5 us -> 28.3 us  [body(): own = lax.all_to_all(send, PLANE, 0, 0)]
    unnamed x14 -> x22, local copies, waits for them, and re-layouts: 0.04 us -> 3.21 us
    all_to_all x1, waiting for transfers between devices: 12.2 us -> 9.96 us  [body(): returned = lax.all_to_all(states.reshape(HEADS, HEAD, LANES), 'sp', 0, 0)]
  transfers between devices with their start and end apart: 6 -> 5, of which waited for: 4 -> 4; matrix products, arithmetic and copies ran while one was open for 0% -> 0% of each run, Pallas kernels for 3% -> 3%
where the time goes in v7:
time: 121 us
  blocking collectives  58.7 us (49%)
  waiting for transfers between devices  34.5 us (29%)
  starting transfers between devices  13.7 us (11%)
  Pallas kernels  10.1 us (8%)
  local copies, waits for them, and re-layouts  3.29 us (3%)
    all_to_all x1, blocking collectives, body(): inbound = lax.all_to_all(payload, 'sp', 0, 0)  30.4 us
    all_to_all x1, blocking collectives, body(): own = lax.all_to_all(send, PLANE, 0, 0)  28.3 us
    ppermute x2, waiting for transfers between devices, body(): arrived = lax.ppermute(mix, 'dp_0', [(i, i ^ flip) for i in range(4)])  21.8 us
    pallas_call x8, Pallas kernels, call(): pl.pallas_call(kernel, out_shape=outs, in_specs=specs, out_specs=(VMEM,)...  10.1 us
    all_to_all x1, waiting for transfers between devices, body(): returned = lax.all_to_all(states.reshape(HEADS, HEAD, LANES), 'sp', 0, 0)  9.96 us
    all_to_all x1, starting transfers between devices, body(): returned = lax.all_to_all(states.reshape(HEADS, HEAD, LANES), 'sp', 0, 0)  5.2 us
    ppermute x2, starting transfers between devices, body(): arrived = lax.ppermute(mix, 'dp_0', [(i, i ^ flip) for i in range(4)])  4.67 us
    ppermute x2, starting transfers between devices, swapped(): return lax.ppermute(x, 'dp_2', [(0, 1), (1, 0)])  3.83 us
  transfers between devices with their start and end apart: 5, of which 4 were waited for; matrix products, arithmetic and copies ran while one was open for 0% of the time, Pallas kernels for 3%

profile of v7, /device:TPU:32, one launch (start us, length us, event | category | flops | bytes accessed | tf_op | source)
XLA Modules:
  0.0 120.6 jit_solution(754209652722857194)
XLA Ops:
  0.0 1.1 shard_map.128
  1.1 0.0 copy-start
  1.1 0.0 copy-start.3
  1.2 0.0 copy-start.1
  1.2 0.0 copy-start.2
  1.2 0.0 copy-start.4
  1.2 0.0 copy-start.5
  1.2 28.3 %all_to_all.15.own_ref = bf16[16,32,1408]{2,1,0:T(8,128)(2,1)S(1)} all-to-all(bf16[16,32,1408]{2,1,0:T(8,128)(2,1)S(1)} %shard_map.128), channel_id=1, replica_groups=mesh['sp'=16,'dp_0'=4,'dp_1'=4,'dp_2'=2] {'dp_0','dp_1'}, dimensions={0} | all-to-all | bytes 2883584 | tf_op jit(solution)/shard_map/all_to_all | solution.py:344
  29.5 1.9 %collective-permute-start = (bf16[16,32,1408]{2,1,0:T(8,128)(2,1)S(1)}, bf16[16,32,1408]{2,1,0:T(8,128)(2,1)S(1)}, u32[]{:S(2)}, u32[]{:S(2)}) collective-permute-start(bf16[16,32,1408]{2,1,0:T(8,128)(2,1)S(1)} %all_to_all.15.own_ref), channel_id=1, source_target_pairs={{0,1},{1,0},{2,3},{3,2},{4,5},{5,4},{6,7},{7,6},{8,9},{9,8},{10,11... | collective-permute-start | bytes 4325384 | tf_op jit(solution)/shard_map/ppermute | solution.py:325
  31.5 0.0 copy-done
  31.5 0.0 copy-done.3
  31.5 0.3 shard_map.127.normed_ref
  31.8 2.8 %collective-permute-done.other_ref = bf16[16,32,1408]{2,1,0:T(8,128)(2,1)S(1)} collective-permute-done((bf16[16,32,1408]{2,1,0:T(8,128)(2,1)S(1)}, bf16[16,32,1408]{2,1,0:T(8,128)(2,1)S(1)}, u32[]{:S(2)}, u32[]{:S(2)}) %collective-permute-start) | collective-permute-done | bytes 1441824 | tf_op jit(solution)/shard_map/ppermute | solution.py:325
  34.7 2.5 %shard_map.129 = (bf16[16,40,128]{2,1,0:T(8,128)(2,1)S(1)}, bf16[128,1152]{1,0:T(8,128)(2,1)S(1)}, bf16[1,16,32,256]{3,2,1,0:T(8,128)(2,1)S(1)}) custom-call(bf16[2,128,512]{2,1,0:T(8,128)(2,1)S(1)} %shard_map.127.normed_ref, bf16[16,32,1408]{2,1,0:T(8,128)(2,1)S(1)} %all_to_all.15.own_ref, bf16[16,32,1408]{2,1,0:T(8,128)(2,1)S(1)} %collective-permute-done.other_ref, ...), custom_call_target="tpu_custom_call" | custom-call | flops 1073741824 | bytes 1048576 | tf_op jit(solution)/shard_map/pallas_call | solution.py:313
  37.2 1.9 %collective-permute-start.1 = (bf16[1,16,32,256]{3,2,1,0:T(8,128)(2,1)S(1)}, bf16[1,16,32,256]{3,2,1,0:T(8,128)(2,1)S(1)}, u32[]{:S(2)}, u32[]{:S(2)}) collective-permute-start(bf16[1,16,32,256]{3,2,1,0:T(8,128)(2,1)S(1)} %get-tuple-element.11.first_ref), channel_id=1, source_target_pairs={{0,8},{8,0},{16,24},{24,16},{1,9},{9,1},{17,25},{25,17},{2,10},{10... | collective-permute-start | bytes 786440 | tf_op jit(solution)/shard_map/ppermute | solution.py:363
  39.1 8.3 %collective-permute-done.1.second_ref = bf16[1,16,32,256]{3,2,1,0:T(8,128)(2,1)S(1)} collective-permute-done((bf16[1,16,32,256]{3,2,1,0:T(8,128)(2,1)S(1)}, bf16[1,16,32,256]{3,2,1,0:T(8,128)(2,1)S(1)}, u32[]{:S(2)}, u32[]{:S(2)}) %collective-permute-start.1) | collective-permute-done | bytes 262176 | tf_op jit(solution)/shard_map/ppermute | solution.py:363
  47.5 0.0 copy-start.10
  47.5 2.8 %collective-permute-start.2 = (bf16[2,16,32,256]{3,2,1,0:T(8,128)(2,1)S(1)}, bf16[2,16,32,256]{3,2,1,0:T(8,128)(2,1)S(1)}, u32[]{:S(2)}, u32[]{:S(2)}) collective-permute-start(bf16[2,16,32,256]{3,2,1,0:T(8,128)(2,1)S(1)} %shard_map.131.first_ref), channel_id=1, source_target_pairs={{0,24},{8,16},{16,8},{24,0},{1,25},{9,17},{17,9},{25,1},{2,26},{10... | collective-permute-start | bytes 1572872 | tf_op jit(solution)/shard_map/ppermute | solution.py:363
  50.3 13.4 %collective-permute-done.2.second_ref = bf16[2,16,32,256]{3,2,1,0:T(8,128)(2,1)S(1)} collective-permute-done((bf16[2,16,32,256]{3,2,1,0:T(8,128)(2,1)S(1)}, bf16[2,16,32,256]{3,2,1,0:T(8,128)(2,1)S(1)}, u32[]{:S(2)}, u32[]{:S(2)}) %collective-permute-start.2) | collective-permute-done | bytes 524320 | tf_op jit(solution)/shard_map/ppermute | solution.py:363
  63.7 0.1 shard_map.132.own_ref
  63.8 1.9 %collective-permute-start.3 = (bf16[4,16,32,256]{3,2,1,0:T(8,128)(2,1)S(1)}, bf16[4,16,32,256]{3,2,1,0:T(8,128)(2,1)S(1)}, u32[]{:S(2)}, u32[]{:S(2)}) collective-permute-start(bf16[4,16,32,256]{3,2,1,0:T(8,128)(2,1)S(1)} %shard_map.132.own_ref), channel_id=1, source_target_pairs={{0,1},{1,0},{2,3},{3,2},{4,5},{5,4},{6,7},{7,6},{8,9},{9,8},{10,11... | collective-permute-start | bytes 3145736 | tf_op jit(solution)/shard_map/ppermute | solution.py:325
  65.7 30.4 %all_to_all.16.payload_ref = bf16[16,40,128]{2,1,0:T(8,128)(2,1)S(1)} all-to-all(bf16[16,40,128]{2,1,0:T(8,128)(2,1)S(1)} %get-tuple-element.10), channel_id=1, replica_groups=mesh['sp'=16,'dp_0'=4,'dp_1'=4,'dp_2'=2] {'sp'}, dimensions={0} | all-to-all | bytes 327680 | tf_op jit(solution)/shard_map/all_to_all | solution.py:361
  96.1 0.9 shard_map.130
  97.0 5.2 %all-to-all-start.2 = ((bf16[16,32,128]{2,1,0:T(8,128)(2,1)}), bf16[16,32,128]{2,1,0:T(8,128)(2,1)S(1)}, u32[]{:S(2)}, u32[]{:S(2)}) async-start(bf16[16,32,128]{2,1,0:T(8,128)(2,1)} %bitcast.6), calls=%async_computation.2 | async-start | bytes 262144 | tf_op jit(solution)/shard_map/all_to_all | solution.py:373
  102.3 0.1 reshape_tile.3.gain_ref
  102.3 0.0 collective-permute-done.3.other_ref
  102.3 1.0 copy-done.9
  103.3 2.5 %shard_map.133 = (f32[128,1536]{1,0:T(8,128)S(1)}, bf16[8,16,2,16,128]{4,3,2,1,0:T(8,128)(2,1)S(1)}) custom-call(bf16[2,128,512]{2,1,0:T(8,128)(2,1)S(1)} %shard_map.127.normed_ref, bf16[4,16,32,256]{3,2,1,0:T(8,128)(2,1)S(1)} %shard_map.132.own_ref, bf16[4,16,32,256]{3,2,1,0:T(8,128)(2,1)S(1)} %collective-permute-done.3.other_ref, ...), custom_call_target="tpu_custom_call" | custom-call | flops 1073741824 | bytes 1048576 | tf_op jit(solution)/shard_map/pallas_call | solution.py:313
  105.8 1.0 copy-done.6
  106.8 10.0 %all-to-all-done.2 = bf16[16,32,128]{2,1,0:T(8,128)(2,1)S(1)} async-done(((bf16[16,32,128]{2,1,0:T(8,128)(2,1)}), bf16[16,32,128]{2,1,0:T(8,128)(2,1)S(1)}, u32[]{:S(2)}, u32[]{:S(2)}) %all-to-all-start.2) | async-done | bytes 131104 | tf_op jit(solution)/shard_map/all_to_all | solution.py:373
  116.8 1.2 %copy-done.7 = bf16[8,16,2,16,128]{4,3,2,1,0:T(8,128)(2,1)S(1)} copy-done((bf16[8,16,2,16,128]{4,3,2,1,0:T(8,128)(2,1)S(1)}, bf16[8,16,2,16,128]{4,3,2,1,0:T(8,128)(2,1)}, u32[]{:S(2)}) %copy-start.7) | copy-done | bytes 1048600
  118.0 2.6 %shard_map.134 = bf16[128,1024]{1,0:T(8,128)(2,1)} custom-call(bf16[512,128]{1,0:T(8,128)(2,1)S(1)} %bitcast.9, f32[128,1536]{1,0:T(8,128)S(1)} %get-tuple-element.13.parts_ref, f32[1,512]{1,0:T(1,128)S(1)} %reshape_tile.3.gain_ref, bf16[8,16,2,16,128]{4,3,2,1,0:T(8,128)(2,1)S(1)} %copy-done.7), custom_call_target="tpu_custom_call" | custom-call | flops 1073741824 | bytes 1048576 | tf_op jit(solution)/shard_map/pallas_call | solution.py:313
  (12 shorter events, 0.1 us)
Async XLA Ops:
  1.1 30.3 %copy-start = (bf16[2,64,1024]{2,1,0:T(8,128)(2,1)S(1)}, bf16[2,64,1024]{2,1,0:T(8,128)(2,1)}, u32[]{:S(2)}) copy-start(bf16[2,64,1024]{2,1,0:T(8,128)(2,1)} %param.13) | copy-start | bytes 786436
  1.1 30.3 %copy-start.3 = (f32[1024]{0:T(1024)S(1)}, f32[1024]{0:T(1024)}, u32[]{:S(2)}) copy-start(f32[1024]{0:T(1024)} %param.14) | copy-start | bytes 12292
  1.2 33.5 %copy-start.1 = (bf16[16,512]{1,0:T(8,128)(2,1)S(1)}, bf16[16,512]{1,0:T(8,128)(2,1)}, u32[]{:S(2)}) copy-start(bf16[16,512]{1,0:T(8,128)(2,1)} %up_forward_ref.3) | copy-start | bytes 49156
  1.2 33.5 %copy-start.2 = (bf16[16,512]{1,0:T(8,128)(2,1)S(1)}, bf16[16,512]{1,0:T(8,128)(2,1)}, u32[]{:S(2)}) copy-start(bf16[16,512]{1,0:T(8,128)(2,1)} %up_backward_ref.3) | copy-start | bytes 49156
  1.2 33.5 %copy-start.4 = (f32[512]{0:T(512)S(1)}, f32[512]{0:T(512)}, u32[]{:S(2)}) copy-start(f32[512]{0:T(512)} %param.22) | copy-start | bytes 6148
  1.2 33.5 %copy-start.5 = (f32[512]{0:T(512)S(1)}, f32[512]{0:T(512)}, u32[]{:S(2)}) copy-start(f32[512]{0:T(512)} %param.23) | copy-start | bytes 6148
  29.5 5.1 %collective-permute-start = (bf16[16,32,1408]{2,1,0:T(8,128)(2,1)S(1)}, bf16[16,32,1408]{2,1,0:T(8,128)(2,1)S(1)}, u32[]{:S(2)}, u32[]{:S(2)}) collective-permute-start(bf16[16,32,1408]{2,1,0:T(8,128)(2,1)S(1)} %all_to_all.15.own_ref), channel_id=1, source_target_pairs={{0,1},{1,0},{2,3},{3,2},{4,5},{5,4},{6,7},{7,6},{8,9},{9,8},{10,11... | collective-permute-start | bytes 4325384 | tf_op jit(solution)/shard_map/ppermute | solution.py:325
  37.2 26.6 %copy-start.8 = (bf16[128,1152]{1,0:T(8,128)(2,1)}, bf16[128,1152]{1,0:T(8,128)(2,1)S(1)}, u32[]{:S(2)}) copy-start(bf16[128,1152]{1,0:T(8,128)(2,1)S(1)} %get-tuple-element.12.rounded_ref) | copy-start | bytes 884740
  37.2 10.2 %collective-permute-start.1 = (bf16[1,16,32,256]{3,2,1,0:T(8,128)(2,1)S(1)}, bf16[1,16,32,256]{3,2,1,0:T(8,128)(2,1)S(1)}, u32[]{:S(2)}, u32[]{:S(2)}) collective-permute-start(bf16[1,16,32,256]{3,2,1,0:T(8,128)(2,1)S(1)} %get-tuple-element.11.first_ref), channel_id=1, source_target_pairs={{0,8},{8,0},{16,24},{24,16},{1,9},{9,1},{17,25},{25,17},{2,10},{10... | collective-permute-start | bytes 786440 | tf_op jit(solution)/shard_map/ppermute | solution.py:363
  47.5 54.8 %copy-start.10 = (f32[32]{0:T(128)S(1)}, f32[32]{0:T(128)}, u32[]{:S(2)}) copy-start(f32[32]{0:T(128)} %param.24) | copy-start | bytes 388
  47.5 16.2 %collective-permute-start.2 = (bf16[2,16,32,256]{3,2,1,0:T(8,128)(2,1)S(1)}, bf16[2,16,32,256]{3,2,1,0:T(8,128)(2,1)S(1)}, u32[]{:S(2)}, u32[]{:S(2)}) collective-permute-start(bf16[2,16,32,256]{3,2,1,0:T(8,128)(2,1)S(1)} %shard_map.131.first_ref), channel_id=1, source_target_pairs={{0,24},{8,16},{16,8},{24,0},{1,25},{9,17},{17,9},{25,1},{2,26},{10... | collective-permute-start | bytes 1572872 | tf_op jit(solution)/shard_map/ppermute | solution.py:363
  63.8 38.5 %collective-permute-start.3 = (bf16[4,16,32,256]{3,2,1,0:T(8,128)(2,1)S(1)}, bf16[4,16,32,256]{3,2,1,0:T(8,128)(2,1)S(1)}, u32[]{:S(2)}, u32[]{:S(2)}) collective-permute-start(bf16[4,16,32,256]{3,2,1,0:T(8,128)(2,1)S(1)} %shard_map.132.own_ref), channel_id=1, source_target_pairs={{0,1},{1,0},{2,3},{3,2},{4,5},{5,4},{6,7},{7,6},{8,9},{9,8},{10,11... | collective-permute-start | bytes 3145736 | tf_op jit(solution)/shard_map/ppermute | solution.py:325
  97.0 19.7 %all-to-all-start.2 = ((bf16[16,32,128]{2,1,0:T(8,128)(2,1)}), bf16[16,32,128]{2,1,0:T(8,128)(2,1)S(1)}, u32[]{:S(2)}, u32[]{:S(2)}) async-start(bf16[16,32,128]{2,1,0:T(8,128)(2,1)} %bitcast.6), calls=%async_computation.2 | async-start | bytes 262144 | tf_op jit(solution)/shard_map/all_to_all | solution.py:373
  102.3 1.0 copy-start.9
  105.8 1.0 copy-start.6
  116.8 1.2 %copy-start.7 = (bf16[8,16,2,16,128]{4,3,2,1,0:T(8,128)(2,1)S(1)}, bf16[8,16,2,16,128]{4,3,2,1,0:T(8,128)(2,1)}, u32[]{:S(2)}) copy-start(bf16[8,16,2,16,128]{4,3,2,1,0:T(8,128)(2,1)} %copy-done.6) | copy-start | bytes 3145732

commit v8 on v7

--- a/solution.py
+++ b/solution.py
@@ -14,7 +14,8 @@
 BLOCK = 64
 LANES = 128
 ALL = 2 * WIDTH + LANES
-SENT = ALL + 2 * LANES
+COLUMNS = 8 * 32
+SENT = COLUMNS + 32 + 32 + 8
 EPS = 1e-06
 f32 = jnp.float32
 bf16 = jnp.bfloat16
@@ -63,15 +64,17 @@
     ranks = dot_tn(forward_ref[...], as_bf16(row == col)) + dot_tn(
         backward_ref[...], as_bf16(row + 16 == col)
     )
-    block = jnp.concatenate(
-        [key_ref[...], value_ref[...], ranks.astype(bf16)], axis=1
-    )
+    packed = jnp.concatenate([ranks[8 * i : 8 * i + 8, :32] for i in range(4)], axis=1)
     for i in range(16):
+        for group in range(4):
+            lanes = slice(group * LANES, (group + 1) * LANES)
+            out_ref[i, group * 32 : (group + 1) * 32] = key_ref[:, lanes]
+            out_ref[i, (4 + group) * 32 : (5 + group) * 32] = value_ref[:, lanes]
         start = (i // 4) * LANES
-        out_ref[i, :, :ALL] = block
-        out_ref[i, :, ALL : ALL + LANES] = query_ref[:, start : start + LANES]
-        out_ref[i, :16, ALL + LANES :] = mix_ref[:, 2 * start : 2 * start + LANES]
-        out_ref[i, 16:, ALL + LANES :] = mix_ref[:, 2 * start + LANES : 2 * start + 2 * LANES]
+        out_ref[i, COLUMNS : COLUMNS + 32] = query_ref[:, start : start + LANES]
+        out_ref[i, COLUMNS + 32 : COLUMNS + 48] = mix_ref[:, 2 * start : 2 * start + LANES]
+        out_ref[i, COLUMNS + 48 : COLUMNS + 64] = mix_ref[:, 2 * start + LANES : 2 * start + 2 * LANES]
+        out_ref[i, COLUMNS + 64 :] = packed.astype(bf16)
 
 
 def join_kernel(first_ref, second_ref, out_ref):
@@ -85,14 +88,21 @@
     return apart ^ (apart >> 1)
 
 
-def norm_kernel(tokens_ref, gain_ref, normed_ref):
+def normed_halves(tokens_ref, gain_ref):
     values = tokens_ref[...].astype(f32)
     scale = lax.rsqrt(jnp.mean(values * values, axis=-1, keepdims=True) + EPS)
     normed = (values * scale * gain_ref[...]).astype(bf16)
-    for core in range(2):
-        normed_ref[core] = jnp.concatenate(
+    return [
+        jnp.concatenate(
             [normed[:, (2 * i + core) * 32 : (2 * i + core) * 32 + 32] for i in range(16)], axis=1
         )
+        for core in range(2)
+    ]
+
+
+def norm_kernel(tokens_ref, gain_ref, normed_ref):
+    for core, half in enumerate(normed_halves(tokens_ref, gain_ref)):
+        normed_ref[core] = half
 
 
 def rates_of(ranks, up_forward_ref, up_backward_ref, bias_forward_ref, bias_backward_ref):
@@ -118,11 +128,26 @@
     bias_forward_ref, bias_backward_ref, payload_ref, rounded_ref, mix_ref,
 ):
     core = lax.axis_index("dp_2")
-    projected = dot(normed_ref[core], own_ref[:, :, :ALL].reshape(WIDTH, ALL)) + dot(
-        normed_ref[1 - core], other_ref[:, :, :ALL].reshape(WIDTH, ALL)
-    )
-    mix_ref[0] = own_ref[:, :, ALL:]
-    rounded = projected.astype(bf16)
+    mix_ref[0] = own_ref[:, COLUMNS : COLUMNS + 64, :]
+
+    def columns(ref, first):
+        return jnp.concatenate(
+            [ref[:, g * 32 : (g + 1) * 32, :].reshape(WIDTH, LANES) for g in (first, first + 1)], axis=1
+        )
+
+    def rank_columns(ref):
+        packed = ref[:, COLUMNS + 64 :, :].astype(f32)
+        rows = jnp.stack([packed[:, :, 32 * i : 32 * i + 32] for i in range(4)], axis=1)
+        return rows.reshape(WIDTH, 32).astype(bf16)
+
+    mine, theirs = normed_ref[core], normed_ref[1 - core]
+    pieces = [
+        dot(mine, columns(own_ref, first)) + dot(theirs, columns(other_ref, first))
+        for first in (0, 2, 4, 6)
+    ]
+    pieces.append(dot(mine, rank_columns(own_ref)) + dot(theirs, rank_columns(other_ref)))
+    pieces.append(jnp.zeros((2 * BLOCK, LANES - 32), f32))
+    rounded = jnp.concatenate(pieces, axis=1).astype(bf16)
     rounded_ref[...] = rounded
     values = rounded[:, WIDTH : 2 * WIDTH]
     parts = rates_of(
@@ -166,9 +191,8 @@
             for seq in range(2):
                 span = slice(seq * BLOCK, (seq + 1) * BLOCK)
                 value = values[span, lanes]
-                state = dot_tn(remain[way][0][span, lanes], value) + dot_tn(
-                    remain[way][1][span, lanes], value
-                )
+                both = jnp.concatenate([half[span, lanes] for half in remain[way]], axis=0)
+                state = dot_tn(both, jnp.concatenate([value, value], axis=0))
                 parts.append(jnp.where(diagonal, state, 0.0).astype(bf16))
         folded = dot(jnp.concatenate(parts, axis=1), fold).astype(bf16)
         payload_ref[4 * group : 4 * group + 4, :HEAD, :] = folded.reshape(4, HEAD, LANES)
@@ -208,30 +232,25 @@
 
 
 def query_kernel(
-    normed_ref, own_ref, other_ref, rounded_ref, up_forward_ref, up_backward_ref,
-    bias_forward_ref, bias_backward_ref, out_ref, mix_ref,
+    tokens_ref, gain_ref, own_ref, other_ref, rounded_ref, up_forward_ref, up_backward_ref,
+    bias_forward_ref, bias_backward_ref, out_ref,
 ):
     core = lax.axis_index("dp_2")
 
     def weights(ref):
         return jnp.concatenate(
             [
-                ref[slot_of(quarter, "dp_0"), :, :, :LANES].reshape(WIDTH, LANES)
+                ref[slot_of(quarter, "dp_0"), :, :32, :].reshape(WIDTH, LANES)
                 for quarter in range(4)
             ],
             axis=1,
         )
 
-    projected = dot(normed_ref[core], weights(own_ref)) + dot(
-        normed_ref[1 - core], weights(other_ref)
+    first, second = normed_halves(tokens_ref, gain_ref)
+    projected = dot(jnp.where(core == 0, first, second), weights(own_ref)) + dot(
+        jnp.where(core == 0, second, first), weights(other_ref)
     )
     queries = projected.astype(bf16).astype(f32) * HEAD ** (-0.5)
-    for quarter in range(4):
-        slot = slot_of(quarter, "dp_0")
-        for half in range(2):
-            rows = slice(16 * half, 16 * half + 16)
-            mix_ref[2 * quarter + half, :, core] = own_ref[slot, :, rows, LANES:]
-            mix_ref[2 * quarter + half, :, 1 - core] = other_ref[slot, :, rows, LANES:]
     keys = rounded_ref[:, :WIDTH].astype(f32)
     parts = rates_of(
         rounded_ref[:, 2 * WIDTH :], up_forward_ref, up_backward_ref, bias_forward_ref, bias_backward_ref
@@ -243,66 +262,92 @@
         out_ref[:, (way + 1) * WIDTH : (way + 2) * WIDTH] = product
         decayed.append(product.astype(bf16))
         inverse.append((keys * jnp.exp(-running)).astype(bf16))
-    row, col = grid_of((4 * BLOCK, LANES))
-    own_lanes = (row // BLOCK) == (col // HEAD)
-    own_lanes_bf = as_bf16(own_lanes)
-    srow, scol = grid_of((4 * BLOCK, BLOCK))
+    row, col = grid_of((WIDTH, WIDTH))
+    natural = ((col % 256) // 16) * HEAD + (col // 256) * 16 + col % 16
+    values = dot(rounded_ref[:, WIDTH : 2 * WIDTH], as_bf16(row == natural)).astype(bf16)
+    row, col = grid_of((WIDTH, 256))
+    own_lanes = as_bf16((row // BLOCK) == (col // HEAD))
+    srow, scol = grid_of((WIDTH, BLOCK))
     lower = (srow % BLOCK) >= scol
     upper = (srow % BLOCK) <= scol
+    vrow, vcol = grid_of((WIDTH, LANES))
+    own_values = (vrow // BLOCK) == (vcol // 16)
     for seq in range(2):
         span = slice(seq * BLOCK, (seq + 1) * BLOCK)
-        for group in range(4):
-            lanes = slice(group * LANES, (group + 1) * LANES)
+        for group in range(2):
+            wide = slice(group * 256, (group + 1) * 256)
             scores = 0.0
             for way, mask in ((0, lower), (1, upper)):
-                one = decayed[way][span, lanes]
-                stacked = jnp.concatenate([one] * 4, axis=0) * own_lanes_bf
-                scores = scores + jnp.where(mask, dot_nt(stacked, inverse[way][span, lanes]), 0.0)
-            spread = jnp.where(own_lanes, dot(scores.astype(bf16), rounded_ref[span, slice(WIDTH + group * LANES, WIDTH + (group + 1) * LANES)]), 0.0)
-            out_ref[span, lanes] = (
-                spread[:BLOCK] + spread[BLOCK : 2 * BLOCK]
-                + spread[2 * BLOCK : 3 * BLOCK] + spread[3 * BLOCK :]
-            )
-
-
-def out_kernel(
-    states_ref, parts_ref, gain_ref, mix_ref, out_ref
-):
-    row, col = grid_of((LANES, LANES))
-    diagonal = (row // HEAD) == (col // HEAD)
-    rows = []
+                stacked = jnp.concatenate([decayed[way][span, wide]] * 8, axis=0) * own_lanes
+                scores = scores + jnp.where(mask, dot_nt(stacked, inverse[way][span, wide]), 0.0)
+            scores = scores.astype(bf16)
+            for half in range(2):
+                start = half * 256 + group * LANES
+                spread = dot(scores, values[span, start : start + LANES])
+                spread = jnp.where(own_values, spread, 0.0)
+                total = spread[:BLOCK]
+                for head in range(1, 8):
+                    total = total + spread[head * BLOCK : (head + 1) * BLOCK]
+                out_ref[span, start : start + LANES] = total
+
+
+def out_kernel(states_ref, parts_ref, gain_ref, own_ref, other_ref, out_ref):
+    core = lax.axis_index("dp_2")
+    row, col = grid_of((LANES, 8 * LANES))
+    source = (col // 256) * HEAD + ((col // LANES) % 2) * 16 + col % 16
+    widen = as_bf16(row == source)
+    row, col = grid_of((256, 8 * LANES))
+    diagonal = (row // HEAD) == ((col % LANES) // 16)
+    full = [
+        jnp.where(diagonal, dot(states_ref[g * 256 : (g + 1) * 256, :], widen), 0.0).astype(bf16)
+        for g in range(2)
+    ]
+    totals = [[], []]
     for seq in range(2):
         span = slice(seq * BLOCK, (seq + 1) * BLOCK)
-        pieces = []
-        for group in range(4):
-            lanes = slice(group * LANES, (group + 1) * LANES)
-            total = parts_ref[span, lanes]
-            for way in range(2):
-                widen = as_bf16(row == (2 * way + seq) * HEAD + col % HEAD)
-                full = dot(states_ref[lanes, :], widen)
-                full = jnp.where(diagonal, full, 0.0).astype(bf16)
-                start = (way + 1) * WIDTH + group * LANES
-                high, low = halves(parts_ref[span, start : start + LANES])
-                total = total + dot(high, full) + dot(low, full)
-            pieces.append(total)
-        rows.append(jnp.concatenate(pieces, axis=1))
-    combined = jnp.concatenate(rows, axis=0)
-    high, low = halves(combined * combined)
-    ones = as_bf16(diagonal)
-    mean = jnp.concatenate(
-        [
-            dot(high[:, g * LANES : (g + 1) * LANES], ones)
-            + dot(low[:, g * LANES : (g + 1) * LANES], ones)
-            for g in range(4)
-        ],
-        axis=1,
-    ) * (1.0 / HEAD)
-    attended = (combined * lax.rsqrt(mean + EPS) * gain_ref[...]).astype(bf16)
-    for part in range(4):
-        weights = jnp.concatenate(
-            [mix_ref[2 * part + half].reshape(WIDTH, LANES) for half in range(2)], axis=1
-        )
-        out_ref[:, part * 2 * LANES : (part + 1) * 2 * LANES] = dot(attended, weights).astype(bf16)
+        sides = [[], []]
+        for group in range(2):
+            queries = jnp.concatenate(
+                [
+                    parts_ref[span, (way + 1) * WIDTH + group * 256 : (way + 1) * WIDTH + group * 256 + 256]
+                    for way in range(2)
+                ],
+                axis=1,
+            )
+            right = jnp.concatenate(
+                [full[group][:, (2 * way + seq) * 256 : (2 * way + seq + 1) * 256] for way in range(2)],
+                axis=0,
+            )
+            across = dot(jnp.concatenate(halves(queries), axis=0), right)
+            across = across[:BLOCK] + across[BLOCK:]
+            for half in range(2):
+                start = half * 256 + group * LANES
+                sides[half].append(
+                    parts_ref[span, start : start + LANES] + across[:, half * LANES : (half + 1) * LANES]
+                )
+        for half in range(2):
+            totals[half].append(jnp.concatenate(sides[half], axis=1))
+    combined = [jnp.concatenate(total, axis=0) for total in totals]
+    high, low = halves(combined[0] * combined[0] + combined[1] * combined[1])
+    row, col = grid_of((256, 256))
+    ones = as_bf16((row // 16) == (col // 16))
+    scale = lax.rsqrt((dot(high, ones) + dot(low, ones)) * (1.0 / HEAD) + EPS)
+    attended = [
+        (combined[half] * scale * gain_ref[half : half + 1, :]).astype(bf16) for half in range(2)
+    ]
+    mine = jnp.where(core == 0, attended[0], attended[1])
+    theirs = jnp.where(core == 0, attended[1], attended[0])
+    for quarter in range(4):
+        slot = slot_of(quarter, "dp_0")
+
+        def weights(ref):
+            return jnp.concatenate(
+                [ref[slot, :, rows : rows + 16, :].reshape(256, LANES) for rows in (32, 48)], axis=1
+            )
+
+        out_ref[:, quarter * 256 : (quarter + 1) * 256] = (
+            dot(mine, weights(own_ref)) + dot(theirs, weights(other_ref))
+        ).astype(bf16)
 
 
 VMEM = pl.BlockSpec(memory_space=pltpu.VMEM)
@@ -321,6 +366,10 @@
     )(*args)
 
 
+def in_hbm(x):
+    return pltpu.with_memory_space_constraint(x, pltpu.HBM)
+
+
 def swapped(x):
     return lax.ppermute(x, "dp_2", [(0, 1), (1, 0)])
 
@@ -332,20 +381,21 @@
     seqs, toks, width = tokens.shape
     rows = seqs * toks
     shape = jax.ShapeDtypeStruct
+    tokens_flat, gain_flat = tokens.reshape(rows, width), norm_gain.reshape(1, width)
     hbm = pl.BlockSpec(memory_space=pltpu.HBM)
     sources = [
-        pltpu.with_memory_space_constraint(x, pltpu.HBM)
+        in_hbm(x)
         for x in (w_key, w_value, w_query, w_rank_forward.T, w_rank_backward.T, w_out)
     ]
     send = call(
-        pack_kernel, shape((16, 32, SENT), bf16), [hbm] * 6, 1 << 26, *sources,
+        pack_kernel, shape((16, SENT, LANES), bf16), [hbm] * 6, 1 << 26, *sources,
         scratch=[pltpu.VMEM(x.shape, bf16) for x in sources] + [pltpu.SemaphoreType.DMA((6,))],
     )
     own = lax.all_to_all(send, PLANE, 0, 0)
     other = swapped(own)
     normed = call(
         norm_kernel, shape((2, rows, 512), bf16), [VMEM, VMEM], 1 << 28,
-        tokens.reshape(rows, width), norm_gain.reshape(1, width),
+        tokens_flat, gain_flat,
     )
     decays = (
         up_forward, up_backward, bias_forward.reshape(1, WIDTH), bias_backward.reshape(1, WIDTH)
@@ -353,8 +403,8 @@
     payload, rounded, mix = call(
         block_kernel,
         (
-            shape((HEADS, 40, LANES), bf16), shape((rows, ALL), bf16),
-            shape((1, 16, 32, 2 * LANES), bf16),
+            shape((HEADS, 40, LANES), bf16), pltpu.HBM((rows, ALL), bf16),
+            shape((1, 16, 64, LANES), bf16),
         ),
         [VMEM] * 7, 1 << 30, normed, own, other, *decays,
     )
@@ -362,7 +412,7 @@
     for flip in (1, 3):
         arrived = lax.ppermute(mix, "dp_0", [(i, i ^ flip) for i in range(4)])
         mix = call(
-            join_kernel, shape((2 * mix.shape[0], 16, 32, 2 * LANES), bf16), [VMEM] * 2, 1 << 26,
+            join_kernel, shape((2 * mix.shape[0], 16, 64, LANES), bf16), [VMEM] * 2, 1 << 26,
             mix, arrived,
         )
     mix_other = swapped(mix)
@@ -371,15 +421,14 @@
         inbound,
     )
     returned = lax.all_to_all(states.reshape(HEADS, HEAD, LANES), "sp", 0, 0)
-    parts, mix_all = call(
-        query_kernel,
-        (shape((rows, 3 * WIDTH), f32), shape((8, 16, 2, 16, LANES), bf16)),
-        [VMEM] * 8, 1 << 30, normed, mix, mix_other, rounded, *decays,
-    )
+    parts = call(
+        query_kernel, pltpu.HBM((rows, 3 * WIDTH), f32), [VMEM] * 9, 1 << 30,
+        in_hbm(tokens_flat), gain_flat, mix, mix_other, in_hbm(rounded), *decays,
+    )
+    gain = jnp.tile(out_gain.reshape(2, 1, 16), (1, HEADS, 1)).reshape(2, 256)
     mixed = call(
-        out_kernel, shape((rows, width), bf16), [VMEM] * 4, 1 << 30,
-        returned.reshape(WIDTH, LANES), parts,
-        jnp.tile(out_gain, HEADS).reshape(1, WIDTH), mix_all,
+        out_kernel, shape((rows, width), bf16), [VMEM] * 5, 1 << 30,
+        returned.reshape(WIDTH, LANES), parts, gain, mix, mix_other,
     )
     return mixed.reshape(seqs, toks, width)
 

time: 121 us -> 119 us (0.983)
  the two profiles are of different devices: /device:TPU:32 before, /device:TPU:24 now
where the time goes in v8:
time: 119 us; the launch traced here: 117 us
  blocking collectives  54.8 us (46%)
  waiting for transfers between devices  32.1 us (27%)
  starting transfers between devices  17 us (14%)
  Pallas kernels  11.2 us (9%)
  local copies, waits for them, and re-layouts  1.35 us (1%)
    all_to_all x1, blocking collectives, body(): inbound = lax.all_to_all(payload, 'sp', 0, 0)  29.6 us
    all_to_all x1, blocking collectives, body(): own = lax.all_to_all(send, PLANE, 0, 0)  25.2 us
    ppermute x2, waiting for transfers between devices, body(): arrived = lax.ppermute(mix, 'dp_0', [(i, i ^ flip) for i in range(4)])  19.2 us
    pallas_call x8, Pallas kernels, call(): pl.pallas_call(kernel, out_shape=outs, in_specs=specs, out_specs=(VMEM,)...  11.2 us
    all_to_all x1, waiting for transfers between devices, body(): returned = lax.all_to_all(states.reshape(HEADS, HEAD, LANES), 'sp', 0, 0)  10.2 us
    ppermute x2, starting transfers between devices, body(): arrived = lax.ppermute(mix, 'dp_0', [(i, i ^ flip) for i in range(4)])  7.2 us
    all_to_all x1, starting transfers between devices, body(): returned = lax.all_to_all(states.reshape(HEADS, HEAD, LANES), 'sp', 0, 0)  5.95 us
    ppermute x2, starting transfers between devices, swapped(): return lax.ppermute(x, 'dp_2', [(0, 1), (1, 0)])  3.83 us
  transfers between devices with their start and end apart: 5, of which 4 were waited for; matrix products, arithmetic and copies ran while one was open for 0% of the time, Pallas kernels for 5%

profile of v8, /device:TPU:24, one launch (start us, length us, event | category | flops | bytes accessed | tf_op | source)
XLA Modules:
  0.0 116.6 jit_solution(5200626433370060050)
XLA Ops:
  0.0 1.3 %shard_map.128 = bf16[16,328,128]{2,1,0:T(8,128)(2,1)S(1)} custom-call(bf16[32,512]{1,0:T(8,128)(2,1)} %key_hbm.1, bf16[32,512]{1,0:T(8,128)(2,1)} %value_hbm.1, bf16[32,512]{1,0:T(8,128)(2,1)} %query_hbm.1, bf16[16,32]{1,0:T(8,128)(2,1)} %bitcast.22, bf16[16,32]{1,0:T(8,128)(2,1)} %bitcast.23, bf16[16,1024]{1,0:T(8,128)(2,1)} %mix_hbm.1), custom_call_target="tpu_custom_call" | custom-call | flops 67108864 | bytes 1048576 | tf_op jit(solution)/shard_map/pallas_call | solution.py:358
  1.3 0.0 copy-start
  1.3 0.0 copy-start.3
  1.3 0.0 copy-start.1
  1.3 0.0 copy-start.2
  1.3 0.0 copy-start.4
  1.3 0.0 copy-start.5
  1.3 25.2 %all_to_all.15.own_ref = bf16[16,328,128]{2,1,0:T(8,128)(2,1)S(1)} all-to-all(bf16[16,328,128]{2,1,0:T(8,128)(2,1)S(1)} %shard_map.128), channel_id=1, replica_groups=mesh['sp'=16,'dp_0'=4,'dp_1'=4,'dp_2'=2] {'dp_0','dp_1'}, dimensions={0} | all-to-all | bytes 2686976 | tf_op jit(solution)/shard_map/all_to_all | solution.py:394
  26.5 1.9 %collective-permute-start = (bf16[16,328,128]{2,1,0:T(8,128)(2,1)S(1)}, bf16[16,328,128]{2,1,0:T(8,128)(2,1)S(1)}, u32[]{:S(2)}, u32[]{:S(2)}) collective-permute-start(bf16[16,328,128]{2,1,0:T(8,128)(2,1)S(1)} %all_to_all.15.own_ref), channel_id=1, source_target_pairs={{0,1},{1,0},{2,3},{3,2},{4,5},{5,4},{6,7},{7,6},{8,9},{9,8},{10,11... | collective-permute-start | bytes 4030472 | tf_op jit(solution)/shard_map/ppermute | solution.py:374
  28.5 0.0 copy-done
  28.5 0.0 copy-done.3
  28.5 0.3 shard_map.127.normed_ref
  28.8 2.7 %collective-permute-done.other_ref = bf16[16,328,128]{2,1,0:T(8,128)(2,1)S(1)} collective-permute-done((bf16[16,328,128]{2,1,0:T(8,128)(2,1)S(1)}, bf16[16,328,128]{2,1,0:T(8,128)(2,1)S(1)}, u32[]{:S(2)}, u32[]{:S(2)}) %collective-permute-start) | collective-permute-done | bytes 1343520 | tf_op jit(solution)/shard_map/ppermute | solution.py:374
  31.5 0.0 copy-done.5
  31.5 2.4 %shard_map.129 = (bf16[16,40,128]{2,1,0:T(8,128)(2,1)S(1)}, bf16[128,1152]{1,0:T(8,128)(2,1)}, bf16[1,16,64,128]{3,2,1,0:T(8,128)(2,1)S(1)}) custom-call(bf16[2,128,512]{2,1,0:T(8,128)(2,1)S(1)} %shard_map.127.normed_ref, bf16[16,328,128]{2,1,0:T(8,128)(2,1)S(1)} %all_to_all.15.own_ref, bf16[16,328,128]{2,1,0:T(8,128)(2,1)S(1)} %collective-permute-done.other_ref, ...), custom_call_target="tpu_custom_call" | custom-call | flops 1073741824 | bytes 1048576 | tf_op jit(solution)/shard_map/pallas_call | solution.py:358
  34.0 2.8 %collective-permute-start.1 = (bf16[1,16,64,128]{3,2,1,0:T(8,128)(2,1)S(1)}, bf16[1,16,64,128]{3,2,1,0:T(8,128)(2,1)S(1)}, u32[]{:S(2)}, u32[]{:S(2)}) collective-permute-start(bf16[1,16,64,128]{3,2,1,0:T(8,128)(2,1)S(1)} %get-tuple-element.9.first_ref), channel_id=1, source_target_pairs={{0,8},{8,0},{16,24},{24,16},{1,9},{9,1},{17,25},{25,17},{2,10},{10... | collective-permute-start | bytes 786440 | tf_op jit(solution)/shard_map/ppermute | solution.py:413
  36.8 7.4 %collective-permute-done.1.second_ref = bf16[1,16,64,128]{3,2,1,0:T(8,128)(2,1)S(1)} collective-permute-done((bf16[1,16,64,128]{3,2,1,0:T(8,128)(2,1)S(1)}, bf16[1,16,64,128]{3,2,1,0:T(8,128)(2,1)S(1)}, u32[]{:S(2)}, u32[]{:S(2)}) %collective-permute-start.1) | collective-permute-done | bytes 262176 | tf_op jit(solution)/shard_map/ppermute | solution.py:413
  44.2 0.0 copy-start.7
  44.2 4.4 %collective-permute-start.2 = (bf16[2,16,64,128]{3,2,1,0:T(8,128)(2,1)S(1)}, bf16[2,16,64,128]{3,2,1,0:T(8,128)(2,1)S(1)}, u32[]{:S(2)}, u32[]{:S(2)}) collective-permute-start(bf16[2,16,64,128]{3,2,1,0:T(8,128)(2,1)S(1)} %shard_map.131.first_ref), channel_id=1, source_target_pairs={{0,24},{8,16},{16,8},{24,0},{1,25},{9,17},{17,9},{25,1},{2,26},{10... | collective-permute-start | bytes 1572872 | tf_op jit(solution)/shard_map/ppermute | solution.py:413
  48.6 11.8 %collective-permute-done.2.second_ref = bf16[2,16,64,128]{3,2,1,0:T(8,128)(2,1)S(1)} collective-permute-done((bf16[2,16,64,128]{3,2,1,0:T(8,128)(2,1)S(1)}, bf16[2,16,64,128]{3,2,1,0:T(8,128)(2,1)S(1)}, u32[]{:S(2)}, u32[]{:S(2)}) %collective-permute-start.2) | collective-permute-done | bytes 524320 | tf_op jit(solution)/shard_map/ppermute | solution.py:413
  60.4 0.1 shard_map.132.own_ref
  60.5 1.9 %collective-permute-start.3 = (bf16[4,16,64,128]{3,2,1,0:T(8,128)(2,1)S(1)}, bf16[4,16,64,128]{3,2,1,0:T(8,128)(2,1)S(1)}, u32[]{:S(2)}, u32[]{:S(2)}) collective-permute-start(bf16[4,16,64,128]{3,2,1,0:T(8,128)(2,1)S(1)} %shard_map.132.own_ref), channel_id=1, source_target_pairs={{0,1},{1,0},{2,3},{3,2},{4,5},{5,4},{6,7},{7,6},{8,9},{9,8},{10,11... | collective-permute-start | bytes 3145736 | tf_op jit(solution)/shard_map/ppermute | solution.py:374
  62.4 29.6 %all_to_all.16.payload_ref = bf16[16,40,128]{2,1,0:T(8,128)(2,1)S(1)} all-to-all(bf16[16,40,128]{2,1,0:T(8,128)(2,1)S(1)} %get-tuple-element.8), channel_id=1, replica_groups=mesh['sp'=16,'dp_0'=4,'dp_1'=4,'dp_2'=2] {'sp'}, dimensions={0} | all-to-all | bytes 327680 | tf_op jit(solution)/shard_map/all_to_all | solution.py:411
  92.0 0.9 shard_map.130
  92.9 6.0 %all-to-all-start.2 = ((bf16[16,32,128]{2,1,0:T(8,128)(2,1)}), bf16[16,32,128]{2,1,0:T(8,128)(2,1)S(1)}, u32[]{:S(2)}, u32[]{:S(2)}) async-start(bf16[16,32,128]{2,1,0:T(8,128)(2,1)} %bitcast.6), calls=%async_computation.2 | async-start | bytes 262144 | tf_op jit(solution)/shard_map/all_to_all | solution.py:423
  98.9 0.1 tile.9
  99.0 0.1 tile.11.gain_ref
  99.1 0.0 collective-permute-done.3.other_ref
  99.1 4.4 %shard_map.133.parts_ref = f32[128,1536]{1,0:T(8,128)} custom-call(bf16[128,1024]{1,0:T(8,128)(2,1)} %bitcast.14, f32[1,1024]{1,0:T(1,128)S(1)} %bitcast.17, bf16[4,16,64,128]{3,2,1,0:T(8,128)(2,1)S(1)} %shard_map.132.own_ref, bf16[4,16,64,128]{3,2,1,0:T(8,128)(2,1)S(1)} %collective-permute-done.3.other_ref, ...), custom_call_target="tpu_custom_call" | custom-call | flops 1073741824 | bytes 1048576 | tf_op jit(solution)/shard_map/pallas_call | solution.py:358
  103.5 10.2 %all-to-all-done.2 = bf16[16,32,128]{2,1,0:T(8,128)(2,1)S(1)} async-done(((bf16[16,32,128]{2,1,0:T(8,128)(2,1)}), bf16[16,32,128]{2,1,0:T(8,128)(2,1)S(1)}, u32[]{:S(2)}, u32[]{:S(2)}) %all-to-all-start.2) | async-done | bytes 131104 | tf_op jit(solution)/shard_map/all_to_all | solution.py:423
  113.7 1.1 copy-done.6
  114.8 1.8 %shard_map.134 = bf16[128,1024]{1,0:T(8,128)(2,1)} custom-call(bf16[512,128]{1,0:T(8,128)(2,1)S(1)} %bitcast.13, f32[128,1536]{1,0:T(8,128)S(1)} %copy-done.6, f32[2,256]{1,0:T(2,128)S(1)} %tile.11.gain_ref, bf16[4,16,64,128]{3,2,1,0:T(8,128)(2,1)S(1)} %shard_map.132.own_ref, bf16[4,16,64,128]{3,2,1,0:T(8,128)(2,1)S(1)} %collective-permute-done.3.other_ref), custom_call_target="tpu_custom_call" | custom-call | flops 1073741824 | bytes 1048576 | tf_op jit(solution)/shard_map/pallas_call | solution.py:358
  (7 shorter events, 0.1 us)
Async XLA Ops:
  1.3 27.2 %copy-start = (bf16[2,64,1024]{2,1,0:T(8,128)(2,1)S(1)}, bf16[2,64,1024]{2,1,0:T(8,128)(2,1)}, u32[]{:S(2)}) copy-start(bf16[2,64,1024]{2,1,0:T(8,128)(2,1)} %param.13) | copy-start | bytes 786436
  1.3 27.2 %copy-start.3 = (f32[1024]{0:T(1024)S(1)}, f32[1024]{0:T(1024)}, u32[]{:S(2)}) copy-start(f32[1024]{0:T(1024)} %param.14) | copy-start | bytes 12292
  1.3 30.2 %copy-start.1 = (bf16[16,512]{1,0:T(8,128)(2,1)S(1)}, bf16[16,512]{1,0:T(8,128)(2,1)}, u32[]{:S(2)}) copy-start(bf16[16,512]{1,0:T(8,128)(2,1)} %up_forward_ref.3) | copy-start | bytes 49156
  1.3 30.2 %copy-start.2 = (bf16[16,512]{1,0:T(8,128)(2,1)S(1)}, bf16[16,512]{1,0:T(8,128)(2,1)}, u32[]{:S(2)}) copy-start(bf16[16,512]{1,0:T(8,128)(2,1)} %up_backward_ref.3) | copy-start | bytes 49156
  1.3 30.2 %copy-start.4 = (f32[512]{0:T(512)S(1)}, f32[512]{0:T(512)}, u32[]{:S(2)}) copy-start(f32[512]{0:T(512)} %param.22) | copy-start | bytes 6148
  1.3 30.2 %copy-start.5 = (f32[512]{0:T(512)S(1)}, f32[512]{0:T(512)}, u32[]{:S(2)}) copy-start(f32[512]{0:T(512)} %param.23) | copy-start | bytes 6148
  26.5 5.0 %collective-permute-start = (bf16[16,328,128]{2,1,0:T(8,128)(2,1)S(1)}, bf16[16,328,128]{2,1,0:T(8,128)(2,1)S(1)}, u32[]{:S(2)}, u32[]{:S(2)}) collective-permute-start(bf16[16,328,128]{2,1,0:T(8,128)(2,1)S(1)} %all_to_all.15.own_ref), channel_id=1, source_target_pairs={{0,1},{1,0},{2,3},{3,2},{4,5},{5,4},{6,7},{7,6},{8,9},{9,8},{10,11... | collective-permute-start | bytes 4030472 | tf_op jit(solution)/shard_map/ppermute | solution.py:374
  34.0 10.2 %collective-permute-start.1 = (bf16[1,16,64,128]{3,2,1,0:T(8,128)(2,1)S(1)}, bf16[1,16,64,128]{3,2,1,0:T(8,128)(2,1)S(1)}, u32[]{:S(2)}, u32[]{:S(2)}) collective-permute-start(bf16[1,16,64,128]{3,2,1,0:T(8,128)(2,1)S(1)} %get-tuple-element.9.first_ref), channel_id=1, source_target_pairs={{0,8},{8,0},{16,24},{24,16},{1,9},{9,1},{17,25},{25,17},{2,10},{10... | collective-permute-start | bytes 786440 | tf_op jit(solution)/shard_map/ppermute | solution.py:413
  44.2 54.7 %copy-start.7 = (f32[32]{0:T(128)S(1)}, f32[32]{0:T(128)}, u32[]{:S(2)}) copy-start(f32[32]{0:T(128)} %param.24) | copy-start | bytes 388
  44.2 16.2 %collective-permute-start.2 = (bf16[2,16,64,128]{3,2,1,0:T(8,128)(2,1)S(1)}, bf16[2,16,64,128]{3,2,1,0:T(8,128)(2,1)S(1)}, u32[]{:S(2)}, u32[]{:S(2)}) collective-permute-start(bf16[2,16,64,128]{3,2,1,0:T(8,128)(2,1)S(1)} %shard_map.131.first_ref), channel_id=1, source_target_pairs={{0,24},{8,16},{16,8},{24,0},{1,25},{9,17},{17,9},{25,1},{2,26},{10... | collective-permute-start | bytes 1572872 | tf_op jit(solution)/shard_map/ppermute | solution.py:413
  60.5 38.6 %collective-permute-start.3 = (bf16[4,16,64,128]{3,2,1,0:T(8,128)(2,1)S(1)}, bf16[4,16,64,128]{3,2,1,0:T(8,128)(2,1)S(1)}, u32[]{:S(2)}, u32[]{:S(2)}) collective-permute-start(bf16[4,16,64,128]{3,2,1,0:T(8,128)(2,1)S(1)} %shard_map.132.own_ref), channel_id=1, source_target_pairs={{0,1},{1,0},{2,3},{3,2},{4,5},{5,4},{6,7},{7,6},{8,9},{9,8},{10,11... | collective-permute-start | bytes 3145736 | tf_op jit(solution)/shard_map/ppermute | solution.py:374
  92.9 20.7 %all-to-all-start.2 = ((bf16[16,32,128]{2,1,0:T(8,128)(2,1)}), bf16[16,32,128]{2,1,0:T(8,128)(2,1)S(1)}, u32[]{:S(2)}, u32[]{:S(2)}) async-start(bf16[16,32,128]{2,1,0:T(8,128)(2,1)} %bitcast.6), calls=%async_computation.2 | async-start | bytes 262144 | tf_op jit(solution)/shard_map/all_to_all | solution.py:423
  113.7 1.1 copy-start.6

commit v9 on v8

--- a/solution.py
+++ b/solution.py
@@ -72,15 +72,24 @@
             out_ref[i, (4 + group) * 32 : (5 + group) * 32] = value_ref[:, lanes]
         start = (i // 4) * LANES
         out_ref[i, COLUMNS : COLUMNS + 32] = query_ref[:, start : start + LANES]
-        out_ref[i, COLUMNS + 32 : COLUMNS + 48] = mix_ref[:, 2 * start : 2 * start + LANES]
-        out_ref[i, COLUMNS + 48 : COLUMNS + 64] = mix_ref[:, 2 * start + LANES : 2 * start + 2 * LANES]
+        start = (i % 4) * 2 * LANES
+        out_ref[i, COLUMNS + 32 : COLUMNS + 48] = mix_ref[:, start : start + LANES]
+        out_ref[i, COLUMNS + 48 : COLUMNS + 64] = mix_ref[:, start + LANES : start + 2 * LANES]
         out_ref[i, COLUMNS + 64 :] = packed.astype(bf16)
 
 
-def join_kernel(first_ref, second_ref, out_ref):
-    count = first_ref.shape[0]
-    out_ref[:count] = first_ref[...]
-    out_ref[count:] = second_ref[...]
+def join_kernel(query_ref, query_in_ref, mix_ref, mix_in_ref, queries_ref, mixes_ref):
+    queries_ref[:1] = query_ref[...]
+    queries_ref[1:] = query_in_ref[...]
+    mixes_ref[:1] = mix_ref[...]
+    mixes_ref[1:] = mix_in_ref[...]
+
+
+def stack_kernel(query_ref, query_in_ref, mix_ref, mix_in_ref, out_ref):
+    out_ref[0, :2] = query_ref[...]
+    out_ref[0, 2:] = query_in_ref[...]
+    out_ref[1, :2] = mix_ref[...]
+    out_ref[1, 2:] = mix_in_ref[...]
 
 
 def slot_of(index, axis):
@@ -125,10 +134,11 @@
 
 def block_kernel(
     normed_ref, own_ref, other_ref, up_forward_ref, up_backward_ref,
-    bias_forward_ref, bias_backward_ref, payload_ref, rounded_ref, mix_ref,
+    bias_forward_ref, bias_backward_ref, payload_ref, rounded_ref, query_ref, mix_ref,
 ):
     core = lax.axis_index("dp_2")
-    mix_ref[0] = own_ref[:, COLUMNS : COLUMNS + 64, :]
+    query_ref[0] = own_ref[:, COLUMNS : COLUMNS + 32, :]
+    mix_ref[0] = own_ref[:, COLUMNS + 32 : COLUMNS + 64, :]
 
     def columns(ref, first):
         return jnp.concatenate(
@@ -240,7 +250,7 @@
     def weights(ref):
         return jnp.concatenate(
             [
-                ref[slot_of(quarter, "dp_0"), :, :32, :].reshape(WIDTH, LANES)
+                ref[0, slot_of(quarter, "dp_0")].reshape(WIDTH, LANES)
                 for quarter in range(4)
             ],
             axis=1,
@@ -291,7 +301,11 @@
                 out_ref[span, start : start + LANES] = total
 
 
-def out_kernel(states_ref, parts_ref, gain_ref, own_ref, other_ref, out_ref):
+def out_kernel(
+    states_ref, parts_hbm, gain_ref, own_ref, other_ref, out_ref, parts_ref, sem
+):
+    fetch = pltpu.make_async_copy(parts_hbm, parts_ref, sem)
+    fetch.start()
     core = lax.axis_index("dp_2")
     row, col = grid_of((LANES, 8 * LANES))
     source = (col // 256) * HEAD + ((col // LANES) % 2) * 16 + col % 16
@@ -302,6 +316,7 @@
         jnp.where(diagonal, dot(states_ref[g * 256 : (g + 1) * 256, :], widen), 0.0).astype(bf16)
         for g in range(2)
     ]
+    fetch.wait()
     totals = [[], []]
     for seq in range(2):
         span = slice(seq * BLOCK, (seq + 1) * BLOCK)
@@ -338,11 +353,11 @@
     mine = jnp.where(core == 0, attended[0], attended[1])
     theirs = jnp.where(core == 0, attended[1], attended[0])
     for quarter in range(4):
-        slot = slot_of(quarter, "dp_0")
+        slot = slot_of(quarter, "dp_1")
 
         def weights(ref):
             return jnp.concatenate(
-                [ref[slot, :, rows : rows + 16, :].reshape(256, LANES) for rows in (32, 48)], axis=1
+                [ref[1, slot, :, rows : rows + 16, :].reshape(256, LANES) for rows in (0, 16)], axis=1
             )
 
         out_ref[:, quarter * 256 : (quarter + 1) * 256] = (
@@ -400,22 +415,30 @@
     decays = (
         up_forward, up_backward, bias_forward.reshape(1, WIDTH), bias_backward.reshape(1, WIDTH)
     )
-    payload, rounded, mix = call(
+    payload, rounded, query, mix = call(
         block_kernel,
         (
             shape((HEADS, 40, LANES), bf16), pltpu.HBM((rows, ALL), bf16),
-            shape((1, 16, 64, LANES), bf16),
+            shape((1, 16, 32, LANES), bf16), shape((1, 16, 32, LANES), bf16),
         ),
         [VMEM] * 7, 1 << 30, normed, own, other, *decays,
     )
     inbound = lax.all_to_all(payload, "sp", 0, 0)
-    for flip in (1, 3):
-        arrived = lax.ppermute(mix, "dp_0", [(i, i ^ flip) for i in range(4)])
-        mix = call(
-            join_kernel, shape((2 * mix.shape[0], 16, 64, LANES), bf16), [VMEM] * 2, 1 << 26,
-            mix, arrived,
-        )
-    mix_other = swapped(mix)
+    for step, flip in enumerate((1, 3)):
+        pairs = [(i, i ^ flip) for i in range(4)]
+        query_in = lax.ppermute(query, "dp_0", pairs)
+        mix_in = lax.ppermute(mix, "dp_1", pairs)
+        if step == 0:
+            query, mix = call(
+                join_kernel, (shape((2, 16, 32, LANES), bf16),) * 2, [VMEM] * 4, 1 << 26,
+                query, query_in, mix, mix_in,
+            )
+        else:
+            later = call(
+                stack_kernel, shape((2, 4, 16, 32, LANES), bf16), [VMEM] * 4, 1 << 26,
+                query, query_in, mix, mix_in,
+            )
+    later_other = swapped(later)
     states = call(
         scan_kernel, shape((WIDTH, LANES), bf16), [VMEM], 1 << 28,
         inbound,
@@ -423,12 +446,13 @@
     returned = lax.all_to_all(states.reshape(HEADS, HEAD, LANES), "sp", 0, 0)
     parts = call(
         query_kernel, pltpu.HBM((rows, 3 * WIDTH), f32), [VMEM] * 9, 1 << 30,
-        in_hbm(tokens_flat), gain_flat, mix, mix_other, in_hbm(rounded), *decays,
+        in_hbm(tokens_flat), gain_flat, later, later_other, in_hbm(rounded), *decays,
     )
     gain = jnp.tile(out_gain.reshape(2, 1, 16), (1, HEADS, 1)).reshape(2, 256)
     mixed = call(
-        out_kernel, shape((rows, width), bf16), [VMEM] * 5, 1 << 30,
-        returned.reshape(WIDTH, LANES), parts, gain, mix, mix_other,
+        out_kernel, shape((rows, width), bf16), [VMEM, hbm] + [VMEM] * 3, 1 << 30,
+        returned.reshape(WIDTH, LANES), in_hbm(parts), gain, later, later_other,
+        scratch=[pltpu.VMEM((rows, 3 * WIDTH), f32), pltpu.SemaphoreType.DMA],
     )
     return mixed.reshape(seqs, toks, width)
 

time: 119 us -> 115 us (0.966); the launches traced: 117 us -> 114 us
  waiting for transfers between devices: 32.1 us -> 25.4 us
  starting transfers between devices: 17 us -> 21.3 us
    ppermute x2 -> x4, waiting for transfers between devices: 19.2 us -> 12.5 us  [the longest x2 6.29 us: body(): mix_in = lax.ppermute(mix, 'dp_1', pairs)]
    ppermute x2 -> x4, starting transfers between devices: 7.2 us -> 11.5 us  [the longest x2 6.56 us: body(): query_in = lax.ppermute(query, 'dp_0', pairs)]
  transfers between devices with their start and end apart: 5 -> 7, of which waited for: 4 -> 6; matrix products, arithmetic and copies ran while one was open for 0% -> 0% of each run, Pallas kernels for 5% -> 5%
where the time goes in v9:
time: 115 us; the launch traced here: 114 us
  blocking collectives  54.7 us (48%)
  waiting for transfers between devices  25.4 us (22%)
  starting transfers between devices  21.3 us (19%)
  Pallas kernels  12.2 us (11%)
    all_to_all x1, blocking collectives, body(): inbound = lax.all_to_all(payload, 'sp', 0, 0)  29.5 us
    all_to_all x1, blocking collectives, body(): own = lax.all_to_all(send, PLANE, 0, 0)  25.2 us
    pallas_call x8, Pallas kernels, call(): pl.pallas_call(kernel, out_shape=outs, in_specs=specs, out_specs=(VMEM,)...  12.2 us
    all_to_all x1, waiting for transfers between devices, body(): returned = lax.all_to_all(states.reshape(HEADS, HEAD, LANES), 'sp', 0, 0)  10.2 us
    ppermute x2, starting transfers between devices, body(): query_in = lax.ppermute(query, 'dp_0', pairs)  6.56 us
    ppermute x2, waiting for transfers between devices, body(): mix_in = lax.ppermute(mix, 'dp_1', pairs)  6.29 us
    ppermute x2, waiting for transfers between devices, body(): query_in = lax.ppermute(query, 'dp_0', pairs)  6.22 us
    all_to_all x1, starting transfers between devices, body(): returned = lax.all_to_all(states.reshape(HEADS, HEAD, LANES), 'sp', 0, 0)  5.96 us
  transfers between devices with their start and end apart: 7, of which 6 were waited for; matrix products, arithmetic and copies ran while one was open for 0% of the time, Pallas kernels for 5%

profile of v9, /device:TPU:24, one launch (start us, length us, event | category | flops | bytes accessed | tf_op | source)
XLA Modules:
  0.0 114.0 jit_solution(12348266409400873535)
XLA Ops:
  0.0 1.3 %shard_map.128 = bf16[16,328,128]{2,1,0:T(8,128)(2,1)S(1)} custom-call(bf16[32,512]{1,0:T(8,128)(2,1)} %key_hbm.1, bf16[32,512]{1,0:T(8,128)(2,1)} %value_hbm.1, bf16[32,512]{1,0:T(8,128)(2,1)} %query_hbm.1, bf16[16,32]{1,0:T(8,128)(2,1)} %bitcast.22, bf16[16,32]{1,0:T(8,128)(2,1)} %bitcast.23, bf16[16,1024]{1,0:T(8,128)(2,1)} %mix_hbm.1), custom_call_target="tpu_custom_call" | custom-call | flops 67108864 | bytes 1048576 | tf_op jit(solution)/shard_map/pallas_call | solution.py:373
  1.3 0.0 copy-start
  1.3 0.0 copy-start.3
  1.3 0.0 copy-start.1
  1.3 0.0 copy-start.2
  1.3 0.0 copy-start.4
  1.3 0.0 copy-start.5
  1.4 25.2 %all_to_all.15.own_ref = bf16[16,328,128]{2,1,0:T(8,128)(2,1)S(1)} all-to-all(bf16[16,328,128]{2,1,0:T(8,128)(2,1)S(1)} %shard_map.128), channel_id=1, replica_groups=mesh['sp'=16,'dp_0'=4,'dp_1'=4,'dp_2'=2] {'dp_0','dp_1'}, dimensions={0} | all-to-all | bytes 2686976 | tf_op jit(solution)/shard_map/all_to_all | solution.py:409
  26.6 1.9 %collective-permute-start = (bf16[16,328,128]{2,1,0:T(8,128)(2,1)S(1)}, bf16[16,328,128]{2,1,0:T(8,128)(2,1)S(1)}, u32[]{:S(2)}, u32[]{:S(2)}) collective-permute-start(bf16[16,328,128]{2,1,0:T(8,128)(2,1)S(1)} %all_to_all.15.own_ref), channel_id=1, source_target_pairs={{0,1},{1,0},{2,3},{3,2},{4,5},{5,4},{6,7},{7,6},{8,9},{9,8},{10,11... | collective-permute-start | bytes 4030472 | tf_op jit(solution)/shard_map/ppermute | solution.py:389
  28.5 0.3 shard_map.127.normed_ref
  28.8 2.7 %collective-permute-done.other_ref = bf16[16,328,128]{2,1,0:T(8,128)(2,1)S(1)} collective-permute-done((bf16[16,328,128]{2,1,0:T(8,128)(2,1)S(1)}, bf16[16,328,128]{2,1,0:T(8,128)(2,1)S(1)}, u32[]{:S(2)}, u32[]{:S(2)}) %collective-permute-start) | collective-permute-done | bytes 1343520 | tf_op jit(solution)/shard_map/ppermute | solution.py:389
  31.5 2.4 %shard_map.129 = (bf16[16,40,128]{2,1,0:T(8,128)(2,1)S(1)}, bf16[128,1152]{1,0:T(8,128)(2,1)}, bf16[1,16,32,128]{3,2,1,0:T(8,128)(2,1)S(1)}, bf16[1,16,32,128]{3,2,1,0:T(8,128)(2,1)S(1)}) custom-call(bf16[2,128,512]{2,1,0:T(8,128)(2,1)S(1)} %shard_map.127.normed_ref, bf16[16,328,128]{2,1,0:T(8,128)(2,1)S(1)} %all_to_all.15.own_ref, ...), custom_call_target="tpu_custom_call" | custom-call | flops 1073741824 | bytes 1048576 | tf_op jit(solution)/shard_map/pallas_call | solution.py:373
  34.0 2.8 %collective-permute-start.1 = (bf16[1,16,32,128]{3,2,1,0:T(8,128)(2,1)S(1)}, bf16[1,16,32,128]{3,2,1,0:T(8,128)(2,1)S(1)}, u32[]{:S(2)}, u32[]{:S(2)}) collective-permute-start(bf16[1,16,32,128]{3,2,1,0:T(8,128)(2,1)S(1)} %get-tuple-element.12.query_ref), channel_id=1, source_target_pairs={{0,8},{8,0},{16,24},{24,16},{1,9},{9,1},{17,25},{25,17},{2,10},{10... | collective-permute-start | bytes 393224 | tf_op jit(solution)/shard_map/ppermute | solution.py:429
  36.8 2.1 %collective-permute-start.2 = (bf16[1,16,32,128]{3,2,1,0:T(8,128)(2,1)S(1)}, bf16[1,16,32,128]{3,2,1,0:T(8,128)(2,1)S(1)}, u32[]{:S(2)}, u32[]{:S(2)}) collective-permute-start(bf16[1,16,32,128]{3,2,1,0:T(8,128)(2,1)S(1)} %get-tuple-element.13.mix_ref), channel_id=1, source_target_pairs={{0,2},{2,0},{4,6},{6,4},{1,3},{3,1},{5,7},{7,5},{8,10},{10,8},{12,... | collective-permute-start | bytes 393224 | tf_op jit(solution)/shard_map/ppermute | solution.py:430
  38.9 2.5 %collective-permute-done.1.query_in_ref = bf16[1,16,32,128]{3,2,1,0:T(8,128)(2,1)S(1)} collective-permute-done((bf16[1,16,32,128]{3,2,1,0:T(8,128)(2,1)S(1)}, bf16[1,16,32,128]{3,2,1,0:T(8,128)(2,1)S(1)}, u32[]{:S(2)}, u32[]{:S(2)}) %collective-permute-start.1) | collective-permute-done | bytes 131104 | tf_op jit(solution)/shard_map/ppermute | solution.py:429
  41.4 2.6 %collective-permute-done.2.mix_in_ref = bf16[1,16,32,128]{3,2,1,0:T(8,128)(2,1)S(1)} collective-permute-done((bf16[1,16,32,128]{3,2,1,0:T(8,128)(2,1)S(1)}, bf16[1,16,32,128]{3,2,1,0:T(8,128)(2,1)S(1)}, u32[]{:S(2)}, u32[]{:S(2)}) %collective-permute-start.2) | collective-permute-done | bytes 131104 | tf_op jit(solution)/shard_map/ppermute | solution.py:430
  44.0 3.7 %collective-permute-start.3 = (bf16[2,16,32,128]{3,2,1,0:T(8,128)(2,1)S(1)}, bf16[2,16,32,128]{3,2,1,0:T(8,128)(2,1)S(1)}, u32[]{:S(2)}, u32[]{:S(2)}) collective-permute-start(bf16[2,16,32,128]{3,2,1,0:T(8,128)(2,1)S(1)} %get-tuple-element.14.query_ref), channel_id=1, source_target_pairs={{0,24},{8,16},{16,8},{24,0},{1,25},{9,17},{17,9},{25,1},{2,26},{10... | collective-permute-start | bytes 786440 | tf_op jit(solution)/shard_map/ppermute | solution.py:429
  47.7 0.0 copy-start.6
  47.7 2.8 %collective-permute-start.4 = (bf16[2,16,32,128]{3,2,1,0:T(8,128)(2,1)S(1)}, bf16[2,16,32,128]{3,2,1,0:T(8,128)(2,1)S(1)}, u32[]{:S(2)}, u32[]{:S(2)}) collective-permute-start(bf16[2,16,32,128]{3,2,1,0:T(8,128)(2,1)S(1)} %get-tuple-element.15.mix_ref), channel_id=1, source_target_pairs={{0,6},{2,4},{4,2},{6,0},{1,7},{3,5},{5,3},{7,1},{8,14},{10,12},{12... | collective-permute-start | bytes 786440 | tf_op jit(solution)/shard_map/ppermute | solution.py:430
  50.5 3.8 %collective-permute-done.3.query_in_ref = bf16[2,16,32,128]{3,2,1,0:T(8,128)(2,1)S(1)} collective-permute-done((bf16[2,16,32,128]{3,2,1,0:T(8,128)(2,1)S(1)}, bf16[2,16,32,128]{3,2,1,0:T(8,128)(2,1)S(1)}, u32[]{:S(2)}, u32[]{:S(2)}) %collective-permute-start.3) | collective-permute-done | bytes 262176 | tf_op jit(solution)/shard_map/ppermute | solution.py:429
  54.3 3.7 %collective-permute-done.4.mix_in_ref = bf16[2,16,32,128]{3,2,1,0:T(8,128)(2,1)S(1)} collective-permute-done((bf16[2,16,32,128]{3,2,1,0:T(8,128)(2,1)S(1)}, bf16[2,16,32,128]{3,2,1,0:T(8,128)(2,1)S(1)}, u32[]{:S(2)}, u32[]{:S(2)}) %collective-permute-start.4) | collective-permute-done | bytes 262176 | tf_op jit(solution)/shard_map/ppermute | solution.py:430
  58.0 0.1 shard_map.132.own_ref
  58.1 1.9 %collective-permute-start.5 = (bf16[2,4,16,32,128]{4,3,2,1,0:T(8,128)(2,1)S(1)}, bf16[2,4,16,32,128]{4,3,2,1,0:T(8,128)(2,1)S(1)}, u32[]{:S(2)}, u32[]{:S(2)}) collective-permute-start(bf16[2,4,16,32,128]{4,3,2,1,0:T(8,128)(2,1)S(1)} %shard_map.132.own_ref), channel_id=1, source_target_pairs={{0,1},{1,0},{2,3},{3,2},{4,5},{5,4},{6,7},{7,6},{8,9},{9,8},{10,11... | collective-permute-start | bytes 3145736 | tf_op jit(solution)/shard_map/ppermute | solution.py:389
  60.0 29.5 %all_to_all.16.payload_ref = bf16[16,40,128]{2,1,0:T(8,128)(2,1)S(1)} all-to-all(bf16[16,40,128]{2,1,0:T(8,128)(2,1)S(1)} %get-tuple-element.11), channel_id=1, replica_groups=mesh['sp'=16,'dp_0'=4,'dp_1'=4,'dp_2'=2] {'sp'}, dimensions={0} | all-to-all | bytes 327680 | tf_op jit(solution)/shard_map/all_to_all | solution.py:426
  89.5 0.9 shard_map.130
  90.5 6.0 %all-to-all-start.2 = ((bf16[16,32,128]{2,1,0:T(8,128)(2,1)}), bf16[16,32,128]{2,1,0:T(8,128)(2,1)S(1)}, u32[]{:S(2)}, u32[]{:S(2)}) async-start(bf16[16,32,128]{2,1,0:T(8,128)(2,1)} %bitcast.6), calls=%async_computation.2 | async-start | bytes 262144 | tf_op jit(solution)/shard_map/all_to_all | solution.py:446
  96.4 0.1 tile.9
  96.5 0.1 tile.11.gain_ref
  96.6 0.0 collective-permute-done.5.other_ref
  96.6 4.4 %shard_map.133.parts_hbm = f32[128,1536]{1,0:T(8,128)} custom-call(bf16[128,1024]{1,0:T(8,128)(2,1)} %bitcast.14, f32[1,1024]{1,0:T(1,128)S(1)} %bitcast.17, bf16[2,4,16,32,128]{4,3,2,1,0:T(8,128)(2,1)S(1)} %shard_map.132.own_ref, bf16[2,4,16,32,128]{4,3,2,1,0:T(8,128)(2,1)S(1)} %collective-permute-done.5.other_ref, ...), custom_call_target="tpu_custom_call" | custom-call | flops 1073741824 | bytes 1048576 | tf_op jit(solution)/shard_map/pallas_call | solution.py:373
  101.0 10.2 %all-to-all-done.2 = bf16[16,32,128]{2,1,0:T(8,128)(2,1)S(1)} async-done(((bf16[16,32,128]{2,1,0:T(8,128)(2,1)}), bf16[16,32,128]{2,1,0:T(8,128)(2,1)S(1)}, u32[]{:S(2)}, u32[]{:S(2)}) %all-to-all-start.2) | async-done | bytes 131104 | tf_op jit(solution)/shard_map/all_to_all | solution.py:446
  111.2 2.8 %shard_map.134 = bf16[128,1024]{1,0:T(8,128)(2,1)} custom-call(bf16[512,128]{1,0:T(8,128)(2,1)S(1)} %bitcast.13, f32[128,1536]{1,0:T(8,128)} %shard_map.133.parts_hbm, f32[2,256]{1,0:T(2,128)S(1)} %tile.11.gain_ref, bf16[2,4,16,32,128]{4,3,2,1,0:T(8,128)(2,1)S(1)} %shard_map.132.own_ref, bf16[2,4,16,32,128]{4,3,2,1,0:T(8,128)(2,1)S(1)} %collective-permute-done.5.other_ref), custom_call_target="tpu_custom_call" | custom-call | flops 1073741824 | bytes 1048576 | tf_op jit(solution)/shard_map/pallas_call | solution.py:373
  (9 shorter events, 0.1 us)
Async XLA Ops:
  1.3 27.2 %copy-start = (bf16[2,64,1024]{2,1,0:T(8,128)(2,1)S(1)}, bf16[2,64,1024]{2,1,0:T(8,128)(2,1)}, u32[]{:S(2)}) copy-start(bf16[2,64,1024]{2,1,0:T(8,128)(2,1)} %param.13) | copy-start | bytes 786436
  1.3 27.2 %copy-start.3 = (f32[1024]{0:T(1024)S(1)}, f32[1024]{0:T(1024)}, u32[]{:S(2)}) copy-start(f32[1024]{0:T(1024)} %param.14) | copy-start | bytes 12292
  1.3 30.2 %copy-start.1 = (bf16[16,512]{1,0:T(8,128)(2,1)S(1)}, bf16[16,512]{1,0:T(8,128)(2,1)}, u32[]{:S(2)}) copy-start(bf16[16,512]{1,0:T(8,128)(2,1)} %up_forward_ref.3) | copy-start | bytes 49156
  1.3 30.2 %copy-start.2 = (bf16[16,512]{1,0:T(8,128)(2,1)S(1)}, bf16[16,512]{1,0:T(8,128)(2,1)}, u32[]{:S(2)}) copy-start(bf16[16,512]{1,0:T(8,128)(2,1)} %up_backward_ref.3) | copy-start | bytes 49156
  1.3 30.2 %copy-start.4 = (f32[512]{0:T(512)S(1)}, f32[512]{0:T(512)}, u32[]{:S(2)}) copy-start(f32[512]{0:T(512)} %param.22) | copy-start | bytes 6148
  1.3 30.2 %copy-start.5 = (f32[512]{0:T(512)S(1)}, f32[512]{0:T(512)}, u32[]{:S(2)}) copy-start(f32[512]{0:T(512)} %param.23) | copy-start | bytes 6148
  26.6 5.0 %collective-permute-start = (bf16[16,328,128]{2,1,0:T(8,128)(2,1)S(1)}, bf16[16,328,128]{2,1,0:T(8,128)(2,1)S(1)}, u32[]{:S(2)}, u32[]{:S(2)}) collective-permute-start(bf16[16,328,128]{2,1,0:T(8,128)(2,1)S(1)} %all_to_all.15.own_ref), channel_id=1, source_target_pairs={{0,1},{1,0},{2,3},{3,2},{4,5},{5,4},{6,7},{7,6},{8,9},{9,8},{10,11... | collective-permute-start | bytes 4030472 | tf_op jit(solution)/shard_map/ppermute | solution.py:389
  34.0 7.4 %collective-permute-start.1 = (bf16[1,16,32,128]{3,2,1,0:T(8,128)(2,1)S(1)}, bf16[1,16,32,128]{3,2,1,0:T(8,128)(2,1)S(1)}, u32[]{:S(2)}, u32[]{:S(2)}) collective-permute-start(bf16[1,16,32,128]{3,2,1,0:T(8,128)(2,1)S(1)} %get-tuple-element.12.query_ref), channel_id=1, source_target_pairs={{0,8},{8,0},{16,24},{24,16},{1,9},{9,1},{17,25},{25,17},{2,10},{10... | collective-permute-start | bytes 393224 | tf_op jit(solution)/shard_map/ppermute | solution.py:429
  36.8 7.2 %collective-permute-start.2 = (bf16[1,16,32,128]{3,2,1,0:T(8,128)(2,1)S(1)}, bf16[1,16,32,128]{3,2,1,0:T(8,128)(2,1)S(1)}, u32[]{:S(2)}, u32[]{:S(2)}) collective-permute-start(bf16[1,16,32,128]{3,2,1,0:T(8,128)(2,1)S(1)} %get-tuple-element.13.mix_ref), channel_id=1, source_target_pairs={{0,2},{2,0},{4,6},{6,4},{1,3},{3,1},{5,7},{7,5},{8,10},{10,8},{12,... | collective-permute-start | bytes 393224 | tf_op jit(solution)/shard_map/ppermute | solution.py:430
  44.0 10.3 %collective-permute-start.3 = (bf16[2,16,32,128]{3,2,1,0:T(8,128)(2,1)S(1)}, bf16[2,16,32,128]{3,2,1,0:T(8,128)(2,1)S(1)}, u32[]{:S(2)}, u32[]{:S(2)}) collective-permute-start(bf16[2,16,32,128]{3,2,1,0:T(8,128)(2,1)S(1)} %get-tuple-element.14.query_ref), channel_id=1, source_target_pairs={{0,24},{8,16},{16,8},{24,0},{1,25},{9,17},{17,9},{25,1},{2,26},{10... | collective-permute-start | bytes 786440 | tf_op jit(solution)/shard_map/ppermute | solution.py:429
  47.7 48.7 %copy-start.6 = (f32[32]{0:T(128)S(1)}, f32[32]{0:T(128)}, u32[]{:S(2)}) copy-start(f32[32]{0:T(128)} %param.24) | copy-start | bytes 388
  47.7 10.3 %collective-permute-start.4 = (bf16[2,16,32,128]{3,2,1,0:T(8,128)(2,1)S(1)}, bf16[2,16,32,128]{3,2,1,0:T(8,128)(2,1)S(1)}, u32[]{:S(2)}, u32[]{:S(2)}) collective-permute-start(bf16[2,16,32,128]{3,2,1,0:T(8,128)(2,1)S(1)} %get-tuple-element.15.mix_ref), channel_id=1, source_target_pairs={{0,6},{2,4},{4,2},{6,0},{1,7},{3,5},{5,3},{7,1},{8,14},{10,12},{12... | collective-permute-start | bytes 786440 | tf_op jit(solution)/shard_map/ppermute | solution.py:430
  58.1 38.5 %collective-permute-start.5 = (bf16[2,4,16,32,128]{4,3,2,1,0:T(8,128)(2,1)S(1)}, bf16[2,4,16,32,128]{4,3,2,1,0:T(8,128)(2,1)S(1)}, u32[]{:S(2)}, u32[]{:S(2)}) collective-permute-start(bf16[2,4,16,32,128]{4,3,2,1,0:T(8,128)(2,1)S(1)} %shard_map.132.own_ref), channel_id=1, source_target_pairs={{0,1},{1,0},{2,3},{3,2},{4,5},{5,4},{6,7},{7,6},{8,9},{9,8},{10,11... | collective-permute-start | bytes 3145736 | tf_op jit(solution)/shard_map/ppermute | solution.py:389
  90.5 20.7 %all-to-all-start.2 = ((bf16[16,32,128]{2,1,0:T(8,128)(2,1)}), bf16[16,32,128]{2,1,0:T(8,128)(2,1)S(1)}, u32[]{:S(2)}, u32[]{:S(2)}) async-start(bf16[16,32,128]{2,1,0:T(8,128)(2,1)} %bitcast.6), calls=%async_computation.2 | async-start | bytes 262144 | tf_op jit(solution)/shard_map/all_to_all | solution.py:446

commit v10 on v8

--- a/solution.py
+++ b/solution.py
@@ -125,10 +125,9 @@
 
 def block_kernel(
     normed_ref, own_ref, other_ref, up_forward_ref, up_backward_ref,
-    bias_forward_ref, bias_backward_ref, payload_ref, rounded_ref, mix_ref,
+    bias_forward_ref, bias_backward_ref, payload_ref, rounded_ref,
 ):
     core = lax.axis_index("dp_2")
-    mix_ref[0] = own_ref[:, COLUMNS : COLUMNS + 64, :]
 
     def columns(ref, first):
         return jnp.concatenate(
@@ -393,28 +392,28 @@
     )
     own = lax.all_to_all(send, PLANE, 0, 0)
     other = swapped(own)
-    normed = call(
-        norm_kernel, shape((2, rows, 512), bf16), [VMEM, VMEM], 1 << 28,
-        tokens_flat, gain_flat,
-    )
-    decays = (
-        up_forward, up_backward, bias_forward.reshape(1, WIDTH), bias_backward.reshape(1, WIDTH)
-    )
-    payload, rounded, mix = call(
-        block_kernel,
-        (
-            shape((HEADS, 40, LANES), bf16), pltpu.HBM((rows, ALL), bf16),
-            shape((1, 16, 64, LANES), bf16),
-        ),
-        [VMEM] * 7, 1 << 30, normed, own, other, *decays,
-    )
-    inbound = lax.all_to_all(payload, "sp", 0, 0)
+    mix = own[None, :, COLUMNS : COLUMNS + 64, :]
     for flip in (1, 3):
         arrived = lax.ppermute(mix, "dp_0", [(i, i ^ flip) for i in range(4)])
         mix = call(
             join_kernel, shape((2 * mix.shape[0], 16, 64, LANES), bf16), [VMEM] * 2, 1 << 26,
             mix, arrived,
         )
+    normed = call(
+        norm_kernel, shape((2, rows, 512), bf16), [VMEM, VMEM], 1 << 28,
+        tokens_flat, gain_flat,
+    )
+    decays = (
+        up_forward, up_backward, bias_forward.reshape(1, WIDTH), bias_backward.reshape(1, WIDTH)
+    )
+    payload, rounded = call(
+        block_kernel,
+        (
+            shape((HEADS, 40, LANES), bf16), pltpu.HBM((rows, ALL), bf16),
+        ),
+        [VMEM] * 7, 1 << 30, normed, own, other, *decays,
+    )
+    inbound = lax.all_to_all(payload, "sp", 0, 0)
     mix_other = swapped(mix)
     states = call(
         scan_kernel, shape((WIDTH, LANES), bf16), [VMEM], 1 << 28,

time: 119 us -> 117 us (0.983)
  the two profiles are of different devices: /device:TPU:24 before, /device:TPU:32 now
where the time goes in v10:
time: 117 us; the launch traced here: 116 us
  blocking collectives  57.6 us (49%)
  waiting for transfers between devices  32 us (27%)
  starting transfers between devices  13.8 us (12%)
  Pallas kernels  11.2 us (10%)
  local copies, waits for them, and re-layouts  1.36 us (1%)
    all_to_all x1, blocking collectives, body(): inbound = lax.all_to_all(payload, 'sp', 0, 0)  30.4 us
    all_to_all x1, blocking collectives, body(): own = lax.all_to_all(send, PLANE, 0, 0)  27.1 us
    ppermute x2, waiting for transfers between devices, body(): arrived = lax.ppermute(mix, 'dp_0', [(i, i ^ flip) for i in range(4)])  22.1 us
    pallas_call x8, Pallas kernels, call(): pl.pallas_call(kernel, out_shape=outs, in_specs=specs, out_specs=(VMEM,)...  11.2 us
    all_to_all x1, waiting for transfers between devices, body(): returned = lax.all_to_all(states.reshape(HEADS, HEAD, LANES), 'sp', 0, 0)  9.97 us
    all_to_all x1, starting transfers between devices, body(): returned = lax.all_to_all(states.reshape(HEADS, HEAD, LANES), 'sp', 0, 0)  5.2 us
    ppermute x2, starting transfers between devices, body(): arrived = lax.ppermute(mix, 'dp_0', [(i, i ^ flip) for i in range(4)])  4.68 us
    ppermute x2, starting transfers between devices, swapped(): return lax.ppermute(x, 'dp_2', [(0, 1), (1, 0)])  3.96 us
  transfers between devices with their start and end apart: 5, of which 3 were waited for; matrix products, arithmetic and copies ran while one was open for 0% of the time, Pallas kernels for 7%

profile of v10, /device:TPU:32, one launch (start us, length us, event | category | flops | bytes accessed | tf_op | source)
XLA Modules:
  0.0 116.2 jit_solution(14212652054769866671)
XLA Ops:
  0.0 1.3 %shard_map.128 = bf16[16,328,128]{2,1,0:T(8,128)(2,1)S(1)} custom-call(bf16[32,512]{1,0:T(8,128)(2,1)} %key_hbm.1, bf16[32,512]{1,0:T(8,128)(2,1)} %value_hbm.1, bf16[32,512]{1,0:T(8,128)(2,1)} %query_hbm.1, bf16[16,32]{1,0:T(8,128)(2,1)} %bitcast.24, bf16[16,32]{1,0:T(8,128)(2,1)} %bitcast.25, bf16[16,1024]{1,0:T(8,128)(2,1)} %mix_hbm.1), custom_call_target="tpu_custom_call" | custom-call | flops 67108864 | bytes 1048576 | tf_op jit(solution)/shard_map/pallas_call | solution.py:357
  1.3 27.1 %all_to_all.15.own_ref = bf16[16,328,128]{2,1,0:T(8,128)(2,1)S(1)} all-to-all(bf16[16,328,128]{2,1,0:T(8,128)(2,1)S(1)} %shard_map.128), channel_id=1, replica_groups=mesh['sp'=16,'dp_0'=4,'dp_1'=4,'dp_2'=2] {'dp_0','dp_1'}, dimensions={0} | all-to-all | bytes 2686976 | tf_op jit(solution)/shard_map/all_to_all | solution.py:393
  28.4 2.0 %collective-permute-start = (bf16[16,328,128]{2,1,0:T(8,128)(2,1)S(1)}, bf16[16,328,128]{2,1,0:T(8,128)(2,1)S(1)}, u32[]{:S(2)}, u32[]{:S(2)}) collective-permute-start(bf16[16,328,128]{2,1,0:T(8,128)(2,1)S(1)} %all_to_all.15.own_ref), channel_id=1, source_target_pairs={{0,1},{1,0},{2,3},{3,2},{4,5},{5,4},{6,7},{7,6},{8,9},{9,8},{10,11... | collective-permute-start | bytes 4030472 | tf_op jit(solution)/shard_map/ppermute | solution.py:373
  30.5 1.9 %collective-permute-start.1 = (bf16[1,16,64,128]{3,2,1,0:T(8,128)(2,1)S(1)}, bf16[1,16,64,128]{3,2,1,0:T(8,128)(2,1)S(1)}, u32[]{:S(2)}, u32[]{:S(2)}) collective-permute-start(bf16[1,16,64,128]{3,2,1,0:T(8,128)(2,1)S(1)} %slice_bitcast_fusion.first_ref), channel_id=1, source_target_pairs={{0,8},{8,0},{16,24},{24,16},{1,9},{9,1},{17,25},{25,17},{2,10},{10... | collective-permute-start | bytes 786440 | tf_op jit(solution)/shard_map/ppermute | solution.py:397
  32.4 8.7 %collective-permute-done.1.second_ref = bf16[1,16,64,128]{3,2,1,0:T(8,128)(2,1)S(1)} collective-permute-done((bf16[1,16,64,128]{3,2,1,0:T(8,128)(2,1)S(1)}, bf16[1,16,64,128]{3,2,1,0:T(8,128)(2,1)S(1)}, u32[]{:S(2)}, u32[]{:S(2)}) %collective-permute-start.1) | collective-permute-done | bytes 262176 | tf_op jit(solution)/shard_map/ppermute | solution.py:397
  41.1 2.8 %collective-permute-start.2 = (bf16[2,16,64,128]{3,2,1,0:T(8,128)(2,1)S(1)}, bf16[2,16,64,128]{3,2,1,0:T(8,128)(2,1)S(1)}, u32[]{:S(2)}, u32[]{:S(2)}) collective-permute-start(bf16[2,16,64,128]{3,2,1,0:T(8,128)(2,1)S(1)} %shard_map.131.first_ref), channel_id=1, source_target_pairs={{0,24},{8,16},{16,8},{24,0},{1,25},{9,17},{17,9},{25,1},{2,26},{10... | collective-permute-start | bytes 1572872 | tf_op jit(solution)/shard_map/ppermute | solution.py:397
  43.9 0.0 copy-done
  43.9 0.0 copy-done.3
  43.9 0.0 copy-start.1
  43.9 0.0 copy-start.2
  43.9 0.0 copy-start.4
  44.0 0.0 copy-start.5
  44.0 0.3 shard_map.127.normed_ref
  44.3 13.4 %collective-permute-done.2.second_ref = bf16[2,16,64,128]{3,2,1,0:T(8,128)(2,1)S(1)} collective-permute-done((bf16[2,16,64,128]{3,2,1,0:T(8,128)(2,1)S(1)}, bf16[2,16,64,128]{3,2,1,0:T(8,128)(2,1)S(1)}, u32[]{:S(2)}, u32[]{:S(2)}) %collective-permute-start.2) | collective-permute-done | bytes 524320 | tf_op jit(solution)/shard_map/ppermute | solution.py:397
  57.7 0.1 shard_map.132.own_ref
  57.8 1.9 %collective-permute-start.3 = (bf16[4,16,64,128]{3,2,1,0:T(8,128)(2,1)S(1)}, bf16[4,16,64,128]{3,2,1,0:T(8,128)(2,1)S(1)}, u32[]{:S(2)}, u32[]{:S(2)}) collective-permute-start(bf16[4,16,64,128]{3,2,1,0:T(8,128)(2,1)S(1)} %shard_map.132.own_ref), channel_id=1, source_target_pairs={{0,1},{1,0},{2,3},{3,2},{4,5},{5,4},{6,7},{7,6},{8,9},{9,8},{10,11... | collective-permute-start | bytes 3145736 | tf_op jit(solution)/shard_map/ppermute | solution.py:373
  59.7 0.0 collective-permute-done.other_ref
  59.7 0.0 copy-done.1
  59.7 0.0 copy-done.2
  59.8 2.4 %shard_map.129 = (bf16[16,40,128]{2,1,0:T(8,128)(2,1)S(1)}, bf16[128,1152]{1,0:T(8,128)(2,1)}) custom-call(bf16[2,128,512]{2,1,0:T(8,128)(2,1)S(1)} %shard_map.127.normed_ref, bf16[16,328,128]{2,1,0:T(8,128)(2,1)S(1)} %all_to_all.15.own_ref, bf16[16,328,128]{2,1,0:T(8,128)(2,1)S(1)} %collective-permute-done.other_ref, bf16[16,512]{1,0:T(8,128)(2,1)S(1)} %copy-done.1, ...), custom_call_target="tpu_custom_call" | custom-call | flops 1073741824 | bytes 1048576 | tf_op jit(solution)/shard_map/pallas_call | solution.py:357
  62.2 0.0 copy-start.7
  62.2 30.4 %all_to_all.16.payload_ref = bf16[16,40,128]{2,1,0:T(8,128)(2,1)S(1)} all-to-all(bf16[16,40,128]{2,1,0:T(8,128)(2,1)S(1)} %get-tuple-element.7), channel_id=1, replica_groups=mesh['sp'=16,'dp_0'=4,'dp_1'=4,'dp_2'=2] {'sp'}, dimensions={0} | all-to-all | bytes 327680 | tf_op jit(solution)/shard_map/all_to_all | solution.py:416
  92.6 0.9 shard_map.130
  93.5 5.2 %all-to-all-start.2 = ((bf16[16,32,128]{2,1,0:T(8,128)(2,1)}), bf16[16,32,128]{2,1,0:T(8,128)(2,1)S(1)}, u32[]{:S(2)}, u32[]{:S(2)}) async-start(bf16[16,32,128]{2,1,0:T(8,128)(2,1)} %bitcast.6), calls=%async_computation.2 | async-start | bytes 262144 | tf_op jit(solution)/shard_map/all_to_all | solution.py:422
  98.7 0.0 copy-done.7
  98.7 0.1 tile.9
  98.8 0.1 tile.11.gain_ref
  98.9 0.0 collective-permute-done.3.other_ref
  98.9 4.4 %shard_map.133.parts_ref = f32[128,1536]{1,0:T(8,128)} custom-call(bf16[128,1024]{1,0:T(8,128)(2,1)} %bitcast.16, f32[1,1024]{1,0:T(1,128)S(1)} %bitcast.19, bf16[4,16,64,128]{3,2,1,0:T(8,128)(2,1)S(1)} %shard_map.132.own_ref, bf16[4,16,64,128]{3,2,1,0:T(8,128)(2,1)S(1)} %collective-permute-done.3.other_ref, bf16[128,1152]{1,0:T(8,128)(2,1)} %get-tuple-element.8.rounded_ref, ...), custom_call_target="tpu_custom_call" | custom-call | flops 1073741824 | bytes 1048576 | tf_op jit(solution)/shard_map/pallas_call | solution.py:357
  103.3 10.0 %all-to-all-done.2 = bf16[16,32,128]{2,1,0:T(8,128)(2,1)S(1)} async-done(((bf16[16,32,128]{2,1,0:T(8,128)(2,1)}), bf16[16,32,128]{2,1,0:T(8,128)(2,1)S(1)}, u32[]{:S(2)}, u32[]{:S(2)}) %all-to-all-start.2) | async-done | bytes 131104 | tf_op jit(solution)/shard_map/all_to_all | solution.py:422
  113.2 1.1 copy-done.6
  114.4 1.8 %shard_map.134 = bf16[128,1024]{1,0:T(8,128)(2,1)} custom-call(bf16[512,128]{1,0:T(8,128)(2,1)S(1)} %bitcast.15, f32[128,1536]{1,0:T(8,128)S(1)} %copy-done.6, f32[2,256]{1,0:T(2,128)S(1)} %tile.11.gain_ref, bf16[4,16,64,128]{3,2,1,0:T(8,128)(2,1)S(1)} %shard_map.132.own_ref, bf16[4,16,64,128]{3,2,1,0:T(8,128)(2,1)S(1)} %collective-permute-done.3.other_ref), custom_call_target="tpu_custom_call" | custom-call | flops 1073741824 | bytes 1048576 | tf_op jit(solution)/shard_map/pallas_call | solution.py:357
  (8 shorter events, 0.1 us)
Async XLA Ops:
  28.4 15.5 %copy-start = (bf16[2,64,1024]{2,1,0:T(8,128)(2,1)S(1)}, bf16[2,64,1024]{2,1,0:T(8,128)(2,1)}, u32[]{:S(2)}) copy-start(bf16[2,64,1024]{2,1,0:T(8,128)(2,1)} %param.13) | copy-start | bytes 786436
  28.4 15.5 %copy-start.3 = (f32[1024]{0:T(1024)S(1)}, f32[1024]{0:T(1024)}, u32[]{:S(2)}) copy-start(f32[1024]{0:T(1024)} %param.14) | copy-start | bytes 12292
  28.4 31.3 %collective-permute-start = (bf16[16,328,128]{2,1,0:T(8,128)(2,1)S(1)}, bf16[16,328,128]{2,1,0:T(8,128)(2,1)S(1)}, u32[]{:S(2)}, u32[]{:S(2)}) collective-permute-start(bf16[16,328,128]{2,1,0:T(8,128)(2,1)S(1)} %all_to_all.15.own_ref), channel_id=1, source_target_pairs={{0,1},{1,0},{2,3},{3,2},{4,5},{5,4},{6,7},{7,6},{8,9},{9,8},{10,11... | collective-permute-start | bytes 4030472 | tf_op jit(solution)/shard_map/ppermute | solution.py:373
  30.5 10.6 %collective-permute-start.1 = (bf16[1,16,64,128]{3,2,1,0:T(8,128)(2,1)S(1)}, bf16[1,16,64,128]{3,2,1,0:T(8,128)(2,1)S(1)}, u32[]{:S(2)}, u32[]{:S(2)}) collective-permute-start(bf16[1,16,64,128]{3,2,1,0:T(8,128)(2,1)S(1)} %slice_bitcast_fusion.first_ref), channel_id=1, source_target_pairs={{0,8},{8,0},{16,24},{24,16},{1,9},{9,1},{17,25},{25,17},{2,10},{10... | collective-permute-start | bytes 786440 | tf_op jit(solution)/shard_map/ppermute | solution.py:397
  41.1 16.6 %collective-permute-start.2 = (bf16[2,16,64,128]{3,2,1,0:T(8,128)(2,1)S(1)}, bf16[2,16,64,128]{3,2,1,0:T(8,128)(2,1)S(1)}, u32[]{:S(2)}, u32[]{:S(2)}) collective-permute-start(bf16[2,16,64,128]{3,2,1,0:T(8,128)(2,1)S(1)} %shard_map.131.first_ref), channel_id=1, source_target_pairs={{0,24},{8,16},{16,8},{24,0},{1,25},{9,17},{17,9},{25,1},{2,26},{10... | collective-permute-start | bytes 1572872 | tf_op jit(solution)/shard_map/ppermute | solution.py:397
  43.9 15.8 %copy-start.1 = (bf16[16,512]{1,0:T(8,128)(2,1)S(1)}, bf16[16,512]{1,0:T(8,128)(2,1)}, u32[]{:S(2)}) copy-start(bf16[16,512]{1,0:T(8,128)(2,1)} %up_forward_ref.3) | copy-start | bytes 49156
  43.9 15.8 %copy-start.2 = (bf16[16,512]{1,0:T(8,128)(2,1)S(1)}, bf16[16,512]{1,0:T(8,128)(2,1)}, u32[]{:S(2)}) copy-start(bf16[16,512]{1,0:T(8,128)(2,1)} %up_backward_ref.3) | copy-start | bytes 49156
  43.9 15.8 %copy-start.4 = (f32[512]{0:T(512)S(1)}, f32[512]{0:T(512)}, u32[]{:S(2)}) copy-start(f32[512]{0:T(512)} %param.22) | copy-start | bytes 6148
  44.0 15.8 %copy-start.5 = (f32[512]{0:T(512)S(1)}, f32[512]{0:T(512)}, u32[]{:S(2)}) copy-start(f32[512]{0:T(512)} %param.23) | copy-start | bytes 6148
  57.8 41.1 %collective-permute-start.3 = (bf16[4,16,64,128]{3,2,1,0:T(8,128)(2,1)S(1)}, bf16[4,16,64,128]{3,2,1,0:T(8,128)(2,1)S(1)}, u32[]{:S(2)}, u32[]{:S(2)}) collective-permute-start(bf16[4,16,64,128]{3,2,1,0:T(8,128)(2,1)S(1)} %shard_map.132.own_ref), channel_id=1, source_target_pairs={{0,1},{1,0},{2,3},{3,2},{4,5},{5,4},{6,7},{7,6},{8,9},{9,8},{10,11... | collective-permute-start | bytes 3145736 | tf_op jit(solution)/shard_map/ppermute | solution.py:373
  62.2 36.5 %copy-start.7 = (f32[32]{0:T(128)S(1)}, f32[32]{0:T(128)}, u32[]{:S(2)}) copy-start(f32[32]{0:T(128)} %param.24) | copy-start | bytes 388
  93.5 19.7 %all-to-all-start.2 = ((bf16[16,32,128]{2,1,0:T(8,128)(2,1)}), bf16[16,32,128]{2,1,0:T(8,128)(2,1)S(1)}, u32[]{:S(2)}, u32[]{:S(2)}) async-start(bf16[16,32,128]{2,1,0:T(8,128)(2,1)} %bitcast.6), calls=%async_computation.2 | async-start | bytes 262144 | tf_op jit(solution)/shard_map/all_to_all | solution.py:422
  113.2 1.1 copy-start.6

commit v11 on v10

--- a/solution.py
+++ b/solution.py
@@ -17,6 +17,7 @@
 COLUMNS = 8 * 32
 SENT = COLUMNS + 32 + 32 + 8
 EPS = 1e-06
+GROUP = [(z + 12) % 16 for z in range(16)]
 f32 = jnp.float32
 bf16 = jnp.bfloat16
 
@@ -217,11 +218,12 @@
         return x[i * HEAD : (i + 1) * HEAD, :]
 
     carried = jnp.zeros((HEAD, LANES), f32)
-    for i in range(HEADS):
+    order = [GROUP.index(z) for z in range(HEADS)]
+    for i in order:
         ahead[i] = carried
         carried = at(decay, i) * carried + at(states, i)
     carried = jnp.zeros((HEAD, LANES), f32)
-    for i in range(HEADS - 1, -1, -1):
+    for i in reversed(order):
         behind[i] = carried
         carried = at(decay, i) * carried + at(states, i)
     for i in range(HEADS):
@@ -413,13 +415,15 @@
         ),
         [VMEM] * 7, 1 << 30, normed, own, other, *decays,
     )
-    inbound = lax.all_to_all(payload, "sp", 0, 0)
+    inbound = lax.all_to_all(payload, "sp", 0, 0, axis_index_groups=[GROUP])
     mix_other = swapped(mix)
     states = call(
         scan_kernel, shape((WIDTH, LANES), bf16), [VMEM], 1 << 28,
         inbound,
     )
-    returned = lax.all_to_all(states.reshape(HEADS, HEAD, LANES), "sp", 0, 0)
+    returned = lax.all_to_all(
+        states.reshape(HEADS, HEAD, LANES), "sp", 0, 0, axis_index_groups=[GROUP]
+    )
     parts = call(
         query_kernel, pltpu.HBM((rows, 3 * WIDTH), f32), [VMEM] * 9, 1 << 30,
         in_hbm(tokens_flat), gain_flat, mix, mix_other, in_hbm(rounded), *decays,

time: 117 us -> 113 us (0.966)
  the two profiles are of different devices: /device:TPU:32 before, /device:TPU:24 now
where the time goes in v11:
time: 113 us; the launch traced here: 111 us
  blocking collectives  53.1 us (47%)
  waiting for transfers between devices  26.1 us (23%)
  starting transfers between devices  19.1 us (17%)
  Pallas kernels  11.2 us (10%)
  local copies, waits for them, and re-layouts  1.36 us (1%)
    all_to_all x1, blocking collectives, body(): inbound = lax.all_to_all(payload, 'sp', 0, 0, axis_index_groups=[GROUP])  28 us
    all_to_all x1, blocking collectives, body(): own = lax.all_to_all(send, PLANE, 0, 0)  25.1 us
    ppermute x2, waiting for transfers between devices, body(): arrived = lax.ppermute(mix, 'dp_0', [(i, i ^ flip) for i in range(4)])  19.6 us
    pallas_call x8, Pallas kernels, call(): pl.pallas_call(kernel, out_shape=outs, in_specs=specs, out_specs=(VMEM,)...  11.2 us
    all_to_all x1, starting transfers between devices, body(): lax.all_to_all(states.reshape(HEADS, HEAD, LANES), 'sp', 0, 0, axis_index...  7.95 us
    ppermute x2, starting transfers between devices, body(): arrived = lax.ppermute(mix, 'dp_0', [(i, i ^ flip) for i in range(4)])  7.19 us
    all_to_all x1, waiting for transfers between devices, body(): lax.all_to_all(states.reshape(HEADS, HEAD, LANES), 'sp', 0, 0, axis_index...  6.59 us
    ppermute x2, starting transfers between devices, swapped(): return lax.ppermute(x, 'dp_2', [(0, 1), (1, 0)])  3.96 us
  transfers between devices with their start and end apart: 5, of which 3 were waited for; matrix products, arithmetic and copies ran while one was open for 0% of the time, Pallas kernels for 7%

profile of v11, /device:TPU:24, one launch (start us, length us, event | category | flops | bytes accessed | tf_op | source)
XLA Modules:
  0.0 111.1 jit_solution(7046950496940890481)
XLA Ops:
  0.0 1.3 %shard_map.128 = bf16[16,328,128]{2,1,0:T(8,128)(2,1)S(1)} custom-call(bf16[32,512]{1,0:T(8,128)(2,1)} %key_hbm.1, bf16[32,512]{1,0:T(8,128)(2,1)} %value_hbm.1, bf16[32,512]{1,0:T(8,128)(2,1)} %query_hbm.1, bf16[16,32]{1,0:T(8,128)(2,1)} %bitcast.24, bf16[16,32]{1,0:T(8,128)(2,1)} %bitcast.25, bf16[16,1024]{1,0:T(8,128)(2,1)} %mix_hbm.1), custom_call_target="tpu_custom_call" | custom-call | flops 67108864 | bytes 1048576 | tf_op jit(solution)/shard_map/pallas_call | solution.py:359
  1.3 25.1 %all_to_all.15.own_ref = bf16[16,328,128]{2,1,0:T(8,128)(2,1)S(1)} all-to-all(bf16[16,328,128]{2,1,0:T(8,128)(2,1)S(1)} %shard_map.128), channel_id=1, replica_groups=mesh['sp'=16,'dp_0'=4,'dp_1'=4,'dp_2'=2] {'dp_0','dp_1'}, dimensions={0} | all-to-all | bytes 2686976 | tf_op jit(solution)/shard_map/all_to_all | solution.py:395
  26.3 2.0 %collective-permute-start = (bf16[16,328,128]{2,1,0:T(8,128)(2,1)S(1)}, bf16[16,328,128]{2,1,0:T(8,128)(2,1)S(1)}, u32[]{:S(2)}, u32[]{:S(2)}) collective-permute-start(bf16[16,328,128]{2,1,0:T(8,128)(2,1)S(1)} %all_to_all.15.own_ref), channel_id=1, source_target_pairs={{0,1},{1,0},{2,3},{3,2},{4,5},{5,4},{6,7},{7,6},{8,9},{9,8},{10,11... | collective-permute-start | bytes 4030472 | tf_op jit(solution)/shard_map/ppermute | solution.py:375
  28.4 2.8 %collective-permute-start.1 = (bf16[1,16,64,128]{3,2,1,0:T(8,128)(2,1)S(1)}, bf16[1,16,64,128]{3,2,1,0:T(8,128)(2,1)S(1)}, u32[]{:S(2)}, u32[]{:S(2)}) collective-permute-start(bf16[1,16,64,128]{3,2,1,0:T(8,128)(2,1)S(1)} %slice_bitcast_fusion.first_ref), channel_id=1, source_target_pairs={{0,8},{8,0},{16,24},{24,16},{1,9},{9,1},{17,25},{25,17},{2,10},{10... | collective-permute-start | bytes 786440 | tf_op jit(solution)/shard_map/ppermute | solution.py:399
  31.2 7.8 %collective-permute-done.1.second_ref = bf16[1,16,64,128]{3,2,1,0:T(8,128)(2,1)S(1)} collective-permute-done((bf16[1,16,64,128]{3,2,1,0:T(8,128)(2,1)S(1)}, bf16[1,16,64,128]{3,2,1,0:T(8,128)(2,1)S(1)}, u32[]{:S(2)}, u32[]{:S(2)}) %collective-permute-start.1) | collective-permute-done | bytes 262176 | tf_op jit(solution)/shard_map/ppermute | solution.py:399
  39.1 4.4 %collective-permute-start.2 = (bf16[2,16,64,128]{3,2,1,0:T(8,128)(2,1)S(1)}, bf16[2,16,64,128]{3,2,1,0:T(8,128)(2,1)S(1)}, u32[]{:S(2)}, u32[]{:S(2)}) collective-permute-start(bf16[2,16,64,128]{3,2,1,0:T(8,128)(2,1)S(1)} %shard_map.131.first_ref), channel_id=1, source_target_pairs={{0,24},{8,16},{16,8},{24,0},{1,25},{9,17},{17,9},{25,1},{2,26},{10... | collective-permute-start | bytes 1572872 | tf_op jit(solution)/shard_map/ppermute | solution.py:399
  43.4 0.0 copy-done
  43.5 0.0 copy-done.3
  43.5 0.0 copy-start.1
  43.5 0.0 copy-start.2
  43.5 0.0 copy-start.4
  43.5 0.0 copy-start.5
  43.5 0.3 shard_map.127.normed_ref
  43.9 11.8 %collective-permute-done.2.second_ref = bf16[2,16,64,128]{3,2,1,0:T(8,128)(2,1)S(1)} collective-permute-done((bf16[2,16,64,128]{3,2,1,0:T(8,128)(2,1)S(1)}, bf16[2,16,64,128]{3,2,1,0:T(8,128)(2,1)S(1)}, u32[]{:S(2)}, u32[]{:S(2)}) %collective-permute-start.2) | collective-permute-done | bytes 524320 | tf_op jit(solution)/shard_map/ppermute | solution.py:399
  55.6 0.1 shard_map.132.own_ref
  55.7 1.9 %collective-permute-start.3 = (bf16[4,16,64,128]{3,2,1,0:T(8,128)(2,1)S(1)}, bf16[4,16,64,128]{3,2,1,0:T(8,128)(2,1)S(1)}, u32[]{:S(2)}, u32[]{:S(2)}) collective-permute-start(bf16[4,16,64,128]{3,2,1,0:T(8,128)(2,1)S(1)} %shard_map.132.own_ref), channel_id=1, source_target_pairs={{0,1},{1,0},{2,3},{3,2},{4,5},{5,4},{6,7},{7,6},{8,9},{9,8},{10,11... | collective-permute-start | bytes 3145736 | tf_op jit(solution)/shard_map/ppermute | solution.py:375
  57.6 0.0 collective-permute-done.other_ref
  57.6 0.0 copy-done.1
  57.7 0.0 copy-done.2
  57.7 0.0 copy-done.4
  57.7 2.4 %shard_map.129 = (bf16[16,40,128]{2,1,0:T(8,128)(2,1)S(1)}, bf16[128,1152]{1,0:T(8,128)(2,1)}) custom-call(bf16[2,128,512]{2,1,0:T(8,128)(2,1)S(1)} %shard_map.127.normed_ref, bf16[16,328,128]{2,1,0:T(8,128)(2,1)S(1)} %all_to_all.15.own_ref, bf16[16,328,128]{2,1,0:T(8,128)(2,1)S(1)} %collective-permute-done.other_ref, bf16[16,512]{1,0:T(8,128)(2,1)S(1)} %copy-done.1, ...), custom_call_target="tpu_custom_call" | custom-call | flops 1073741824 | bytes 1048576 | tf_op jit(solution)/shard_map/pallas_call | solution.py:359
  60.1 0.0 copy-start.7
  60.1 28.0 %all_to_all.16.payload_ref = bf16[16,40,128]{2,1,0:T(8,128)(2,1)S(1)} all-to-all(bf16[16,40,128]{2,1,0:T(8,128)(2,1)S(1)} %get-tuple-element.7), channel_id=1, replica_groups={{384,416,448,480,0,32,64,96,128,160,192,224,256,288,320,352},{385,417,4..., dimensions={0} | all-to-all | bytes 327680 | tf_op jit(solution)/shard_map/all_to_all | solution.py:418
  88.1 0.9 shard_map.130
  89.1 7.9 %all-to-all-start.2 = ((bf16[16,32,128]{2,1,0:T(8,128)(2,1)}), bf16[16,32,128]{2,1,0:T(8,128)(2,1)S(1)}, u32[]{:S(2)}, u32[]{:S(2)}) async-start(bf16[16,32,128]{2,1,0:T(8,128)(2,1)} %bitcast.6), calls=%async_computation.2 | async-start | bytes 262144 | tf_op jit(solution)/shard_map/all_to_all | solution.py:424
  97.0 0.1 tile.9
  97.1 0.1 tile.11.gain_ref
  97.2 0.0 collective-permute-done.3.other_ref
  97.2 4.4 %shard_map.133.parts_ref = f32[128,1536]{1,0:T(8,128)} custom-call(bf16[128,1024]{1,0:T(8,128)(2,1)} %bitcast.16, f32[1,1024]{1,0:T(1,128)S(1)} %bitcast.19, bf16[4,16,64,128]{3,2,1,0:T(8,128)(2,1)S(1)} %shard_map.132.own_ref, bf16[4,16,64,128]{3,2,1,0:T(8,128)(2,1)S(1)} %collective-permute-done.3.other_ref, bf16[128,1152]{1,0:T(8,128)(2,1)} %get-tuple-element.8.rounded_ref, ...), custom_call_target="tpu_custom_call" | custom-call | flops 1073741824 | bytes 1048576 | tf_op jit(solution)/shard_map/pallas_call | solution.py:359
  101.6 6.6 %all-to-all-done.2 = bf16[16,32,128]{2,1,0:T(8,128)(2,1)S(1)} async-done(((bf16[16,32,128]{2,1,0:T(8,128)(2,1)}), bf16[16,32,128]{2,1,0:T(8,128)(2,1)S(1)}, u32[]{:S(2)}, u32[]{:S(2)}) %all-to-all-start.2) | async-done | bytes 131104 | tf_op jit(solution)/shard_map/all_to_all | solution.py:424
  108.2 1.1 %copy-done.6 = f32[128,1536]{1,0:T(8,128)S(1)} copy-done((f32[128,1536]{1,0:T(8,128)S(1)}, f32[128,1536]{1,0:T(8,128)}, u32[]{:S(2)}) %copy-start.6) | copy-done | bytes 786456
  109.3 1.8 %shard_map.134 = bf16[128,1024]{1,0:T(8,128)(2,1)} custom-call(bf16[512,128]{1,0:T(8,128)(2,1)S(1)} %bitcast.15, f32[128,1536]{1,0:T(8,128)S(1)} %copy-done.6, f32[2,256]{1,0:T(2,128)S(1)} %tile.11.gain_ref, bf16[4,16,64,128]{3,2,1,0:T(8,128)(2,1)S(1)} %shard_map.132.own_ref, bf16[4,16,64,128]{3,2,1,0:T(8,128)(2,1)S(1)} %collective-permute-done.3.other_ref), custom_call_target="tpu_custom_call" | custom-call | flops 1073741824 | bytes 1048576 | tf_op jit(solution)/shard_map/pallas_call | solution.py:359
  (8 shorter events, 0.1 us)
Async XLA Ops:
  26.3 17.1 %copy-start = (bf16[2,64,1024]{2,1,0:T(8,128)(2,1)S(1)}, bf16[2,64,1024]{2,1,0:T(8,128)(2,1)}, u32[]{:S(2)}) copy-start(bf16[2,64,1024]{2,1,0:T(8,128)(2,1)} %param.13) | copy-start | bytes 786436
  26.3 17.1 %copy-start.3 = (f32[1024]{0:T(1024)S(1)}, f32[1024]{0:T(1024)}, u32[]{:S(2)}) copy-start(f32[1024]{0:T(1024)} %param.14) | copy-start | bytes 12292
  26.3 31.3 %collective-permute-start = (bf16[16,328,128]{2,1,0:T(8,128)(2,1)S(1)}, bf16[16,328,128]{2,1,0:T(8,128)(2,1)S(1)}, u32[]{:S(2)}, u32[]{:S(2)}) collective-permute-start(bf16[16,328,128]{2,1,0:T(8,128)(2,1)S(1)} %all_to_all.15.own_ref), channel_id=1, source_target_pairs={{0,1},{1,0},{2,3},{3,2},{4,5},{5,4},{6,7},{7,6},{8,9},{9,8},{10,11... | collective-permute-start | bytes 4030472 | tf_op jit(solution)/shard_map/ppermute | solution.py:375
  28.4 10.6 %collective-permute-start.1 = (bf16[1,16,64,128]{3,2,1,0:T(8,128)(2,1)S(1)}, bf16[1,16,64,128]{3,2,1,0:T(8,128)(2,1)S(1)}, u32[]{:S(2)}, u32[]{:S(2)}) collective-permute-start(bf16[1,16,64,128]{3,2,1,0:T(8,128)(2,1)S(1)} %slice_bitcast_fusion.first_ref), channel_id=1, source_target_pairs={{0,8},{8,0},{16,24},{24,16},{1,9},{9,1},{17,25},{25,17},{2,10},{10... | collective-permute-start | bytes 786440 | tf_op jit(solution)/shard_map/ppermute | solution.py:399
  39.1 16.6 %collective-permute-start.2 = (bf16[2,16,64,128]{3,2,1,0:T(8,128)(2,1)S(1)}, bf16[2,16,64,128]{3,2,1,0:T(8,128)(2,1)S(1)}, u32[]{:S(2)}, u32[]{:S(2)}) collective-permute-start(bf16[2,16,64,128]{3,2,1,0:T(8,128)(2,1)S(1)} %shard_map.131.first_ref), channel_id=1, source_target_pairs={{0,24},{8,16},{16,8},{24,0},{1,25},{9,17},{17,9},{25,1},{2,26},{10... | collective-permute-start | bytes 1572872 | tf_op jit(solution)/shard_map/ppermute | solution.py:399
  43.5 14.2 %copy-start.1 = (bf16[16,512]{1,0:T(8,128)(2,1)S(1)}, bf16[16,512]{1,0:T(8,128)(2,1)}, u32[]{:S(2)}) copy-start(bf16[16,512]{1,0:T(8,128)(2,1)} %up_forward_ref.3) | copy-start | bytes 49156
  43.5 14.2 %copy-start.2 = (bf16[16,512]{1,0:T(8,128)(2,1)S(1)}, bf16[16,512]{1,0:T(8,128)(2,1)}, u32[]{:S(2)}) copy-start(bf16[16,512]{1,0:T(8,128)(2,1)} %up_backward_ref.3) | copy-start | bytes 49156
  43.5 14.2 %copy-start.4 = (f32[512]{0:T(512)S(1)}, f32[512]{0:T(512)}, u32[]{:S(2)}) copy-start(f32[512]{0:T(512)} %param.22) | copy-start | bytes 6148
  43.5 14.2 %copy-start.5 = (f32[512]{0:T(512)S(1)}, f32[512]{0:T(512)}, u32[]{:S(2)}) copy-start(f32[512]{0:T(512)} %param.23) | copy-start | bytes 6148
  55.7 41.5 %collective-permute-start.3 = (bf16[4,16,64,128]{3,2,1,0:T(8,128)(2,1)S(1)}, bf16[4,16,64,128]{3,2,1,0:T(8,128)(2,1)S(1)}, u32[]{:S(2)}, u32[]{:S(2)}) collective-permute-start(bf16[4,16,64,128]{3,2,1,0:T(8,128)(2,1)S(1)} %shard_map.132.own_ref), channel_id=1, source_target_pairs={{0,1},{1,0},{2,3},{3,2},{4,5},{5,4},{6,7},{7,6},{8,9},{9,8},{10,11... | collective-permute-start | bytes 3145736 | tf_op jit(solution)/shard_map/ppermute | solution.py:375
  60.1 36.9 %copy-start.7 = (f32[32]{0:T(128)S(1)}, f32[32]{0:T(128)}, u32[]{:S(2)}) copy-start(f32[32]{0:T(128)} %param.24) | copy-start | bytes 388
  89.1 19.1 %all-to-all-start.2 = ((bf16[16,32,128]{2,1,0:T(8,128)(2,1)}), bf16[16,32,128]{2,1,0:T(8,128)(2,1)S(1)}, u32[]{:S(2)}, u32[]{:S(2)}) async-start(bf16[16,32,128]{2,1,0:T(8,128)(2,1)} %bitcast.6), calls=%async_computation.2 | async-start | bytes 262144 | tf_op jit(solution)/shard_map/all_to_all | solution.py:424
  108.2 1.1 %copy-start.6 = (f32[128,1536]{1,0:T(8,128)S(1)}, f32[128,1536]{1,0:T(8,128)}, u32[]{:S(2)}) copy-start(f32[128,1536]{1,0:T(8,128)} %shard_map.133.parts_ref) | copy-start | bytes 2359300

commit v12 on v11

--- a/solution.py
+++ b/solution.py
@@ -18,6 +18,7 @@
 SENT = COLUMNS + 32 + 32 + 8
 EPS = 1e-06
 GROUP = [(z + 12) % 16 for z in range(16)]
+PLANE_GROUP = [(i + 15) % 16 for i in range(16)]
 f32 = jnp.float32
 bf16 = jnp.bfloat16
 
@@ -59,19 +60,21 @@
     ]
     for copy in copies:
         copy.start()
-    for copy in copies:
+    for which, (ref, first) in enumerate(((key_ref, 0), (value_ref, 4))):
+        copies[which].wait()
+        for i in range(16):
+            for group in range(4):
+                lanes = slice(group * LANES, (group + 1) * LANES)
+                out_ref[i, (first + group) * 32 : (first + group + 1) * 32] = ref[:, lanes]
+    for copy in copies[2:]:
         copy.wait()
     row, col = grid_of((16, LANES))
     ranks = dot_tn(forward_ref[...], as_bf16(row == col)) + dot_tn(
         backward_ref[...], as_bf16(row + 16 == col)
     )
     packed = jnp.concatenate([ranks[8 * i : 8 * i + 8, :32] for i in range(4)], axis=1)
-    for i in range(16):
-        for group in range(4):
-            lanes = slice(group * LANES, (group + 1) * LANES)
-            out_ref[i, group * 32 : (group + 1) * 32] = key_ref[:, lanes]
-            out_ref[i, (4 + group) * 32 : (5 + group) * 32] = value_ref[:, lanes]
-        start = (i // 4) * LANES
+    for i, peer in enumerate(PLANE_GROUP):
+        start = (peer // 4) * LANES
         out_ref[i, COLUMNS : COLUMNS + 32] = query_ref[:, start : start + LANES]
         out_ref[i, COLUMNS + 32 : COLUMNS + 48] = mix_ref[:, 2 * start : 2 * start + LANES]
         out_ref[i, COLUMNS + 48 : COLUMNS + 64] = mix_ref[:, 2 * start + LANES : 2 * start + 2 * LANES]
@@ -95,7 +98,7 @@
     normed = (values * scale * gain_ref[...]).astype(bf16)
     return [
         jnp.concatenate(
-            [normed[:, (2 * i + core) * 32 : (2 * i + core) * 32 + 32] for i in range(16)], axis=1
+            [normed[:, (2 * i + core) * 32 : (2 * i + core) * 32 + 32] for i in PLANE_GROUP], axis=1
         )
         for core in range(2)
     ]
@@ -114,7 +117,8 @@
         ],
         axis=1,
     )
-    return halves(jax.nn.log_sigmoid(gates) * (2.0 / (BLOCK * HEADS)))
+    log_sigmoid = jnp.minimum(gates, 0.0) - jnp.log1p(jnp.exp(-jnp.abs(gates)))
+    return halves(log_sigmoid * (2.0 / (BLOCK * HEADS)))
 
 
 def summed(parts, mask, way):
@@ -164,17 +168,19 @@
     hrow, hcol = grid_of((HEADS, WIDTH))
     mine = hrow == hcol // HEAD
     erow, ecol = grid_of((WIDTH, LANES))
+    fold = as_bf16(((erow // LANES) * HEAD + erow % HEAD) == ecol)
     srow, scol = grid_of((8, 128))
-    close = 0.0
-    for way, span in ((0, fwd), (1, bwd)):
-        pick = as_bf16(srow == scol // BLOCK)
+    pick = as_bf16(srow == scol // BLOCK)
+    lines = []
+    for span in (fwd, bwd):
         sums = dot(pick, high[:, span]) + dot(pick, low[:, span])
         for seq in range(2):
             line = jnp.where(mine, sums[seq : seq + 1], 0.0)
-            place = as_bf16(ecol == (2 * way + seq) * HEAD + erow % HEAD)
-            line_high, line_low = halves(line)
-            both = jnp.concatenate([line_high, line_low], axis=0)
-            close = close + dot(both, place)
+            lines.append(
+                line[:, :LANES] + line[:, LANES : 2 * LANES]
+                + line[:, 2 * LANES : 3 * LANES] + line[:, 3 * LANES :]
+            )
+    close = dot(jnp.concatenate(halves(jnp.concatenate(lines, axis=1)), axis=0), fold)
     tail = lax.broadcasted_iota(jnp.int32, (HEADS, 8, LANES), 1)
     payload_ref[:, HEAD:, :] = jnp.where(
         tail == 0,
@@ -182,8 +188,6 @@
         jnp.where(tail == 1, close[HEADS:][:, None, :], 0.0),
     ).astype(bf16)
     diagonal = (row // HEAD) == (col // HEAD)
-    erow, ecol = grid_of((4 * LANES, LANES))
-    fold = as_bf16(((erow // LANES) * HEAD + erow % HEAD) == ecol)
     for group in range(4):
         lanes = slice(group * LANES, (group + 1) * LANES)
         parts = []
@@ -292,7 +296,16 @@
                 out_ref[span, start : start + LANES] = total
 
 
-def out_kernel(states_ref, parts_ref, gain_ref, own_ref, other_ref, out_ref):
+def out_kernel(
+    states_ref, parts_hbm, gain_ref, own_ref, other_ref, out_ref, parts_ref, sems
+):
+    spans = [slice(seq * BLOCK, (seq + 1) * BLOCK) for seq in range(2)]
+    fetches = [
+        pltpu.make_async_copy(parts_hbm.at[span], parts_ref.at[span], sems.at[seq])
+        for seq, span in enumerate(spans)
+    ]
+    for fetch in fetches:
+        fetch.start()
     core = lax.axis_index("dp_2")
     row, col = grid_of((LANES, 8 * LANES))
     source = (col // 256) * HEAD + ((col // LANES) % 2) * 16 + col % 16
@@ -304,8 +317,8 @@
         for g in range(2)
     ]
     totals = [[], []]
-    for seq in range(2):
-        span = slice(seq * BLOCK, (seq + 1) * BLOCK)
+    for seq, span in enumerate(spans):
+        fetches[seq].wait()
         sides = [[], []]
         for group in range(2):
             queries = jnp.concatenate(
@@ -343,7 +356,13 @@
 
         def weights(ref):
             return jnp.concatenate(
-                [ref[slot, :, rows : rows + 16, :].reshape(256, LANES) for rows in (32, 48)], axis=1
+                [
+                    jnp.concatenate(
+                        [ref[slot, 1:, rows : rows + 16, :], ref[slot, :1, rows : rows + 16, :]], axis=0
+                    ).reshape(256, LANES)
+                    for rows in (32, 48)
+                ],
+                axis=1,
             )
 
         out_ref[:, quarter * 256 : (quarter + 1) * 256] = (
@@ -392,7 +411,7 @@
         pack_kernel, shape((16, SENT, LANES), bf16), [hbm] * 6, 1 << 26, *sources,
         scratch=[pltpu.VMEM(x.shape, bf16) for x in sources] + [pltpu.SemaphoreType.DMA((6,))],
     )
-    own = lax.all_to_all(send, PLANE, 0, 0)
+    own = lax.all_to_all(send, PLANE, 0, 0, axis_index_groups=[PLANE_GROUP])
     other = swapped(own)
     mix = own[None, :, COLUMNS : COLUMNS + 64, :]
     for flip in (1, 3):
@@ -430,8 +449,9 @@
     )
     gain = jnp.tile(out_gain.reshape(2, 1, 16), (1, HEADS, 1)).reshape(2, 256)
     mixed = call(
-        out_kernel, shape((rows, width), bf16), [VMEM] * 5, 1 << 30,
-        returned.reshape(WIDTH, LANES), parts, gain, mix, mix_other,
+        out_kernel, shape((rows, width), bf16), [VMEM, hbm] + [VMEM] * 3, 1 << 30,
+        returned.reshape(WIDTH, LANES), in_hbm(parts), gain, mix, mix_other,
+        scratch=[pltpu.VMEM((rows, 3 * WIDTH), f32), pltpu.SemaphoreType.DMA((2,))],
     )
     return mixed.reshape(seqs, toks, width)
 

time: 113 us -> 111 us (0.982)
  blocking collectives: 53.1 us -> 51.7 us
  starting transfers between devices: 19.1 us -> 17.8 us
  waiting for transfers between devices: 26.1 us -> 27.4 us
  local copies, waits for them, and re-layouts: 1.36 us -> 0.23 us
    all_to_all x1, blocking collectives: 25.1 us -> 23.8 us  [body(): own = lax.all_to_all(send, PLANE, 0, 0, axis_index_groups=[PLANE_GROUP])]
    ppermute x2, starting transfers between devices: 7.19 us -> 5.93 us  [body(): arrived = lax.ppermute(mix, 'dp_0', [(i, i ^ flip) for i in range(4)])]
    ppermute x2, waiting for transfers between devices: 19.6 us -> 20.8 us  [body(): arrived = lax.ppermute(mix, 'dp_0', [(i, i ^ flip) for i in range(4)])]
    unnamed x16 -> x14, local copies, waits for them, and re-layouts: 1.17 us -> 0.04 us
where the time goes in v12:
time: 111 us; the launch traced here: 109 us
  blocking collectives  51.7 us (47%)
  waiting for transfers between devices  27.4 us (25%)
  starting transfers between devices  17.8 us (16%)
  Pallas kernels  11.9 us (11%)
    all_to_all x1, blocking collectives, body(): inbound = lax.all_to_all(payload, 'sp', 0, 0, axis_index_groups=[GROUP])  28 us
    all_to_all x1, blocking collectives, body(): own = lax.all_to_all(send, PLANE, 0, 0, axis_index_groups=[PLANE_GROUP])  23.8 us
    ppermute x2, waiting for transfers between devices, body(): arrived = lax.ppermute(mix, 'dp_0', [(i, i ^ flip) for i in range(4)])  20.8 us
    pallas_call x8, Pallas kernels, call(): pl.pallas_call(kernel, out_shape=outs, in_specs=specs, out_specs=(VMEM,)...  11.9 us
    all_to_all x1, starting transfers between devices, body(): lax.all_to_all(states.reshape(HEADS, HEAD, LANES), 'sp', 0, 0, axis_index...  7.95 us
    all_to_all x1, waiting for transfers between devices, body(): lax.all_to_all(states.reshape(HEADS, HEAD, LANES), 'sp', 0, 0, axis_index...  6.65 us
    ppermute x2, starting transfers between devices, body(): arrived = lax.ppermute(mix, 'dp_0', [(i, i ^ flip) for i in range(4)])  5.93 us
    ppermute x2, starting transfers between devices, swapped(): return lax.ppermute(x, 'dp_2', [(0, 1), (1, 0)])  3.96 us
  transfers between devices with their start and end apart: 5, of which 3 were waited for; matrix products, arithmetic and copies ran while one was open for 0% of the time, Pallas kernels for 7%

profile of v12, /device:TPU:24, one launch (start us, length us, event | category | flops | bytes accessed | tf_op | source)
XLA Modules:
  0.0 109.4 jit_solution(8356970620774996271)
XLA Ops:
  0.0 1.2 %shard_map.128 = bf16[16,328,128]{2,1,0:T(8,128)(2,1)S(1)} custom-call(bf16[32,512]{1,0:T(8,128)(2,1)} %key_hbm.1, bf16[32,512]{1,0:T(8,128)(2,1)} %value_hbm.1, bf16[32,512]{1,0:T(8,128)(2,1)} %query_hbm.1, bf16[16,32]{1,0:T(8,128)(2,1)} %bitcast.24, bf16[16,32]{1,0:T(8,128)(2,1)} %bitcast.25, bf16[16,1024]{1,0:T(8,128)(2,1)} %mix_hbm.1), custom_call_target="tpu_custom_call" | custom-call | flops 67108864 | bytes 1048576 | tf_op jit(solution)/shard_map/pallas_call | solution.py:378
  1.2 23.8 %all_to_all.15.own_ref = bf16[16,328,128]{2,1,0:T(8,128)(2,1)S(1)} all-to-all(bf16[16,328,128]{2,1,0:T(8,128)(2,1)S(1)} %shard_map.128), channel_id=1, replica_groups={{30,0,2,4,6,8,10,12,14,16,18,20,22,24,26,28},{31,1,3,5,7,9,11,13,15,17,..., dimensions={0} | all-to-all | bytes 2686976 | tf_op jit(solution)/shard_map/all_to_all | solution.py:414
  25.0 2.0 %collective-permute-start = (bf16[16,328,128]{2,1,0:T(8,128)(2,1)S(1)}, bf16[16,328,128]{2,1,0:T(8,128)(2,1)S(1)}, u32[]{:S(2)}, u32[]{:S(2)}) collective-permute-start(bf16[16,328,128]{2,1,0:T(8,128)(2,1)S(1)} %all_to_all.15.own_ref), channel_id=1, source_target_pairs={{0,1},{1,0},{2,3},{3,2},{4,5},{5,4},{6,7},{7,6},{8,9},{9,8},{10,11... | collective-permute-start | bytes 4030472 | tf_op jit(solution)/shard_map/ppermute | solution.py:394
  27.1 2.8 %collective-permute-start.1 = (bf16[1,16,64,128]{3,2,1,0:T(8,128)(2,1)S(1)}, bf16[1,16,64,128]{3,2,1,0:T(8,128)(2,1)S(1)}, u32[]{:S(2)}, u32[]{:S(2)}) collective-permute-start(bf16[1,16,64,128]{3,2,1,0:T(8,128)(2,1)S(1)} %slice_bitcast_fusion.first_ref), channel_id=1, source_target_pairs={{0,8},{8,0},{16,24},{24,16},{1,9},{9,1},{17,25},{25,17},{2,10},{10... | collective-permute-start | bytes 786440 | tf_op jit(solution)/shard_map/ppermute | solution.py:418
  29.8 7.8 %collective-permute-done.1.second_ref = bf16[1,16,64,128]{3,2,1,0:T(8,128)(2,1)S(1)} collective-permute-done((bf16[1,16,64,128]{3,2,1,0:T(8,128)(2,1)S(1)}, bf16[1,16,64,128]{3,2,1,0:T(8,128)(2,1)S(1)}, u32[]{:S(2)}, u32[]{:S(2)}) %collective-permute-start.1) | collective-permute-done | bytes 262176 | tf_op jit(solution)/shard_map/ppermute | solution.py:418
  37.7 3.2 %collective-permute-start.2 = (bf16[2,16,64,128]{3,2,1,0:T(8,128)(2,1)S(1)}, bf16[2,16,64,128]{3,2,1,0:T(8,128)(2,1)S(1)}, u32[]{:S(2)}, u32[]{:S(2)}) collective-permute-start(bf16[2,16,64,128]{3,2,1,0:T(8,128)(2,1)S(1)} %shard_map.131.first_ref), channel_id=1, source_target_pairs={{0,24},{8,16},{16,8},{24,0},{1,25},{9,17},{17,9},{25,1},{2,26},{10... | collective-permute-start | bytes 1572872 | tf_op jit(solution)/shard_map/ppermute | solution.py:418
  40.9 0.0 copy-done
  40.9 0.0 copy-done.3
  40.9 0.0 copy-start.1
  40.9 0.0 copy-start.2
  40.9 0.0 copy-start.4
  40.9 0.0 copy-start.5
  41.0 0.4 shard_map.127.normed_ref
  41.3 12.9 %collective-permute-done.2.second_ref = bf16[2,16,64,128]{3,2,1,0:T(8,128)(2,1)S(1)} collective-permute-done((bf16[2,16,64,128]{3,2,1,0:T(8,128)(2,1)S(1)}, bf16[2,16,64,128]{3,2,1,0:T(8,128)(2,1)S(1)}, u32[]{:S(2)}, u32[]{:S(2)}) %collective-permute-start.2) | collective-permute-done | bytes 524320 | tf_op jit(solution)/shard_map/ppermute | solution.py:418
  54.3 0.1 shard_map.132.own_ref
  54.3 1.9 %collective-permute-start.3 = (bf16[4,16,64,128]{3,2,1,0:T(8,128)(2,1)S(1)}, bf16[4,16,64,128]{3,2,1,0:T(8,128)(2,1)S(1)}, u32[]{:S(2)}, u32[]{:S(2)}) collective-permute-start(bf16[4,16,64,128]{3,2,1,0:T(8,128)(2,1)S(1)} %shard_map.132.own_ref), channel_id=1, source_target_pairs={{0,1},{1,0},{2,3},{3,2},{4,5},{5,4},{6,7},{7,6},{8,9},{9,8},{10,11... | collective-permute-start | bytes 3145736 | tf_op jit(solution)/shard_map/ppermute | solution.py:394
  56.3 0.0 collective-permute-done.other_ref
  56.3 0.0 copy-done.1
  56.3 0.0 copy-done.2
  56.3 0.0 copy-done.4
  56.3 0.0 copy-done.5
  56.3 2.2 %shard_map.129 = (bf16[16,40,128]{2,1,0:T(8,128)(2,1)S(1)}, bf16[128,1152]{1,0:T(8,128)(2,1)}) custom-call(bf16[2,128,512]{2,1,0:T(8,128)(2,1)S(1)} %shard_map.127.normed_ref, bf16[16,328,128]{2,1,0:T(8,128)(2,1)S(1)} %all_to_all.15.own_ref, bf16[16,328,128]{2,1,0:T(8,128)(2,1)S(1)} %collective-permute-done.other_ref, bf16[16,512]{1,0:T(8,128)(2,1)S(1)} %copy-done.1, ...), custom_call_target="tpu_custom_call" | custom-call | flops 1073741824 | bytes 1048576 | tf_op jit(solution)/shard_map/pallas_call | solution.py:378
  58.5 0.0 copy-start.6
  58.5 28.0 %all_to_all.16.payload_ref = bf16[16,40,128]{2,1,0:T(8,128)(2,1)S(1)} all-to-all(bf16[16,40,128]{2,1,0:T(8,128)(2,1)S(1)} %get-tuple-element.7), channel_id=1, replica_groups={{384,416,448,480,0,32,64,96,128,160,192,224,256,288,320,352},{385,417,4..., dimensions={0} | all-to-all | bytes 327680 | tf_op jit(solution)/shard_map/all_to_all | solution.py:437
  86.5 0.9 shard_map.130
  87.4 8.0 %all-to-all-start.2 = ((bf16[16,32,128]{2,1,0:T(8,128)(2,1)}), bf16[16,32,128]{2,1,0:T(8,128)(2,1)S(1)}, u32[]{:S(2)}, u32[]{:S(2)}) async-start(bf16[16,32,128]{2,1,0:T(8,128)(2,1)} %bitcast.6), calls=%async_computation.2 | async-start | bytes 262144 | tf_op jit(solution)/shard_map/all_to_all | solution.py:443
  95.4 0.1 tile.9
  95.4 0.1 tile.11.gain_ref
  95.5 0.0 collective-permute-done.3.other_ref
  95.5 4.3 %shard_map.133.parts_hbm = f32[128,1536]{1,0:T(8,128)} custom-call(bf16[128,1024]{1,0:T(8,128)(2,1)} %bitcast.16, f32[1,1024]{1,0:T(1,128)S(1)} %bitcast.19, bf16[4,16,64,128]{3,2,1,0:T(8,128)(2,1)S(1)} %shard_map.132.own_ref, bf16[4,16,64,128]{3,2,1,0:T(8,128)(2,1)S(1)} %collective-permute-done.3.other_ref, bf16[128,1152]{1,0:T(8,128)(2,1)} %get-tuple-element.8.rounded_ref, ...), custom_call_target="tpu_custom_call" | custom-call | flops 1073741824 | bytes 1048576 | tf_op jit(solution)/shard_map/pallas_call | solution.py:378
  99.9 6.7 %all-to-all-done.2 = bf16[16,32,128]{2,1,0:T(8,128)(2,1)S(1)} async-done(((bf16[16,32,128]{2,1,0:T(8,128)(2,1)}), bf16[16,32,128]{2,1,0:T(8,128)(2,1)S(1)}, u32[]{:S(2)}, u32[]{:S(2)}) %all-to-all-start.2) | async-done | bytes 131104 | tf_op jit(solution)/shard_map/all_to_all | solution.py:443
  106.5 2.9 %shard_map.134 = bf16[128,1024]{1,0:T(8,128)(2,1)} custom-call(bf16[512,128]{1,0:T(8,128)(2,1)S(1)} %bitcast.15, f32[128,1536]{1,0:T(8,128)} %shard_map.133.parts_hbm, f32[2,256]{1,0:T(2,128)S(1)} %tile.11.gain_ref, bf16[4,16,64,128]{3,2,1,0:T(8,128)(2,1)S(1)} %shard_map.132.own_ref, bf16[4,16,64,128]{3,2,1,0:T(8,128)(2,1)S(1)} %collective-permute-done.3.other_ref), custom_call_target="tpu_custom_call" | custom-call | flops 1073741824 | bytes 1048576 | tf_op jit(solution)/shard_map/pallas_call | solution.py:378
  (6 shorter events, 0.1 us)
Async XLA Ops:
  25.0 15.9 %copy-start = (bf16[2,64,1024]{2,1,0:T(8,128)(2,1)S(1)}, bf16[2,64,1024]{2,1,0:T(8,128)(2,1)}, u32[]{:S(2)}) copy-start(bf16[2,64,1024]{2,1,0:T(8,128)(2,1)} %param.13) | copy-start | bytes 786436
  25.0 15.9 %copy-start.3 = (f32[1024]{0:T(1024)S(1)}, f32[1024]{0:T(1024)}, u32[]{:S(2)}) copy-start(f32[1024]{0:T(1024)} %param.14) | copy-start | bytes 12292
  25.0 31.3 %collective-permute-start = (bf16[16,328,128]{2,1,0:T(8,128)(2,1)S(1)}, bf16[16,328,128]{2,1,0:T(8,128)(2,1)S(1)}, u32[]{:S(2)}, u32[]{:S(2)}) collective-permute-start(bf16[16,328,128]{2,1,0:T(8,128)(2,1)S(1)} %all_to_all.15.own_ref), channel_id=1, source_target_pairs={{0,1},{1,0},{2,3},{3,2},{4,5},{5,4},{6,7},{7,6},{8,9},{9,8},{10,11... | collective-permute-start | bytes 4030472 | tf_op jit(solution)/shard_map/ppermute | solution.py:394
  27.1 10.6 %collective-permute-start.1 = (bf16[1,16,64,128]{3,2,1,0:T(8,128)(2,1)S(1)}, bf16[1,16,64,128]{3,2,1,0:T(8,128)(2,1)S(1)}, u32[]{:S(2)}, u32[]{:S(2)}) collective-permute-start(bf16[1,16,64,128]{3,2,1,0:T(8,128)(2,1)S(1)} %slice_bitcast_fusion.first_ref), channel_id=1, source_target_pairs={{0,8},{8,0},{16,24},{24,16},{1,9},{9,1},{17,25},{25,17},{2,10},{10... | collective-permute-start | bytes 786440 | tf_op jit(solution)/shard_map/ppermute | solution.py:418
  37.7 16.6 %collective-permute-start.2 = (bf16[2,16,64,128]{3,2,1,0:T(8,128)(2,1)S(1)}, bf16[2,16,64,128]{3,2,1,0:T(8,128)(2,1)S(1)}, u32[]{:S(2)}, u32[]{:S(2)}) collective-permute-start(bf16[2,16,64,128]{3,2,1,0:T(8,128)(2,1)S(1)} %shard_map.131.first_ref), channel_id=1, source_target_pairs={{0,24},{8,16},{16,8},{24,0},{1,25},{9,17},{17,9},{25,1},{2,26},{10... | collective-permute-start | bytes 1572872 | tf_op jit(solution)/shard_map/ppermute | solution.py:418
  40.9 15.4 %copy-start.1 = (bf16[16,512]{1,0:T(8,128)(2,1)S(1)}, bf16[16,512]{1,0:T(8,128)(2,1)}, u32[]{:S(2)}) copy-start(bf16[16,512]{1,0:T(8,128)(2,1)} %up_forward_ref.3) | copy-start | bytes 49156
  40.9 15.4 %copy-start.2 = (bf16[16,512]{1,0:T(8,128)(2,1)S(1)}, bf16[16,512]{1,0:T(8,128)(2,1)}, u32[]{:S(2)}) copy-start(bf16[16,512]{1,0:T(8,128)(2,1)} %up_backward_ref.3) | copy-start | bytes 49156
  40.9 15.4 %copy-start.4 = (f32[512]{0:T(512)S(1)}, f32[512]{0:T(512)}, u32[]{:S(2)}) copy-start(f32[512]{0:T(512)} %param.22) | copy-start | bytes 6148
  40.9 15.4 %copy-start.5 = (f32[512]{0:T(512)S(1)}, f32[512]{0:T(512)}, u32[]{:S(2)}) copy-start(f32[512]{0:T(512)} %param.23) | copy-start | bytes 6148
  54.3 41.2 %collective-permute-start.3 = (bf16[4,16,64,128]{3,2,1,0:T(8,128)(2,1)S(1)}, bf16[4,16,64,128]{3,2,1,0:T(8,128)(2,1)S(1)}, u32[]{:S(2)}, u32[]{:S(2)}) collective-permute-start(bf16[4,16,64,128]{3,2,1,0:T(8,128)(2,1)S(1)} %shard_map.132.own_ref), channel_id=1, source_target_pairs={{0,1},{1,0},{2,3},{3,2},{4,5},{5,4},{6,7},{7,6},{8,9},{9,8},{10,11... | collective-permute-start | bytes 3145736 | tf_op jit(solution)/shard_map/ppermute | solution.py:394
  58.5 36.9 %copy-start.6 = (f32[32]{0:T(128)S(1)}, f32[32]{0:T(128)}, u32[]{:S(2)}) copy-start(f32[32]{0:T(128)} %param.24) | copy-start | bytes 388
  87.4 19.1 %all-to-all-start.2 = ((bf16[16,32,128]{2,1,0:T(8,128)(2,1)}), bf16[16,32,128]{2,1,0:T(8,128)(2,1)S(1)}, u32[]{:S(2)}, u32[]{:S(2)}) async-start(bf16[16,32,128]{2,1,0:T(8,128)(2,1)} %bitcast.6), calls=%async_computation.2 | async-start | bytes 262144 | tf_op jit(solution)/shard_map/all_to_all | solution.py:443

commit v13 on v12

--- a/solution.py
+++ b/solution.py
@@ -85,6 +85,12 @@
     count = first_ref.shape[0]
     out_ref[:count] = first_ref[...]
     out_ref[count:] = second_ref[...]
+
+
+def split_kernel(first_ref, second_ref, query_ref, mix_ref):
+    for part, ref in enumerate((first_ref, second_ref)):
+        query_ref[2 * part : 2 * part + 2] = ref[:, :, :32, :]
+        mix_ref[2 * part : 2 * part + 2] = ref[:, :, 32:, :]
 
 
 def slot_of(index, axis):
@@ -245,7 +251,7 @@
     def weights(ref):
         return jnp.concatenate(
             [
-                ref[slot_of(quarter, "dp_0"), :, :32, :].reshape(WIDTH, LANES)
+                ref[slot_of(quarter, "dp_0")].reshape(WIDTH, LANES)
                 for quarter in range(4)
             ],
             axis=1,
@@ -297,15 +303,11 @@
 
 
 def out_kernel(
-    states_ref, parts_hbm, gain_ref, own_ref, other_ref, out_ref, parts_ref, sems
+    states_ref, parts_ref, gain_ref, own_hbm, other_ref, out_ref, own_ref, sem
 ):
+    fetch = pltpu.make_async_copy(own_hbm, own_ref, sem)
+    fetch.start()
     spans = [slice(seq * BLOCK, (seq + 1) * BLOCK) for seq in range(2)]
-    fetches = [
-        pltpu.make_async_copy(parts_hbm.at[span], parts_ref.at[span], sems.at[seq])
-        for seq, span in enumerate(spans)
-    ]
-    for fetch in fetches:
-        fetch.start()
     core = lax.axis_index("dp_2")
     row, col = grid_of((LANES, 8 * LANES))
     source = (col // 256) * HEAD + ((col // LANES) % 2) * 16 + col % 16
@@ -318,7 +320,6 @@
     ]
     totals = [[], []]
     for seq, span in enumerate(spans):
-        fetches[seq].wait()
         sides = [[], []]
         for group in range(2):
             queries = jnp.concatenate(
@@ -351,6 +352,7 @@
     ]
     mine = jnp.where(core == 0, attended[0], attended[1])
     theirs = jnp.where(core == 0, attended[1], attended[0])
+    fetch.wait()
     for quarter in range(4):
         slot = slot_of(quarter, "dp_0")
 
@@ -360,7 +362,7 @@
                     jnp.concatenate(
                         [ref[slot, 1:, rows : rows + 16, :], ref[slot, :1, rows : rows + 16, :]], axis=0
                     ).reshape(256, LANES)
-                    for rows in (32, 48)
+                    for rows in (0, 16)
                 ],
                 axis=1,
             )
@@ -414,12 +416,19 @@
     own = lax.all_to_all(send, PLANE, 0, 0, axis_index_groups=[PLANE_GROUP])
     other = swapped(own)
     mix = own[None, :, COLUMNS : COLUMNS + 64, :]
-    for flip in (1, 3):
+    for step, flip in enumerate((1, 3)):
         arrived = lax.ppermute(mix, "dp_0", [(i, i ^ flip) for i in range(4)])
-        mix = call(
-            join_kernel, shape((2 * mix.shape[0], 16, 64, LANES), bf16), [VMEM] * 2, 1 << 26,
-            mix, arrived,
-        )
+        if step == 0:
+            mix = call(
+                join_kernel, shape((2, 16, 64, LANES), bf16), [VMEM] * 2, 1 << 26, mix, arrived
+            )
+        else:
+            query, mix = call(
+                split_kernel,
+                (shape((4, 16, 32, LANES), bf16), pltpu.HBM((4, 16, 32, LANES), bf16)),
+                [VMEM] * 2, 1 << 26,
+                mix, arrived,
+            )
     normed = call(
         norm_kernel, shape((2, rows, 512), bf16), [VMEM, VMEM], 1 << 28,
         tokens_flat, gain_flat,
@@ -435,6 +444,7 @@
         [VMEM] * 7, 1 << 30, normed, own, other, *decays,
     )
     inbound = lax.all_to_all(payload, "sp", 0, 0, axis_index_groups=[GROUP])
+    query_other = swapped(query)
     mix_other = swapped(mix)
     states = call(
         scan_kernel, shape((WIDTH, LANES), bf16), [VMEM], 1 << 28,
@@ -444,14 +454,14 @@
         states.reshape(HEADS, HEAD, LANES), "sp", 0, 0, axis_index_groups=[GROUP]
     )
     parts = call(
-        query_kernel, pltpu.HBM((rows, 3 * WIDTH), f32), [VMEM] * 9, 1 << 30,
-        in_hbm(tokens_flat), gain_flat, mix, mix_other, in_hbm(rounded), *decays,
+        query_kernel, shape((rows, 3 * WIDTH), f32), [VMEM] * 9, 1 << 30,
+        in_hbm(tokens_flat), gain_flat, query, query_other, in_hbm(rounded), *decays,
     )
     gain = jnp.tile(out_gain.reshape(2, 1, 16), (1, HEADS, 1)).reshape(2, 256)
     mixed = call(
-        out_kernel, shape((rows, width), bf16), [VMEM, hbm] + [VMEM] * 3, 1 << 30,
-        returned.reshape(WIDTH, LANES), in_hbm(parts), gain, mix, mix_other,
-        scratch=[pltpu.VMEM((rows, 3 * WIDTH), f32), pltpu.SemaphoreType.DMA((2,))],
+        out_kernel, shape((rows, width), bf16), [VMEM] * 3 + [hbm, VMEM], 1 << 30,
+        returned.reshape(WIDTH, LANES), parts, gain, in_hbm(mix), mix_other,
+        scratch=[pltpu.VMEM((4, 16, 32, LANES), bf16), pltpu.SemaphoreType.DMA],
     )
     return mixed.reshape(seqs, toks, width)
 

time: 111 us -> 94.8 us (0.85)
  the two profiles are of different devices: /device:TPU:24 before, /device:TPU:2 now
where the time goes in v13:
time: 94.8 us; the launch traced here: 94.2 us
  starting transfers between devices  36.1 us (38%)
  blocking collectives  24.6 us (26%)
  waiting for transfers between devices  20.7 us (22%)
  Pallas kernels  12.4 us (13%)
    all_to_all x1, blocking collectives, body(): own = lax.all_to_all(send, PLANE, 0, 0, axis_index_groups=[PLANE_GROUP])  24.6 us
    all_to_all x1, starting transfers between devices, body(): inbound = lax.all_to_all(payload, 'sp', 0, 0, axis_index_groups=[GROUP])  15.7 us
    pallas_call x8, Pallas kernels, call(): pl.pallas_call(kernel, out_shape=outs, in_specs=specs, out_specs=(VMEM,)...  12.4 us
    ppermute x2, waiting for transfers between devices, body(): arrived = lax.ppermute(mix, 'dp_0', [(i, i ^ flip) for i in range(4)])  7.93 us
    all_to_all x1, starting transfers between devices, body(): lax.all_to_all(states.reshape(HEADS, HEAD, LANES), 'sp', 0, 0, axis_index...  7.91 us
    all_to_all x1, waiting for transfers between devices, body(): lax.all_to_all(states.reshape(HEADS, HEAD, LANES), 'sp', 0, 0, axis_index...  6.44 us
    ppermute x3, starting transfers between devices, swapped(): return lax.ppermute(x, 'dp_2', [(0, 1), (1, 0)])  6.37 us
    all_to_all x1, waiting for transfers between devices, body(): inbound = lax.all_to_all(payload, 'sp', 0, 0, axis_index_groups=[GROUP])  6.36 us
  transfers between devices with their start and end apart: 7, of which 3 were waited for; matrix products, arithmetic and copies ran while one was open for 0% of the time, Pallas kernels for 9%

profile of v13, /device:TPU:2, one launch (start us, length us, event | category | flops | bytes accessed | tf_op | source)
XLA Modules:
  0.0 94.2 jit_solution(1429785130690671392)
XLA Ops:
  0.0 1.2 %shard_map.128 = bf16[16,328,128]{2,1,0:T(8,128)(2,1)S(1)} custom-call(bf16[32,512]{1,0:T(8,128)(2,1)} %key_hbm.1, bf16[32,512]{1,0:T(8,128)(2,1)} %value_hbm.1, bf16[32,512]{1,0:T(8,128)(2,1)} %query_hbm.1, bf16[16,32]{1,0:T(8,128)(2,1)} %bitcast.24, bf16[16,32]{1,0:T(8,128)(2,1)} %bitcast.25, bf16[16,1024]{1,0:T(8,128)(2,1)} %mix_hbm.1), custom_call_target="tpu_custom_call" | custom-call | flops 67108864 | bytes 1048576 | tf_op jit(solution)/shard_map/pallas_call | solution.py:380
  1.2 0.0 copy-start
  1.2 0.0 copy-start.3
  1.3 24.6 %all_to_all.15.own_ref = bf16[16,328,128]{2,1,0:T(8,128)(2,1)S(1)} all-to-all(bf16[16,328,128]{2,1,0:T(8,128)(2,1)S(1)} %shard_map.128), channel_id=1, replica_groups={{30,0,2,4,6,8,10,12,14,16,18,20,22,24,26,28},{31,1,3,5,7,9,11,13,15,17,..., dimensions={0} | all-to-all | bytes 2686976 | tf_op jit(solution)/shard_map/all_to_all | solution.py:416
  25.8 2.1 %collective-permute-start = (bf16[16,328,128]{2,1,0:T(8,128)(2,1)S(1)}, bf16[16,328,128]{2,1,0:T(8,128)(2,1)S(1)}, u32[]{:S(2)}, u32[]{:S(2)}) collective-permute-start(bf16[16,328,128]{2,1,0:T(8,128)(2,1)S(1)} %all_to_all.15.own_ref), channel_id=1, source_target_pairs={{0,1},{1,0},{2,3},{3,2},{4,5},{5,4},{6,7},{7,6},{8,9},{9,8},{10,11... | collective-permute-start | bytes 4030472 | tf_op jit(solution)/shard_map/ppermute | solution.py:396
  27.9 2.3 %collective-permute-start.1 = (bf16[1,16,64,128]{3,2,1,0:T(8,128)(2,1)S(1)}, bf16[1,16,64,128]{3,2,1,0:T(8,128)(2,1)S(1)}, u32[]{:S(2)}, u32[]{:S(2)}) collective-permute-start(bf16[1,16,64,128]{3,2,1,0:T(8,128)(2,1)S(1)} %slice_bitcast_fusion.first_ref), channel_id=1, source_target_pairs={{0,8},{8,0},{16,24},{24,16},{1,9},{9,1},{17,25},{25,17},{2,10},{10... | collective-permute-start | bytes 786440 | tf_op jit(solution)/shard_map/ppermute | solution.py:420
  30.2 0.0 copy-done
  30.2 0.0 copy-done.3
  30.2 0.4 shard_map.127.normed_ref
  30.6 7.9 %collective-permute-done.1.second_ref = bf16[1,16,64,128]{3,2,1,0:T(8,128)(2,1)S(1)} collective-permute-done((bf16[1,16,64,128]{3,2,1,0:T(8,128)(2,1)S(1)}, bf16[1,16,64,128]{3,2,1,0:T(8,128)(2,1)S(1)}, u32[]{:S(2)}, u32[]{:S(2)}) %collective-permute-start.1) | collective-permute-done | bytes 262176 | tf_op jit(solution)/shard_map/ppermute | solution.py:420
  38.6 3.9 %collective-permute-start.2 = (bf16[2,16,64,128]{3,2,1,0:T(8,128)(2,1)S(1)}, bf16[2,16,64,128]{3,2,1,0:T(8,128)(2,1)S(1)}, u32[]{:S(2)}, u32[]{:S(2)}) collective-permute-start(bf16[2,16,64,128]{3,2,1,0:T(8,128)(2,1)S(1)} %shard_map.131.first_ref), channel_id=1, source_target_pairs={{0,24},{8,16},{16,8},{24,0},{1,25},{9,17},{17,9},{25,1},{2,26},{10... | collective-permute-start | bytes 1572872 | tf_op jit(solution)/shard_map/ppermute | solution.py:420
  42.5 0.0 collective-permute-done.other_ref
  42.5 0.0 copy-done.1
  42.5 0.0 copy-done.2
  42.5 0.0 copy-done.4
  42.6 0.0 copy-done.5
  42.6 2.8 %shard_map.129 = (bf16[16,40,128]{2,1,0:T(8,128)(2,1)}, bf16[128,1152]{1,0:T(8,128)(2,1)}) custom-call(bf16[2,128,512]{2,1,0:T(8,128)(2,1)S(1)} %shard_map.127.normed_ref, bf16[16,328,128]{2,1,0:T(8,128)(2,1)S(1)} %all_to_all.15.own_ref, bf16[16,328,128]{2,1,0:T(8,128)(2,1)S(1)} %collective-permute-done.other_ref, bf16[16,512]{1,0:T(8,128)(2,1)S(1)} %copy-done.1, ...), custom_call_target="tpu_custom_call" | custom-call | flops 1073741824 | bytes 1048576 | tf_op jit(solution)/shard_map/pallas_call | solution.py:380
  45.4 15.7 %all-to-all-start.1 = ((bf16[16,40,128]{2,1,0:T(8,128)(2,1)}), bf16[16,40,128]{2,1,0:T(8,128)(2,1)S(1)}, u32[]{:S(2)}, u32[]{:S(2)}) async-start(bf16[16,40,128]{2,1,0:T(8,128)(2,1)} %get-tuple-element.9), calls=%async_computation.1 | async-start | bytes 327680 | tf_op jit(solution)/shard_map/all_to_all | solution.py:446
  61.1 0.0 collective-permute-done.2.second_ref
  61.1 0.9 shard_map.132
  61.9 1.9 %collective-permute-start.3 = (bf16[4,16,32,128]{3,2,1,0:T(8,128)(2,1)S(1)}, bf16[4,16,32,128]{3,2,1,0:T(8,128)(2,1)S(1)}, u32[]{:S(2)}, u32[]{:S(2)}) collective-permute-start(bf16[4,16,32,128]{3,2,1,0:T(8,128)(2,1)S(1)} %get-tuple-element.10.own_ref), channel_id=1, source_target_pairs={{0,1},{1,0},{2,3},{3,2},{4,5},{5,4},{6,7},{7,6},{8,9},{9,8},{10,11... | collective-permute-start | bytes 1572872 | tf_op jit(solution)/shard_map/ppermute | solution.py:396
  63.8 2.4 %collective-permute-start.4 = (bf16[4,16,32,128]{3,2,1,0:T(8,128)(2,1)}, bf16[4,16,32,128]{3,2,1,0:T(8,128)(2,1)S(1)}, u32[]{:S(2)}, u32[]{:S(2)}) collective-permute-start(bf16[4,16,32,128]{3,2,1,0:T(8,128)(2,1)} %get-tuple-element.12.own_hbm), channel_id=1, source_target_pairs={{0,1},{1,0},{2,3},{3,2},{4,5},{5,4},{6,7},{7,6},{8,9},{9,8},{10,11... | collective-permute-start | bytes 1572872 | tf_op jit(solution)/shard_map/ppermute | solution.py:396
  66.3 6.4 %all-to-all-done.1.payload_ref = bf16[16,40,128]{2,1,0:T(8,128)(2,1)S(1)} async-done(((bf16[16,40,128]{2,1,0:T(8,128)(2,1)}), bf16[16,40,128]{2,1,0:T(8,128)(2,1)S(1)}, u32[]{:S(2)}, u32[]{:S(2)}) %all-to-all-start.1) | async-done | bytes 163872 | tf_op jit(solution)/shard_map/all_to_all | solution.py:446
  72.6 0.9 shard_map.130
  73.5 7.9 %all-to-all-start.2 = ((bf16[16,32,128]{2,1,0:T(8,128)(2,1)}), bf16[16,32,128]{2,1,0:T(8,128)(2,1)S(1)}, u32[]{:S(2)}, u32[]{:S(2)}) async-start(bf16[16,32,128]{2,1,0:T(8,128)(2,1)} %bitcast.6), calls=%async_computation.2 | async-start | bytes 262144 | tf_op jit(solution)/shard_map/all_to_all | solution.py:453
  81.5 0.1 tile.9
  81.6 0.1 tile.11.gain_ref
  81.6 0.0 collective-permute-done.3.other_ref
  81.6 3.4 %shard_map.133.parts_ref = f32[128,1536]{1,0:T(8,128)S(1)} custom-call(bf16[128,1024]{1,0:T(8,128)(2,1)} %bitcast.16, f32[1,1024]{1,0:T(1,128)S(1)} %bitcast.19, bf16[4,16,32,128]{3,2,1,0:T(8,128)(2,1)S(1)} %get-tuple-element.10.own_ref, bf16[4,16,32,128]{3,2,1,0:T(8,128)(2,1)S(1)} %collective-permute-done.3.other_ref, ...), custom_call_target="tpu_custom_call" | custom-call | flops 1073741824 | bytes 1048576 | tf_op jit(solution)/shard_map/pallas_call | solution.py:380
  85.1 0.0 collective-permute-done.4.other_ref
  85.1 6.4 %all-to-all-done.2 = bf16[16,32,128]{2,1,0:T(8,128)(2,1)S(1)} async-done(((bf16[16,32,128]{2,1,0:T(8,128)(2,1)}), bf16[16,32,128]{2,1,0:T(8,128)(2,1)S(1)}, u32[]{:S(2)}, u32[]{:S(2)}) %all-to-all-start.2) | async-done | bytes 131104 | tf_op jit(solution)/shard_map/all_to_all | solution.py:453
  91.5 2.7 %shard_map.134 = bf16[128,1024]{1,0:T(8,128)(2,1)} custom-call(bf16[512,128]{1,0:T(8,128)(2,1)S(1)} %bitcast.15, f32[128,1536]{1,0:T(8,128)S(1)} %shard_map.133.parts_ref, f32[2,256]{1,0:T(2,128)S(1)} %tile.11.gain_ref, bf16[4,16,32,128]{3,2,1,0:T(8,128)(2,1)} %get-tuple-element.12.own_hbm, bf16[4,16,32,128]{3,2,1,0:T(8,128)(2,1)S(1)} %collective-permute-done.4.other_ref), custom_call_target="tpu_custom_call" | custom-call | flops 1073741824 | bytes 1048576 | tf_op jit(solution)/shard_map/pallas_call | solution.py:380
  (9 shorter events, 0.1 us)
Async XLA Ops:
  1.2 29.0 %copy-start = (bf16[2,64,1024]{2,1,0:T(8,128)(2,1)S(1)}, bf16[2,64,1024]{2,1,0:T(8,128)(2,1)}, u32[]{:S(2)}) copy-start(bf16[2,64,1024]{2,1,0:T(8,128)(2,1)} %param.13) | copy-start | bytes 786436
  1.2 29.0 %copy-start.3 = (f32[1024]{0:T(1024)S(1)}, f32[1024]{0:T(1024)}, u32[]{:S(2)}) copy-start(f32[1024]{0:T(1024)} %param.14) | copy-start | bytes 12292
  25.8 16.7 %copy-start.1 = (bf16[16,512]{1,0:T(8,128)(2,1)S(1)}, bf16[16,512]{1,0:T(8,128)(2,1)}, u32[]{:S(2)}) copy-start(bf16[16,512]{1,0:T(8,128)(2,1)} %up_forward_ref.3) | copy-start | bytes 49156
  25.8 16.7 %copy-start.2 = (bf16[16,512]{1,0:T(8,128)(2,1)S(1)}, bf16[16,512]{1,0:T(8,128)(2,1)}, u32[]{:S(2)}) copy-start(bf16[16,512]{1,0:T(8,128)(2,1)} %up_backward_ref.3) | copy-start | bytes 49156
  25.8 16.7 %copy-start.4 = (f32[512]{0:T(512)S(1)}, f32[512]{0:T(512)}, u32[]{:S(2)}) copy-start(f32[512]{0:T(512)} %param.22) | copy-start | bytes 6148
  25.8 16.7 %copy-start.5 = (f32[512]{0:T(512)S(1)}, f32[512]{0:T(512)}, u32[]{:S(2)}) copy-start(f32[512]{0:T(512)} %param.23) | copy-start | bytes 6148
  25.8 16.7 %collective-permute-start = (bf16[16,328,128]{2,1,0:T(8,128)(2,1)S(1)}, bf16[16,328,128]{2,1,0:T(8,128)(2,1)S(1)}, u32[]{:S(2)}, u32[]{:S(2)}) collective-permute-start(bf16[16,328,128]{2,1,0:T(8,128)(2,1)S(1)} %all_to_all.15.own_ref), channel_id=1, source_target_pairs={{0,1},{1,0},{2,3},{3,2},{4,5},{5,4},{6,7},{7,6},{8,9},{9,8},{10,11... | collective-permute-start | bytes 4030472 | tf_op jit(solution)/shard_map/ppermute | solution.py:396
  27.9 10.6 %collective-permute-start.1 = (bf16[1,16,64,128]{3,2,1,0:T(8,128)(2,1)S(1)}, bf16[1,16,64,128]{3,2,1,0:T(8,128)(2,1)S(1)}, u32[]{:S(2)}, u32[]{:S(2)}) collective-permute-start(bf16[1,16,64,128]{3,2,1,0:T(8,128)(2,1)S(1)} %slice_bitcast_fusion.first_ref), channel_id=1, source_target_pairs={{0,8},{8,0},{16,24},{24,16},{1,9},{9,1},{17,25},{25,17},{2,10},{10... | collective-permute-start | bytes 786440 | tf_op jit(solution)/shard_map/ppermute | solution.py:420
  38.6 22.5 %collective-permute-start.2 = (bf16[2,16,64,128]{3,2,1,0:T(8,128)(2,1)S(1)}, bf16[2,16,64,128]{3,2,1,0:T(8,128)(2,1)S(1)}, u32[]{:S(2)}, u32[]{:S(2)}) collective-permute-start(bf16[2,16,64,128]{3,2,1,0:T(8,128)(2,1)S(1)} %shard_map.131.first_ref), channel_id=1, source_target_pairs={{0,24},{8,16},{16,8},{24,0},{1,25},{9,17},{17,9},{25,1},{2,26},{10... | collective-permute-start | bytes 1572872 | tf_op jit(solution)/shard_map/ppermute | solution.py:420
  45.4 36.1 %copy-start.6 = (f32[32]{0:T(128)S(1)}, f32[32]{0:T(128)}, u32[]{:S(2)}) copy-start(f32[32]{0:T(128)} %param.24) | copy-start | bytes 388
  45.4 27.2 %all-to-all-start.1 = ((bf16[16,40,128]{2,1,0:T(8,128)(2,1)}), bf16[16,40,128]{2,1,0:T(8,128)(2,1)S(1)}, u32[]{:S(2)}, u32[]{:S(2)}) async-start(bf16[16,40,128]{2,1,0:T(8,128)(2,1)} %get-tuple-element.9), calls=%async_computation.1 | async-start | bytes 327680 | tf_op jit(solution)/shard_map/all_to_all | solution.py:446
  61.9 19.7 %collective-permute-start.3 = (bf16[4,16,32,128]{3,2,1,0:T(8,128)(2,1)S(1)}, bf16[4,16,32,128]{3,2,1,0:T(8,128)(2,1)S(1)}, u32[]{:S(2)}, u32[]{:S(2)}) collective-permute-start(bf16[4,16,32,128]{3,2,1,0:T(8,128)(2,1)S(1)} %get-tuple-element.10.own_ref), channel_id=1, source_target_pairs={{0,1},{1,0},{2,3},{3,2},{4,5},{5,4},{6,7},{7,6},{8,9},{9,8},{10,11... | collective-permute-start | bytes 1572872 | tf_op jit(solution)/shard_map/ppermute | solution.py:396
  63.8 21.2 %collective-permute-start.4 = (bf16[4,16,32,128]{3,2,1,0:T(8,128)(2,1)}, bf16[4,16,32,128]{3,2,1,0:T(8,128)(2,1)S(1)}, u32[]{:S(2)}, u32[]{:S(2)}) collective-permute-start(bf16[4,16,32,128]{3,2,1,0:T(8,128)(2,1)} %get-tuple-element.12.own_hbm), channel_id=1, source_target_pairs={{0,1},{1,0},{2,3},{3,2},{4,5},{5,4},{6,7},{7,6},{8,9},{9,8},{10,11... | collective-permute-start | bytes 1572872 | tf_op jit(solution)/shard_map/ppermute | solution.py:396
  73.5 18.0 %all-to-all-start.2 = ((bf16[16,32,128]{2,1,0:T(8,128)(2,1)}), bf16[16,32,128]{2,1,0:T(8,128)(2,1)S(1)}, u32[]{:S(2)}, u32[]{:S(2)}) async-start(bf16[16,32,128]{2,1,0:T(8,128)(2,1)} %bitcast.6), calls=%async_computation.2 | async-start | bytes 262144 | tf_op jit(solution)/shard_map/all_to_all | solution.py:453

commit v14 on v13

--- a/solution.py
+++ b/solution.py
@@ -303,10 +303,8 @@
 
 
 def out_kernel(
-    states_ref, parts_ref, gain_ref, own_hbm, other_ref, out_ref, own_ref, sem
+    states_ref, parts_ref, gain_ref, own_ref, other_ref, out_ref
 ):
-    fetch = pltpu.make_async_copy(own_hbm, own_ref, sem)
-    fetch.start()
     spans = [slice(seq * BLOCK, (seq + 1) * BLOCK) for seq in range(2)]
     core = lax.axis_index("dp_2")
     row, col = grid_of((LANES, 8 * LANES))
@@ -352,7 +350,6 @@
     ]
     mine = jnp.where(core == 0, attended[0], attended[1])
     theirs = jnp.where(core == 0, attended[1], attended[0])
-    fetch.wait()
     for quarter in range(4):
         slot = slot_of(quarter, "dp_0")
 
@@ -425,7 +422,7 @@
         else:
             query, mix = call(
                 split_kernel,
-                (shape((4, 16, 32, LANES), bf16), pltpu.HBM((4, 16, 32, LANES), bf16)),
+                (pltpu.HBM((4, 16, 32, LANES), bf16), shape((4, 16, 32, LANES), bf16)),
                 [VMEM] * 2, 1 << 26,
                 mix, arrived,
             )
@@ -459,9 +456,8 @@
     )
     gain = jnp.tile(out_gain.reshape(2, 1, 16), (1, HEADS, 1)).reshape(2, 256)
     mixed = call(
-        out_kernel, shape((rows, width), bf16), [VMEM] * 3 + [hbm, VMEM], 1 << 30,
-        returned.reshape(WIDTH, LANES), parts, gain, in_hbm(mix), mix_other,
-        scratch=[pltpu.VMEM((4, 16, 32, LANES), bf16), pltpu.SemaphoreType.DMA],
+        out_kernel, shape((rows, width), bf16), [VMEM] * 5, 1 << 30,
+        returned.reshape(WIDTH, LANES), parts, gain, mix, mix_other,
     )
     return mixed.reshape(seqs, toks, width)
 

time: 94.8 us -> 93.9 us (level)
  local copies, waits for them, and re-layouts: 0.22 us -> 1.26 us
  waiting for transfers between devices: 20.7 us -> 19.7 us
    all_to_all x1, waiting for transfers between devices: 6.44 us -> 5.38 us  [body(): lax.all_to_all(states.reshape(HEADS, HEAD, LANES), 'sp', 0, 0, axis_index...]
    unnamed x14 -> x16, local copies, waits for them, and re-layouts: 0.03 us -> 1.07 us
where the time goes in v14:
time: 93.9 us; the launch traced here: 93.3 us
  starting transfers between devices  36.1 us (38%)
  blocking collectives  24.6 us (26%)
  waiting for transfers between devices  19.7 us (21%)
  Pallas kernels  11.5 us (12%)
  local copies, waits for them, and re-layouts  1.26 us (1%)
    all_to_all x1, blocking collectives, body(): own = lax.all_to_all(send, PLANE, 0, 0, axis_index_groups=[PLANE_GROUP])  24.6 us
    all_to_all x1, starting transfers between devices, body(): inbound = lax.all_to_all(payload, 'sp', 0, 0, axis_index_groups=[GROUP])  15.7 us
    pallas_call x8, Pallas kernels, call(): pl.pallas_call(kernel, out_shape=outs, in_specs=specs, out_specs=(VMEM,)...  11.5 us
    ppermute x2, waiting for transfers between devices, body(): arrived = lax.ppermute(mix, 'dp_0', [(i, i ^ flip) for i in range(4)])  7.93 us
    all_to_all x1, starting transfers between devices, body(): lax.all_to_all(states.reshape(HEADS, HEAD, LANES), 'sp', 0, 0, axis_index...  7.91 us
    ppermute x3, starting transfers between devices, swapped(): return lax.ppermute(x, 'dp_2', [(0, 1), (1, 0)])  6.37 us
    all_to_all x1, waiting for transfers between devices, body(): inbound = lax.all_to_all(payload, 'sp', 0, 0, axis_index_groups=[GROUP])  6.34 us
    ppermute x2, starting transfers between devices, body(): arrived = lax.ppermute(mix, 'dp_0', [(i, i ^ flip) for i in range(4)])  6.2 us
  transfers between devices with their start and end apart: 7, of which 3 were waited for; matrix products, arithmetic and copies ran while one was open for 0% of the time, Pallas kernels for 9%

profile of v14, /device:TPU:2, one launch (start us, length us, event | category | flops | bytes accessed | tf_op | source)
XLA Modules:
  0.0 93.3 jit_solution(18209017880652031161)
XLA Ops:
  0.0 1.2 %shard_map.128 = bf16[16,328,128]{2,1,0:T(8,128)(2,1)S(1)} custom-call(bf16[32,512]{1,0:T(8,128)(2,1)} %key_hbm.1, bf16[32,512]{1,0:T(8,128)(2,1)} %value_hbm.1, bf16[32,512]{1,0:T(8,128)(2,1)} %query_hbm.1, bf16[16,32]{1,0:T(8,128)(2,1)} %bitcast.24, bf16[16,32]{1,0:T(8,128)(2,1)} %bitcast.25, bf16[16,1024]{1,0:T(8,128)(2,1)} %mix_hbm.1), custom_call_target="tpu_custom_call" | custom-call | flops 67108864 | bytes 1048576 | tf_op jit(solution)/shard_map/pallas_call | solution.py:377
  1.2 0.0 copy-start.1
  1.2 0.0 copy-start.4
  1.3 24.6 %all_to_all.15.own_ref = bf16[16,328,128]{2,1,0:T(8,128)(2,1)S(1)} all-to-all(bf16[16,328,128]{2,1,0:T(8,128)(2,1)S(1)} %shard_map.128), channel_id=1, replica_groups={{30,0,2,4,6,8,10,12,14,16,18,20,22,24,26,28},{31,1,3,5,7,9,11,13,15,17,..., dimensions={0} | all-to-all | bytes 2686976 | tf_op jit(solution)/shard_map/all_to_all | solution.py:413
  25.8 2.1 %collective-permute-start = (bf16[16,328,128]{2,1,0:T(8,128)(2,1)S(1)}, bf16[16,328,128]{2,1,0:T(8,128)(2,1)S(1)}, u32[]{:S(2)}, u32[]{:S(2)}) collective-permute-start(bf16[16,328,128]{2,1,0:T(8,128)(2,1)S(1)} %all_to_all.15.own_ref), channel_id=1, source_target_pairs={{0,1},{1,0},{2,3},{3,2},{4,5},{5,4},{6,7},{7,6},{8,9},{9,8},{10,11... | collective-permute-start | bytes 4030472 | tf_op jit(solution)/shard_map/ppermute | solution.py:393
  27.9 2.3 %collective-permute-start.1 = (bf16[1,16,64,128]{3,2,1,0:T(8,128)(2,1)S(1)}, bf16[1,16,64,128]{3,2,1,0:T(8,128)(2,1)S(1)}, u32[]{:S(2)}, u32[]{:S(2)}) collective-permute-start(bf16[1,16,64,128]{3,2,1,0:T(8,128)(2,1)S(1)} %slice_bitcast_fusion.first_ref), channel_id=1, source_target_pairs={{0,8},{8,0},{16,24},{24,16},{1,9},{9,1},{17,25},{25,17},{2,10},{10... | collective-permute-start | bytes 786440 | tf_op jit(solution)/shard_map/ppermute | solution.py:417
  30.2 0.0 copy-done.1
  30.2 0.4 shard_map.127.normed_ref
  30.6 7.9 %collective-permute-done.1.second_ref = bf16[1,16,64,128]{3,2,1,0:T(8,128)(2,1)S(1)} collective-permute-done((bf16[1,16,64,128]{3,2,1,0:T(8,128)(2,1)S(1)}, bf16[1,16,64,128]{3,2,1,0:T(8,128)(2,1)S(1)}, u32[]{:S(2)}, u32[]{:S(2)}) %collective-permute-start.1) | collective-permute-done | bytes 262176 | tf_op jit(solution)/shard_map/ppermute | solution.py:417
  38.6 3.9 %collective-permute-start.2 = (bf16[2,16,64,128]{3,2,1,0:T(8,128)(2,1)S(1)}, bf16[2,16,64,128]{3,2,1,0:T(8,128)(2,1)S(1)}, u32[]{:S(2)}, u32[]{:S(2)}) collective-permute-start(bf16[2,16,64,128]{3,2,1,0:T(8,128)(2,1)S(1)} %shard_map.131.first_ref), channel_id=1, source_target_pairs={{0,24},{8,16},{16,8},{24,0},{1,25},{9,17},{17,9},{25,1},{2,26},{10... | collective-permute-start | bytes 1572872 | tf_op jit(solution)/shard_map/ppermute | solution.py:417
  42.5 0.0 collective-permute-done.other_ref
  42.5 0.0 copy-done.2
  42.5 0.0 copy-done.3
  42.5 0.0 copy-done.5
  42.6 0.0 copy-done.6
  42.6 2.8 %shard_map.129 = (bf16[16,40,128]{2,1,0:T(8,128)(2,1)}, bf16[128,1152]{1,0:T(8,128)(2,1)}) custom-call(bf16[2,128,512]{2,1,0:T(8,128)(2,1)S(1)} %shard_map.127.normed_ref, bf16[16,328,128]{2,1,0:T(8,128)(2,1)S(1)} %all_to_all.15.own_ref, bf16[16,328,128]{2,1,0:T(8,128)(2,1)S(1)} %collective-permute-done.other_ref, bf16[16,512]{1,0:T(8,128)(2,1)S(1)} %copy-done.2, ...), custom_call_target="tpu_custom_call" | custom-call | flops 1073741824 | bytes 1048576 | tf_op jit(solution)/shard_map/pallas_call | solution.py:377
  45.4 15.7 %all-to-all-start.1 = ((bf16[16,40,128]{2,1,0:T(8,128)(2,1)}), bf16[16,40,128]{2,1,0:T(8,128)(2,1)S(1)}, u32[]{:S(2)}, u32[]{:S(2)}) async-start(bf16[16,40,128]{2,1,0:T(8,128)(2,1)} %get-tuple-element.9), calls=%async_computation.1 | async-start | bytes 327680 | tf_op jit(solution)/shard_map/all_to_all | solution.py:443
  61.1 0.0 collective-permute-done.2.second_ref
  61.1 0.9 shard_map.132
  61.9 1.9 %collective-permute-start.3 = (bf16[4,16,32,128]{3,2,1,0:T(8,128)(2,1)}, bf16[4,16,32,128]{3,2,1,0:T(8,128)(2,1)S(1)}, u32[]{:S(2)}, u32[]{:S(2)}) collective-permute-start(bf16[4,16,32,128]{3,2,1,0:T(8,128)(2,1)} %get-tuple-element.10.own_ref), channel_id=1, source_target_pairs={{0,1},{1,0},{2,3},{3,2},{4,5},{5,4},{6,7},{7,6},{8,9},{9,8},{10,11... | collective-permute-start | bytes 1572872 | tf_op jit(solution)/shard_map/ppermute | solution.py:393
  63.9 2.4 %collective-permute-start.4 = (bf16[4,16,32,128]{3,2,1,0:T(8,128)(2,1)S(1)}, bf16[4,16,32,128]{3,2,1,0:T(8,128)(2,1)S(1)}, u32[]{:S(2)}, u32[]{:S(2)}) collective-permute-start(bf16[4,16,32,128]{3,2,1,0:T(8,128)(2,1)S(1)} %get-tuple-element.12.own_ref), channel_id=1, source_target_pairs={{0,1},{1,0},{2,3},{3,2},{4,5},{5,4},{6,7},{7,6},{8,9},{9,8},{10,11... | collective-permute-start | bytes 1572872 | tf_op jit(solution)/shard_map/ppermute | solution.py:393
  66.3 6.3 %all-to-all-done.1.payload_ref = bf16[16,40,128]{2,1,0:T(8,128)(2,1)S(1)} async-done(((bf16[16,40,128]{2,1,0:T(8,128)(2,1)}), bf16[16,40,128]{2,1,0:T(8,128)(2,1)S(1)}, u32[]{:S(2)}, u32[]{:S(2)}) %all-to-all-start.1) | async-done | bytes 163872 | tf_op jit(solution)/shard_map/all_to_all | solution.py:443
  72.6 0.9 shard_map.130
  73.5 7.9 %all-to-all-start.2 = ((bf16[16,32,128]{2,1,0:T(8,128)(2,1)}), bf16[16,32,128]{2,1,0:T(8,128)(2,1)S(1)}, u32[]{:S(2)}, u32[]{:S(2)}) async-start(bf16[16,32,128]{2,1,0:T(8,128)(2,1)} %bitcast.6), calls=%async_computation.2 | async-start | bytes 262144 | tf_op jit(solution)/shard_map/all_to_all | solution.py:450
  81.5 0.1 tile.9
  81.6 0.1 tile.11.gain_ref
  81.6 0.0 collective-permute-done.3.other_ref
  81.7 1.0 %copy-done = bf16[4,16,32,128]{3,2,1,0:T(8,128)(2,1)S(1)} copy-done((bf16[4,16,32,128]{3,2,1,0:T(8,128)(2,1)S(1)}, bf16[4,16,32,128]{3,2,1,0:T(8,128)(2,1)}, u32[]{:S(2)}) %copy-start) | copy-done | bytes 524312
  82.7 3.4 %shard_map.133.parts_ref = f32[128,1536]{1,0:T(8,128)S(1)} custom-call(bf16[128,1024]{1,0:T(8,128)(2,1)} %bitcast.16, f32[1,1024]{1,0:T(1,128)S(1)} %bitcast.19, bf16[4,16,32,128]{3,2,1,0:T(8,128)(2,1)S(1)} %copy-done, bf16[4,16,32,128]{3,2,1,0:T(8,128)(2,1)S(1)} %collective-permute-done.3.other_ref, bf16[128,1152]{1,0:T(8,128)(2,1)} %get-tuple-element.11.rounded_ref, ...), custom_call_target="tpu_custom_call" | custom-call | flops 1073741824 | bytes 1048576 | tf_op jit(solution)/shard_map/pallas_call | solution.py:377
  86.1 0.0 collective-permute-done.4.other_ref
  86.1 5.4 %all-to-all-done.2 = bf16[16,32,128]{2,1,0:T(8,128)(2,1)S(1)} async-done(((bf16[16,32,128]{2,1,0:T(8,128)(2,1)}), bf16[16,32,128]{2,1,0:T(8,128)(2,1)S(1)}, u32[]{:S(2)}, u32[]{:S(2)}) %all-to-all-start.2) | async-done | bytes 131104 | tf_op jit(solution)/shard_map/all_to_all | solution.py:450
  91.5 1.8 %shard_map.134 = bf16[128,1024]{1,0:T(8,128)(2,1)} custom-call(bf16[512,128]{1,0:T(8,128)(2,1)S(1)} %bitcast.15, f32[128,1536]{1,0:T(8,128)S(1)} %shard_map.133.parts_ref, f32[2,256]{1,0:T(2,128)S(1)} %tile.11.gain_ref, bf16[4,16,32,128]{3,2,1,0:T(8,128)(2,1)S(1)} %get-tuple-element.12.own_ref, bf16[4,16,32,128]{3,2,1,0:T(8,128)(2,1)S(1)} %collective-permute-done.4.other_ref), custom_call_target="tpu_custom_call" | custom-call | flops 1073741824 | bytes 1048576 | tf_op jit(solution)/shard_map/pallas_call | solution.py:377
  (11 shorter events, 0.1 us)
Async XLA Ops:
  1.2 29.0 %copy-start.1 = (bf16[2,64,1024]{2,1,0:T(8,128)(2,1)S(1)}, bf16[2,64,1024]{2,1,0:T(8,128)(2,1)}, u32[]{:S(2)}) copy-start(bf16[2,64,1024]{2,1,0:T(8,128)(2,1)} %param.13) | copy-start | bytes 786436
  1.2 29.0 %copy-start.4 = (f32[1024]{0:T(1024)S(1)}, f32[1024]{0:T(1024)}, u32[]{:S(2)}) copy-start(f32[1024]{0:T(1024)} %param.14) | copy-start | bytes 12292
  25.8 16.7 %copy-start.2 = (bf16[16,512]{1,0:T(8,128)(2,1)S(1)}, bf16[16,512]{1,0:T(8,128)(2,1)}, u32[]{:S(2)}) copy-start(bf16[16,512]{1,0:T(8,128)(2,1)} %up_forward_ref.3) | copy-start | bytes 49156
  25.8 16.7 %copy-start.3 = (bf16[16,512]{1,0:T(8,128)(2,1)S(1)}, bf16[16,512]{1,0:T(8,128)(2,1)}, u32[]{:S(2)}) copy-start(bf16[16,512]{1,0:T(8,128)(2,1)} %up_backward_ref.3) | copy-start | bytes 49156
  25.8 16.7 %copy-start.5 = (f32[512]{0:T(512)S(1)}, f32[512]{0:T(512)}, u32[]{:S(2)}) copy-start(f32[512]{0:T(512)} %param.22) | copy-start | bytes 6148
  25.8 16.7 %copy-start.6 = (f32[512]{0:T(512)S(1)}, f32[512]{0:T(512)}, u32[]{:S(2)}) copy-start(f32[512]{0:T(512)} %param.23) | copy-start | bytes 6148
  25.8 16.7 %collective-permute-start = (bf16[16,328,128]{2,1,0:T(8,128)(2,1)S(1)}, bf16[16,328,128]{2,1,0:T(8,128)(2,1)S(1)}, u32[]{:S(2)}, u32[]{:S(2)}) collective-permute-start(bf16[16,328,128]{2,1,0:T(8,128)(2,1)S(1)} %all_to_all.15.own_ref), channel_id=1, source_target_pairs={{0,1},{1,0},{2,3},{3,2},{4,5},{5,4},{6,7},{7,6},{8,9},{9,8},{10,11... | collective-permute-start | bytes 4030472 | tf_op jit(solution)/shard_map/ppermute | solution.py:393
  27.9 10.6 %collective-permute-start.1 = (bf16[1,16,64,128]{3,2,1,0:T(8,128)(2,1)S(1)}, bf16[1,16,64,128]{3,2,1,0:T(8,128)(2,1)S(1)}, u32[]{:S(2)}, u32[]{:S(2)}) collective-permute-start(bf16[1,16,64,128]{3,2,1,0:T(8,128)(2,1)S(1)} %slice_bitcast_fusion.first_ref), channel_id=1, source_target_pairs={{0,8},{8,0},{16,24},{24,16},{1,9},{9,1},{17,25},{25,17},{2,10},{10... | collective-permute-start | bytes 786440 | tf_op jit(solution)/shard_map/ppermute | solution.py:417
  38.6 22.5 %collective-permute-start.2 = (bf16[2,16,64,128]{3,2,1,0:T(8,128)(2,1)S(1)}, bf16[2,16,64,128]{3,2,1,0:T(8,128)(2,1)S(1)}, u32[]{:S(2)}, u32[]{:S(2)}) collective-permute-start(bf16[2,16,64,128]{3,2,1,0:T(8,128)(2,1)S(1)} %shard_map.131.first_ref), channel_id=1, source_target_pairs={{0,24},{8,16},{16,8},{24,0},{1,25},{9,17},{17,9},{25,1},{2,26},{10... | collective-permute-start | bytes 1572872 | tf_op jit(solution)/shard_map/ppermute | solution.py:417
  45.4 36.1 %copy-start.7 = (f32[32]{0:T(128)S(1)}, f32[32]{0:T(128)}, u32[]{:S(2)}) copy-start(f32[32]{0:T(128)} %param.24) | copy-start | bytes 388
  45.4 27.2 %all-to-all-start.1 = ((bf16[16,40,128]{2,1,0:T(8,128)(2,1)}), bf16[16,40,128]{2,1,0:T(8,128)(2,1)S(1)}, u32[]{:S(2)}, u32[]{:S(2)}) async-start(bf16[16,40,128]{2,1,0:T(8,128)(2,1)} %get-tuple-element.9), calls=%async_computation.1 | async-start | bytes 327680 | tf_op jit(solution)/shard_map/all_to_all | solution.py:443
  61.9 19.7 %collective-permute-start.3 = (bf16[4,16,32,128]{3,2,1,0:T(8,128)(2,1)}, bf16[4,16,32,128]{3,2,1,0:T(8,128)(2,1)S(1)}, u32[]{:S(2)}, u32[]{:S(2)}) collective-permute-start(bf16[4,16,32,128]{3,2,1,0:T(8,128)(2,1)} %get-tuple-element.10.own_ref), channel_id=1, source_target_pairs={{0,1},{1,0},{2,3},{3,2},{4,5},{5,4},{6,7},{7,6},{8,9},{9,8},{10,11... | collective-permute-start | bytes 1572872 | tf_op jit(solution)/shard_map/ppermute | solution.py:393
  63.9 22.3 %collective-permute-start.4 = (bf16[4,16,32,128]{3,2,1,0:T(8,128)(2,1)S(1)}, bf16[4,16,32,128]{3,2,1,0:T(8,128)(2,1)S(1)}, u32[]{:S(2)}, u32[]{:S(2)}) collective-permute-start(bf16[4,16,32,128]{3,2,1,0:T(8,128)(2,1)S(1)} %get-tuple-element.12.own_ref), channel_id=1, source_target_pairs={{0,1},{1,0},{2,3},{3,2},{4,5},{5,4},{6,7},{7,6},{8,9},{9,8},{10,11... | collective-permute-start | bytes 1572872 | tf_op jit(solution)/shard_map/ppermute | solution.py:393
  73.5 18.0 %all-to-all-start.2 = ((bf16[16,32,128]{2,1,0:T(8,128)(2,1)}), bf16[16,32,128]{2,1,0:T(8,128)(2,1)S(1)}, u32[]{:S(2)}, u32[]{:S(2)}) async-start(bf16[16,32,128]{2,1,0:T(8,128)(2,1)} %bitcast.6), calls=%async_computation.2 | async-start | bytes 262144 | tf_op jit(solution)/shard_map/all_to_all | solution.py:450
  81.6 1.0 %copy-start = (bf16[4,16,32,128]{3,2,1,0:T(8,128)(2,1)S(1)}, bf16[4,16,32,128]{3,2,1,0:T(8,128)(2,1)}, u32[]{:S(2)}) copy-start(bf16[4,16,32,128]{3,2,1,0:T(8,128)(2,1)} %get-tuple-element.10.own_ref) | copy-start | bytes 1572868

commit v15 on v14

--- a/solution.py
+++ b/solution.py
@@ -18,6 +18,7 @@
 SENT = COLUMNS + 32 + 32 + 8
 EPS = 1e-06
 GROUP = [(z + 12) % 16 for z in range(16)]
+RETURN_GROUP = [(z + 14) % 16 for z in range(16)]
 PLANE_GROUP = [(i + 15) % 16 for i in range(16)]
 f32 = jnp.float32
 bf16 = jnp.bfloat16
@@ -136,7 +137,8 @@
 
 def block_kernel(
     normed_ref, own_ref, other_ref, up_forward_ref, up_backward_ref,
-    bias_forward_ref, bias_backward_ref, payload_ref, rounded_ref,
+    bias_forward_ref, bias_backward_ref, payload_ref, rounded_hbm,
+    rounded_ref, sem,
 ):
     core = lax.axis_index("dp_2")
 
@@ -159,6 +161,8 @@
     pieces.append(jnp.zeros((2 * BLOCK, LANES - 32), f32))
     rounded = jnp.concatenate(pieces, axis=1).astype(bf16)
     rounded_ref[...] = rounded
+    send = pltpu.make_async_copy(rounded_ref, rounded_hbm, sem)
+    send.start()
     values = rounded[:, WIDTH : 2 * WIDTH]
     parts = rates_of(
         rounded[:, 2 * WIDTH :], up_forward_ref, up_backward_ref, bias_forward_ref, bias_backward_ref
@@ -206,6 +210,7 @@
                 parts.append(jnp.where(diagonal, state, 0.0).astype(bf16))
         folded = dot(jnp.concatenate(parts, axis=1), fold).astype(bf16)
         payload_ref[4 * group : 4 * group + 4, :HEAD, :] = folded.reshape(4, HEAD, LANES)
+    send.wait()
 
 
 def scan_kernel(payload_ref, out_ref):
@@ -237,7 +242,8 @@
         behind[i] = carried
         carried = at(decay, i) * carried + at(states, i)
     for i in range(HEADS):
-        out_ref[i * HEAD : (i + 1) * HEAD, :] = jnp.where(
+        place = RETURN_GROUP.index(GROUP[i])
+        out_ref[place * HEAD : (place + 1) * HEAD, :] = jnp.where(
             lane < LANES // 2, ahead[i], behind[i]
         ).astype(bf16)
 
@@ -312,10 +318,11 @@
     widen = as_bf16(row == source)
     row, col = grid_of((256, 8 * LANES))
     diagonal = (row // HEAD) == ((col % LANES) // 16)
-    full = [
-        jnp.where(diagonal, dot(states_ref[g * 256 : (g + 1) * 256, :], widen), 0.0).astype(bf16)
-        for g in range(2)
-    ]
+    by_group = (
+        jnp.concatenate([states_ref[14 * HEAD :, :], states_ref[: 6 * HEAD, :]], axis=0),
+        states_ref[6 * HEAD : 14 * HEAD, :],
+    )
+    full = [jnp.where(diagonal, dot(rows, widen), 0.0).astype(bf16) for rows in by_group]
     totals = [[], []]
     for seq, span in enumerate(spans):
         sides = [[], []]
@@ -372,13 +379,13 @@
 VMEM = pl.BlockSpec(memory_space=pltpu.VMEM)
 
 
-def call(kernel, outs, specs, cycles, *args, scratch=()):
+def call(kernel, outs, specs, cycles, *args, scratch=(), out_specs=None):
     many = isinstance(outs, tuple)
     return pl.pallas_call(
         kernel,
         out_shape=outs,
         in_specs=specs,
-        out_specs=(VMEM,) * len(outs) if many else VMEM,
+        out_specs=out_specs or ((VMEM,) * len(outs) if many else VMEM),
         scratch_shapes=scratch,
         cost_estimate=pl.CostEstimate(flops=cycles, bytes_accessed=1 << 20, transcendentals=0),
         compiler_params=pltpu.CompilerParams(vmem_limit_bytes=16 << 20),
@@ -434,11 +441,9 @@
         up_forward, up_backward, bias_forward.reshape(1, WIDTH), bias_backward.reshape(1, WIDTH)
     )
     payload, rounded = call(
-        block_kernel,
-        (
-            shape((HEADS, 40, LANES), bf16), pltpu.HBM((rows, ALL), bf16),
-        ),
-        [VMEM] * 7, 1 << 30, normed, own, other, *decays,
+        block_kernel, (shape((HEADS, 40, LANES), bf16), pltpu.HBM((rows, ALL), bf16)),
+        [VMEM] * 7, 1 << 30, normed, own, other, *decays, out_specs=(VMEM, hbm),
+        scratch=[pltpu.VMEM((rows, ALL), bf16), pltpu.SemaphoreType.DMA],
     )
     inbound = lax.all_to_all(payload, "sp", 0, 0, axis_index_groups=[GROUP])
     query_other = swapped(query)
@@ -448,11 +453,11 @@
         inbound,
     )
     returned = lax.all_to_all(
-        states.reshape(HEADS, HEAD, LANES), "sp", 0, 0, axis_index_groups=[GROUP]
+        states.reshape(HEADS, HEAD, LANES), "sp", 0, 0, axis_index_groups=[RETURN_GROUP]
     )
     parts = call(
         query_kernel, shape((rows, 3 * WIDTH), f32), [VMEM] * 9, 1 << 30,
-        in_hbm(tokens_flat), gain_flat, query, query_other, in_hbm(rounded), *decays,
+        in_hbm(tokens_flat), gain_flat, in_hbm(query), query_other, in_hbm(rounded), *decays,
     )
     gain = jnp.tile(out_gain.reshape(2, 1, 16), (1, HEADS, 1)).reshape(2, 256)
     mixed = call(

time: 93.9 us -> 94.4 us (level)
  waiting for transfers between devices: 19.7 us -> 21.2 us
  local copies, waits for them, and re-layouts: 1.26 us -> 0.22 us
    all_to_all x1, waiting for transfers between devices: 5.38 us -> 6.93 us  [body(): lax.all_to_all(states.reshape(HEADS, HEAD, LANES), 'sp', 0, 0, axis_index...]
    unnamed x16 -> x14, local copies, waits for them, and re-layouts: 1.07 us -> 0.03 us
where the time goes in v15:
time: 94.4 us; the launch traced here: 93.9 us
  starting transfers between devices  36 us (38%)
  blocking collectives  24.6 us (26%)
  waiting for transfers between devices  21.2 us (22%)
  Pallas kernels  11.6 us (12%)
    all_to_all x1, blocking collectives, body(): own = lax.all_to_all(send, PLANE, 0, 0, axis_index_groups=[PLANE_GROUP])  24.6 us
    all_to_all x1, starting transfers between devices, body(): inbound = lax.all_to_all(payload, 'sp', 0, 0, axis_index_groups=[GROUP])  15.5 us
    pallas_call x8, Pallas kernels, call(): pl.pallas_call(kernel, out_shape=outs, in_specs=specs, out_specs=out_spec...  11.6 us
    ppermute x2, waiting for transfers between devices, body(): arrived = lax.ppermute(mix, 'dp_0', [(i, i ^ flip) for i in range(4)])  7.93 us
    all_to_all x1, starting transfers between devices, body(): lax.all_to_all(states.reshape(HEADS, HEAD, LANES), 'sp', 0, 0, axis_index...  7.92 us
    all_to_all x1, waiting for transfers between devices, body(): lax.all_to_all(states.reshape(HEADS, HEAD, LANES), 'sp', 0, 0, axis_index...  6.93 us
    ppermute x3, starting transfers between devices, swapped(): return lax.ppermute(x, 'dp_2', [(0, 1), (1, 0)])  6.37 us
    all_to_all x1, waiting for transfers between devices, body(): inbound = lax.all_to_all(payload, 'sp', 0, 0, axis_index_groups=[GROUP])  6.36 us
  transfers between devices with their start and end apart: 7, of which 3 were waited for; matrix products, arithmetic and copies ran while one was open for 0% of the time, Pallas kernels for 9%

profile of v15, /device:TPU:2, one launch (start us, length us, event | category | flops | bytes accessed | tf_op | source)
XLA Modules:
  0.0 93.9 jit_solution(7125264600548844512)
XLA Ops:
  0.0 1.2 %shard_map.128 = bf16[16,328,128]{2,1,0:T(8,128)(2,1)S(1)} custom-call(bf16[32,512]{1,0:T(8,128)(2,1)} %key_hbm.1, bf16[32,512]{1,0:T(8,128)(2,1)} %value_hbm.1, bf16[32,512]{1,0:T(8,128)(2,1)} %query_hbm.1, bf16[16,32]{1,0:T(8,128)(2,1)} %bitcast.24, bf16[16,32]{1,0:T(8,128)(2,1)} %bitcast.25, bf16[16,1024]{1,0:T(8,128)(2,1)} %mix_hbm.1), custom_call_target="tpu_custom_call" | custom-call | flops 67108864 | bytes 1048576 | tf_op jit(solution)/shard_map/pallas_call | solution.py:384
  1.2 0.0 copy-start
  1.2 0.0 copy-start.3
  1.3 24.6 %all_to_all.15.own_ref = bf16[16,328,128]{2,1,0:T(8,128)(2,1)S(1)} all-to-all(bf16[16,328,128]{2,1,0:T(8,128)(2,1)S(1)} %shard_map.128), channel_id=1, replica_groups={{30,0,2,4,6,8,10,12,14,16,18,20,22,24,26,28},{31,1,3,5,7,9,11,13,15,17,..., dimensions={0} | all-to-all | bytes 2686976 | tf_op jit(solution)/shard_map/all_to_all | solution.py:420
  25.8 2.1 %collective-permute-start = (bf16[16,328,128]{2,1,0:T(8,128)(2,1)S(1)}, bf16[16,328,128]{2,1,0:T(8,128)(2,1)S(1)}, u32[]{:S(2)}, u32[]{:S(2)}) collective-permute-start(bf16[16,328,128]{2,1,0:T(8,128)(2,1)S(1)} %all_to_all.15.own_ref), channel_id=1, source_target_pairs={{0,1},{1,0},{2,3},{3,2},{4,5},{5,4},{6,7},{7,6},{8,9},{9,8},{10,11... | collective-permute-start | bytes 4030472 | tf_op jit(solution)/shard_map/ppermute | solution.py:400
  27.9 2.3 %collective-permute-start.1 = (bf16[1,16,64,128]{3,2,1,0:T(8,128)(2,1)S(1)}, bf16[1,16,64,128]{3,2,1,0:T(8,128)(2,1)S(1)}, u32[]{:S(2)}, u32[]{:S(2)}) collective-permute-start(bf16[1,16,64,128]{3,2,1,0:T(8,128)(2,1)S(1)} %slice_bitcast_fusion.first_ref), channel_id=1, source_target_pairs={{0,8},{8,0},{16,24},{24,16},{1,9},{9,1},{17,25},{25,17},{2,10},{10... | collective-permute-start | bytes 786440 | tf_op jit(solution)/shard_map/ppermute | solution.py:424
  30.2 0.4 shard_map.127.normed_ref
  30.6 7.9 %collective-permute-done.1.second_ref = bf16[1,16,64,128]{3,2,1,0:T(8,128)(2,1)S(1)} collective-permute-done((bf16[1,16,64,128]{3,2,1,0:T(8,128)(2,1)S(1)}, bf16[1,16,64,128]{3,2,1,0:T(8,128)(2,1)S(1)}, u32[]{:S(2)}, u32[]{:S(2)}) %collective-permute-start.1) | collective-permute-done | bytes 262176 | tf_op jit(solution)/shard_map/ppermute | solution.py:424
  38.6 3.9 %collective-permute-start.2 = (bf16[2,16,64,128]{3,2,1,0:T(8,128)(2,1)S(1)}, bf16[2,16,64,128]{3,2,1,0:T(8,128)(2,1)S(1)}, u32[]{:S(2)}, u32[]{:S(2)}) collective-permute-start(bf16[2,16,64,128]{3,2,1,0:T(8,128)(2,1)S(1)} %shard_map.131.first_ref), channel_id=1, source_target_pairs={{0,24},{8,16},{16,8},{24,0},{1,25},{9,17},{17,9},{25,1},{2,26},{10... | collective-permute-start | bytes 1572872 | tf_op jit(solution)/shard_map/ppermute | solution.py:424
  42.5 0.0 collective-permute-done.other_ref
  42.5 0.0 copy-done.1
  42.5 0.0 copy-done.2
  42.5 0.0 copy-done.4
  42.6 0.0 copy-done.5
  42.6 2.8 %shard_map.129 = (bf16[16,40,128]{2,1,0:T(8,128)(2,1)}, bf16[128,1152]{1,0:T(8,128)(2,1)}) custom-call(bf16[2,128,512]{2,1,0:T(8,128)(2,1)S(1)} %shard_map.127.normed_ref, bf16[16,328,128]{2,1,0:T(8,128)(2,1)S(1)} %all_to_all.15.own_ref, bf16[16,328,128]{2,1,0:T(8,128)(2,1)S(1)} %collective-permute-done.other_ref, bf16[16,512]{1,0:T(8,128)(2,1)S(1)} %copy-done.1, ...), custom_call_target="tpu_custom_call" | custom-call | flops 1073741824 | bytes 1048576 | tf_op jit(solution)/shard_map/pallas_call | solution.py:384
  45.4 0.0 copy-start.6
  45.4 15.5 %all-to-all-start.1 = ((bf16[16,40,128]{2,1,0:T(8,128)(2,1)}), bf16[16,40,128]{2,1,0:T(8,128)(2,1)S(1)}, u32[]{:S(2)}, u32[]{:S(2)}) async-start(bf16[16,40,128]{2,1,0:T(8,128)(2,1)} %get-tuple-element.9), calls=%async_computation.1 | async-start | bytes 327680 | tf_op jit(solution)/shard_map/all_to_all | solution.py:448
  61.0 0.0 collective-permute-done.2.second_ref
  61.0 0.9 shard_map.132
  61.8 1.9 %collective-permute-start.3 = (bf16[4,16,32,128]{3,2,1,0:T(8,128)(2,1)}, bf16[4,16,32,128]{3,2,1,0:T(8,128)(2,1)S(1)}, u32[]{:S(2)}, u32[]{:S(2)}) collective-permute-start(bf16[4,16,32,128]{3,2,1,0:T(8,128)(2,1)} %get-tuple-element.10.own_ref), channel_id=1, source_target_pairs={{0,1},{1,0},{2,3},{3,2},{4,5},{5,4},{6,7},{7,6},{8,9},{9,8},{10,11... | collective-permute-start | bytes 1572872 | tf_op jit(solution)/shard_map/ppermute | solution.py:400
  63.8 2.4 %collective-permute-start.4 = (bf16[4,16,32,128]{3,2,1,0:T(8,128)(2,1)S(1)}, bf16[4,16,32,128]{3,2,1,0:T(8,128)(2,1)S(1)}, u32[]{:S(2)}, u32[]{:S(2)}) collective-permute-start(bf16[4,16,32,128]{3,2,1,0:T(8,128)(2,1)S(1)} %get-tuple-element.12.own_ref), channel_id=1, source_target_pairs={{0,1},{1,0},{2,3},{3,2},{4,5},{5,4},{6,7},{7,6},{8,9},{9,8},{10,11... | collective-permute-start | bytes 1572872 | tf_op jit(solution)/shard_map/ppermute | solution.py:400
  66.2 6.4 %all-to-all-done.1.payload_ref = bf16[16,40,128]{2,1,0:T(8,128)(2,1)S(1)} async-done(((bf16[16,40,128]{2,1,0:T(8,128)(2,1)}), bf16[16,40,128]{2,1,0:T(8,128)(2,1)S(1)}, u32[]{:S(2)}, u32[]{:S(2)}) %all-to-all-start.1) | async-done | bytes 163872 | tf_op jit(solution)/shard_map/all_to_all | solution.py:448
  72.5 0.9 shard_map.130
  73.4 7.9 %all-to-all-start.2 = ((bf16[16,32,128]{2,1,0:T(8,128)(2,1)}), bf16[16,32,128]{2,1,0:T(8,128)(2,1)S(1)}, u32[]{:S(2)}, u32[]{:S(2)}) async-start(bf16[16,32,128]{2,1,0:T(8,128)(2,1)} %bitcast.6), calls=%async_computation.2 | async-start | bytes 262144 | tf_op jit(solution)/shard_map/all_to_all | solution.py:455
  81.4 0.0 copy-done.6
  81.4 0.1 tile.9
  81.5 0.1 tile.11.gain_ref
  81.5 0.0 collective-permute-done.3.other_ref
  81.5 3.6 %shard_map.133.parts_ref = f32[128,1536]{1,0:T(8,128)S(1)} custom-call(bf16[128,1024]{1,0:T(8,128)(2,1)} %bitcast.16, f32[1,1024]{1,0:T(1,128)S(1)} %bitcast.19, bf16[4,16,32,128]{3,2,1,0:T(8,128)(2,1)} %get-tuple-element.10.own_ref, bf16[4,16,32,128]{3,2,1,0:T(8,128)(2,1)S(1)} %collective-permute-done.3.other_ref, ...), custom_call_target="tpu_custom_call" | custom-call | flops 1073741824 | bytes 1048576 | tf_op jit(solution)/shard_map/pallas_call | solution.py:384
  85.1 0.0 collective-permute-done.4.other_ref
  85.1 6.9 %all-to-all-done.2 = bf16[16,32,128]{2,1,0:T(8,128)(2,1)S(1)} async-done(((bf16[16,32,128]{2,1,0:T(8,128)(2,1)}), bf16[16,32,128]{2,1,0:T(8,128)(2,1)S(1)}, u32[]{:S(2)}, u32[]{:S(2)}) %all-to-all-start.2) | async-done | bytes 131104 | tf_op jit(solution)/shard_map/all_to_all | solution.py:455
  92.1 1.8 %shard_map.134 = bf16[128,1024]{1,0:T(8,128)(2,1)} custom-call(bf16[512,128]{1,0:T(8,128)(2,1)S(1)} %bitcast.15, f32[128,1536]{1,0:T(8,128)S(1)} %shard_map.133.parts_ref, f32[2,256]{1,0:T(2,128)S(1)} %tile.11.gain_ref, bf16[4,16,32,128]{3,2,1,0:T(8,128)(2,1)S(1)} %get-tuple-element.12.own_ref, bf16[4,16,32,128]{3,2,1,0:T(8,128)(2,1)S(1)} %collective-permute-done.4.other_ref), custom_call_target="tpu_custom_call" | custom-call | flops 1073741824 | bytes 1048576 | tf_op jit(solution)/shard_map/pallas_call | solution.py:384
  (9 shorter events, 0.1 us)
Async XLA Ops:
  1.2 29.0 %copy-start = (bf16[2,64,1024]{2,1,0:T(8,128)(2,1)S(1)}, bf16[2,64,1024]{2,1,0:T(8,128)(2,1)}, u32[]{:S(2)}) copy-start(bf16[2,64,1024]{2,1,0:T(8,128)(2,1)} %param.13) | copy-start | bytes 786436
  1.2 29.0 %copy-start.3 = (f32[1024]{0:T(1024)S(1)}, f32[1024]{0:T(1024)}, u32[]{:S(2)}) copy-start(f32[1024]{0:T(1024)} %param.14) | copy-start | bytes 12292
  25.8 16.7 %copy-start.1 = (bf16[16,512]{1,0:T(8,128)(2,1)S(1)}, bf16[16,512]{1,0:T(8,128)(2,1)}, u32[]{:S(2)}) copy-start(bf16[16,512]{1,0:T(8,128)(2,1)} %up_forward_ref.3) | copy-start | bytes 49156
  25.8 16.7 %copy-start.2 = (bf16[16,512]{1,0:T(8,128)(2,1)S(1)}, bf16[16,512]{1,0:T(8,128)(2,1)}, u32[]{:S(2)}) copy-start(bf16[16,512]{1,0:T(8,128)(2,1)} %up_backward_ref.3) | copy-start | bytes 49156
  25.8 16.7 %copy-start.4 = (f32[512]{0:T(512)S(1)}, f32[512]{0:T(512)}, u32[]{:S(2)}) copy-start(f32[512]{0:T(512)} %param.22) | copy-start | bytes 6148
  25.8 16.7 %copy-start.5 = (f32[512]{0:T(512)S(1)}, f32[512]{0:T(512)}, u32[]{:S(2)}) copy-start(f32[512]{0:T(512)} %param.23) | copy-start | bytes 6148
  25.8 16.7 %collective-permute-start = (bf16[16,328,128]{2,1,0:T(8,128)(2,1)S(1)}, bf16[16,328,128]{2,1,0:T(8,128)(2,1)S(1)}, u32[]{:S(2)}, u32[]{:S(2)}) collective-permute-start(bf16[16,328,128]{2,1,0:T(8,128)(2,1)S(1)} %all_to_all.15.own_ref), channel_id=1, source_target_pairs={{0,1},{1,0},{2,3},{3,2},{4,5},{5,4},{6,7},{7,6},{8,9},{9,8},{10,11... | collective-permute-start | bytes 4030472 | tf_op jit(solution)/shard_map/ppermute | solution.py:400
  27.9 10.6 %collective-permute-start.1 = (bf16[1,16,64,128]{3,2,1,0:T(8,128)(2,1)S(1)}, bf16[1,16,64,128]{3,2,1,0:T(8,128)(2,1)S(1)}, u32[]{:S(2)}, u32[]{:S(2)}) collective-permute-start(bf16[1,16,64,128]{3,2,1,0:T(8,128)(2,1)S(1)} %slice_bitcast_fusion.first_ref), channel_id=1, source_target_pairs={{0,8},{8,0},{16,24},{24,16},{1,9},{9,1},{17,25},{25,17},{2,10},{10... | collective-permute-start | bytes 786440 | tf_op jit(solution)/shard_map/ppermute | solution.py:424
  38.6 22.4 %collective-permute-start.2 = (bf16[2,16,64,128]{3,2,1,0:T(8,128)(2,1)S(1)}, bf16[2,16,64,128]{3,2,1,0:T(8,128)(2,1)S(1)}, u32[]{:S(2)}, u32[]{:S(2)}) collective-permute-start(bf16[2,16,64,128]{3,2,1,0:T(8,128)(2,1)S(1)} %shard_map.131.first_ref), channel_id=1, source_target_pairs={{0,24},{8,16},{16,8},{24,0},{1,25},{9,17},{17,9},{25,1},{2,26},{10... | collective-permute-start | bytes 1572872 | tf_op jit(solution)/shard_map/ppermute | solution.py:424
  45.4 35.9 %copy-start.6 = (f32[32]{0:T(128)S(1)}, f32[32]{0:T(128)}, u32[]{:S(2)}) copy-start(f32[32]{0:T(128)} %param.24) | copy-start | bytes 388
  45.4 27.1 %all-to-all-start.1 = ((bf16[16,40,128]{2,1,0:T(8,128)(2,1)}), bf16[16,40,128]{2,1,0:T(8,128)(2,1)S(1)}, u32[]{:S(2)}, u32[]{:S(2)}) async-start(bf16[16,40,128]{2,1,0:T(8,128)(2,1)} %get-tuple-element.9), calls=%async_computation.1 | async-start | bytes 327680 | tf_op jit(solution)/shard_map/all_to_all | solution.py:448
  61.8 19.7 %collective-permute-start.3 = (bf16[4,16,32,128]{3,2,1,0:T(8,128)(2,1)}, bf16[4,16,32,128]{3,2,1,0:T(8,128)(2,1)S(1)}, u32[]{:S(2)}, u32[]{:S(2)}) collective-permute-start(bf16[4,16,32,128]{3,2,1,0:T(8,128)(2,1)} %get-tuple-element.10.own_ref), channel_id=1, source_target_pairs={{0,1},{1,0},{2,3},{3,2},{4,5},{5,4},{6,7},{7,6},{8,9},{9,8},{10,11... | collective-permute-start | bytes 1572872 | tf_op jit(solution)/shard_map/ppermute | solution.py:400
  63.8 21.4 %collective-permute-start.4 = (bf16[4,16,32,128]{3,2,1,0:T(8,128)(2,1)S(1)}, bf16[4,16,32,128]{3,2,1,0:T(8,128)(2,1)S(1)}, u32[]{:S(2)}, u32[]{:S(2)}) collective-permute-start(bf16[4,16,32,128]{3,2,1,0:T(8,128)(2,1)S(1)} %get-tuple-element.12.own_ref), channel_id=1, source_target_pairs={{0,1},{1,0},{2,3},{3,2},{4,5},{5,4},{6,7},{7,6},{8,9},{9,8},{10,11... | collective-permute-start | bytes 1572872 | tf_op jit(solution)/shard_map/ppermute | solution.py:400
  73.4 18.6 %all-to-all-start.2 = ((bf16[16,32,128]{2,1,0:T(8,128)(2,1)}), bf16[16,32,128]{2,1,0:T(8,128)(2,1)S(1)}, u32[]{:S(2)}, u32[]{:S(2)}) async-start(bf16[16,32,128]{2,1,0:T(8,128)(2,1)} %bitcast.6), calls=%async_computation.2 | async-start | bytes 262144 | tf_op jit(solution)/shard_map/all_to_all | solution.py:455

commit v16 on v14

--- a/solution.py
+++ b/solution.py
@@ -123,7 +123,7 @@
         ],
         axis=1,
     )
-    log_sigmoid = jnp.minimum(gates, 0.0) - jnp.log1p(jnp.exp(-jnp.abs(gates)))
+    log_sigmoid = jnp.minimum(gates, 0.0) - jnp.log(1.0 + jnp.exp(-jnp.abs(gates)))
     return halves(log_sigmoid * (2.0 / (BLOCK * HEADS)))
 
 
@@ -131,7 +131,8 @@
     row, col = grid_of((LANES, LANES))
     ones = as_bf16(mask(row, col) & ((row // BLOCK) == (col // BLOCK)))
     lanes = slice(way * WIDTH, (way + 1) * WIDTH)
-    return dot(ones, parts[0][:, lanes]) + dot(ones, parts[1][:, lanes])
+    both = jnp.concatenate([part[:, lanes] for part in parts], axis=0)
+    return dot(jnp.concatenate([ones, ones], axis=1), both)
 
 
 def block_kernel(
@@ -150,12 +151,17 @@
         rows = jnp.stack([packed[:, :, 32 * i : 32 * i + 32] for i in range(4)], axis=1)
         return rows.reshape(WIDTH, 32).astype(bf16)
 
-    mine, theirs = normed_ref[core], normed_ref[1 - core]
+    rows = jnp.concatenate([normed_ref[core], normed_ref[1 - core]], axis=1)
     pieces = [
-        dot(mine, columns(own_ref, first)) + dot(theirs, columns(other_ref, first))
+        dot(
+            rows,
+            jnp.concatenate([columns(own_ref, first), columns(other_ref, first)], axis=0),
+        )
         for first in (0, 2, 4, 6)
     ]
-    pieces.append(dot(mine, rank_columns(own_ref)) + dot(theirs, rank_columns(other_ref)))
+    pieces.append(
+        dot(rows, jnp.concatenate([rank_columns(own_ref), rank_columns(other_ref)], axis=0))
+    )
     pieces.append(jnp.zeros((2 * BLOCK, LANES - 32), f32))
     rounded = jnp.concatenate(pieces, axis=1).astype(bf16)
     rounded_ref[...] = rounded
@@ -179,7 +185,10 @@
     pick = as_bf16(srow == scol // BLOCK)
     lines = []
     for span in (fwd, bwd):
-        sums = dot(pick, high[:, span]) + dot(pick, low[:, span])
+        sums = dot(
+            jnp.concatenate([pick, pick], axis=1),
+            jnp.concatenate([high[:, span], low[:, span]], axis=0),
+        )
         for seq in range(2):
             line = jnp.where(mine, sums[seq : seq + 1], 0.0)
             lines.append(
@@ -193,17 +202,25 @@
         close[:HEADS][:, None, :],
         jnp.where(tail == 1, close[HEADS:][:, None, :], 0.0),
     ).astype(bf16)
-    diagonal = (row // HEAD) == (col // HEAD)
+    drow, dcol = grid_of((LANES, 2 * LANES))
+    diagonal = (drow // HEAD) == ((dcol % LANES) // HEAD)
     for group in range(4):
         lanes = slice(group * LANES, (group + 1) * LANES)
+        value = values[:, lanes]
+        empty = jnp.zeros((BLOCK, LANES), bf16)
+        by_seq = jnp.concatenate(
+            [
+                jnp.concatenate([value[:BLOCK], empty], axis=0),
+                jnp.concatenate([empty, value[BLOCK:]], axis=0),
+            ],
+            axis=1,
+        )
+        by_seq = jnp.concatenate([by_seq, by_seq], axis=0)
         parts = []
         for way in range(2):
-            for seq in range(2):
-                span = slice(seq * BLOCK, (seq + 1) * BLOCK)
-                value = values[span, lanes]
-                both = jnp.concatenate([half[span, lanes] for half in remain[way]], axis=0)
-                state = dot_tn(both, jnp.concatenate([value, value], axis=0))
-                parts.append(jnp.where(diagonal, state, 0.0).astype(bf16))
+            both = jnp.concatenate([half[:, lanes] for half in remain[way]], axis=0)
+            state = dot_tn(both, by_seq)
+            parts.append(jnp.where(diagonal, state, 0.0).astype(bf16))
         folded = dot(jnp.concatenate(parts, axis=1), fold).astype(bf16)
         payload_ref[4 * group : 4 * group + 4, :HEAD, :] = folded.reshape(4, HEAD, LANES)
 

time: 93.9 us -> 93.7 us (level)
  no operation moved by 1% of the time
where the time goes in v16:
time: 93.7 us; the launch traced here: 93.1 us
  starting transfers between devices  36.2 us (39%)
  blocking collectives  24.6 us (26%)
  waiting for transfers between devices  19.8 us (21%)
  Pallas kernels  11.1 us (12%)
  local copies, waits for them, and re-layouts  1.26 us (1%)
    all_to_all x1, blocking collectives, body(): own = lax.all_to_all(send, PLANE, 0, 0, axis_index_groups=[PLANE_GROUP])  24.6 us
    all_to_all x1, starting transfers between devices, body(): inbound = lax.all_to_all(payload, 'sp', 0, 0, axis_index_groups=[GROUP])  15.7 us
    pallas_call x8, Pallas kernels, call(): pl.pallas_call(kernel, out_shape=outs, in_specs=specs, out_specs=(VMEM,)...  11.1 us
    ppermute x2, waiting for transfers between devices, body(): arrived = lax.ppermute(mix, 'dp_0', [(i, i ^ flip) for i in range(4)])  7.93 us
    all_to_all x1, starting transfers between devices, body(): lax.all_to_all(states.reshape(HEADS, HEAD, LANES), 'sp', 0, 0, axis_index...  7.91 us
    ppermute x3, starting transfers between devices, swapped(): return lax.ppermute(x, 'dp_2', [(0, 1), (1, 0)])  6.37 us
    all_to_all x1, waiting for transfers between devices, body(): inbound = lax.all_to_all(payload, 'sp', 0, 0, axis_index_groups=[GROUP])  6.34 us
    ppermute x2, starting transfers between devices, body(): arrived = lax.ppermute(mix, 'dp_0', [(i, i ^ flip) for i in range(4)])  6.2 us
  transfers between devices with their start and end apart: 7, of which 3 were waited for; matrix products, arithmetic and copies ran while one was open for 0% of the time, Pallas kernels for 9%

profile of v16, /device:TPU:2, one launch (start us, length us, event | category | flops | bytes accessed | tf_op | source)
XLA Modules:
  0.0 93.1 jit_solution(16187490035218909536)
XLA Ops:
  0.0 1.2 %shard_map.128 = bf16[16,328,128]{2,1,0:T(8,128)(2,1)S(1)} custom-call(bf16[32,512]{1,0:T(8,128)(2,1)} %key_hbm.1, bf16[32,512]{1,0:T(8,128)(2,1)} %value_hbm.1, bf16[32,512]{1,0:T(8,128)(2,1)} %query_hbm.1, bf16[16,32]{1,0:T(8,128)(2,1)} %bitcast.24, bf16[16,32]{1,0:T(8,128)(2,1)} %bitcast.25, bf16[16,1024]{1,0:T(8,128)(2,1)} %mix_hbm.1), custom_call_target="tpu_custom_call" | custom-call | flops 67108864 | bytes 1048576 | tf_op jit(solution)/shard_map/pallas_call | solution.py:394
  1.2 0.0 copy-start.1
  1.2 0.0 copy-start.4
  1.3 24.6 %all_to_all.15.own_ref = bf16[16,328,128]{2,1,0:T(8,128)(2,1)S(1)} all-to-all(bf16[16,328,128]{2,1,0:T(8,128)(2,1)S(1)} %shard_map.128), channel_id=1, replica_groups={{30,0,2,4,6,8,10,12,14,16,18,20,22,24,26,28},{31,1,3,5,7,9,11,13,15,17,..., dimensions={0} | all-to-all | bytes 2686976 | tf_op jit(solution)/shard_map/all_to_all | solution.py:430
  25.8 2.1 %collective-permute-start = (bf16[16,328,128]{2,1,0:T(8,128)(2,1)S(1)}, bf16[16,328,128]{2,1,0:T(8,128)(2,1)S(1)}, u32[]{:S(2)}, u32[]{:S(2)}) collective-permute-start(bf16[16,328,128]{2,1,0:T(8,128)(2,1)S(1)} %all_to_all.15.own_ref), channel_id=1, source_target_pairs={{0,1},{1,0},{2,3},{3,2},{4,5},{5,4},{6,7},{7,6},{8,9},{9,8},{10,11... | collective-permute-start | bytes 4030472 | tf_op jit(solution)/shard_map/ppermute | solution.py:410
  27.9 2.3 %collective-permute-start.1 = (bf16[1,16,64,128]{3,2,1,0:T(8,128)(2,1)S(1)}, bf16[1,16,64,128]{3,2,1,0:T(8,128)(2,1)S(1)}, u32[]{:S(2)}, u32[]{:S(2)}) collective-permute-start(bf16[1,16,64,128]{3,2,1,0:T(8,128)(2,1)S(1)} %slice_bitcast_fusion.first_ref), channel_id=1, source_target_pairs={{0,8},{8,0},{16,24},{24,16},{1,9},{9,1},{17,25},{25,17},{2,10},{10... | collective-permute-start | bytes 786440 | tf_op jit(solution)/shard_map/ppermute | solution.py:434
  30.2 0.4 shard_map.127.normed_ref
  30.6 7.9 %collective-permute-done.1.second_ref = bf16[1,16,64,128]{3,2,1,0:T(8,128)(2,1)S(1)} collective-permute-done((bf16[1,16,64,128]{3,2,1,0:T(8,128)(2,1)S(1)}, bf16[1,16,64,128]{3,2,1,0:T(8,128)(2,1)S(1)}, u32[]{:S(2)}, u32[]{:S(2)}) %collective-permute-start.1) | collective-permute-done | bytes 262176 | tf_op jit(solution)/shard_map/ppermute | solution.py:434
  38.6 3.9 %collective-permute-start.2 = (bf16[2,16,64,128]{3,2,1,0:T(8,128)(2,1)S(1)}, bf16[2,16,64,128]{3,2,1,0:T(8,128)(2,1)S(1)}, u32[]{:S(2)}, u32[]{:S(2)}) collective-permute-start(bf16[2,16,64,128]{3,2,1,0:T(8,128)(2,1)S(1)} %shard_map.131.first_ref), channel_id=1, source_target_pairs={{0,24},{8,16},{16,8},{24,0},{1,25},{9,17},{17,9},{25,1},{2,26},{10... | collective-permute-start | bytes 1572872 | tf_op jit(solution)/shard_map/ppermute | solution.py:434
  42.5 0.0 collective-permute-done.other_ref
  42.5 0.0 copy-done.2
  42.5 0.0 copy-done.3
  42.5 0.0 copy-done.5
  42.6 0.0 copy-done.6
  42.6 2.6 %shard_map.129 = (bf16[16,40,128]{2,1,0:T(8,128)(2,1)}, bf16[128,1152]{1,0:T(8,128)(2,1)}) custom-call(bf16[2,128,512]{2,1,0:T(8,128)(2,1)S(1)} %shard_map.127.normed_ref, bf16[16,328,128]{2,1,0:T(8,128)(2,1)S(1)} %all_to_all.15.own_ref, bf16[16,328,128]{2,1,0:T(8,128)(2,1)S(1)} %collective-permute-done.other_ref, bf16[16,512]{1,0:T(8,128)(2,1)S(1)} %copy-done.2, ...), custom_call_target="tpu_custom_call" | custom-call | flops 1073741824 | bytes 1048576 | tf_op jit(solution)/shard_map/pallas_call | solution.py:394
  45.2 15.7 %all-to-all-start.1 = ((bf16[16,40,128]{2,1,0:T(8,128)(2,1)}), bf16[16,40,128]{2,1,0:T(8,128)(2,1)S(1)}, u32[]{:S(2)}, u32[]{:S(2)}) async-start(bf16[16,40,128]{2,1,0:T(8,128)(2,1)} %get-tuple-element.9), calls=%async_computation.1 | async-start | bytes 327680 | tf_op jit(solution)/shard_map/all_to_all | solution.py:460
  60.8 0.0 collective-permute-done.2.second_ref
  60.8 0.9 shard_map.132
  61.7 1.9 %collective-permute-start.3 = (bf16[4,16,32,128]{3,2,1,0:T(8,128)(2,1)}, bf16[4,16,32,128]{3,2,1,0:T(8,128)(2,1)S(1)}, u32[]{:S(2)}, u32[]{:S(2)}) collective-permute-start(bf16[4,16,32,128]{3,2,1,0:T(8,128)(2,1)} %get-tuple-element.10.own_ref), channel_id=1, source_target_pairs={{0,1},{1,0},{2,3},{3,2},{4,5},{5,4},{6,7},{7,6},{8,9},{9,8},{10,11... | collective-permute-start | bytes 1572872 | tf_op jit(solution)/shard_map/ppermute | solution.py:410
  63.6 2.4 %collective-permute-start.4 = (bf16[4,16,32,128]{3,2,1,0:T(8,128)(2,1)S(1)}, bf16[4,16,32,128]{3,2,1,0:T(8,128)(2,1)S(1)}, u32[]{:S(2)}, u32[]{:S(2)}) collective-permute-start(bf16[4,16,32,128]{3,2,1,0:T(8,128)(2,1)S(1)} %get-tuple-element.12.own_ref), channel_id=1, source_target_pairs={{0,1},{1,0},{2,3},{3,2},{4,5},{5,4},{6,7},{7,6},{8,9},{9,8},{10,11... | collective-permute-start | bytes 1572872 | tf_op jit(solution)/shard_map/ppermute | solution.py:410
  66.0 6.3 %all-to-all-done.1.payload_ref = bf16[16,40,128]{2,1,0:T(8,128)(2,1)S(1)} async-done(((bf16[16,40,128]{2,1,0:T(8,128)(2,1)}), bf16[16,40,128]{2,1,0:T(8,128)(2,1)S(1)}, u32[]{:S(2)}, u32[]{:S(2)}) %all-to-all-start.1) | async-done | bytes 163872 | tf_op jit(solution)/shard_map/all_to_all | solution.py:460
  72.4 0.9 shard_map.130
  73.3 7.9 %all-to-all-start.2 = ((bf16[16,32,128]{2,1,0:T(8,128)(2,1)}), bf16[16,32,128]{2,1,0:T(8,128)(2,1)S(1)}, u32[]{:S(2)}, u32[]{:S(2)}) async-start(bf16[16,32,128]{2,1,0:T(8,128)(2,1)} %bitcast.6), calls=%async_computation.2 | async-start | bytes 262144 | tf_op jit(solution)/shard_map/all_to_all | solution.py:467
  81.2 0.0 copy-done.7
  81.2 0.1 tile.9
  81.3 0.1 tile.11.gain_ref
  81.4 0.0 collective-permute-done.3.other_ref
  81.4 1.0 %copy-done = bf16[4,16,32,128]{3,2,1,0:T(8,128)(2,1)S(1)} copy-done((bf16[4,16,32,128]{3,2,1,0:T(8,128)(2,1)S(1)}, bf16[4,16,32,128]{3,2,1,0:T(8,128)(2,1)}, u32[]{:S(2)}) %copy-start) | copy-done | bytes 524312
  82.5 3.3 %shard_map.133.parts_ref = f32[128,1536]{1,0:T(8,128)S(1)} custom-call(bf16[128,1024]{1,0:T(8,128)(2,1)} %bitcast.16, f32[1,1024]{1,0:T(1,128)S(1)} %bitcast.19, bf16[4,16,32,128]{3,2,1,0:T(8,128)(2,1)S(1)} %copy-done, bf16[4,16,32,128]{3,2,1,0:T(8,128)(2,1)S(1)} %collective-permute-done.3.other_ref, bf16[128,1152]{1,0:T(8,128)(2,1)} %get-tuple-element.11.rounded_ref, ...), custom_call_target="tpu_custom_call" | custom-call | flops 1073741824 | bytes 1048576 | tf_op jit(solution)/shard_map/pallas_call | solution.py:394
  85.7 0.0 collective-permute-done.4.other_ref
  85.7 5.5 %all-to-all-done.2 = bf16[16,32,128]{2,1,0:T(8,128)(2,1)S(1)} async-done(((bf16[16,32,128]{2,1,0:T(8,128)(2,1)}), bf16[16,32,128]{2,1,0:T(8,128)(2,1)S(1)}, u32[]{:S(2)}, u32[]{:S(2)}) %all-to-all-start.2) | async-done | bytes 131104 | tf_op jit(solution)/shard_map/all_to_all | solution.py:467
  91.3 1.8 %shard_map.134 = bf16[128,1024]{1,0:T(8,128)(2,1)} custom-call(bf16[512,128]{1,0:T(8,128)(2,1)S(1)} %bitcast.15, f32[128,1536]{1,0:T(8,128)S(1)} %shard_map.133.parts_ref, f32[2,256]{1,0:T(2,128)S(1)} %tile.11.gain_ref, bf16[4,16,32,128]{3,2,1,0:T(8,128)(2,1)S(1)} %get-tuple-element.12.own_ref, bf16[4,16,32,128]{3,2,1,0:T(8,128)(2,1)S(1)} %collective-permute-done.4.other_ref), custom_call_target="tpu_custom_call" | custom-call | flops 1073741824 | bytes 1048576 | tf_op jit(solution)/shard_map/pallas_call | solution.py:394
  (11 shorter events, 0.1 us)
Async XLA Ops:
  1.2 29.0 %copy-start.1 = (bf16[2,64,1024]{2,1,0:T(8,128)(2,1)S(1)}, bf16[2,64,1024]{2,1,0:T(8,128)(2,1)}, u32[]{:S(2)}) copy-start(bf16[2,64,1024]{2,1,0:T(8,128)(2,1)} %param.13) | copy-start | bytes 786436
  1.2 29.0 %copy-start.4 = (f32[1024]{0:T(1024)S(1)}, f32[1024]{0:T(1024)}, u32[]{:S(2)}) copy-start(f32[1024]{0:T(1024)} %param.14) | copy-start | bytes 12292
  25.8 16.7 %copy-start.2 = (bf16[16,512]{1,0:T(8,128)(2,1)S(1)}, bf16[16,512]{1,0:T(8,128)(2,1)}, u32[]{:S(2)}) copy-start(bf16[16,512]{1,0:T(8,128)(2,1)} %up_forward_ref.3) | copy-start | bytes 49156
  25.8 16.7 %copy-start.3 = (bf16[16,512]{1,0:T(8,128)(2,1)S(1)}, bf16[16,512]{1,0:T(8,128)(2,1)}, u32[]{:S(2)}) copy-start(bf16[16,512]{1,0:T(8,128)(2,1)} %up_backward_ref.3) | copy-start | bytes 49156
  25.8 16.7 %copy-start.5 = (f32[512]{0:T(512)S(1)}, f32[512]{0:T(512)}, u32[]{:S(2)}) copy-start(f32[512]{0:T(512)} %param.22) | copy-start | bytes 6148
  25.8 16.7 %copy-start.6 = (f32[512]{0:T(512)S(1)}, f32[512]{0:T(512)}, u32[]{:S(2)}) copy-start(f32[512]{0:T(512)} %param.23) | copy-start | bytes 6148
  25.8 16.7 %collective-permute-start = (bf16[16,328,128]{2,1,0:T(8,128)(2,1)S(1)}, bf16[16,328,128]{2,1,0:T(8,128)(2,1)S(1)}, u32[]{:S(2)}, u32[]{:S(2)}) collective-permute-start(bf16[16,328,128]{2,1,0:T(8,128)(2,1)S(1)} %all_to_all.15.own_ref), channel_id=1, source_target_pairs={{0,1},{1,0},{2,3},{3,2},{4,5},{5,4},{6,7},{7,6},{8,9},{9,8},{10,11... | collective-permute-start | bytes 4030472 | tf_op jit(solution)/shard_map/ppermute | solution.py:410
  27.9 10.6 %collective-permute-start.1 = (bf16[1,16,64,128]{3,2,1,0:T(8,128)(2,1)S(1)}, bf16[1,16,64,128]{3,2,1,0:T(8,128)(2,1)S(1)}, u32[]{:S(2)}, u32[]{:S(2)}) collective-permute-start(bf16[1,16,64,128]{3,2,1,0:T(8,128)(2,1)S(1)} %slice_bitcast_fusion.first_ref), channel_id=1, source_target_pairs={{0,8},{8,0},{16,24},{24,16},{1,9},{9,1},{17,25},{25,17},{2,10},{10... | collective-permute-start | bytes 786440 | tf_op jit(solution)/shard_map/ppermute | solution.py:434
  38.6 22.3 %collective-permute-start.2 = (bf16[2,16,64,128]{3,2,1,0:T(8,128)(2,1)S(1)}, bf16[2,16,64,128]{3,2,1,0:T(8,128)(2,1)S(1)}, u32[]{:S(2)}, u32[]{:S(2)}) collective-permute-start(bf16[2,16,64,128]{3,2,1,0:T(8,128)(2,1)S(1)} %shard_map.131.first_ref), channel_id=1, source_target_pairs={{0,24},{8,16},{16,8},{24,0},{1,25},{9,17},{17,9},{25,1},{2,26},{10... | collective-permute-start | bytes 1572872 | tf_op jit(solution)/shard_map/ppermute | solution.py:434
  45.2 36.1 %copy-start.7 = (f32[32]{0:T(128)S(1)}, f32[32]{0:T(128)}, u32[]{:S(2)}) copy-start(f32[32]{0:T(128)} %param.24) | copy-start | bytes 388
  45.2 27.2 %all-to-all-start.1 = ((bf16[16,40,128]{2,1,0:T(8,128)(2,1)}), bf16[16,40,128]{2,1,0:T(8,128)(2,1)S(1)}, u32[]{:S(2)}, u32[]{:S(2)}) async-start(bf16[16,40,128]{2,1,0:T(8,128)(2,1)} %get-tuple-element.9), calls=%async_computation.1 | async-start | bytes 327680 | tf_op jit(solution)/shard_map/all_to_all | solution.py:460
  61.7 19.7 %collective-permute-start.3 = (bf16[4,16,32,128]{3,2,1,0:T(8,128)(2,1)}, bf16[4,16,32,128]{3,2,1,0:T(8,128)(2,1)S(1)}, u32[]{:S(2)}, u32[]{:S(2)}) collective-permute-start(bf16[4,16,32,128]{3,2,1,0:T(8,128)(2,1)} %get-tuple-element.10.own_ref), channel_id=1, source_target_pairs={{0,1},{1,0},{2,3},{3,2},{4,5},{5,4},{6,7},{7,6},{8,9},{9,8},{10,11... | collective-permute-start | bytes 1572872 | tf_op jit(solution)/shard_map/ppermute | solution.py:410
  63.6 22.1 %collective-permute-start.4 = (bf16[4,16,32,128]{3,2,1,0:T(8,128)(2,1)S(1)}, bf16[4,16,32,128]{3,2,1,0:T(8,128)(2,1)S(1)}, u32[]{:S(2)}, u32[]{:S(2)}) collective-permute-start(bf16[4,16,32,128]{3,2,1,0:T(8,128)(2,1)S(1)} %get-tuple-element.12.own_ref), channel_id=1, source_target_pairs={{0,1},{1,0},{2,3},{3,2},{4,5},{5,4},{6,7},{7,6},{8,9},{9,8},{10,11... | collective-permute-start | bytes 1572872 | tf_op jit(solution)/shard_map/ppermute | solution.py:410
  73.3 17.9 %all-to-all-start.2 = ((bf16[16,32,128]{2,1,0:T(8,128)(2,1)}), bf16[16,32,128]{2,1,0:T(8,128)(2,1)S(1)}, u32[]{:S(2)}, u32[]{:S(2)}) async-start(bf16[16,32,128]{2,1,0:T(8,128)(2,1)} %bitcast.6), calls=%async_computation.2 | async-start | bytes 262144 | tf_op jit(solution)/shard_map/all_to_all | solution.py:467
  81.4 1.0 %copy-start = (bf16[4,16,32,128]{3,2,1,0:T(8,128)(2,1)S(1)}, bf16[4,16,32,128]{3,2,1,0:T(8,128)(2,1)}, u32[]{:S(2)}) copy-start(bf16[4,16,32,128]{3,2,1,0:T(8,128)(2,1)} %get-tuple-element.10.own_ref) | copy-start | bytes 1572868

commit v17 on v16

--- a/solution.py
+++ b/solution.py
@@ -18,7 +18,7 @@
 SENT = COLUMNS + 32 + 32 + 8
 EPS = 1e-06
 GROUP = [(z + 12) % 16 for z in range(16)]
-PLANE_GROUP = [(i + 15) % 16 for i in range(16)]
+PLANE_GROUP = [(5 * i + 15) % 16 for i in range(16)]
 f32 = jnp.float32
 bf16 = jnp.bfloat16
 
@@ -324,15 +324,20 @@
 ):
     spans = [slice(seq * BLOCK, (seq + 1) * BLOCK) for seq in range(2)]
     core = lax.axis_index("dp_2")
-    row, col = grid_of((LANES, 8 * LANES))
-    source = (col // 256) * HEAD + ((col // LANES) % 2) * 16 + col % 16
-    widen = as_bf16(row == source)
-    row, col = grid_of((256, 8 * LANES))
-    diagonal = (row // HEAD) == ((col % LANES) // 16)
-    full = [
-        jnp.where(diagonal, dot(states_ref[g * 256 : (g + 1) * 256, :], widen), 0.0).astype(bf16)
-        for g in range(2)
-    ]
+    row, col = grid_of((LANES, LANES))
+    lead = row - col % 16
+    widen = jnp.concatenate([as_bf16(lead == 16 * i) for i in range(8)], axis=1)
+    row, col = grid_of((256, LANES))
+    diagonal = (row // HEAD) == (col // 16)
+    full = []
+    for g in range(2):
+        wide = dot(states_ref[g * 256 : (g + 1) * 256, :], widen)
+        full.append(
+            [
+                jnp.where(diagonal, wide[:, i * LANES : (i + 1) * LANES], 0.0).astype(bf16)
+                for i in range(8)
+            ]
+        )
     totals = [[], []]
     for seq, span in enumerate(spans):
         sides = [[], []]
@@ -345,7 +350,10 @@
                 axis=1,
             )
             right = jnp.concatenate(
-                [full[group][:, (2 * way + seq) * 256 : (2 * way + seq + 1) * 256] for way in range(2)],
+                [
+                    jnp.concatenate(full[group][4 * way + 2 * seq : 4 * way + 2 * seq + 2], axis=1)
+                    for way in range(2)
+                ],
                 axis=0,
             )
             across = dot(jnp.concatenate(halves(queries), axis=0), right)
@@ -361,12 +369,14 @@
     high, low = halves(combined[0] * combined[0] + combined[1] * combined[1])
     row, col = grid_of((256, 256))
     ones = as_bf16((row // 16) == (col // 16))
-    scale = lax.rsqrt((dot(high, ones) + dot(low, ones)) * (1.0 / HEAD) + EPS)
+    sums = dot(jnp.concatenate([high, low], axis=1), jnp.concatenate([ones, ones], axis=0))
+    scale = lax.rsqrt(sums * (1.0 / HEAD) + EPS)
     attended = [
         (combined[half] * scale * gain_ref[half : half + 1, :]).astype(bf16) for half in range(2)
     ]
     mine = jnp.where(core == 0, attended[0], attended[1])
     theirs = jnp.where(core == 0, attended[1], attended[0])
+    both = jnp.concatenate([mine, theirs], axis=1)
     for quarter in range(4):
         slot = slot_of(quarter, "dp_0")
 
@@ -374,15 +384,15 @@
             return jnp.concatenate(
                 [
                     jnp.concatenate(
-                        [ref[slot, 1:, rows : rows + 16, :], ref[slot, :1, rows : rows + 16, :]], axis=0
-                    ).reshape(256, LANES)
+                        [ref[slot, PLANE_GROUP.index(h), rows : rows + 16, :] for h in range(16)], axis=0
+                    )
                     for rows in (0, 16)
                 ],
                 axis=1,
             )
 
-        out_ref[:, quarter * 256 : (quarter + 1) * 256] = (
-            dot(mine, weights(own_ref)) + dot(theirs, weights(other_ref))
+        out_ref[:, quarter * 256 : (quarter + 1) * 256] = dot(
+            both, jnp.concatenate([weights(own_ref), weights(other_ref)], axis=0)
         ).astype(bf16)
 
 
@@ -469,7 +479,7 @@
     )
     parts = call(
         query_kernel, shape((rows, 3 * WIDTH), f32), [VMEM] * 9, 1 << 30,
-        in_hbm(tokens_flat), gain_flat, query, query_other, in_hbm(rounded), *decays,
+        in_hbm(tokens_flat), gain_flat, in_hbm(query), query_other, in_hbm(rounded), *decays,
     )
     gain = jnp.tile(out_gain.reshape(2, 1, 16), (1, HEADS, 1)).reshape(2, 256)
     mixed = call(

time: 93.7 us -> 94.1 us (level)
  the two profiles are of different devices: /device:TPU:2 before, /device:TPU:6 now
where the time goes in v17:
time: 94.1 us; the launch traced here: 93.6 us
  starting transfers between devices  35.9 us (38%)
  blocking collectives  25 us (27%)
  waiting for transfers between devices  21.1 us (22%)
  Pallas kernels  11.2 us (12%)
    all_to_all x1, blocking collectives, body(): own = lax.all_to_all(send, PLANE, 0, 0, axis_index_groups=[PLANE_GROUP])  25 us
    all_to_all x1, starting transfers between devices, body(): inbound = lax.all_to_all(payload, 'sp', 0, 0, axis_index_groups=[GROUP])  15.7 us
    pallas_call x8, Pallas kernels, call(): pl.pallas_call(kernel, out_shape=outs, in_specs=specs, out_specs=(VMEM,)...  11.2 us
    ppermute x2, waiting for transfers between devices, body(): arrived = lax.ppermute(mix, 'dp_0', [(i, i ^ flip) for i in range(4)])  8.28 us
    all_to_all x1, starting transfers between devices, body(): lax.all_to_all(states.reshape(HEADS, HEAD, LANES), 'sp', 0, 0, axis_index...  7.92 us
    all_to_all x1, waiting for transfers between devices, body(): lax.all_to_all(states.reshape(HEADS, HEAD, LANES), 'sp', 0, 0, axis_index...  6.45 us
    ppermute x3, starting transfers between devices, swapped(): return lax.ppermute(x, 'dp_2', [(0, 1), (1, 0)])  6.37 us
    all_to_all x1, waiting for transfers between devices, body(): inbound = lax.all_to_all(payload, 'sp', 0, 0, axis_index_groups=[GROUP])  6.36 us
  transfers between devices with their start and end apart: 7, of which 3 were waited for; matrix products, arithmetic and copies ran while one was open for 0% of the time, Pallas kernels for 9%

profile of v17, /device:TPU:6, one launch (start us, length us, event | category | flops | bytes accessed | tf_op | source)
XLA Modules:
  0.0 93.6 jit_solution(14321980440503014139)
XLA Ops:
  0.0 1.2 %shard_map.128 = bf16[16,328,128]{2,1,0:T(8,128)(2,1)S(1)} custom-call(bf16[32,512]{1,0:T(8,128)(2,1)} %key_hbm.1, bf16[32,512]{1,0:T(8,128)(2,1)} %value_hbm.1, bf16[32,512]{1,0:T(8,128)(2,1)} %query_hbm.1, bf16[16,32]{1,0:T(8,128)(2,1)} %bitcast.24, bf16[16,32]{1,0:T(8,128)(2,1)} %bitcast.25, bf16[16,1024]{1,0:T(8,128)(2,1)} %mix_hbm.1), custom_call_target="tpu_custom_call" | custom-call | flops 67108864 | bytes 1048576 | tf_op jit(solution)/shard_map/pallas_call | solution.py:404
  1.2 0.0 copy-start
  1.2 0.0 copy-start.3
  1.3 25.0 %all_to_all.15.own_ref = bf16[16,328,128]{2,1,0:T(8,128)(2,1)S(1)} all-to-all(bf16[16,328,128]{2,1,0:T(8,128)(2,1)S(1)} %shard_map.128), channel_id=1, replica_groups={{30,8,18,28,6,16,26,4,14,24,2,12,22,0,10,20},{31,9,19,29,7,17,27,5,15,2..., dimensions={0} | all-to-all | bytes 2686976 | tf_op jit(solution)/shard_map/all_to_all | solution.py:440
  26.3 2.1 %collective-permute-start = (bf16[16,328,128]{2,1,0:T(8,128)(2,1)S(1)}, bf16[16,328,128]{2,1,0:T(8,128)(2,1)S(1)}, u32[]{:S(2)}, u32[]{:S(2)}) collective-permute-start(bf16[16,328,128]{2,1,0:T(8,128)(2,1)S(1)} %all_to_all.15.own_ref), channel_id=1, source_target_pairs={{0,1},{1,0},{2,3},{3,2},{4,5},{5,4},{6,7},{7,6},{8,9},{9,8},{10,11... | collective-permute-start | bytes 4030472 | tf_op jit(solution)/shard_map/ppermute | solution.py:420
  28.4 1.9 %collective-permute-start.1 = (bf16[1,16,64,128]{3,2,1,0:T(8,128)(2,1)S(1)}, bf16[1,16,64,128]{3,2,1,0:T(8,128)(2,1)S(1)}, u32[]{:S(2)}, u32[]{:S(2)}) collective-permute-start(bf16[1,16,64,128]{3,2,1,0:T(8,128)(2,1)S(1)} %slice_bitcast_fusion.first_ref), channel_id=1, source_target_pairs={{0,8},{8,0},{16,24},{24,16},{1,9},{9,1},{17,25},{25,17},{2,10},{10... | collective-permute-start | bytes 786440 | tf_op jit(solution)/shard_map/ppermute | solution.py:444
  30.3 0.0 copy-done
  30.3 0.0 copy-done.3
  30.3 0.4 shard_map.127.normed_ref
  30.7 8.3 %collective-permute-done.1.second_ref = bf16[1,16,64,128]{3,2,1,0:T(8,128)(2,1)S(1)} collective-permute-done((bf16[1,16,64,128]{3,2,1,0:T(8,128)(2,1)S(1)}, bf16[1,16,64,128]{3,2,1,0:T(8,128)(2,1)S(1)}, u32[]{:S(2)}, u32[]{:S(2)}) %collective-permute-start.1) | collective-permute-done | bytes 262176 | tf_op jit(solution)/shard_map/ppermute | solution.py:444
  39.0 4.0 %collective-permute-start.2 = (bf16[2,16,64,128]{3,2,1,0:T(8,128)(2,1)S(1)}, bf16[2,16,64,128]{3,2,1,0:T(8,128)(2,1)S(1)}, u32[]{:S(2)}, u32[]{:S(2)}) collective-permute-start(bf16[2,16,64,128]{3,2,1,0:T(8,128)(2,1)S(1)} %shard_map.131.first_ref), channel_id=1, source_target_pairs={{0,24},{8,16},{16,8},{24,0},{1,25},{9,17},{17,9},{25,1},{2,26},{10... | collective-permute-start | bytes 1572872 | tf_op jit(solution)/shard_map/ppermute | solution.py:444
  43.0 0.0 collective-permute-done.other_ref
  43.0 0.0 copy-done.1
  43.0 0.0 copy-done.2
  43.0 0.0 copy-done.4
  43.1 0.0 copy-done.5
  43.1 2.6 %shard_map.129 = (bf16[16,40,128]{2,1,0:T(8,128)(2,1)}, bf16[128,1152]{1,0:T(8,128)(2,1)}) custom-call(bf16[2,128,512]{2,1,0:T(8,128)(2,1)S(1)} %shard_map.127.normed_ref, bf16[16,328,128]{2,1,0:T(8,128)(2,1)S(1)} %all_to_all.15.own_ref, bf16[16,328,128]{2,1,0:T(8,128)(2,1)S(1)} %collective-permute-done.other_ref, bf16[16,512]{1,0:T(8,128)(2,1)S(1)} %copy-done.1, ...), custom_call_target="tpu_custom_call" | custom-call | flops 1073741824 | bytes 1048576 | tf_op jit(solution)/shard_map/pallas_call | solution.py:404
  45.7 15.7 %all-to-all-start.1 = ((bf16[16,40,128]{2,1,0:T(8,128)(2,1)}), bf16[16,40,128]{2,1,0:T(8,128)(2,1)S(1)}, u32[]{:S(2)}, u32[]{:S(2)}) async-start(bf16[16,40,128]{2,1,0:T(8,128)(2,1)} %get-tuple-element.9), calls=%async_computation.1 | async-start | bytes 327680 | tf_op jit(solution)/shard_map/all_to_all | solution.py:470
  61.4 0.0 collective-permute-done.2.second_ref
  61.4 0.9 shard_map.132
  62.2 1.9 %collective-permute-start.3 = (bf16[4,16,32,128]{3,2,1,0:T(8,128)(2,1)}, bf16[4,16,32,128]{3,2,1,0:T(8,128)(2,1)S(1)}, u32[]{:S(2)}, u32[]{:S(2)}) collective-permute-start(bf16[4,16,32,128]{3,2,1,0:T(8,128)(2,1)} %get-tuple-element.10.own_ref), channel_id=1, source_target_pairs={{0,1},{1,0},{2,3},{3,2},{4,5},{5,4},{6,7},{7,6},{8,9},{9,8},{10,11... | collective-permute-start | bytes 1572872 | tf_op jit(solution)/shard_map/ppermute | solution.py:420
  64.1 2.4 %collective-permute-start.4 = (bf16[4,16,32,128]{3,2,1,0:T(8,128)(2,1)S(1)}, bf16[4,16,32,128]{3,2,1,0:T(8,128)(2,1)S(1)}, u32[]{:S(2)}, u32[]{:S(2)}) collective-permute-start(bf16[4,16,32,128]{3,2,1,0:T(8,128)(2,1)S(1)} %get-tuple-element.12.own_ref), channel_id=1, source_target_pairs={{0,1},{1,0},{2,3},{3,2},{4,5},{5,4},{6,7},{7,6},{8,9},{9,8},{10,11... | collective-permute-start | bytes 1572872 | tf_op jit(solution)/shard_map/ppermute | solution.py:420
  66.6 6.4 %all-to-all-done.1.payload_ref = bf16[16,40,128]{2,1,0:T(8,128)(2,1)S(1)} async-done(((bf16[16,40,128]{2,1,0:T(8,128)(2,1)}), bf16[16,40,128]{2,1,0:T(8,128)(2,1)S(1)}, u32[]{:S(2)}, u32[]{:S(2)}) %all-to-all-start.1) | async-done | bytes 163872 | tf_op jit(solution)/shard_map/all_to_all | solution.py:470
  72.9 0.9 shard_map.130
  73.8 7.9 %all-to-all-start.2 = ((bf16[16,32,128]{2,1,0:T(8,128)(2,1)}), bf16[16,32,128]{2,1,0:T(8,128)(2,1)S(1)}, u32[]{:S(2)}, u32[]{:S(2)}) async-start(bf16[16,32,128]{2,1,0:T(8,128)(2,1)} %bitcast.6), calls=%async_computation.2 | async-start | bytes 262144 | tf_op jit(solution)/shard_map/all_to_all | solution.py:477
  81.8 0.1 tile.9
  81.9 0.1 tile.11.gain_ref
  81.9 0.0 collective-permute-done.3.other_ref
  81.9 3.4 %shard_map.133.parts_ref = f32[128,1536]{1,0:T(8,128)S(1)} custom-call(bf16[128,1024]{1,0:T(8,128)(2,1)} %bitcast.16, f32[1,1024]{1,0:T(1,128)S(1)} %bitcast.19, bf16[4,16,32,128]{3,2,1,0:T(8,128)(2,1)} %get-tuple-element.10.own_ref, bf16[4,16,32,128]{3,2,1,0:T(8,128)(2,1)S(1)} %collective-permute-done.3.other_ref, ...), custom_call_target="tpu_custom_call" | custom-call | flops 1073741824 | bytes 1048576 | tf_op jit(solution)/shard_map/pallas_call | solution.py:404
  85.4 0.0 collective-permute-done.4.other_ref
  85.4 6.4 %all-to-all-done.2 = bf16[16,32,128]{2,1,0:T(8,128)(2,1)S(1)} async-done(((bf16[16,32,128]{2,1,0:T(8,128)(2,1)}), bf16[16,32,128]{2,1,0:T(8,128)(2,1)S(1)}, u32[]{:S(2)}, u32[]{:S(2)}) %all-to-all-start.2) | async-done | bytes 131104 | tf_op jit(solution)/shard_map/all_to_all | solution.py:477
  91.8 1.8 %shard_map.134 = bf16[128,1024]{1,0:T(8,128)(2,1)} custom-call(bf16[512,128]{1,0:T(8,128)(2,1)S(1)} %bitcast.15, f32[128,1536]{1,0:T(8,128)S(1)} %shard_map.133.parts_ref, f32[2,256]{1,0:T(2,128)S(1)} %tile.11.gain_ref, bf16[4,16,32,128]{3,2,1,0:T(8,128)(2,1)S(1)} %get-tuple-element.12.own_ref, bf16[4,16,32,128]{3,2,1,0:T(8,128)(2,1)S(1)} %collective-permute-done.4.other_ref), custom_call_target="tpu_custom_call" | custom-call | flops 1073741824 | bytes 1048576 | tf_op jit(solution)/shard_map/pallas_call | solution.py:404
  (9 shorter events, 0.1 us)
Async XLA Ops:
  1.2 29.1 %copy-start = (bf16[2,64,1024]{2,1,0:T(8,128)(2,1)S(1)}, bf16[2,64,1024]{2,1,0:T(8,128)(2,1)}, u32[]{:S(2)}) copy-start(bf16[2,64,1024]{2,1,0:T(8,128)(2,1)} %param.13) | copy-start | bytes 786436
  1.2 29.1 %copy-start.3 = (f32[1024]{0:T(1024)S(1)}, f32[1024]{0:T(1024)}, u32[]{:S(2)}) copy-start(f32[1024]{0:T(1024)} %param.14) | copy-start | bytes 12292
  26.3 16.7 %copy-start.1 = (bf16[16,512]{1,0:T(8,128)(2,1)S(1)}, bf16[16,512]{1,0:T(8,128)(2,1)}, u32[]{:S(2)}) copy-start(bf16[16,512]{1,0:T(8,128)(2,1)} %up_forward_ref.3) | copy-start | bytes 49156
  26.3 16.8 %copy-start.2 = (bf16[16,512]{1,0:T(8,128)(2,1)S(1)}, bf16[16,512]{1,0:T(8,128)(2,1)}, u32[]{:S(2)}) copy-start(bf16[16,512]{1,0:T(8,128)(2,1)} %up_backward_ref.3) | copy-start | bytes 49156
  26.3 16.8 %copy-start.4 = (f32[512]{0:T(512)S(1)}, f32[512]{0:T(512)}, u32[]{:S(2)}) copy-start(f32[512]{0:T(512)} %param.22) | copy-start | bytes 6148
  26.3 16.8 %copy-start.5 = (f32[512]{0:T(512)S(1)}, f32[512]{0:T(512)}, u32[]{:S(2)}) copy-start(f32[512]{0:T(512)} %param.23) | copy-start | bytes 6148
  26.3 16.7 %collective-permute-start = (bf16[16,328,128]{2,1,0:T(8,128)(2,1)S(1)}, bf16[16,328,128]{2,1,0:T(8,128)(2,1)S(1)}, u32[]{:S(2)}, u32[]{:S(2)}) collective-permute-start(bf16[16,328,128]{2,1,0:T(8,128)(2,1)S(1)} %all_to_all.15.own_ref), channel_id=1, source_target_pairs={{0,1},{1,0},{2,3},{3,2},{4,5},{5,4},{6,7},{7,6},{8,9},{9,8},{10,11... | collective-permute-start | bytes 4030472 | tf_op jit(solution)/shard_map/ppermute | solution.py:420
  28.4 10.6 %collective-permute-start.1 = (bf16[1,16,64,128]{3,2,1,0:T(8,128)(2,1)S(1)}, bf16[1,16,64,128]{3,2,1,0:T(8,128)(2,1)S(1)}, u32[]{:S(2)}, u32[]{:S(2)}) collective-permute-start(bf16[1,16,64,128]{3,2,1,0:T(8,128)(2,1)S(1)} %slice_bitcast_fusion.first_ref), channel_id=1, source_target_pairs={{0,8},{8,0},{16,24},{24,16},{1,9},{9,1},{17,25},{25,17},{2,10},{10... | collective-permute-start | bytes 786440 | tf_op jit(solution)/shard_map/ppermute | solution.py:444
  39.0 22.4 %collective-permute-start.2 = (bf16[2,16,64,128]{3,2,1,0:T(8,128)(2,1)S(1)}, bf16[2,16,64,128]{3,2,1,0:T(8,128)(2,1)S(1)}, u32[]{:S(2)}, u32[]{:S(2)}) collective-permute-start(bf16[2,16,64,128]{3,2,1,0:T(8,128)(2,1)S(1)} %shard_map.131.first_ref), channel_id=1, source_target_pairs={{0,24},{8,16},{16,8},{24,0},{1,25},{9,17},{17,9},{25,1},{2,26},{10... | collective-permute-start | bytes 1572872 | tf_op jit(solution)/shard_map/ppermute | solution.py:444
  45.7 36.1 %copy-start.6 = (f32[32]{0:T(128)S(1)}, f32[32]{0:T(128)}, u32[]{:S(2)}) copy-start(f32[32]{0:T(128)} %param.24) | copy-start | bytes 388
  45.7 27.3 %all-to-all-start.1 = ((bf16[16,40,128]{2,1,0:T(8,128)(2,1)}), bf16[16,40,128]{2,1,0:T(8,128)(2,1)S(1)}, u32[]{:S(2)}, u32[]{:S(2)}) async-start(bf16[16,40,128]{2,1,0:T(8,128)(2,1)} %get-tuple-element.9), calls=%async_computation.1 | async-start | bytes 327680 | tf_op jit(solution)/shard_map/all_to_all | solution.py:470
  62.2 19.7 %collective-permute-start.3 = (bf16[4,16,32,128]{3,2,1,0:T(8,128)(2,1)}, bf16[4,16,32,128]{3,2,1,0:T(8,128)(2,1)S(1)}, u32[]{:S(2)}, u32[]{:S(2)}) collective-permute-start(bf16[4,16,32,128]{3,2,1,0:T(8,128)(2,1)} %get-tuple-element.10.own_ref), channel_id=1, source_target_pairs={{0,1},{1,0},{2,3},{3,2},{4,5},{5,4},{6,7},{7,6},{8,9},{9,8},{10,11... | collective-permute-start | bytes 1572872 | tf_op jit(solution)/shard_map/ppermute | solution.py:420
  64.1 21.2 %collective-permute-start.4 = (bf16[4,16,32,128]{3,2,1,0:T(8,128)(2,1)S(1)}, bf16[4,16,32,128]{3,2,1,0:T(8,128)(2,1)S(1)}, u32[]{:S(2)}, u32[]{:S(2)}) collective-permute-start(bf16[4,16,32,128]{3,2,1,0:T(8,128)(2,1)S(1)} %get-tuple-element.12.own_ref), channel_id=1, source_target_pairs={{0,1},{1,0},{2,3},{3,2},{4,5},{5,4},{6,7},{7,6},{8,9},{9,8},{10,11... | collective-permute-start | bytes 1572872 | tf_op jit(solution)/shard_map/ppermute | solution.py:420
  73.8 18.0 %all-to-all-start.2 = ((bf16[16,32,128]{2,1,0:T(8,128)(2,1)}), bf16[16,32,128]{2,1,0:T(8,128)(2,1)S(1)}, u32[]{:S(2)}, u32[]{:S(2)}) async-start(bf16[16,32,128]{2,1,0:T(8,128)(2,1)} %bitcast.6), calls=%async_computation.2 | async-start | bytes 262144 | tf_op jit(solution)/shard_map/all_to_all | solution.py:477

commit v18 on v17

--- a/solution.py
+++ b/solution.py
@@ -17,8 +17,8 @@
 COLUMNS = 8 * 32
 SENT = COLUMNS + 32 + 32 + 8
 EPS = 1e-06
-GROUP = [(z + 12) % 16 for z in range(16)]
-PLANE_GROUP = [(5 * i + 15) % 16 for i in range(16)]
+GROUP = [(z + 10) % 16 for z in range(16)]
+PLANE_GROUP = [(i + 15) % 16 for i in range(16)]
 f32 = jnp.float32
 bf16 = jnp.bfloat16
 
@@ -384,8 +384,8 @@
             return jnp.concatenate(
                 [
                     jnp.concatenate(
-                        [ref[slot, PLANE_GROUP.index(h), rows : rows + 16, :] for h in range(16)], axis=0
-                    )
+                        [ref[slot, 1:, rows : rows + 16, :], ref[slot, :1, rows : rows + 16, :]], axis=0
+                    ).reshape(256, LANES)
                     for rows in (0, 16)
                 ],
                 axis=1,

time: 94.1 us -> 92.2 us (0.980)
  the two profiles are of different devices: /device:TPU:6 before, /device:TPU:2 now
where the time goes in v18:
time: 92.2 us; the launch traced here: 91.6 us
  starting transfers between devices  40.1 us (43%)
  blocking collectives  24.6 us (27%)
  waiting for transfers between devices  15.4 us (17%)
  Pallas kernels  11.2 us (12%)
    all_to_all x1, blocking collectives, body(): own = lax.all_to_all(send, PLANE, 0, 0, axis_index_groups=[PLANE_GROUP])  24.6 us
    all_to_all x1, starting transfers between devices, body(): inbound = lax.all_to_all(payload, 'sp', 0, 0, axis_index_groups=[GROUP])  17.1 us
    pallas_call x8, Pallas kernels, call(): pl.pallas_call(kernel, out_shape=outs, in_specs=specs, out_specs=(VMEM,)...  11.2 us
    all_to_all x1, starting transfers between devices, body(): lax.all_to_all(states.reshape(HEADS, HEAD, LANES), 'sp', 0, 0, axis_index...  10.5 us
    ppermute x2, waiting for transfers between devices, body(): arrived = lax.ppermute(mix, 'dp_0', [(i, i ^ flip) for i in range(4)])  7.93 us
    ppermute x3, starting transfers between devices, swapped(): return lax.ppermute(x, 'dp_2', [(0, 1), (1, 0)])  6.37 us
    ppermute x2, starting transfers between devices, body(): arrived = lax.ppermute(mix, 'dp_0', [(i, i ^ flip) for i in range(4)])  6.2 us
    all_to_all x1, waiting for transfers between devices, body(): inbound = lax.all_to_all(payload, 'sp', 0, 0, axis_index_groups=[GROUP])  3.82 us
  transfers between devices with their start and end apart: 7, of which 3 were waited for; matrix products, arithmetic and copies ran while one was open for 0% of the time, Pallas kernels for 9%

profile of v18, /device:TPU:2, one launch (start us, length us, event | category | flops | bytes accessed | tf_op | source)
XLA Modules:
  0.0 91.6 jit_solution(4490411976157888214)
XLA Ops:
  0.0 1.2 %shard_map.128 = bf16[16,328,128]{2,1,0:T(8,128)(2,1)S(1)} custom-call(bf16[32,512]{1,0:T(8,128)(2,1)} %key_hbm.1, bf16[32,512]{1,0:T(8,128)(2,1)} %value_hbm.1, bf16[32,512]{1,0:T(8,128)(2,1)} %query_hbm.1, bf16[16,32]{1,0:T(8,128)(2,1)} %bitcast.24, bf16[16,32]{1,0:T(8,128)(2,1)} %bitcast.25, bf16[16,1024]{1,0:T(8,128)(2,1)} %mix_hbm.1), custom_call_target="tpu_custom_call" | custom-call | flops 67108864 | bytes 1048576 | tf_op jit(solution)/shard_map/pallas_call | solution.py:404
  1.2 0.0 copy-start
  1.2 0.0 copy-start.3
  1.3 24.6 %all_to_all.15.own_ref = bf16[16,328,128]{2,1,0:T(8,128)(2,1)S(1)} all-to-all(bf16[16,328,128]{2,1,0:T(8,128)(2,1)S(1)} %shard_map.128), channel_id=1, replica_groups={{30,0,2,4,6,8,10,12,14,16,18,20,22,24,26,28},{31,1,3,5,7,9,11,13,15,17,..., dimensions={0} | all-to-all | bytes 2686976 | tf_op jit(solution)/shard_map/all_to_all | solution.py:440
  25.8 2.1 %collective-permute-start = (bf16[16,328,128]{2,1,0:T(8,128)(2,1)S(1)}, bf16[16,328,128]{2,1,0:T(8,128)(2,1)S(1)}, u32[]{:S(2)}, u32[]{:S(2)}) collective-permute-start(bf16[16,328,128]{2,1,0:T(8,128)(2,1)S(1)} %all_to_all.15.own_ref), channel_id=1, source_target_pairs={{0,1},{1,0},{2,3},{3,2},{4,5},{5,4},{6,7},{7,6},{8,9},{9,8},{10,11... | collective-permute-start | bytes 4030472 | tf_op jit(solution)/shard_map/ppermute | solution.py:420
  27.9 2.3 %collective-permute-start.1 = (bf16[1,16,64,128]{3,2,1,0:T(8,128)(2,1)S(1)}, bf16[1,16,64,128]{3,2,1,0:T(8,128)(2,1)S(1)}, u32[]{:S(2)}, u32[]{:S(2)}) collective-permute-start(bf16[1,16,64,128]{3,2,1,0:T(8,128)(2,1)S(1)} %slice_bitcast_fusion.first_ref), channel_id=1, source_target_pairs={{0,8},{8,0},{16,24},{24,16},{1,9},{9,1},{17,25},{25,17},{2,10},{10... | collective-permute-start | bytes 786440 | tf_op jit(solution)/shard_map/ppermute | solution.py:444
  30.2 0.0 copy-done
  30.2 0.4 shard_map.127.normed_ref
  30.6 7.9 %collective-permute-done.1.second_ref = bf16[1,16,64,128]{3,2,1,0:T(8,128)(2,1)S(1)} collective-permute-done((bf16[1,16,64,128]{3,2,1,0:T(8,128)(2,1)S(1)}, bf16[1,16,64,128]{3,2,1,0:T(8,128)(2,1)S(1)}, u32[]{:S(2)}, u32[]{:S(2)}) %collective-permute-start.1) | collective-permute-done | bytes 262176 | tf_op jit(solution)/shard_map/ppermute | solution.py:444
  38.6 3.9 %collective-permute-start.2 = (bf16[2,16,64,128]{3,2,1,0:T(8,128)(2,1)S(1)}, bf16[2,16,64,128]{3,2,1,0:T(8,128)(2,1)S(1)}, u32[]{:S(2)}, u32[]{:S(2)}) collective-permute-start(bf16[2,16,64,128]{3,2,1,0:T(8,128)(2,1)S(1)} %shard_map.131.first_ref), channel_id=1, source_target_pairs={{0,24},{8,16},{16,8},{24,0},{1,25},{9,17},{17,9},{25,1},{2,26},{10... | collective-permute-start | bytes 1572872 | tf_op jit(solution)/shard_map/ppermute | solution.py:444
  42.5 0.0 collective-permute-done.other_ref
  42.5 0.0 copy-done.1
  42.5 0.0 copy-done.2
  42.5 0.0 copy-done.4
  42.6 0.0 copy-done.5
  42.6 2.6 %shard_map.129 = (bf16[16,40,128]{2,1,0:T(8,128)(2,1)}, bf16[128,1152]{1,0:T(8,128)(2,1)}) custom-call(bf16[2,128,512]{2,1,0:T(8,128)(2,1)S(1)} %shard_map.127.normed_ref, bf16[16,328,128]{2,1,0:T(8,128)(2,1)S(1)} %all_to_all.15.own_ref, bf16[16,328,128]{2,1,0:T(8,128)(2,1)S(1)} %collective-permute-done.other_ref, bf16[16,512]{1,0:T(8,128)(2,1)S(1)} %copy-done.1, ...), custom_call_target="tpu_custom_call" | custom-call | flops 1073741824 | bytes 1048576 | tf_op jit(solution)/shard_map/pallas_call | solution.py:404
  45.2 17.1 %all-to-all-start.1 = ((bf16[16,40,128]{2,1,0:T(8,128)(2,1)}), bf16[16,40,128]{2,1,0:T(8,128)(2,1)S(1)}, u32[]{:S(2)}, u32[]{:S(2)}) async-start(bf16[16,40,128]{2,1,0:T(8,128)(2,1)} %get-tuple-element.9), calls=%async_computation.1 | async-start | bytes 327680 | tf_op jit(solution)/shard_map/all_to_all | solution.py:470
  62.2 0.0 collective-permute-done.2.second_ref
  62.2 0.9 shard_map.132
  63.1 1.9 %collective-permute-start.3 = (bf16[4,16,32,128]{3,2,1,0:T(8,128)(2,1)}, bf16[4,16,32,128]{3,2,1,0:T(8,128)(2,1)S(1)}, u32[]{:S(2)}, u32[]{:S(2)}) collective-permute-start(bf16[4,16,32,128]{3,2,1,0:T(8,128)(2,1)} %get-tuple-element.10.own_ref), channel_id=1, source_target_pairs={{0,1},{1,0},{2,3},{3,2},{4,5},{5,4},{6,7},{7,6},{8,9},{9,8},{10,11... | collective-permute-start | bytes 1572872 | tf_op jit(solution)/shard_map/ppermute | solution.py:420
  65.0 2.4 %collective-permute-start.4 = (bf16[4,16,32,128]{3,2,1,0:T(8,128)(2,1)S(1)}, bf16[4,16,32,128]{3,2,1,0:T(8,128)(2,1)S(1)}, u32[]{:S(2)}, u32[]{:S(2)}) collective-permute-start(bf16[4,16,32,128]{3,2,1,0:T(8,128)(2,1)S(1)} %get-tuple-element.12.own_ref), channel_id=1, source_target_pairs={{0,1},{1,0},{2,3},{3,2},{4,5},{5,4},{6,7},{7,6},{8,9},{9,8},{10,11... | collective-permute-start | bytes 1572872 | tf_op jit(solution)/shard_map/ppermute | solution.py:420
  67.4 3.8 %all-to-all-done.1.payload_ref = bf16[16,40,128]{2,1,0:T(8,128)(2,1)S(1)} async-done(((bf16[16,40,128]{2,1,0:T(8,128)(2,1)}), bf16[16,40,128]{2,1,0:T(8,128)(2,1)S(1)}, u32[]{:S(2)}, u32[]{:S(2)}) %all-to-all-start.1) | async-done | bytes 163872 | tf_op jit(solution)/shard_map/all_to_all | solution.py:470
  71.2 0.9 shard_map.130
  72.2 10.5 %all-to-all-start.2 = ((bf16[16,32,128]{2,1,0:T(8,128)(2,1)}), bf16[16,32,128]{2,1,0:T(8,128)(2,1)S(1)}, u32[]{:S(2)}, u32[]{:S(2)}) async-start(bf16[16,32,128]{2,1,0:T(8,128)(2,1)} %bitcast.6), calls=%async_computation.2 | async-start | bytes 262144 | tf_op jit(solution)/shard_map/all_to_all | solution.py:477
  82.6 0.0 copy-done.6
  82.6 0.1 tile.9
  82.7 0.1 tile.11.gain_ref
  82.8 0.0 collective-permute-done.3.other_ref
  82.8 3.4 %shard_map.133.parts_ref = f32[128,1536]{1,0:T(8,128)S(1)} custom-call(bf16[128,1024]{1,0:T(8,128)(2,1)} %bitcast.16, f32[1,1024]{1,0:T(1,128)S(1)} %bitcast.19, bf16[4,16,32,128]{3,2,1,0:T(8,128)(2,1)} %get-tuple-element.10.own_ref, bf16[4,16,32,128]{3,2,1,0:T(8,128)(2,1)S(1)} %collective-permute-done.3.other_ref, ...), custom_call_target="tpu_custom_call" | custom-call | flops 1073741824 | bytes 1048576 | tf_op jit(solution)/shard_map/pallas_call | solution.py:404
  86.2 0.0 collective-permute-done.4.other_ref
  86.2 3.6 %all-to-all-done.2 = bf16[16,32,128]{2,1,0:T(8,128)(2,1)S(1)} async-done(((bf16[16,32,128]{2,1,0:T(8,128)(2,1)}), bf16[16,32,128]{2,1,0:T(8,128)(2,1)S(1)}, u32[]{:S(2)}, u32[]{:S(2)}) %all-to-all-start.2) | async-done | bytes 131104 | tf_op jit(solution)/shard_map/all_to_all | solution.py:477
  89.8 1.8 %shard_map.134 = bf16[128,1024]{1,0:T(8,128)(2,1)} custom-call(bf16[512,128]{1,0:T(8,128)(2,1)S(1)} %bitcast.15, f32[128,1536]{1,0:T(8,128)S(1)} %shard_map.133.parts_ref, f32[2,256]{1,0:T(2,128)S(1)} %tile.11.gain_ref, bf16[4,16,32,128]{3,2,1,0:T(8,128)(2,1)S(1)} %get-tuple-element.12.own_ref, bf16[4,16,32,128]{3,2,1,0:T(8,128)(2,1)S(1)} %collective-permute-done.4.other_ref), custom_call_target="tpu_custom_call" | custom-call | flops 1073741824 | bytes 1048576 | tf_op jit(solution)/shard_map/pallas_call | solution.py:404
  (9 shorter events, 0.1 us)
Async XLA Ops:
  1.2 29.0 %copy-start = (bf16[2,64,1024]{2,1,0:T(8,128)(2,1)S(1)}, bf16[2,64,1024]{2,1,0:T(8,128)(2,1)}, u32[]{:S(2)}) copy-start(bf16[2,64,1024]{2,1,0:T(8,128)(2,1)} %param.13) | copy-start | bytes 786436
  1.2 29.0 %copy-start.3 = (f32[1024]{0:T(1024)S(1)}, f32[1024]{0:T(1024)}, u32[]{:S(2)}) copy-start(f32[1024]{0:T(1024)} %param.14) | copy-start | bytes 12292
  25.8 16.7 %copy-start.1 = (bf16[16,512]{1,0:T(8,128)(2,1)S(1)}, bf16[16,512]{1,0:T(8,128)(2,1)}, u32[]{:S(2)}) copy-start(bf16[16,512]{1,0:T(8,128)(2,1)} %up_forward_ref.3) | copy-start | bytes 49156
  25.8 16.7 %copy-start.2 = (bf16[16,512]{1,0:T(8,128)(2,1)S(1)}, bf16[16,512]{1,0:T(8,128)(2,1)}, u32[]{:S(2)}) copy-start(bf16[16,512]{1,0:T(8,128)(2,1)} %up_backward_ref.3) | copy-start | bytes 49156
  25.8 16.7 %copy-start.4 = (f32[512]{0:T(512)S(1)}, f32[512]{0:T(512)}, u32[]{:S(2)}) copy-start(f32[512]{0:T(512)} %param.22) | copy-start | bytes 6148
  25.8 16.7 %copy-start.5 = (f32[512]{0:T(512)S(1)}, f32[512]{0:T(512)}, u32[]{:S(2)}) copy-start(f32[512]{0:T(512)} %param.23) | copy-start | bytes 6148
  25.8 16.7 %collective-permute-start = (bf16[16,328,128]{2,1,0:T(8,128)(2,1)S(1)}, bf16[16,328,128]{2,1,0:T(8,128)(2,1)S(1)}, u32[]{:S(2)}, u32[]{:S(2)}) collective-permute-start(bf16[16,328,128]{2,1,0:T(8,128)(2,1)S(1)} %all_to_all.15.own_ref), channel_id=1, source_target_pairs={{0,1},{1,0},{2,3},{3,2},{4,5},{5,4},{6,7},{7,6},{8,9},{9,8},{10,11... | collective-permute-start | bytes 4030472 | tf_op jit(solution)/shard_map/ppermute | solution.py:420
  27.9 10.6 %collective-permute-start.1 = (bf16[1,16,64,128]{3,2,1,0:T(8,128)(2,1)S(1)}, bf16[1,16,64,128]{3,2,1,0:T(8,128)(2,1)S(1)}, u32[]{:S(2)}, u32[]{:S(2)}) collective-permute-start(bf16[1,16,64,128]{3,2,1,0:T(8,128)(2,1)S(1)} %slice_bitcast_fusion.first_ref), channel_id=1, source_target_pairs={{0,8},{8,0},{16,24},{24,16},{1,9},{9,1},{17,25},{25,17},{2,10},{10... | collective-permute-start | bytes 786440 | tf_op jit(solution)/shard_map/ppermute | solution.py:444
  38.6 23.6 %collective-permute-start.2 = (bf16[2,16,64,128]{3,2,1,0:T(8,128)(2,1)S(1)}, bf16[2,16,64,128]{3,2,1,0:T(8,128)(2,1)S(1)}, u32[]{:S(2)}, u32[]{:S(2)}) collective-permute-start(bf16[2,16,64,128]{3,2,1,0:T(8,128)(2,1)S(1)} %shard_map.131.first_ref), channel_id=1, source_target_pairs={{0,24},{8,16},{16,8},{24,0},{1,25},{9,17},{17,9},{25,1},{2,26},{10... | collective-permute-start | bytes 1572872 | tf_op jit(solution)/shard_map/ppermute | solution.py:444
  45.2 37.4 %copy-start.6 = (f32[32]{0:T(128)S(1)}, f32[32]{0:T(128)}, u32[]{:S(2)}) copy-start(f32[32]{0:T(128)} %param.24) | copy-start | bytes 388
  45.2 26.1 %all-to-all-start.1 = ((bf16[16,40,128]{2,1,0:T(8,128)(2,1)}), bf16[16,40,128]{2,1,0:T(8,128)(2,1)S(1)}, u32[]{:S(2)}, u32[]{:S(2)}) async-start(bf16[16,40,128]{2,1,0:T(8,128)(2,1)} %get-tuple-element.9), calls=%async_computation.1 | async-start | bytes 327680 | tf_op jit(solution)/shard_map/all_to_all | solution.py:470
  63.1 19.7 %collective-permute-start.3 = (bf16[4,16,32,128]{3,2,1,0:T(8,128)(2,1)}, bf16[4,16,32,128]{3,2,1,0:T(8,128)(2,1)S(1)}, u32[]{:S(2)}, u32[]{:S(2)}) collective-permute-start(bf16[4,16,32,128]{3,2,1,0:T(8,128)(2,1)} %get-tuple-element.10.own_ref), channel_id=1, source_target_pairs={{0,1},{1,0},{2,3},{3,2},{4,5},{5,4},{6,7},{7,6},{8,9},{9,8},{10,11... | collective-permute-start | bytes 1572872 | tf_op jit(solution)/shard_map/ppermute | solution.py:420
  65.0 21.2 %collective-permute-start.4 = (bf16[4,16,32,128]{3,2,1,0:T(8,128)(2,1)S(1)}, bf16[4,16,32,128]{3,2,1,0:T(8,128)(2,1)S(1)}, u32[]{:S(2)}, u32[]{:S(2)}) collective-permute-start(bf16[4,16,32,128]{3,2,1,0:T(8,128)(2,1)S(1)} %get-tuple-element.12.own_ref), channel_id=1, source_target_pairs={{0,1},{1,0},{2,3},{3,2},{4,5},{5,4},{6,7},{7,6},{8,9},{9,8},{10,11... | collective-permute-start | bytes 1572872 | tf_op jit(solution)/shard_map/ppermute | solution.py:420
  72.2 17.7 %all-to-all-start.2 = ((bf16[16,32,128]{2,1,0:T(8,128)(2,1)}), bf16[16,32,128]{2,1,0:T(8,128)(2,1)S(1)}, u32[]{:S(2)}, u32[]{:S(2)}) async-start(bf16[16,32,128]{2,1,0:T(8,128)(2,1)} %bitcast.6), calls=%async_computation.2 | async-start | bytes 262144 | tf_op jit(solution)/shard_map/all_to_all | solution.py:477
